TPU v7x, 512 devices: a whole 4x8x8 slice. The times are simulated.
512 devices in a mesh: rep: 2 (over z_hi), fs: 32 (over z_lo, y), tp: 8 (over x, core).
Axes of the slice: x: 4, y: 8, z: 8 (z_hi: 2, z_lo: 4; z = z_hi * 4 + z_lo), core: 2. Of those that a mesh axis runs over, the one named last changes fastest.
Arguments:
- tokens: bfloat16 [16384, 2048], P(('rep', 'fs')), may hold values from -6 to 6
- mid_tokens: bfloat16 [16384, 2048], P(('rep', 'fs')), may hold values from -6 to 6
- out_grad: bfloat16 [16384, 2048], P(('rep', 'fs')), may hold values from -16 to 16
- gate_first: bfloat16 [2048, 3072], P('fs', 'tp'), may hold values from -0.125 to 0.125
- up_first: bfloat16 [2048, 3072], P('fs', 'tp'), may hold values from -0.125 to 0.125
- down_first: bfloat16 [3072, 2048], P('tp', 'fs'), may hold values from -0.109375 to 0.109375
- gate_second: bfloat16 [2048, 3072], P('fs', 'tp'), may hold values from -0.125 to 0.125
- up_second: bfloat16 [2048, 3072], P('fs', 'tp'), may hold values from -0.125 to 0.125
- down_second: bfloat16 [3072, 2048], P('tp', 'fs'), may hold values from -0.109375 to 0.109375
Outputs:
- input_grad: bfloat16 [16384, 2048], P(('rep', 'fs'))
- down_grad: float32 [3072, 2048], P('tp', 'fs')
- row_norms: float32 [3072], P('tp')
All inputs are finite; a program needn't handle non-finite values.
Results may differ from a plain program's by a relative error of at most 0.025.
Values may be sent and summed in bfloat16 or wider, within the bound.
No kernel may reach another device: no remote copies, remote signals or barrier semaphores. Data moves between devices by JAX's collectives and lax.ppermute only.
A program may use at most 64 MiB of HBM per device.

v0:
```python
import jax
import jax.numpy as jnp
from jax import lax
from jax.sharding import Mesh
from jax.sharding import PartitionSpec as P

FS = ("fs_0", "fs_1")
REP_FS = ("rep", "fs_0", "fs_1")


eps = 1e-06


def in_one_piece(arrays, axis, dim, along):
    both = jnp.concatenate(arrays, axis=along)
    filled, at, done = (lax.all_gather(both, axis, axis=dim, tiled=True), 0, [])
    for a in arrays:
        done.append(lax.slice_in_dim(filled, at, at + a.shape[along], axis=along))
        at += a.shape[along]
    return tuple(done)


def from_everyone(value, axis):
    length = lax.axis_size(axis)
    return lax.all_to_all(
        jnp.broadcast_to(value[None], (length, *value.shape)), axis, 0, 0, tiled=True
    )


def in_order(pieces, dim):
    pieces = jnp.moveaxis(pieces, 0, dim)
    lengths = pieces.shape
    return pieces.reshape(*lengths[:dim], lengths[dim] * lengths[dim + 1], *lengths[dim + 2 :])


def collect(value, axis, dim):
    pieces = from_everyone(value, axis)
    return in_order(pieces, dim)


def gathered_total(value, axis):
    pieces = lax.all_gather(value, axis).astype(jnp.float32)
    return pieces.sum(axis=0)


def own_block(pieces, axes, order):
    lengths = [lax.axis_size(a) for a in axes]
    pieces = pieces.reshape(*lengths, *pieces.shape[1:])
    pieces = pieces.transpose(*order, *range(len(axes), pieces.ndim))
    pieces = pieces.reshape(-1, *pieces.shape[len(axes) :])
    for k in order:
        pieces = lax.psum_scatter(pieces, axes[k], scatter_dimension=0, tiled=True)
    return pieces[0]


def cut_along(value, dim, length):
    before, after = (value.shape[:dim], value.shape[dim + 1 :])
    return jnp.moveaxis(value.reshape(*before, length, -1, *after), dim, 0)


def summed_rows_2(value, axes, order, dim):
    length = lax.axis_size(axes)
    return own_block(cut_along(value, dim, length), axes, order)


def of_everyone(value, axis):
    return from_everyone(value, axis).astype(jnp.float32).sum(axis=0)


def of_everyone_2(value, axis):
    everything = from_everyone(value, axis)
    return jnp.sum(everything, axis=0)


def half_back(field, carried, gate_w, up_w, down_w):
    scale = lax.rsqrt(jnp.mean(field * field, axis=1, keepdims=True) + eps)
    normed = field * scale
    normed_b = normed.astype(jnp.bfloat16)
    gates, uppers = in_one_piece((gate_w, up_w), FS, 0, 1)
    gate = jnp.dot(normed_b, gates, preferred_element_type=jnp.float32)
    upper = jnp.dot(normed_b, uppers, preferred_element_type=jnp.float32)
    back = 0.5 * lax.dot_general(
        carried,
        collect(down_w, FS, 1),
        (((1,), (1,)), ((), ())),
        preferred_element_type=jnp.float32,
    )
    logistic = jax.nn.sigmoid(gate)
    activated = gate * logistic
    hidden = (activated * upper).astype(jnp.bfloat16)
    d_gate = (back * upper * logistic * (1.0 + gate * (1.0 - logistic))).astype(jnp.bfloat16)
    d_up = (back * activated).astype(jnp.bfloat16)
    dims = (((1,), (1,)), ((), ()))
    partial_sum = lax.dot_general(d_gate, gates, dims, preferred_element_type=jnp.float32)
    partial_sum = partial_sum + lax.dot_general(
        d_up, uppers, dims, preferred_element_type=jnp.float32
    )
    d_normed = gathered_total(partial_sum.astype(jnp.bfloat16), "tp").astype(jnp.float32)
    d_field = carried.astype(jnp.float32) + scale * (
        d_normed - normed * jnp.mean(d_normed * normed, axis=1, keepdims=True)
    )
    return (d_field, hidden)


def on_device(
    tokens,
    mid_tokens,
    out_grad,
    gate_first,
    up_first,
    down_first,
    gate_second,
    up_second,
    down_second,
):
    d_mid, unused = half_back(
        mid_tokens.astype(jnp.float32), out_grad, gate_second, up_second, down_second
    )
    mid_grad = d_mid.astype(jnp.bfloat16)
    d_input, hidden = half_back(
        tokens.astype(jnp.float32), mid_grad, gate_first, up_first, down_first
    )
    share = summed_rows_2(
        (
            0.5
            * lax.dot_general(
                mid_grad, hidden, (((0,), (0,)), ((), ())), preferred_element_type=jnp.float32
            )
        ).astype(jnp.bfloat16),
        FS,
        (1, 0),
        0,
    ).astype(jnp.float32)
    share = of_everyone(share.astype(jnp.bfloat16), "rep").astype(jnp.float32)
    norms = of_everyone_2(jnp.sum(share * share, axis=0), FS)
    return (d_input.astype(jnp.bfloat16), share.T, norms)


def solution(mesh):
    torus = Mesh(
        mesh.devices.reshape(mesh.shape["rep"], 4, 8, mesh.shape["tp"]),
        ("rep", "fs_0", "fs_1", "tp"),
    )
    placed = (
        P(REP_FS, None),
        P(REP_FS, None),
        P(REP_FS, None),
        P(FS, "tp"),
        P(FS, "tp"),
        P("tp", FS),
        P(FS, "tp"),
        P(FS, "tp"),
        P("tp", FS),
    )
    return jax.shard_map(
        on_device,
        mesh=torus,
        in_specs=placed,
        out_specs=(P(REP_FS, None), P("tp", FS), P("tp")),
        check_vma=False,
    )
```

profile of v0, /device:TPU:1, one launch (start us, length us, event | category | flops | bytes accessed | tf_op | source)
XLA Modules:
  0.0 552.2 jit_solution(11396152390987948231)
XLA Ops:
  7.2 0.0 all-gather.7.cloned.1.call-start
  7.2 1.5 pad_maximum_fusion
  8.7 0.0 all-gather.9.cloned.1.call-start
  8.8 1.5 pad_maximum_fusion.1
  10.3 2.3 broadcast_in_dim.10
  12.6 13.7 %all-to-all-start = ((bf16[32,384,64]{1,2,0:T(8,128)(2,1)}), bf16[32,384,64]{1,2,0:T(8,128)(2,1)}, u32[]{:S(2)}, u32[]{:S(2)}) async-start(bf16[32,384,64]{1,2,0:T(8,128)(2,1)} %broadcast_in_dim.10), calls=%async_computation | async-start | bytes 3145728 | tf_op jit(solution)/shard_map/all_to_all | solution.py:25
  26.3 0.0 all-gather.11.cloned.1.call-start
  26.3 0.3 fusion.13
  26.6 41.0 %all-to-all-done = bf16[32,384,64]{1,2,0:T(8,128)(2,1)} async-done(((bf16[32,384,64]{1,2,0:T(8,128)(2,1)}), bf16[32,384,64]{1,2,0:T(8,128)(2,1)}, u32[]{:S(2)}, u32[]{:S(2)}) %all-to-all-start) | async-done | bytes 1572896 | tf_op jit(solution)/shard_map/all_to_all | solution.py:25
  67.6 2.1 convolution_multiply_fusion.1
  69.8 92.2 %all-gather.7.cloned.1.call-done = bf16[2048,768]{1,0:T(8,128)(2,1)} async-done(((bf16[64,768]{1,0:T(8,128)(2,1)}), bf16[2048,768]{1,0:T(8,128)(2,1)}) %all-gather.7.cloned.1.call-update) | async-done | bytes 3145744 | tf_op jit(solution)/shard_map/all_gather | solution.py:16
  162.0 2.2 fusion.29
  164.1 4.7 fusion.27
  168.8 3.8 fusion.6
  172.6 0.0 all-gather.11.cloned.1.call-update
  172.7 1.4 broadcast_in_dim.11
  174.1 5.8 %all-to-all-start.1 = ((bf16[32,384,64]{1,2,0:T(8,128)(2,1)}), bf16[32,384,64]{1,2,0:T(8,128)(2,1)}, u32[]{:S(2)}, u32[]{:S(2)}) async-start(bf16[32,384,64]{1,2,0:T(8,128)(2,1)} %broadcast_in_dim.11), calls=%async_computation.1 | async-start | bytes 3145728 | tf_op jit(solution)/shard_map/all_to_all | solution.py:25
  179.8 0.0 reduce-scatter.3.cloned.1.call-start
  179.9 0.3 fusion.19
  180.2 145.1 %all-gather.9.cloned.1.call-done = bf16[2048,768]{1,0:T(8,128)(2,1)} async-done(((bf16[64,768]{1,0:T(8,128)(2,1)}), bf16[2048,768]{1,0:T(8,128)(2,1)}) %all-gather.9.cloned.1.call-update) | async-done | bytes 3145744 | tf_op jit(solution)/shard_map/all_gather | solution.py:16
  325.3 2.3 fusion.22
  327.6 0.0 copy-done.4
  327.6 1.5 fusion.25
  329.1 69.8 %all-gather.11.cloned.1.call-done = bf16[2048,2048]{1,0:T(8,128)(2,1)} async-done(((bf16[256,2048]{1,0:T(8,128)(2,1)}), bf16[2048,2048]{1,0:T(8,128)(2,1)}) %all-gather.11.cloned.1.call-update) | async-done | bytes 8388624 | tf_op jit(solution)/shard_map/all_gather | solution.py:42
  398.9 5.4 convert_reduce_fusion.1
  404.4 0.4 fusion.8
  404.8 0.8 copy-done.3
  405.6 0.6 fusion.12
  406.2 0.3 copy-done.6
  406.6 0.8 multiply_convert_fusion
  407.4 1.3 copy.16
  408.7 0.0 reduce-scatter.3.cloned.1.call-update
  408.8 0.0 reduce-scatter.5.cloned.1.call-start
  408.8 2.1 convolution_multiply_fusion
  411.0 36.9 %reduce-scatter.3.cloned.1.call-done = bf16[4,64,384]{2,1,0:T(8,128)(2,1)} async-done(((bf16[32,64,384]{2,1,0:T(8,128)(2,1)}), bf16[4,64,384]{2,1,0:T(8,128)(2,1)}) %reduce-scatter.3.cloned.1.call-update) | async-done | bytes 196624 | tf_op jit(solution)/shard_map/reduce_scatter | solution.py:52
  447.9 0.2 all-gather.13.cloned.1.call-start
  448.2 2.3 fusion.20
  450.5 1.7 fusion.7
  452.3 0.0 all-gather.13.cloned.1.call-update
  452.3 26.7 %reduce-scatter.5.cloned.1.call-done = bf16[1,64,384]{2,1,0:T(8,128)(2,1)} async-done(((bf16[4,64,384]{2,1,0:T(8,128)(2,1)}), bf16[1,64,384]{2,1,0:T(8,128)(2,1)}) %reduce-scatter.5.cloned.1.call-update) | async-done | bytes 49168 | tf_op jit(solution)/shard_map/reduce_scatter | solution.py:52
  479.0 0.8 broadcast_in_dim.13
  479.8 11.8 %all_to_all.21 = bf16[2,64,384]{2,1,0:T(8,128)(2,1)S(1)} all-to-all(bf16[2,64,384]{2,1,0:T(8,128)(2,1)S(1)} %broadcast_in_dim.13), channel_id=1, replica_groups=mesh['rep'=2,'fs_0'=4,'fs_1'=8,'tp'=8] {'rep'}, dimensions={0} | all-to-all | bytes 196608 | tf_op jit(solution)/shard_map/all_to_all | solution.py:25
  491.7 17.5 %all_to_all.22 = f32[32,1,384]{2,1,0:T(1,128)S(1)} all-to-all(f32[32,1,384]{2,1,0:T(1,128)S(1)} %broadcast_in_dim.14), channel_id=1, replica_groups=mesh['rep'=2,'fs_0'=4,'fs_1'=8,'tp'=8] {'fs_0','fs_1'}, dimensions={0} | all-to-all | bytes 98304 | tf_op jit(solution)/shard_map/all_to_all | solution.py:25
  509.2 0.6 reduce_sum.89
  509.8 28.1 %all-gather.13.cloned.1.call-done = bf16[2048,2048]{1,0:T(8,128)(2,1)} async-done(((bf16[256,2048]{1,0:T(8,128)(2,1)}), bf16[2048,2048]{1,0:T(8,128)(2,1)}) %all-gather.13.cloned.1.call-update) | async-done | bytes 8388624 | tf_op jit(solution)/shard_map/all_gather | solution.py:42
  537.9 5.4 convert_reduce_fusion
  543.4 0.4 fusion.14
  543.8 1.6 fusion.18
  (28 shorter events, 0.2 us)
Async XLA Ops:
  7.2 154.8 %all-gather.7.cloned.1.call-start = ((), (), s32[]{:S(2)}) async-start(), calls=%async_computation.6 | async-start | bytes 3244032 | tf_op jit(solution)/shard_map/all_gather | solution.py:16
  8.7 316.5 %all-gather.9.cloned.1.call-start = ((), (), s32[]{:S(2)}) async-start(), calls=%async_computation.7 | async-start | bytes 3244032 | tf_op jit(solution)/shard_map/all_gather | solution.py:16
  10.3 16.1 %copy-start = (bf16[256,2048]{1,0:T(8,128)(2,1)S(1)}, bf16[256,2048]{1,0:T(8,128)(2,1)}, u32[]{:S(2)}) copy-start(bf16[256,2048]{1,0:T(8,128)(2,1)} %param.10) | copy-start | bytes 3145732
  12.6 55.1 %copy-start.2 = (bf16[256,2048]{1,0:T(8,128)(2,1)S(1)}, bf16[256,2048]{1,0:T(8,128)(2,1)}, u32[]{:S(2)}) copy-start(bf16[256,2048]{1,0:T(8,128)(2,1)} %param.11) | copy-start | bytes 3145732
  12.6 55.1 %all-to-all-start = ((bf16[32,384,64]{1,2,0:T(8,128)(2,1)}), bf16[32,384,64]{1,2,0:T(8,128)(2,1)}, u32[]{:S(2)}, u32[]{:S(2)}) async-start(bf16[32,384,64]{1,2,0:T(8,128)(2,1)} %broadcast_in_dim.10), calls=%async_computation | async-start | bytes 3145728 | tf_op jit(solution)/shard_map/all_to_all | solution.py:25
  26.3 372.7 %all-gather.11.cloned.1.call-start = ((), (), s32[]{:S(2)}) async-start(), calls=%async_computation.10 | async-start | bytes 9437184 | tf_op jit(solution)/shard_map/all_gather | solution.py:42
  168.8 3.8 copy-start.9
  172.7 7.2 %copy-start.1 = (bf16[256,2048]{1,0:T(8,128)(2,1)S(1)}, bf16[256,2048]{1,0:T(8,128)(2,1)}, u32[]{:S(2)}) copy-start(bf16[256,2048]{1,0:T(8,128)(2,1)} %param.9) | copy-start | bytes 3145732
  174.1 234.7 %all-to-all-start.1 = ((bf16[32,384,64]{1,2,0:T(8,128)(2,1)}), bf16[32,384,64]{1,2,0:T(8,128)(2,1)}, u32[]{:S(2)}, u32[]{:S(2)}) async-start(bf16[32,384,64]{1,2,0:T(8,128)(2,1)} %broadcast_in_dim.11), calls=%async_computation.1 | async-start | bytes 3145728 | tf_op jit(solution)/shard_map/all_to_all | solution.py:25
  179.8 268.1 %reduce-scatter.3.cloned.1.call-start = ((), (), s32[]{:S(2)}) async-start(), calls=%async_computation.8 | async-start | bytes 1769472 | tf_op jit(solution)/shard_map/reduce_scatter | solution.py:52
  325.3 2.4 copy-start.4
  404.3 1.2 copy-start.3
  405.6 1.0 copy-start.6
  408.7 39.4 %copy-start.7 = (f32[256,384]{1,0:T(8,128)S(1)}, f32[256,384]{1,0:T(8,128)}, u32[]{:S(2)}) copy-start(f32[256,384]{1,0:T(8,128)} %fusion.25) | copy-start | bytes 1179652
  408.8 70.3 %reduce-scatter.5.cloned.1.call-start = ((), (), s32[]{:S(2)}) async-start(), calls=%async_computation.9 | async-start | bytes 245760 | tf_op jit(solution)/shard_map/reduce_scatter | solution.py:52
  447.9 90.0 %all-gather.13.cloned.1.call-start = ((), (), s32[]{:S(2)}) async-start(), calls=%async_computation.11 | async-start | bytes 9437184 | tf_op jit(solution)/shard_map/all_gather | solution.py:42
  448.2 2.4 copy-start.5
  491.6 51.7 %copy-start.8 = (f32[64,384]{1,0:T(8,128)}, f32[64,384]{1,0:T(8,128)S(1)}, u32[]{:S(2)}) copy-start(f32[64,384]{1,0:T(8,128)S(1)} %convert_reduce_fusion.2) | copy-start | bytes 294916
Sparse Core Ops, SparseCore 0:
  10.6 151.2 all-gather.6
  164.6 160.5 all-gather.8
  328.0 70.9 all-gather.10
  408.9 38.9 reduce-scatter.2
  450.6 28.4 reduce-scatter.4
  481.6 56.2 all-gather.12
where the time goes:
time: 553 us; the launch traced here: 552 us
  waiting for transfers between devices  440 us (80%)
  blocking collectives  29.2 us (5%)
  matrix products  23.6 us (4%)
  starting transfers between devices  19.9 us (4%)
  other arithmetic  18.2 us (3%)
  between operations  14.3 us (3%)
  local copies, waits for them, and re-layouts  7.05 us (1%)
    all_gather x2, waiting for transfers between devices, in_one_piece(): filled, at, done = (lax.all_gather(both, axis, axis=dim, tiled=True), 0, [])  237 us
    all_gather x2, waiting for transfers between devices, gathered_total(): pieces = lax.all_gather(value, axis).astype(jnp.float32)  97.9 us
    reduce_scatter x2, waiting for transfers between devices, own_block(): pieces = lax.psum_scatter(pieces, axes[k], scatter_dimension=0, tiled=True)  63.7 us
    all_to_all x2, waiting for transfers between devices, from_everyone(): lax.all_to_all(jnp.broadcast_to(value[None], (length, *value.shape)), axi...  41 us
    all_to_all x2, blocking collectives, from_everyone(): lax.all_to_all(jnp.broadcast_to(value[None], (length, *value.shape)), axi...  29.2 us
    all_to_all x2, starting transfers between devices, from_everyone(): lax.all_to_all(jnp.broadcast_to(value[None], (length, *value.shape)), axi...  19.5 us
  transfers between devices with their start and end apart: 8, of which 7 were waited for; matrix products, arithmetic and copies ran while one was open for 7% of the time, Pallas kernels for 0%

commit v1 on v0

v1 whole, which is shorter than its diff:
```python
import jax
import jax.numpy as jnp
from jax import lax
from jax.sharding import Mesh
from jax.sharding import PartitionSpec as P

FS = ("fs_0", "fs_1")
Z = ("rep", "fs_0")
REP_FS = ("rep", "fs_0", "fs_1")
f32 = jnp.float32
bf16 = jnp.bfloat16

eps = 1e-06


def take_from(value, axis, step):
    n = lax.axis_size(axis)
    return lax.ppermute(value, axis, [((i + step) % n, i) for i in range(n)])


def from_everyone(value, axis):
    n = lax.axis_size(axis)
    return lax.all_to_all(
        jnp.broadcast_to(value[None], (n, *value.shape)), axis, 0, 0, tiled=True
    )


def along_y(value):
    whole = from_everyone(value, "fs_1")
    return whole.reshape(-1, value.shape[1])


def along_z(value):
    half = value.shape[0] // 2
    after = take_from(value, Z, 1)
    before = take_from(value, Z, -1)
    top = take_from(after[:half], Z, 1)
    bottom = take_from(before[half:], Z, -1)
    return ((0, 0, value), (1, 0, after), (3, 0, before), (2, 0, top), (2, half, bottom))


def columns(x, z, piece):
    m, first, w = piece
    span = x.shape[1] // 4
    start = ((z + m) % 4) * span + first
    return lax.dynamic_slice_in_dim(x, start, w.shape[0], axis=1)


def contract(x, z, pieces):
    total = None
    for piece in pieces:
        part = jnp.dot(columns(x, z, piece), piece[2], preferred_element_type=f32)
        total = part if total is None else total + part
    return total


def spread(x, z, pieces):
    dims = (((1,), (1,)), ((), ()))
    out = {
        (m, first): lax.dot_general(x, w, dims, preferred_element_type=f32).astype(bf16)
        for m, first, w in pieces
    }
    half = pieces[3][2].shape[0]
    rel = jnp.concatenate(
        [out[0, 0], out[1, 0], out[2, 0], out[2, half], out[3, 0]], axis=1
    )
    return jnp.roll(rel, z * (2 * half), axis=1)


def swap_cores(value):
    return lax.ppermute(value, "tp", [(i, i ^ 1) for i in range(lax.axis_size("tp"))])


def take_x(value, step):
    n = lax.axis_size("tp")
    return lax.ppermute(value, "tp", [((i + 2 * step) % n, i) for i in range(n)])


def own_rows(partial, core, x):
    rows = partial.shape[0]
    other = lax.dynamic_slice_in_dim(partial, (1 - core) * (rows // 2), rows // 2, axis=0)
    mine = lax.dynamic_slice_in_dim(partial, core * (rows // 2), rows // 2, axis=0)
    chip = (mine.astype(f32) + swap_cores(other).astype(f32)).astype(bf16)
    n = rows // 8

    def block(j):
        return lax.dynamic_slice_in_dim(chip, ((x + j) % 4) * n, n, axis=0)

    total = block(0).astype(f32)
    for j in (1, 3, 2):
        total = total + take_x(block(j), -j).astype(f32)
    return total


def all_rows(value, core, x):
    n = value.shape[0]
    quarter = jnp.concatenate([value] + [take_x(value, j) for j in (1, 2, 3)], axis=0)
    half = jnp.roll(quarter, x * n, axis=0)
    other = swap_cores(half)
    both = jnp.concatenate([half, other], axis=0)
    return jnp.roll(both, core * (4 * n), axis=0)


def half_back(u, c, z, core, x, gate_up, down):
    field = u.astype(f32)
    scale = lax.rsqrt(jnp.mean(field * field, axis=1, keepdims=True) + eps)
    normed_b = (field * scale).astype(bf16)
    both = contract(normed_b, z, gate_up)
    n = both.shape[1] // 2
    gate, upper = both[:, :n], both[:, n:]
    back = 0.5 * contract(c, z, down)
    logistic = jax.nn.sigmoid(gate)
    activated = gate * logistic
    hidden = (activated * upper).astype(bf16)
    d_gate = (back * upper * logistic * (1.0 + gate * (1.0 - logistic))).astype(bf16)
    d_up = (back * activated).astype(bf16)
    partial = spread(jnp.concatenate([d_gate, d_up], axis=1), z, gate_up)
    rows = u.shape[0] // 8
    start = core * (4 * rows) + x * rows
    d_normed = own_rows(partial, core, x)
    field = lax.dynamic_slice_in_dim(u, start, rows, axis=0).astype(f32)
    scale = lax.rsqrt(jnp.mean(field * field, axis=1, keepdims=True) + eps)
    normed = field * scale
    carried = lax.dynamic_slice_in_dim(c, start, rows, axis=0).astype(f32)
    d_field = carried + scale * (
        d_normed - normed * jnp.mean(d_normed * normed, axis=1, keepdims=True)
    )
    return all_rows(d_field.astype(bf16), core, x), hidden


def down_share(hidden, grad, z):
    span = grad.shape[1] // 4
    half = span // 2

    def part(m):
        cols = lax.dynamic_slice_in_dim(grad, ((z + m) % 4) * span, span, axis=1)
        return 0.5 * lax.dot_general(
            cols, hidden, (((0,), (0,)), ((), ())), preferred_element_type=f32
        )

    far = part(2).astype(bf16)
    top = take_from(far[:half], Z, -1).astype(f32)
    bottom = take_from(far[half:], Z, 1).astype(f32)
    after = part(1)
    before = part(3)
    after = jnp.concatenate([after[:half] + top, after[half:]], axis=0).astype(bf16)
    before = jnp.concatenate([before[:half], before[half:] + bottom], axis=0).astype(bf16)
    column = part(0) + take_from(after, Z, -1).astype(f32) + take_from(before, Z, 1).astype(f32)
    column = column.astype(bf16).reshape(lax.axis_size("fs_1"), -1, hidden.shape[1])
    share = lax.all_to_all(column, "fs_1", 0, 0, tiled=True).astype(f32).sum(axis=0)
    share = share.astype(bf16)
    return share.astype(f32) + take_from(share, "rep", 1).astype(f32)


def on_device(
    tokens,
    mid_tokens,
    out_grad,
    gate_first,
    up_first,
    down_first,
    gate_second,
    up_second,
    down_second,
):
    z = lax.axis_index("fs_0")
    tp = lax.axis_index("tp")
    core, x = tp % 2, tp // 2
    gate_up_2 = along_z(along_y(jnp.concatenate([gate_second, up_second], axis=1)))
    down_2 = along_z(along_y(down_second.T))
    gate_up_1 = along_z(along_y(jnp.concatenate([gate_first, up_first], axis=1)))
    down_1 = along_z(along_y(down_first.T))
    mid_grad, _ = half_back(mid_tokens, out_grad, z, core, x, gate_up_2, down_2)
    input_grad, hidden = half_back(tokens, mid_grad, z, core, x, gate_up_1, down_1)
    share = down_share(hidden, mid_grad, z)
    norms = from_everyone(jnp.sum(share * share, axis=0), FS).sum(axis=0)
    return (input_grad, share.T, norms)


def solution(mesh):
    torus = Mesh(
        mesh.devices.reshape(mesh.shape["rep"], 4, 8, mesh.shape["tp"]),
        ("rep", "fs_0", "fs_1", "tp"),
    )
    placed = (
        P(REP_FS, None),
        P(REP_FS, None),
        P(REP_FS, None),
        P(FS, "tp"),
        P(FS, "tp"),
        P("tp", FS),
        P(FS, "tp"),
        P(FS, "tp"),
        P("tp", FS),
    )
    return jax.shard_map(
        on_device,
        mesh=torus,
        in_specs=placed,
        out_specs=(P(REP_FS, None), P("tp", FS), P("tp")),
        check_vma=False,
    )
```

time: 553 us -> 317 us (0.57)
  waiting for transfers between devices: 440 us -> 53.5 us
  starting transfers between devices: 19.9 us -> 170 us
  between operations: 14.3 us -> 1.85 us
  matrix products: 23.6 us -> 33.7 us
  local copies, waits for them, and re-layouts: 7.05 us -> 16.3 us
  blocking collectives: 29.2 us -> 20 us
    all_gather x4 -> x0, waiting for transfers between devices: 335 us -> none  [the longest x2 237 us: in_one_piece(): filled, at, done = (lax.all_gather(both, axis, axis=dim, tiled=True), 0, [])]
    ppermute x0 -> x37, starting transfers between devices: none -> 140 us  [the longest x21 84.6 us: take_from(): return lax.ppermute(value, axis, [((i + step) % n, i) for i in range(n)])]
    reduce_scatter x2 -> x0, waiting for transfers between devices: 63.7 us -> none  [own_block(): pieces = lax.psum_scatter(pieces, axes[k], scatter_dimension=0, tiled=True)]
    ppermute x0 -> x37, waiting for transfers between devices: none -> 33.7 us  [the longest x21 27.2 us: take_from(): return lax.ppermute(value, axis, [((i + step) % n, i) for i in range(n)])]
    all_to_all x2 -> x5, waiting for transfers between devices: 41 us -> 19.8 us  [the longest x4 19.8 us: from_everyone(): lax.all_to_all(jnp.broadcast_to(value[None], (n, *value.shape)), axis, 0,...]
    all_to_all x2 -> x5, starting transfers between devices: 19.5 us -> 29.6 us  [the longest x4 23.1 us: from_everyone(): lax.all_to_all(jnp.broadcast_to(value[None], (n, *value.shape)), axis, 0,...]
    reduce_sum x5 -> x3, other arithmetic: 11.5 us -> 1.36 us  [the longest x2 1.3 us: on_device(): norms = from_everyone(jnp.sum(share * share, axis=0), FS).sum(axis=0)]
    dot_general x10 -> x34, matrix products: 23.6 us -> 33.7 us  [the longest x20 21.8 us: contract(): part = jnp.dot(columns(x, z, piece), piece[2], preferred_element_type=f32)]
  transfers between devices with their start and end apart: 8 -> 42, of which waited for: 7 -> 13; matrix products, arithmetic and copies ran while one was open for 7% -> 19% of each run, Pallas kernels for 0% -> 0%
where the time goes in v1:
time: 317 us; the launch traced here: 315 us
  starting transfers between devices  170 us (54%)
  waiting for transfers between devices  53.5 us (17%)
  matrix products  33.7 us (11%)
  blocking collectives  20 us (6%)
  other arithmetic  19.5 us (6%)
  local copies, waits for them, and re-layouts  16.3 us (5%)
    ppermute x21, starting transfers between devices, take_from(): return lax.ppermute(value, axis, [((i + step) % n, i) for i in range(n)])  84.6 us
    ppermute x12, starting transfers between devices, take_x(): lax.ppermute(value, 'tp', [((i + 2 * step) % n, i) for i in range(n)])  36.3 us
    ppermute x21, waiting for transfers between devices, take_from(): return lax.ppermute(value, axis, [((i + step) % n, i) for i in range(n)])  27.2 us
    all_to_all x4, starting transfers between devices, from_everyone(): lax.all_to_all(jnp.broadcast_to(value[None], (n, *value.shape)), axis, 0,...  23.1 us
    dot_general x20, matrix products, contract(): part = jnp.dot(columns(x, z, piece), piece[2], preferred_element_type=f32)  21.8 us
    all_to_all x1, blocking collectives, from_everyone(): lax.all_to_all(jnp.broadcast_to(value[None], (n, *value.shape)), axis, 0,...  20 us
    all_to_all x4, waiting for transfers between devices, from_everyone(): lax.all_to_all(jnp.broadcast_to(value[None], (n, *value.shape)), axis, 0,...  19.8 us
    ppermute x4, starting transfers between devices, swap_cores(): lax.ppermute(value, 'tp', [(i, i ^ 1) for i in range(lax.axis_size('tp'))])  19.2 us
  transfers between devices with their start and end apart: 42, of which 13 were waited for; matrix products, arithmetic and copies ran while one was open for 19% of the time, Pallas kernels for 0%

profile of v1, /device:TPU:1, one launch (start us, length us, event | category | flops | bytes accessed | tf_op | source)
XLA Modules:
  0.0 314.6 jit_solution(16601042618215085049)
XLA Ops:
  1.5 20.0 %all_to_all.31 = bf16[8,64,384]{2,1,0:T(8,128)(2,1)S(1)} all-to-all(bf16[8,64,384]{2,1,0:T(8,128)(2,1)S(1)} %broadcast_in_dim.10), channel_id=1, replica_groups=mesh['rep'=2,'fs_0'=4,'fs_1'=8,'tp'=8] {'fs_1'}, dimensions={0} | all-to-all | bytes 786432 | tf_op jit(solution)/shard_map/all_to_all | solution.py:23
  23.2 3.5 %all-to-all-start.2 = ((bf16[8,64,384]{2,1,0:T(8,128)(2,1)}), bf16[8,64,384]{2,1,0:T(8,128)(2,1)S(1)}, u32[]{:S(2)}, u32[]{:S(2)}) async-start(bf16[8,64,384]{2,1,0:T(8,128)(2,1)} %broadcast_in_dim.12), calls=%async_computation.2 | async-start | bytes 786432 | tf_op jit(solution)/shard_map/all_to_all | solution.py:23
  26.7 10.5 %all-to-all-done.2 = bf16[8,64,384]{2,1,0:T(8,128)(2,1)S(1)} async-done(((bf16[8,64,384]{2,1,0:T(8,128)(2,1)}), bf16[8,64,384]{2,1,0:T(8,128)(2,1)S(1)}, u32[]{:S(2)}, u32[]{:S(2)}) %all-to-all-start.2) | async-done | bytes 393248 | tf_op jit(solution)/shard_map/all_to_all | solution.py:23
  38.2 4.2 %all-to-all-start.1 = ((bf16[8,64,768]{2,1,0:T(8,128)(2,1)}), bf16[8,64,768]{2,1,0:T(8,128)(2,1)}, u32[]{:S(2)}, u32[]{:S(2)}) async-start(bf16[8,64,768]{2,1,0:T(8,128)(2,1)} %broadcast_in_dim.11), calls=%async_computation.1 | async-start | bytes 1572864 | tf_op jit(solution)/shard_map/all_to_all | solution.py:23
  44.0 6.8 %collective-permute-start.1 = (bf16[512,384]{1,0:T(8,128)(2,1)S(1)}, bf16[512,384]{1,0:T(8,128)(2,1)}, u32[]{:S(2)}, u32[]{:S(2)}) collective-permute-start(bf16[512,384]{1,0:T(8,128)(2,1)S(1)} %bitcast.43), channel_id=1, source_target_pairs={{448,0},{0,64},{64,128},{128,192},{192,256},{256,320},{320,384},{3... | collective-permute-start | bytes 1179656 | tf_op jit(solution)/shard_map/ppermute | solution.py:18
  50.7 8.6 %collective-permute-start = (bf16[512,384]{1,0:T(8,128)(2,1)S(1)}, bf16[512,384]{1,0:T(8,128)(2,1)}, u32[]{:S(2)}, u32[]{:S(2)}) collective-permute-start(bf16[512,384]{1,0:T(8,128)(2,1)S(1)} %bitcast.44), channel_id=1, source_target_pairs={{64,0},{128,64},{192,128},{256,192},{320,256},{384,320},{448,384},... | collective-permute-start | bytes 1179656 | tf_op jit(solution)/shard_map/ppermute | solution.py:18
  59.3 2.9 all-to-all-done.1
  64.1 4.2 %all-to-all-start.3 = ((bf16[8,64,768]{2,1,0:T(8,128)(2,1)}), bf16[8,64,768]{2,1,0:T(8,128)(2,1)}, u32[]{:S(2)}, u32[]{:S(2)}) async-start(bf16[8,64,768]{2,1,0:T(8,128)(2,1)} %broadcast_in_dim.13), calls=%async_computation.3 | async-start | bytes 1572864 | tf_op jit(solution)/shard_map/all_to_all | solution.py:23
  69.6 7.5 %collective-permute-start.17 = (bf16[512,384]{1,0:T(8,128)(2,1)}, bf16[512,384]{1,0:T(8,128)(2,1)}, u32[]{:S(2)}, u32[]{:S(2)}) collective-permute-start(bf16[512,384]{1,0:T(8,128)(2,1)} %bitcast.47), channel_id=1, source_target_pairs={{448,0},{0,64},{64,128},{128,192},{192,256},{256,320},{320,384},{3... | collective-permute-start | bytes 1179656 | tf_op jit(solution)/shard_map/ppermute | solution.py:18
  77.1 8.6 %collective-permute-start.16 = (bf16[512,384]{1,0:T(8,128)(2,1)}, bf16[512,384]{1,0:T(8,128)(2,1)}, u32[]{:S(2)}, u32[]{:S(2)}) collective-permute-start(bf16[512,384]{1,0:T(8,128)(2,1)} %bitcast.48), channel_id=1, source_target_pairs={{64,0},{128,64},{192,128},{256,192},{320,256},{384,320},{448,384},... | collective-permute-start | bytes 1179656 | tf_op jit(solution)/shard_map/ppermute | solution.py:18
  91.8 4.6 %collective-permute-start.4 = (bf16[512,768]{1,0:T(8,128)(2,1)}, bf16[512,768]{1,0:T(8,128)(2,1)}, u32[]{:S(2)}, u32[]{:S(2)}) collective-permute-start(bf16[512,768]{1,0:T(8,128)(2,1)} %bitcast.2), channel_id=1, source_target_pairs={{64,0},{128,64},{192,128},{256,192},{320,256},{384,320},{448,384},... | collective-permute-start | bytes 2359304 | tf_op jit(solution)/shard_map/ppermute | solution.py:18
  96.4 2.1 convolution_add_fusion.6
  99.5 12.9 %collective-permute-done.3 = bf16[256,384]{1,0:T(8,128)(2,1)S(1)} collective-permute-done((bf16[256,384]{1,0:T(8,128)(2,1)S(1)}, bf16[256,384]{1,0:T(8,128)(2,1)S(1)}, u32[]{:S(2)}, u32[]{:S(2)}) %collective-permute-start.3) | collective-permute-done | bytes 196640 | tf_op jit(solution)/shard_map/ppermute | solution.py:18
  112.4 2.7 collective-permute-start.2
  116.2 2.6 collective-permute-done.2
  124.3 2.4 fusion.79
  126.6 2.6 collective-permute-start.21
  130.3 4.0 %collective-permute-start.6 = (bf16[256,768]{1,0:T(8,128)(2,1)S(1)}, bf16[256,768]{1,0:T(8,128)(2,1)S(1)}, u32[]{:S(2)}, u32[]{:S(2)}) collective-permute-start(bf16[256,768]{1,0:T(8,128)(2,1)S(1)} %slice.76), channel_id=1, source_target_pairs={{64,0},{128,64},{192,128},{256,192},{320,256},{384,320},{448,384},... | collective-permute-start | bytes 1179656 | tf_op jit(solution)/shard_map/ppermute | solution.py:18
  148.8 6.6 %collective-permute-start.8 = (bf16[128,2048]{1,0:T(8,128)(2,1)}, bf16[128,2048]{1,0:T(8,128)(2,1)}, u32[]{:S(2)}, u32[]{:S(2)}) collective-permute-start(bf16[128,2048]{1,0:T(8,128)(2,1)} %fusion.48), channel_id=1, source_target_pairs={{0,1},{1,0},{2,3},{3,2},{4,5},{5,4},{6,7},{7,6},{8,9},{9,8},{10,11... | collective-permute-start | bytes 1572872 | tf_op jit(solution)/shard_map/ppermute | solution.py:71
  156.7 3.5 %collective-permute-start.19 = (bf16[256,384]{1,0:T(8,128)(2,1)S(1)}, bf16[256,384]{1,0:T(8,128)(2,1)S(1)}, u32[]{:S(2)}, u32[]{:S(2)}) collective-permute-start(bf16[256,384]{1,0:T(8,128)(2,1)S(1)} %slice.81), channel_id=1, source_target_pairs={{448,0},{0,64},{64,128},{128,192},{192,256},{256,320},{320,384},{3... | collective-permute-start | bytes 589832 | tf_op jit(solution)/shard_map/ppermute | solution.py:18
  161.1 3.8 %collective-permute-start.20 = (bf16[512,768]{1,0:T(8,128)(2,1)}, bf16[512,768]{1,0:T(8,128)(2,1)S(1)}, u32[]{:S(2)}, u32[]{:S(2)}) collective-permute-start(bf16[512,768]{1,0:T(8,128)(2,1)} %bitcast.5), channel_id=1, source_target_pairs={{64,0},{128,64},{192,128},{256,192},{320,256},{384,320},{448,384},... | collective-permute-start | bytes 2359304 | tf_op jit(solution)/shard_map/ppermute | solution.py:18
  171.3 4.6 %collective-permute-start.11 = (bf16[32,2048]{1,0:T(8,128)(2,1)S(1)}, bf16[32,2048]{1,0:T(8,128)(2,1)S(1)}, u32[]{:S(2)}, u32[]{:S(2)}) collective-permute-start(bf16[32,2048]{1,0:T(8,128)(2,1)S(1)} %get-tuple-element.15), channel_id=1, source_target_pairs={{4,0},{5,1},{6,2},{7,3},{0,4},{1,5},{2,6},{3,7},{12,8},{13,9},{14,... | collective-permute-start | bytes 393224 | tf_op jit(solution)/shard_map/ppermute | solution.py:76
  176.0 2.8 collective-permute-start.10
  178.7 3.8 %collective-permute-done.20 = bf16[512,768]{1,0:T(8,128)(2,1)S(1)} collective-permute-done((bf16[512,768]{1,0:T(8,128)(2,1)}, bf16[512,768]{1,0:T(8,128)(2,1)S(1)}, u32[]{:S(2)}, u32[]{:S(2)}) %collective-permute-start.20) | collective-permute-done | bytes 786464 | tf_op jit(solution)/shard_map/ppermute | solution.py:18
  182.6 3.1 collective-permute-start.9
  186.1 4.7 %collective-permute-start.22 = (bf16[256,768]{1,0:T(8,128)(2,1)S(1)}, bf16[256,768]{1,0:T(8,128)(2,1)S(1)}, u32[]{:S(2)}, u32[]{:S(2)}) collective-permute-start(bf16[256,768]{1,0:T(8,128)(2,1)S(1)} %slice.82), channel_id=1, source_target_pairs={{64,0},{128,64},{192,128},{256,192},{320,256},{384,320},{448,384},... | collective-permute-start | bytes 1179656 | tf_op jit(solution)/shard_map/ppermute | solution.py:18
  192.2 3.4 %collective-permute-start.12 = (bf16[32,2048]{1,0:T(8,128)(2,1)S(1)}, bf16[32,2048]{1,0:T(8,128)(2,1)S(1)}, u32[]{:S(2)}, u32[]{:S(2)}) collective-permute-start(bf16[32,2048]{1,0:T(8,128)(2,1)S(1)} %fusion.69), channel_id=1, source_target_pairs={{2,0},{3,1},{4,2},{5,3},{6,4},{7,5},{0,6},{1,7},{10,8},{11,9},{12,... | collective-permute-start | bytes 393224 | tf_op jit(solution)/shard_map/ppermute | solution.py:76
  195.6 3.4 %collective-permute-start.13 = (bf16[32,2048]{1,0:T(8,128)(2,1)S(1)}, bf16[32,2048]{1,0:T(8,128)(2,1)S(1)}, u32[]{:S(2)}, u32[]{:S(2)}) collective-permute-start(bf16[32,2048]{1,0:T(8,128)(2,1)S(1)} %fusion.69), channel_id=1, source_target_pairs={{4,0},{5,1},{6,2},{7,3},{0,4},{1,5},{2,6},{3,7},{12,8},{13,9},{14,... | collective-permute-start | bytes 393224 | tf_op jit(solution)/shard_map/ppermute | solution.py:76
  199.0 2.2 collective-permute-start.14
  201.5 2.9 collective-permute-start.18
  204.5 2.2 collective-permute-done.14
  208.2 4.3 %collective-permute-start.15 = (bf16[128,2048]{1,0:T(8,128)(2,1)S(1)}, bf16[128,2048]{1,0:T(8,128)(2,1)S(1)}, u32[]{:S(2)}, u32[]{:S(2)}) collective-permute-start(bf16[128,2048]{1,0:T(8,128)(2,1)S(1)} %fusion.42), channel_id=1, source_target_pairs={{0,1},{1,0},{2,3},{3,2},{4,5},{5,4},{6,7},{7,6},{8,9},{9,8},{10,11... | collective-permute-start | bytes 1572872 | tf_op jit(solution)/shard_map/ppermute | solution.py:71
  226.3 2.8 collective-permute-start.34
  229.7 2.4 collective-permute-start.32
  234.3 4.1 %collective-permute-start.35 = (bf16[512,384]{1,0:T(8,128)(2,1)S(1)}, bf16[512,384]{1,0:T(8,128)(2,1)S(1)}, u32[]{:S(2)}, u32[]{:S(2)}) collective-permute-start(bf16[512,384]{1,0:T(8,128)(2,1)S(1)} %pad_maximum_fusion.3), channel_id=1, source_target_pairs={{64,0},{128,64},{192,128},{256,192},{320,256},{384,320},{448,384},... | collective-permute-start | bytes 1179656 | tf_op jit(solution)/shard_map/ppermute | solution.py:18
  243.8 3.1 collective-permute-start.27
  246.9 2.5 collective-permute-start.26
  249.3 2.8 collective-permute-start.25
  253.4 6.5 %all-to-all-start.4 = ((bf16[8,64,384]{2,1,0:T(8,128)(2,1)}), bf16[8,64,384]{2,1,0:T(8,128)(2,1)S(1)}, u32[]{:S(2)}, u32[]{:S(2)}) async-start(bf16[8,64,384]{2,1,0:T(8,128)(2,1)} %bitcast.46), calls=%async_computation.4 | async-start | bytes 786432 | tf_op jit(solution)/shard_map/all_to_all | solution.py:150
  262.6 3.7 %collective-permute-start.28 = (bf16[32,2048]{1,0:T(8,128)(2,1)S(1)}, bf16[32,2048]{1,0:T(8,128)(2,1)S(1)}, u32[]{:S(2)}, u32[]{:S(2)}) collective-permute-start(bf16[32,2048]{1,0:T(8,128)(2,1)S(1)} %fusion.64), channel_id=1, source_target_pairs={{2,0},{3,1},{4,2},{5,3},{6,4},{7,5},{0,6},{1,7},{10,8},{11,9},{12,... | collective-permute-start | bytes 393224 | tf_op jit(solution)/shard_map/ppermute | solution.py:76
  268.4 2.6 collective-permute-start.30
  271.0 2.5 collective-permute-done.29
  276.8 6.3 %collective-permute-start.31 = (bf16[128,2048]{1,0:T(8,128)(2,1)S(1)}, bf16[128,2048]{1,0:T(8,128)(2,1)S(1)}, u32[]{:S(2)}, u32[]{:S(2)}) collective-permute-start(bf16[128,2048]{1,0:T(8,128)(2,1)S(1)} %fusion.35), channel_id=1, source_target_pairs={{0,1},{1,0},{2,3},{3,2},{4,5},{5,4},{6,7},{7,6},{8,9},{9,8},{10,11... | collective-permute-start | bytes 1572872 | tf_op jit(solution)/shard_map/ppermute | solution.py:71
  283.3 5.4 %collective-permute-start.36 = (bf16[64,384]{1,0:T(8,128)(2,1)S(1)}, bf16[64,384]{1,0:T(8,128)(2,1)S(1)}, u32[]{:S(2)}, u32[]{:S(2)}) collective-permute-start(bf16[64,384]{1,0:T(8,128)(2,1)S(1)} %reduce_sum.90), channel_id=1, source_target_pairs={{256,0},{0,256},{257,1},{1,257},{258,2},{2,258},{259,3},{3,259},{2... | collective-permute-start | bytes 147464 | tf_op jit(solution)/shard_map/ppermute | solution.py:18
  288.7 3.7 %collective-permute-done.36 = bf16[64,384]{1,0:T(8,128)(2,1)S(1)} collective-permute-done((bf16[64,384]{1,0:T(8,128)(2,1)S(1)}, bf16[64,384]{1,0:T(8,128)(2,1)S(1)}, u32[]{:S(2)}, u32[]{:S(2)}) %collective-permute-start.36) | collective-permute-done | bytes 49184 | tf_op jit(solution)/shard_map/ppermute | solution.py:18
  293.6 11.2 %all-to-all-start.5 = ((f32[32,1,384]{2,1,0:T(1,128)}), f32[32,1,384]{2,1,0:T(1,128)S(1)}, u32[]{:S(2)}, u32[]{:S(2)}) async-start(f32[32,1,384]{2,1,0:T(1,128)} %broadcast_in_dim.14), calls=%async_computation.5 | async-start | bytes 98304 | tf_op jit(solution)/shard_map/all_to_all | solution.py:23
  304.9 2.7 fusion.30
  307.6 6.3 %all-to-all-done.5 = f32[32,1,384]{2,1,0:T(1,128)S(1)} async-done(((f32[32,1,384]{2,1,0:T(1,128)}), f32[32,1,384]{2,1,0:T(1,128)S(1)}, u32[]{:S(2)}, u32[]{:S(2)}) %all-to-all-start.5) | async-done | bytes 49184 | tf_op jit(solution)/shard_map/all_to_all | solution.py:23
  (148 shorter events, 82.1 us)
Async XLA Ops:
  0.6 26.0 %copy-start.9 = (bf16[64,384]{1,0:T(8,128)(2,1)S(1)}, bf16[64,384]{1,0:T(8,128)(2,1)}, u32[]{:S(2)}) copy-start(bf16[64,384]{1,0:T(8,128)(2,1)} %param.22) | copy-start | bytes 147460
  0.6 26.0 %copy-start.10 = (bf16[64,384]{1,0:T(8,128)(2,1)S(1)}, bf16[64,384]{1,0:T(8,128)(2,1)}, u32[]{:S(2)}) copy-start(bf16[64,384]{1,0:T(8,128)(2,1)} %param.21) | copy-start | bytes 147460
  21.5 21.0 %copy-start.11 = (bf16[64,384]{1,0:T(8,128)(2,1)S(1)}, bf16[64,384]{1,0:T(8,128)(2,1)}, u32[]{:S(2)}) copy-start(bf16[64,384]{1,0:T(8,128)(2,1)} %param.19) | copy-start | bytes 147460
  21.5 21.0 %copy-start.12 = (bf16[64,384]{1,0:T(8,128)(2,1)S(1)}, bf16[64,384]{1,0:T(8,128)(2,1)}, u32[]{:S(2)}) copy-start(bf16[64,384]{1,0:T(8,128)(2,1)} %param.18) | copy-start | bytes 147460
  21.5 21.6 %copy-start = (bf16[256,2048]{1,0:T(8,128)(2,1)S(1)}, bf16[256,2048]{1,0:T(8,128)(2,1)}, u32[]{:S(2)}) copy-start(bf16[256,2048]{1,0:T(8,128)(2,1)} %param.16) | copy-start | bytes 3145732
  23.2 14.0 %all-to-all-start.2 = ((bf16[8,64,384]{2,1,0:T(8,128)(2,1)}), bf16[8,64,384]{2,1,0:T(8,128)(2,1)S(1)}, u32[]{:S(2)}, u32[]{:S(2)}) async-start(bf16[8,64,384]{2,1,0:T(8,128)(2,1)} %broadcast_in_dim.12), calls=%async_computation.2 | async-start | bytes 786432 | tf_op jit(solution)/shard_map/all_to_all | solution.py:23
  38.2 24.0 %all-to-all-start.1 = ((bf16[8,64,768]{2,1,0:T(8,128)(2,1)}), bf16[8,64,768]{2,1,0:T(8,128)(2,1)}, u32[]{:S(2)}, u32[]{:S(2)}) async-start(bf16[8,64,768]{2,1,0:T(8,128)(2,1)} %broadcast_in_dim.11), calls=%async_computation.1 | async-start | bytes 1572864 | tf_op jit(solution)/shard_map/all_to_all | solution.py:23
  44.0 44.9 %collective-permute-start.1 = (bf16[512,384]{1,0:T(8,128)(2,1)S(1)}, bf16[512,384]{1,0:T(8,128)(2,1)}, u32[]{:S(2)}, u32[]{:S(2)}) collective-permute-start(bf16[512,384]{1,0:T(8,128)(2,1)S(1)} %bitcast.43), channel_id=1, source_target_pairs={{448,0},{0,64},{64,128},{128,192},{192,256},{256,320},{320,384},{3... | collective-permute-start | bytes 1179656 | tf_op jit(solution)/shard_map/ppermute | solution.py:18
  50.7 41.1 %collective-permute-start = (bf16[512,384]{1,0:T(8,128)(2,1)S(1)}, bf16[512,384]{1,0:T(8,128)(2,1)}, u32[]{:S(2)}, u32[]{:S(2)}) collective-permute-start(bf16[512,384]{1,0:T(8,128)(2,1)S(1)} %bitcast.44), channel_id=1, source_target_pairs={{64,0},{128,64},{192,128},{256,192},{320,256},{384,320},{448,384},... | collective-permute-start | bytes 1179656 | tf_op jit(solution)/shard_map/ppermute | solution.py:18
  64.1 62.6 %all-to-all-start.3 = ((bf16[8,64,768]{2,1,0:T(8,128)(2,1)}), bf16[8,64,768]{2,1,0:T(8,128)(2,1)}, u32[]{:S(2)}, u32[]{:S(2)}) async-start(bf16[8,64,768]{2,1,0:T(8,128)(2,1)} %broadcast_in_dim.13), calls=%async_computation.3 | async-start | bytes 1572864 | tf_op jit(solution)/shard_map/all_to_all | solution.py:23
  69.6 86.1 %collective-permute-start.17 = (bf16[512,384]{1,0:T(8,128)(2,1)}, bf16[512,384]{1,0:T(8,128)(2,1)}, u32[]{:S(2)}, u32[]{:S(2)}) collective-permute-start(bf16[512,384]{1,0:T(8,128)(2,1)} %bitcast.47), channel_id=1, source_target_pairs={{448,0},{0,64},{64,128},{128,192},{192,256},{256,320},{320,384},{3... | collective-permute-start | bytes 1179656 | tf_op jit(solution)/shard_map/ppermute | solution.py:18
  77.1 83.0 %collective-permute-start.16 = (bf16[512,384]{1,0:T(8,128)(2,1)}, bf16[512,384]{1,0:T(8,128)(2,1)}, u32[]{:S(2)}, u32[]{:S(2)}) collective-permute-start(bf16[512,384]{1,0:T(8,128)(2,1)} %bitcast.48), channel_id=1, source_target_pairs={{64,0},{128,64},{192,128},{256,192},{320,256},{384,320},{448,384},... | collective-permute-start | bytes 1179656 | tf_op jit(solution)/shard_map/ppermute | solution.py:18
  85.7 34.9 %collective-permute-start.5 = (bf16[512,768]{1,0:T(8,128)(2,1)}, bf16[512,768]{1,0:T(8,128)(2,1)S(1)}, u32[]{:S(2)}, u32[]{:S(2)}) collective-permute-start(bf16[512,768]{1,0:T(8,128)(2,1)} %bitcast.2), channel_id=1, source_target_pairs={{448,0},{0,64},{64,128},{128,192},{192,256},{256,320},{320,384},{3... | collective-permute-start | bytes 2359304 | tf_op jit(solution)/shard_map/ppermute | solution.py:18
  89.9 22.5 %collective-permute-start.3 = (bf16[256,384]{1,0:T(8,128)(2,1)S(1)}, bf16[256,384]{1,0:T(8,128)(2,1)S(1)}, u32[]{:S(2)}, u32[]{:S(2)}) collective-permute-start(bf16[256,384]{1,0:T(8,128)(2,1)S(1)} %slice.75), channel_id=1, source_target_pairs={{448,0},{0,64},{64,128},{128,192},{192,256},{256,320},{320,384},{3... | collective-permute-start | bytes 589832 | tf_op jit(solution)/shard_map/ppermute | solution.py:18
  91.8 37.5 %collective-permute-start.4 = (bf16[512,768]{1,0:T(8,128)(2,1)}, bf16[512,768]{1,0:T(8,128)(2,1)}, u32[]{:S(2)}, u32[]{:S(2)}) collective-permute-start(bf16[512,768]{1,0:T(8,128)(2,1)} %bitcast.2), channel_id=1, source_target_pairs={{64,0},{128,64},{192,128},{256,192},{320,256},{384,320},{448,384},... | collective-permute-start | bytes 2359304 | tf_op jit(solution)/shard_map/ppermute | solution.py:18
  112.4 6.4 %collective-permute-start.2 = (bf16[256,384]{1,0:T(8,128)(2,1)S(1)}, bf16[256,384]{1,0:T(8,128)(2,1)S(1)}, u32[]{:S(2)}, u32[]{:S(2)}) collective-permute-start(bf16[256,384]{1,0:T(8,128)(2,1)S(1)} %slice.74), channel_id=1, source_target_pairs={{64,0},{128,64},{192,128},{256,192},{320,256},{384,320},{448,384},... | collective-permute-start | bytes 589832 | tf_op jit(solution)/shard_map/ppermute | solution.py:18
  122.3 13.8 %collective-permute-start.7 = (bf16[256,768]{1,0:T(8,128)(2,1)}, bf16[256,768]{1,0:T(8,128)(2,1)}, u32[]{:S(2)}, u32[]{:S(2)}) collective-permute-start(bf16[256,768]{1,0:T(8,128)(2,1)} %slice.77), channel_id=1, source_target_pairs={{448,0},{0,64},{64,128},{128,192},{192,256},{256,320},{320,384},{3... | collective-permute-start | bytes 1179656 | tf_op jit(solution)/shard_map/ppermute | solution.py:18
  126.6 39.9 %collective-permute-start.21 = (bf16[512,768]{1,0:T(8,128)(2,1)}, bf16[512,768]{1,0:T(8,128)(2,1)}, u32[]{:S(2)}, u32[]{:S(2)}) collective-permute-start(bf16[512,768]{1,0:T(8,128)(2,1)} %bitcast.5), channel_id=1, source_target_pairs={{448,0},{0,64},{64,128},{128,192},{192,256},{256,320},{320,384},{3... | collective-permute-start | bytes 2359304 | tf_op jit(solution)/shard_map/ppermute | solution.py:18
  130.3 9.1 %collective-permute-start.6 = (bf16[256,768]{1,0:T(8,128)(2,1)S(1)}, bf16[256,768]{1,0:T(8,128)(2,1)S(1)}, u32[]{:S(2)}, u32[]{:S(2)}) collective-permute-start(bf16[256,768]{1,0:T(8,128)(2,1)S(1)} %slice.76), channel_id=1, source_target_pairs={{64,0},{128,64},{192,128},{256,192},{320,256},{384,320},{448,384},... | collective-permute-start | bytes 1179656 | tf_op jit(solution)/shard_map/ppermute | solution.py:18
  148.8 20.8 %collective-permute-start.8 = (bf16[128,2048]{1,0:T(8,128)(2,1)}, bf16[128,2048]{1,0:T(8,128)(2,1)}, u32[]{:S(2)}, u32[]{:S(2)}) collective-permute-start(bf16[128,2048]{1,0:T(8,128)(2,1)} %fusion.48), channel_id=1, source_target_pairs={{0,1},{1,0},{2,3},{3,2},{4,5},{5,4},{6,7},{7,6},{8,9},{9,8},{10,11... | collective-permute-start | bytes 1572872 | tf_op jit(solution)/shard_map/ppermute | solution.py:71
  156.7 60.7 %collective-permute-start.19 = (bf16[256,384]{1,0:T(8,128)(2,1)S(1)}, bf16[256,384]{1,0:T(8,128)(2,1)S(1)}, u32[]{:S(2)}, u32[]{:S(2)}) collective-permute-start(bf16[256,384]{1,0:T(8,128)(2,1)S(1)} %slice.81), channel_id=1, source_target_pairs={{448,0},{0,64},{64,128},{128,192},{192,256},{256,320},{320,384},{3... | collective-permute-start | bytes 589832 | tf_op jit(solution)/shard_map/ppermute | solution.py:18
  161.1 21.4 %collective-permute-start.20 = (bf16[512,768]{1,0:T(8,128)(2,1)}, bf16[512,768]{1,0:T(8,128)(2,1)S(1)}, u32[]{:S(2)}, u32[]{:S(2)}) collective-permute-start(bf16[512,768]{1,0:T(8,128)(2,1)} %bitcast.5), channel_id=1, source_target_pairs={{64,0},{128,64},{192,128},{256,192},{320,256},{384,320},{448,384},... | collective-permute-start | bytes 2359304 | tf_op jit(solution)/shard_map/ppermute | solution.py:18
  166.5 19.2 %copy-start.2 = (bf16[256,2048]{1,0:T(8,128)(2,1)S(1)}, bf16[256,2048]{1,0:T(8,128)(2,1)}, u32[]{:S(2)}) copy-start(bf16[256,2048]{1,0:T(8,128)(2,1)} %fusion.3) | copy-start | bytes 3145732
  167.7 31.4 %collective-permute-start.23 = (bf16[256,768]{1,0:T(8,128)(2,1)S(1)}, bf16[256,768]{1,0:T(8,128)(2,1)S(1)}, u32[]{:S(2)}, u32[]{:S(2)}) collective-permute-start(bf16[256,768]{1,0:T(8,128)(2,1)S(1)} %slice.83), channel_id=1, source_target_pairs={{448,0},{0,64},{64,128},{128,192},{192,256},{256,320},{320,384},{3... | collective-permute-start | bytes 1179656 | tf_op jit(solution)/shard_map/ppermute | solution.py:18
  171.3 14.8 %collective-permute-start.11 = (bf16[32,2048]{1,0:T(8,128)(2,1)S(1)}, bf16[32,2048]{1,0:T(8,128)(2,1)S(1)}, u32[]{:S(2)}, u32[]{:S(2)}) collective-permute-start(bf16[32,2048]{1,0:T(8,128)(2,1)S(1)} %get-tuple-element.15), channel_id=1, source_target_pairs={{4,0},{5,1},{6,2},{7,3},{0,4},{1,5},{2,6},{3,7},{12,8},{13,9},{14,... | collective-permute-start | bytes 393224 | tf_op jit(solution)/shard_map/ppermute | solution.py:76
  176.0 14.9 %collective-permute-start.10 = (bf16[32,2048]{1,0:T(8,128)(2,1)S(1)}, bf16[32,2048]{1,0:T(8,128)(2,1)S(1)}, u32[]{:S(2)}, u32[]{:S(2)}) collective-permute-start(bf16[32,2048]{1,0:T(8,128)(2,1)S(1)} %get-tuple-element.16), channel_id=1, source_target_pairs={{2,0},{3,1},{4,2},{5,3},{6,4},{7,5},{0,6},{1,7},{10,8},{11,9},{12,... | collective-permute-start | bytes 393224 | tf_op jit(solution)/shard_map/ppermute | solution.py:76
  182.6 8.3 %collective-permute-start.9 = (bf16[32,2048]{1,0:T(8,128)(2,1)S(1)}, bf16[32,2048]{1,0:T(8,128)(2,1)S(1)}, u32[]{:S(2)}, u32[]{:S(2)}) collective-permute-start(bf16[32,2048]{1,0:T(8,128)(2,1)S(1)} %get-tuple-element.14), channel_id=1, source_target_pairs={{6,0},{7,1},{0,2},{1,3},{2,4},{3,5},{4,6},{5,7},{14,8},{15,9},{8,1... | collective-permute-start | bytes 393224 | tf_op jit(solution)/shard_map/ppermute | solution.py:76
  186.1 26.4 %collective-permute-start.22 = (bf16[256,768]{1,0:T(8,128)(2,1)S(1)}, bf16[256,768]{1,0:T(8,128)(2,1)S(1)}, u32[]{:S(2)}, u32[]{:S(2)}) collective-permute-start(bf16[256,768]{1,0:T(8,128)(2,1)S(1)} %slice.82), channel_id=1, source_target_pairs={{64,0},{128,64},{192,128},{256,192},{320,256},{384,320},{448,384},... | collective-permute-start | bytes 1179656 | tf_op jit(solution)/shard_map/ppermute | solution.py:18
  192.2 9.4 %collective-permute-start.12 = (bf16[32,2048]{1,0:T(8,128)(2,1)S(1)}, bf16[32,2048]{1,0:T(8,128)(2,1)S(1)}, u32[]{:S(2)}, u32[]{:S(2)}) collective-permute-start(bf16[32,2048]{1,0:T(8,128)(2,1)S(1)} %fusion.69), channel_id=1, source_target_pairs={{2,0},{3,1},{4,2},{5,3},{6,4},{7,5},{0,6},{1,7},{10,8},{11,9},{12,... | collective-permute-start | bytes 393224 | tf_op jit(solution)/shard_map/ppermute | solution.py:76
  195.6 8.9 %collective-permute-start.13 = (bf16[32,2048]{1,0:T(8,128)(2,1)S(1)}, bf16[32,2048]{1,0:T(8,128)(2,1)S(1)}, u32[]{:S(2)}, u32[]{:S(2)}) collective-permute-start(bf16[32,2048]{1,0:T(8,128)(2,1)S(1)} %fusion.69), channel_id=1, source_target_pairs={{4,0},{5,1},{6,2},{7,3},{0,4},{1,5},{2,6},{3,7},{12,8},{13,9},{14,... | collective-permute-start | bytes 393224 | tf_op jit(solution)/shard_map/ppermute | solution.py:76
  199.0 7.7 %collective-permute-start.14 = (bf16[32,2048]{1,0:T(8,128)(2,1)S(1)}, bf16[32,2048]{1,0:T(8,128)(2,1)S(1)}, u32[]{:S(2)}, u32[]{:S(2)}) collective-permute-start(bf16[32,2048]{1,0:T(8,128)(2,1)S(1)} %fusion.69), channel_id=1, source_target_pairs={{6,0},{7,1},{0,2},{1,3},{2,4},{3,5},{4,6},{5,7},{14,8},{15,9},{8,1... | collective-permute-start | bytes 393224 | tf_op jit(solution)/shard_map/ppermute | solution.py:76
  201.5 16.2 %collective-permute-start.18 = (bf16[256,384]{1,0:T(8,128)(2,1)S(1)}, bf16[256,384]{1,0:T(8,128)(2,1)S(1)}, u32[]{:S(2)}, u32[]{:S(2)}) collective-permute-start(bf16[256,384]{1,0:T(8,128)(2,1)S(1)} %slice.80), channel_id=1, source_target_pairs={{64,0},{128,64},{192,128},{256,192},{320,256},{384,320},{448,384},... | collective-permute-start | bytes 589832 | tf_op jit(solution)/shard_map/ppermute | solution.py:18
  208.2 6.2 %collective-permute-start.15 = (bf16[128,2048]{1,0:T(8,128)(2,1)S(1)}, bf16[128,2048]{1,0:T(8,128)(2,1)S(1)}, u32[]{:S(2)}, u32[]{:S(2)}) collective-permute-start(bf16[128,2048]{1,0:T(8,128)(2,1)S(1)} %fusion.42), channel_id=1, source_target_pairs={{0,1},{1,0},{2,3},{3,2},{4,5},{5,4},{6,7},{7,6},{8,9},{9,8},{10,11... | collective-permute-start | bytes 1572872 | tf_op jit(solution)/shard_map/ppermute | solution.py:71
  223.3 17.3 %collective-permute-start.24 = (bf16[128,2048]{1,0:T(8,128)(2,1)S(1)}, bf16[128,2048]{1,0:T(8,128)(2,1)S(1)}, u32[]{:S(2)}, u32[]{:S(2)}) collective-permute-start(bf16[128,2048]{1,0:T(8,128)(2,1)S(1)} %fusion.46), channel_id=1, source_target_pairs={{0,1},{1,0},{2,3},{3,2},{4,5},{5,4},{6,7},{7,6},{8,9},{9,8},{10,11... | collective-permute-start | bytes 1572872 | tf_op jit(solution)/shard_map/ppermute | solution.py:71
  226.3 7.9 %collective-permute-start.34 = (bf16[256,384]{1,0:T(8,128)(2,1)S(1)}, bf16[256,384]{1,0:T(8,128)(2,1)S(1)}, u32[]{:S(2)}, u32[]{:S(2)}) collective-permute-start(bf16[256,384]{1,0:T(8,128)(2,1)S(1)} %get-tuple-element.18), channel_id=1, source_target_pairs={{64,0},{128,64},{192,128},{256,192},{320,256},{384,320},{448,384},... | collective-permute-start | bytes 589832 | tf_op jit(solution)/shard_map/ppermute | solution.py:18
  229.7 8.8 %collective-permute-start.32 = (bf16[256,384]{1,0:T(8,128)(2,1)S(1)}, bf16[256,384]{1,0:T(8,128)(2,1)S(1)}, u32[]{:S(2)}, u32[]{:S(2)}) collective-permute-start(bf16[256,384]{1,0:T(8,128)(2,1)S(1)} %get-tuple-element.17), channel_id=1, source_target_pairs={{448,0},{0,64},{64,128},{128,192},{192,256},{256,320},{320,384},{3... | collective-permute-start | bytes 589832 | tf_op jit(solution)/shard_map/ppermute | solution.py:18
  234.3 17.9 %collective-permute-start.35 = (bf16[512,384]{1,0:T(8,128)(2,1)S(1)}, bf16[512,384]{1,0:T(8,128)(2,1)S(1)}, u32[]{:S(2)}, u32[]{:S(2)}) collective-permute-start(bf16[512,384]{1,0:T(8,128)(2,1)S(1)} %pad_maximum_fusion.3), channel_id=1, source_target_pairs={{64,0},{128,64},{192,128},{256,192},{320,256},{384,320},{448,384},... | collective-permute-start | bytes 1179656 | tf_op jit(solution)/shard_map/ppermute | solution.py:18
  238.6 13.6 %collective-permute-start.33 = (bf16[512,384]{1,0:T(8,128)(2,1)S(1)}, bf16[512,384]{1,0:T(8,128)(2,1)S(1)}, u32[]{:S(2)}, u32[]{:S(2)}) collective-permute-start(bf16[512,384]{1,0:T(8,128)(2,1)S(1)} %pad_maximum_fusion.2), channel_id=1, source_target_pairs={{448,0},{0,64},{64,128},{128,192},{192,256},{256,320},{320,384},{3... | collective-permute-start | bytes 1179656 | tf_op jit(solution)/shard_map/ppermute | solution.py:18
  243.8 16.2 %collective-permute-start.27 = (bf16[32,2048]{1,0:T(8,128)(2,1)}, bf16[32,2048]{1,0:T(8,128)(2,1)}, u32[]{:S(2)}, u32[]{:S(2)}) collective-permute-start(bf16[32,2048]{1,0:T(8,128)(2,1)} %get-tuple-element.12), channel_id=1, source_target_pairs={{4,0},{5,1},{6,2},{7,3},{0,4},{1,5},{2,6},{3,7},{12,8},{13,9},{14,... | collective-permute-start | bytes 393224 | tf_op jit(solution)/shard_map/ppermute | solution.py:76
  246.9 13.1 %collective-permute-start.26 = (bf16[32,2048]{1,0:T(8,128)(2,1)}, bf16[32,2048]{1,0:T(8,128)(2,1)}, u32[]{:S(2)}, u32[]{:S(2)}) collective-permute-start(bf16[32,2048]{1,0:T(8,128)(2,1)} %get-tuple-element.13), channel_id=1, source_target_pairs={{2,0},{3,1},{4,2},{5,3},{6,4},{7,5},{0,6},{1,7},{10,8},{11,9},{12,... | collective-permute-start | bytes 393224 | tf_op jit(solution)/shard_map/ppermute | solution.py:76
  249.3 10.7 %collective-permute-start.25 = (bf16[32,2048]{1,0:T(8,128)(2,1)}, bf16[32,2048]{1,0:T(8,128)(2,1)}, u32[]{:S(2)}, u32[]{:S(2)}) collective-permute-start(bf16[32,2048]{1,0:T(8,128)(2,1)} %get-tuple-element.11), channel_id=1, source_target_pairs={{6,0},{7,1},{0,2},{1,3},{2,4},{3,5},{4,6},{5,7},{14,8},{15,9},{8,1... | collective-permute-start | bytes 393224 | tf_op jit(solution)/shard_map/ppermute | solution.py:76
  253.4 29.8 %all-to-all-start.4 = ((bf16[8,64,384]{2,1,0:T(8,128)(2,1)}), bf16[8,64,384]{2,1,0:T(8,128)(2,1)S(1)}, u32[]{:S(2)}, u32[]{:S(2)}) async-start(bf16[8,64,384]{2,1,0:T(8,128)(2,1)} %bitcast.46), calls=%async_computation.4 | async-start | bytes 786432 | tf_op jit(solution)/shard_map/all_to_all | solution.py:150
  262.6 8.4 %collective-permute-start.28 = (bf16[32,2048]{1,0:T(8,128)(2,1)S(1)}, bf16[32,2048]{1,0:T(8,128)(2,1)S(1)}, u32[]{:S(2)}, u32[]{:S(2)}) collective-permute-start(bf16[32,2048]{1,0:T(8,128)(2,1)S(1)} %fusion.64), channel_id=1, source_target_pairs={{2,0},{3,1},{4,2},{5,3},{6,4},{7,5},{0,6},{1,7},{10,8},{11,9},{12,... | collective-permute-start | bytes 393224 | tf_op jit(solution)/shard_map/ppermute | solution.py:76
  266.3 7.2 %collective-permute-start.29 = (bf16[32,2048]{1,0:T(8,128)(2,1)S(1)}, bf16[32,2048]{1,0:T(8,128)(2,1)S(1)}, u32[]{:S(2)}, u32[]{:S(2)}) collective-permute-start(bf16[32,2048]{1,0:T(8,128)(2,1)S(1)} %fusion.64), channel_id=1, source_target_pairs={{4,0},{5,1},{6,2},{7,3},{0,4},{1,5},{2,6},{3,7},{12,8},{13,9},{14,... | collective-permute-start | bytes 393224 | tf_op jit(solution)/shard_map/ppermute | solution.py:76
  268.4 6.9 %collective-permute-start.30 = (bf16[32,2048]{1,0:T(8,128)(2,1)S(1)}, bf16[32,2048]{1,0:T(8,128)(2,1)S(1)}, u32[]{:S(2)}, u32[]{:S(2)}) collective-permute-start(bf16[32,2048]{1,0:T(8,128)(2,1)S(1)} %fusion.64), channel_id=1, source_target_pairs={{6,0},{7,1},{0,2},{1,3},{2,4},{3,5},{4,6},{5,7},{14,8},{15,9},{8,1... | collective-permute-start | bytes 393224 | tf_op jit(solution)/shard_map/ppermute | solution.py:76
  276.8 28.0 %collective-permute-start.31 = (bf16[128,2048]{1,0:T(8,128)(2,1)S(1)}, bf16[128,2048]{1,0:T(8,128)(2,1)S(1)}, u32[]{:S(2)}, u32[]{:S(2)}) collective-permute-start(bf16[128,2048]{1,0:T(8,128)(2,1)S(1)} %fusion.35), channel_id=1, source_target_pairs={{0,1},{1,0},{2,3},{3,2},{4,5},{5,4},{6,7},{7,6},{8,9},{9,8},{10,11... | collective-permute-start | bytes 1572872 | tf_op jit(solution)/shard_map/ppermute | solution.py:71
  283.3 9.1 %collective-permute-start.36 = (bf16[64,384]{1,0:T(8,128)(2,1)S(1)}, bf16[64,384]{1,0:T(8,128)(2,1)S(1)}, u32[]{:S(2)}, u32[]{:S(2)}) collective-permute-start(bf16[64,384]{1,0:T(8,128)(2,1)S(1)} %reduce_sum.90), channel_id=1, source_target_pairs={{256,0},{0,256},{257,1},{1,257},{258,2},{2,258},{259,3},{3,259},{2... | collective-permute-start | bytes 147464 | tf_op jit(solution)/shard_map/ppermute | solution.py:18
  293.6 20.3 %all-to-all-start.5 = ((f32[32,1,384]{2,1,0:T(1,128)}), f32[32,1,384]{2,1,0:T(1,128)S(1)}, u32[]{:S(2)}, u32[]{:S(2)}) async-start(f32[32,1,384]{2,1,0:T(1,128)} %broadcast_in_dim.14), calls=%async_computation.5 | async-start | bytes 98304 | tf_op jit(solution)/shard_map/all_to_all | solution.py:23
  (7 other events, 39.0 us)

commit v2 on v1

v2 whole, which is shorter than its diff:
```python
import jax
import jax.numpy as jnp
from jax import lax
from jax.sharding import Mesh
from jax.sharding import PartitionSpec as P

FS = ("fs_0", "fs_1")
Z = ("rep", "fs_0")
REP_FS = ("rep", "fs_0", "fs_1")
f32 = jnp.float32
bf16 = jnp.bfloat16

eps = 1e-06


def take_from(value, axis, step):
    n = lax.axis_size(axis)
    return lax.ppermute(value, axis, [((i + step) % n, i) for i in range(n)])


def from_everyone(value, axis):
    n = lax.axis_size(axis)
    return lax.all_to_all(
        jnp.broadcast_to(value[None], (n, *value.shape)), axis, 0, 0, tiled=True
    )


def along_y(value):
    whole = from_everyone(value, "fs_1")
    return whole.reshape(-1, value.shape[1])


def along_z(value):
    half = value.shape[0] // 2
    next_ = take_from(value, Z, 1)
    last = take_from(value, Z, -1)
    top = take_from(next_[:half], Z, 1)
    bottom = take_from(last[half:], Z, -1)
    return ((0, 0, value), (1, 0, next_), (3, 0, last), (2, 0, top), (2, half, bottom))


def columns(x, z, piece):
    m, first, w = piece
    span = x.shape[1] // 4
    start = ((z + m) % 4) * span + first
    return lax.dynamic_slice_in_dim(x, start, w.shape[0], axis=1)


def contract(x, z, pieces):
    total = None
    for piece in pieces:
        part = jnp.dot(columns(x, z, piece), piece[2], preferred_element_type=f32)
        total = part if total is None else total + part
    return total


def spread(x, z, pieces):
    dims = (((1,), (1,)), ((), ()))
    out = {
        (m, first): lax.dot_general(x, w, dims, preferred_element_type=f32).astype(bf16)
        for m, first, w in pieces
    }
    half = pieces[3][2].shape[0]
    rel = jnp.concatenate(
        [out[0, 0], out[1, 0], out[2, 0], out[2, half], out[3, 0]], axis=1
    )
    return jnp.roll(rel, z * (2 * half), axis=1)


def after(value, *others):
    return lax.optimization_barrier((value, *others))[0]


def own_rows(partial):
    n = lax.axis_size("tp")
    pieces = partial.reshape(n, -1, partial.shape[1])
    return lax.all_to_all(pieces, "tp", 0, 0, tiled=True).astype(f32).sum(axis=0)


def half_back(u, c, z, tp, gate_up, down):
    field = u.astype(f32)
    scale = lax.rsqrt(jnp.mean(field * field, axis=1, keepdims=True) + eps)
    normed_b = (field * scale).astype(bf16)
    both = contract(normed_b, z, gate_up)
    n = both.shape[1] // 2
    gate, upper = both[:, :n], both[:, n:]
    back = 0.5 * contract(c, z, down)
    logistic = jax.nn.sigmoid(gate)
    activated = gate * logistic
    hidden = (activated * upper).astype(bf16)
    d_gate = (back * upper * logistic * (1.0 + gate * (1.0 - logistic))).astype(bf16)
    d_up = (back * activated).astype(bf16)
    partial = spread(jnp.concatenate([d_gate, d_up], axis=1), z, gate_up)
    rows = u.shape[0] // lax.axis_size("tp")
    d_normed = own_rows(partial)
    field = lax.dynamic_slice_in_dim(u, tp * rows, rows, axis=0).astype(f32)
    scale = lax.rsqrt(jnp.mean(field * field, axis=1, keepdims=True) + eps)
    normed = field * scale
    carried = lax.dynamic_slice_in_dim(c, tp * rows, rows, axis=0).astype(f32)
    d_field = carried + scale * (
        d_normed - normed * jnp.mean(d_normed * normed, axis=1, keepdims=True)
    )
    return from_everyone(d_field.astype(bf16), "tp").reshape(u.shape), hidden


def down_share(hidden, grad, z):
    span = grad.shape[1] // 4
    half = span // 2

    def part(m):
        cols = lax.dynamic_slice_in_dim(grad, ((z + m) % 4) * span, span, axis=1)
        return 0.5 * lax.dot_general(
            cols, hidden, (((0,), (0,)), ((), ())), preferred_element_type=f32
        )

    far = part(2).astype(bf16)
    top = take_from(far[:half], Z, -2).astype(f32)
    bottom = take_from(far[half:], Z, 2).astype(f32)
    next_ = take_from(part(1).astype(bf16), Z, -1).astype(f32)
    last = take_from(part(3).astype(bf16), Z, 1).astype(f32)
    column = part(0) + next_ + last + jnp.concatenate([top, bottom], axis=0)
    column = column.astype(bf16).reshape(lax.axis_size("fs_1"), -1, hidden.shape[1])
    share = lax.all_to_all(column, "fs_1", 0, 0, tiled=True).astype(f32).sum(axis=0)
    share = share.astype(bf16)
    return share.astype(f32) + take_from(share, "rep", 1).astype(f32)


def on_device(
    tokens,
    mid_tokens,
    out_grad,
    gate_first,
    up_first,
    down_first,
    gate_second,
    up_second,
    down_second,
):
    z = lax.axis_index("fs_0")
    tp = lax.axis_index("tp")
    gu2 = along_y(jnp.concatenate([gate_second, up_second], axis=1))
    dn2 = along_y(after(down_second.T, gu2))
    gu1 = along_y(after(jnp.concatenate([gate_first, up_first], axis=1), dn2))
    dn1 = along_y(after(down_first.T, gu1))
    gate_up_2 = along_z(gu2)
    down_2 = along_z(after(dn2, gate_up_2[1][2], gate_up_2[2][2]))
    gate_up_1 = along_z(after(gu1, down_2[1][2], down_2[2][2]))
    down_1 = along_z(after(dn1, gate_up_1[1][2], gate_up_1[2][2]))
    mid_grad, _ = half_back(mid_tokens, out_grad, z, tp, gate_up_2, down_2)
    input_grad, hidden = half_back(tokens, mid_grad, z, tp, gate_up_1, down_1)
    share = down_share(hidden, mid_grad, z)
    norms = from_everyone(jnp.sum(share * share, axis=0), FS).sum(axis=0)
    return (input_grad, share.T, norms)


def solution(mesh):
    torus = Mesh(
        mesh.devices.reshape(mesh.shape["rep"], 4, 8, mesh.shape["tp"]),
        ("rep", "fs_0", "fs_1", "tp"),
    )
    placed = (
        P(REP_FS, None),
        P(REP_FS, None),
        P(REP_FS, None),
        P(FS, "tp"),
        P(FS, "tp"),
        P("tp", FS),
        P(FS, "tp"),
        P(FS, "tp"),
        P("tp", FS),
    )
    return jax.shard_map(
        on_device,
        mesh=torus,
        in_specs=placed,
        out_specs=(P(REP_FS, None), P("tp", FS), P("tp")),
        check_vma=False,
    )
```

time: 317 us -> 307 us (0.968)
  waiting for transfers between devices: 53.5 us -> 104 us
  starting transfers between devices: 170 us -> 138 us
  blocking collectives: 20 us -> 0 us
  other arithmetic: 19.5 us -> 10.6 us
    ppermute x16 -> x0, starting transfers between devices: 55.5 us -> none  [the longest x12 36.3 us: take_x(): lax.ppermute(value, 'tp', [((i + 2 * step) % n, i) for i in range(n)])]
    all_to_all x4 -> x7, waiting for transfers between devices: 19.8 us -> 70.7 us  [from_everyone(): lax.all_to_all(jnp.broadcast_to(value[None], (n, *value.shape)), axis, 0,...]
    all_to_all x1 -> x0, blocking collectives: 20 us -> none  [from_everyone(): lax.all_to_all(jnp.broadcast_to(value[None], (n, *value.shape)), axis, 0,...]
    all_to_all x4 -> x7, starting transfers between devices: 23.1 us -> 40.3 us  [from_everyone(): lax.all_to_all(jnp.broadcast_to(value[None], (n, *value.shape)), axis, 0,...]
    ppermute x21, waiting for transfers between devices: 27.2 us -> 10.9 us  [take_from(): return lax.ppermute(value, axis, [((i + step) % n, i) for i in range(n)])]
    all_to_all x0 -> x2, starting transfers between devices: none -> 14.8 us  [own_rows(): lax.all_to_all(pieces, 'tp', 0, 0, tiled=True).astype(f32).sum(axis=0)]
    all_to_all x1, waiting for transfers between devices: 0.01 us -> 14.6 us  [down_share(): lax.all_to_all(column, 'fs_1', 0, 0, tiled=True).astype(f32).sum(axis=0)]
    all_to_all x0 -> x2, waiting for transfers between devices: none -> 7.97 us  [own_rows(): lax.all_to_all(pieces, 'tp', 0, 0, tiled=True).astype(f32).sum(axis=0)]
  transfers between devices with their start and end apart: 42 -> 31, of which waited for: 13 -> 12; matrix products, arithmetic and copies ran while one was open for 19% -> 16% of each run, Pallas kernels for 0% -> 0%
where the time goes in v2:
time: 307 us; the launch traced here: 304 us
  starting transfers between devices  138 us (45%)
  waiting for transfers between devices  104 us (34%)
  matrix products  34.6 us (11%)
  local copies, waits for them, and re-layouts  15.6 us (5%)
  other arithmetic  10.6 us (3%)
    ppermute x21, starting transfers between devices, take_from(): return lax.ppermute(value, axis, [((i + step) % n, i) for i in range(n)])  78.6 us
    all_to_all x7, waiting for transfers between devices, from_everyone(): lax.all_to_all(jnp.broadcast_to(value[None], (n, *value.shape)), axis, 0,...  70.7 us
    all_to_all x7, starting transfers between devices, from_everyone(): lax.all_to_all(jnp.broadcast_to(value[None], (n, *value.shape)), axis, 0,...  40.3 us
    dot_general x20, matrix products, contract(): part = jnp.dot(columns(x, z, piece), piece[2], preferred_element_type=f32)  18.6 us
    all_to_all x2, starting transfers between devices, own_rows(): lax.all_to_all(pieces, 'tp', 0, 0, tiled=True).astype(f32).sum(axis=0)  14.8 us
    all_to_all x1, waiting for transfers between devices, down_share(): lax.all_to_all(column, 'fs_1', 0, 0, tiled=True).astype(f32).sum(axis=0)  14.6 us
    ppermute x21, waiting for transfers between devices, take_from(): return lax.ppermute(value, axis, [((i + step) % n, i) for i in range(n)])  10.9 us
    dot_general x10, matrix products, spread(): lax.dot_general(x, w, dims, preferred_element_type=f32).astype(bf16)  10.3 us
  transfers between devices with their start and end apart: 31, of which 12 were waited for; matrix products, arithmetic and copies ran while one was open for 16% of the time, Pallas kernels for 0%

profile of v2, /device:TPU:1, one launch (start us, length us, event | category | flops | bytes accessed | tf_op | source)
XLA Modules:
  0.0 304.3 jit_solution(8545814245701333893)
XLA Ops:
  2.4 7.8 %all-to-all-start = ((bf16[8,64,768]{2,1,0:T(8,128)(2,1)}), bf16[8,64,768]{2,1,0:T(8,128)(2,1)S(1)}, u32[]{:S(2)}, u32[]{:S(2)}) async-start(bf16[8,64,768]{2,1,0:T(8,128)(2,1)} %broadcast_in_dim.14), calls=%async_computation | async-start | bytes 1572864 | tf_op jit(solution)/shard_map/all_to_all | solution.py:23
  10.7 20.6 %all-to-all-done = bf16[8,64,768]{2,1,0:T(8,128)(2,1)S(1)} async-done(((bf16[8,64,768]{2,1,0:T(8,128)(2,1)}), bf16[8,64,768]{2,1,0:T(8,128)(2,1)S(1)}, u32[]{:S(2)}, u32[]{:S(2)}) %all-to-all-start) | async-done | bytes 786464 | tf_op jit(solution)/shard_map/all_to_all | solution.py:23
  31.3 13.1 %collective-permute-start = (bf16[512,768]{1,0:T(8,128)(2,1)S(1)}, bf16[512,768]{1,0:T(8,128)(2,1)}, u32[]{:S(2)}, u32[]{:S(2)}) collective-permute-start(bf16[512,768]{1,0:T(8,128)(2,1)S(1)} %bitcast.59), channel_id=1, source_target_pairs={{64,0},{128,64},{192,128},{256,192},{320,256},{384,320},{448,384},... | collective-permute-start | bytes 2359304 | tf_op jit(solution)/shard_map/ppermute | solution.py:18
  44.4 1.9 collective-permute-start.1
  47.2 4.1 %all-to-all-start.1 = ((bf16[8,64,384]{2,1,0:T(8,128)(2,1)}), bf16[8,64,384]{2,1,0:T(8,128)(2,1)}, u32[]{:S(2)}, u32[]{:S(2)}) async-start(bf16[8,64,384]{2,1,0:T(8,128)(2,1)} %broadcast_in_dim.15), calls=%async_computation.1 | async-start | bytes 786432 | tf_op jit(solution)/shard_map/all_to_all | solution.py:23
  51.5 14.8 %all-to-all-done.1 = bf16[8,64,384]{2,1,0:T(8,128)(2,1)} async-done(((bf16[8,64,384]{2,1,0:T(8,128)(2,1)}), bf16[8,64,384]{2,1,0:T(8,128)(2,1)}, u32[]{:S(2)}, u32[]{:S(2)}) %all-to-all-start.1) | async-done | bytes 393248 | tf_op jit(solution)/shard_map/all_to_all | solution.py:23
  66.4 1.9 collective-permute-start.3
  68.3 4.6 %collective-permute-start.2 = (bf16[512,384]{1,0:T(8,128)(2,1)}, bf16[512,384]{1,0:T(8,128)(2,1)S(1)}, u32[]{:S(2)}, u32[]{:S(2)}) collective-permute-start(bf16[512,384]{1,0:T(8,128)(2,1)} %bitcast.2), channel_id=1, source_target_pairs={{64,0},{128,64},{192,128},{256,192},{320,256},{384,320},{448,384},... | collective-permute-start | bytes 1179656 | tf_op jit(solution)/shard_map/ppermute | solution.py:18
  72.9 1.8 slice.59
  74.6 1.9 collective-permute-start.7
  78.8 4.2 %all-to-all-start.4 = ((bf16[8,64,768]{2,1,0:T(8,128)(2,1)}), bf16[8,64,768]{2,1,0:T(8,128)(2,1)}, u32[]{:S(2)}, u32[]{:S(2)}) async-start(bf16[8,64,768]{2,1,0:T(8,128)(2,1)} %broadcast_in_dim.17), calls=%async_computation.4 | async-start | bytes 1572864 | tf_op jit(solution)/shard_map/all_to_all | solution.py:23
  84.1 4.6 %collective-permute-start.6 = (bf16[256,768]{1,0:T(8,128)(2,1)S(1)}, bf16[256,768]{1,0:T(8,128)(2,1)S(1)}, u32[]{:S(2)}, u32[]{:S(2)}) collective-permute-start(bf16[256,768]{1,0:T(8,128)(2,1)S(1)} %slice.58), channel_id=1, source_target_pairs={{64,0},{128,64},{192,128},{256,192},{320,256},{384,320},{448,384},... | collective-permute-start | bytes 1179656 | tf_op jit(solution)/shard_map/ppermute | solution.py:18
  91.2 1.9 collective-permute-start.5
  93.1 4.7 %collective-permute-start.4 = (bf16[256,384]{1,0:T(8,128)(2,1)S(1)}, bf16[256,384]{1,0:T(8,128)(2,1)S(1)}, u32[]{:S(2)}, u32[]{:S(2)}) collective-permute-start(bf16[256,384]{1,0:T(8,128)(2,1)S(1)} %slice.56), channel_id=1, source_target_pairs={{64,0},{128,64},{192,128},{256,192},{320,256},{384,320},{448,384},... | collective-permute-start | bytes 589832 | tf_op jit(solution)/shard_map/ppermute | solution.py:18
  104.9 1.5 fusion.13
  109.6 1.6 fusion.31
  111.1 7.3 %all-to-all-start.2 = ((bf16[8,32,2048]{2,1,0:T(8,128)(2,1)}), bf16[8,32,2048]{2,1,0:T(8,128)(2,1)S(1)}, u32[]{:S(2)}, u32[]{:S(2)}) async-start(bf16[8,32,2048]{2,1,0:T(8,128)(2,1)} %bitcast.47), calls=%async_computation.2 | async-start | bytes 2097152 | tf_op jit(solution)/shard_map/all_to_all | solution.py:77
  120.0 3.5 %collective-permute-start.8 = (bf16[512,768]{1,0:T(8,128)(2,1)}, bf16[512,768]{1,0:T(8,128)(2,1)}, u32[]{:S(2)}, u32[]{:S(2)}) collective-permute-start(bf16[512,768]{1,0:T(8,128)(2,1)} %bitcast.6), channel_id=1, source_target_pairs={{64,0},{128,64},{192,128},{256,192},{320,256},{384,320},{448,384},... | collective-permute-start | bytes 2359304 | tf_op jit(solution)/shard_map/ppermute | solution.py:18
  123.5 1.9 collective-permute-start.9
  125.4 8.0 %all-to-all-done.2 = bf16[8,32,2048]{2,1,0:T(8,128)(2,1)S(1)} async-done(((bf16[8,32,2048]{2,1,0:T(8,128)(2,1)}), bf16[8,32,2048]{2,1,0:T(8,128)(2,1)S(1)}, u32[]{:S(2)}, u32[]{:S(2)}) %all-to-all-start.2) | async-done | bytes 1048608 | tf_op jit(solution)/shard_map/all_to_all | solution.py:77
  134.2 6.8 %all-to-all-start.5 = ((bf16[8,64,384]{2,1,0:T(8,128)(2,1)}), bf16[8,64,384]{2,1,0:T(8,128)(2,1)S(1)}, u32[]{:S(2)}, u32[]{:S(2)}) async-start(bf16[8,64,384]{2,1,0:T(8,128)(2,1)} %broadcast_in_dim.18), calls=%async_computation.5 | async-start | bytes 786432 | tf_op jit(solution)/shard_map/all_to_all | solution.py:23
  142.4 12.1 %all-to-all-done.5 = bf16[8,64,384]{2,1,0:T(8,128)(2,1)S(1)} async-done(((bf16[8,64,384]{2,1,0:T(8,128)(2,1)}), bf16[8,64,384]{2,1,0:T(8,128)(2,1)S(1)}, u32[]{:S(2)}, u32[]{:S(2)}) %all-to-all-start.5) | async-done | bytes 393248 | tf_op jit(solution)/shard_map/all_to_all | solution.py:23
  155.6 5.6 %all-to-all-start.3 = ((bf16[8,32,2048]{2,1,0:T(8,128)(2,1)}), bf16[8,32,2048]{2,1,0:T(8,128)(2,1)S(1)}, u32[]{:S(2)}, u32[]{:S(2)}) async-start(bf16[8,32,2048]{2,1,0:T(8,128)(2,1)} %broadcast_in_dim.16), calls=%async_computation.3 | async-start | bytes 2097152 | tf_op jit(solution)/shard_map/all_to_all | solution.py:23
  161.2 3.7 %collective-permute-start.10 = (bf16[512,384]{1,0:T(8,128)(2,1)S(1)}, bf16[512,384]{1,0:T(8,128)(2,1)S(1)}, u32[]{:S(2)}, u32[]{:S(2)}) collective-permute-start(bf16[512,384]{1,0:T(8,128)(2,1)S(1)} %bitcast.63), channel_id=1, source_target_pairs={{64,0},{128,64},{192,128},{256,192},{320,256},{384,320},{448,384},... | collective-permute-start | bytes 1179656 | tf_op jit(solution)/shard_map/ppermute | solution.py:18
  164.9 1.9 collective-permute-start.11
  167.9 4.6 %collective-permute-start.14 = (bf16[256,768]{1,0:T(8,128)(2,1)S(1)}, bf16[256,768]{1,0:T(8,128)(2,1)S(1)}, u32[]{:S(2)}, u32[]{:S(2)}) collective-permute-start(bf16[256,768]{1,0:T(8,128)(2,1)S(1)} %slice.64), channel_id=1, source_target_pairs={{64,0},{128,64},{192,128},{256,192},{320,256},{384,320},{448,384},... | collective-permute-start | bytes 1179656 | tf_op jit(solution)/shard_map/ppermute | solution.py:18
  173.5 1.9 collective-permute-start.15
  178.5 4.5 %collective-permute-start.12 = (bf16[256,384]{1,0:T(8,128)(2,1)S(1)}, bf16[256,384]{1,0:T(8,128)(2,1)}, u32[]{:S(2)}, u32[]{:S(2)}) collective-permute-start(bf16[256,384]{1,0:T(8,128)(2,1)S(1)} %slice.62), channel_id=1, source_target_pairs={{64,0},{128,64},{192,128},{256,192},{320,256},{384,320},{448,384},... | collective-permute-start | bytes 589832 | tf_op jit(solution)/shard_map/ppermute | solution.py:18
  183.8 1.9 collective-permute-start.13
  187.5 2.4 fusion.6
  195.9 1.9 collective-permute-start.16
  197.9 4.8 %collective-permute-start.17 = (bf16[512,384]{1,0:T(8,128)(2,1)}, bf16[512,384]{1,0:T(8,128)(2,1)}, u32[]{:S(2)}, u32[]{:S(2)}) collective-permute-start(bf16[512,384]{1,0:T(8,128)(2,1)} %fusion.10), channel_id=1, source_target_pairs={{64,0},{128,64},{192,128},{256,192},{320,256},{384,320},{448,384},... | collective-permute-start | bytes 1179656 | tf_op jit(solution)/shard_map/ppermute | solution.py:18
  204.2 1.6 fusion.16
  208.6 1.6 fusion.30
  210.2 7.5 %all-to-all-start.6 = ((bf16[8,32,2048]{2,1,0:T(8,128)(2,1)}), bf16[8,32,2048]{2,1,0:T(8,128)(2,1)S(1)}, u32[]{:S(2)}, u32[]{:S(2)}) async-start(bf16[8,32,2048]{2,1,0:T(8,128)(2,1)} %bitcast.8), calls=%async_computation.6 | async-start | bytes 2097152 | tf_op jit(solution)/shard_map/all_to_all | solution.py:77
  219.1 1.9 collective-permute-start.18
  221.0 5.5 %collective-permute-start.19 = (bf16[256,384]{1,0:T(8,128)(2,1)S(1)}, bf16[256,384]{1,0:T(8,128)(2,1)S(1)}, u32[]{:S(2)}, u32[]{:S(2)}) collective-permute-start(bf16[256,384]{1,0:T(8,128)(2,1)S(1)} %get-tuple-element.22), channel_id=1, source_target_pairs={{128,0},{192,64},{256,128},{320,192},{384,256},{448,320},{0,384},{... | collective-permute-start | bytes 589832 | tf_op jit(solution)/shard_map/ppermute | solution.py:18
  226.5 5.7 %collective-permute-done.18 = bf16[256,384]{1,0:T(8,128)(2,1)S(1)} collective-permute-done((bf16[256,384]{1,0:T(8,128)(2,1)S(1)}, bf16[256,384]{1,0:T(8,128)(2,1)S(1)}, u32[]{:S(2)}, u32[]{:S(2)}) %collective-permute-start.18) | collective-permute-done | bytes 196640 | tf_op jit(solution)/shard_map/ppermute | solution.py:18
  232.2 1.6 collective-permute-done.19
  233.8 2.2 add_convert_fusion
  236.0 4.1 %all-to-all-start.8 = ((bf16[8,64,384]{2,1,0:T(8,128)(2,1)}), bf16[8,64,384]{2,1,0:T(8,128)(2,1)}, u32[]{:S(2)}, u32[]{:S(2)}) async-start(bf16[8,64,384]{2,1,0:T(8,128)(2,1)} %bitcast.10), calls=%async_computation.8 | async-start | bytes 786432 | tf_op jit(solution)/shard_map/all_to_all | solution.py:123
  240.6 14.6 %all-to-all-done.8 = bf16[8,64,384]{2,1,0:T(8,128)(2,1)} async-done(((bf16[8,64,384]{2,1,0:T(8,128)(2,1)}), bf16[8,64,384]{2,1,0:T(8,128)(2,1)}, u32[]{:S(2)}, u32[]{:S(2)}) %all-to-all-start.8) | async-done | bytes 393248 | tf_op jit(solution)/shard_map/all_to_all | solution.py:123
  256.3 5.9 %collective-permute-start.20 = (bf16[64,384]{1,0:T(8,128)(2,1)S(1)}, bf16[64,384]{1,0:T(8,128)(2,1)S(1)}, u32[]{:S(2)}, u32[]{:S(2)}) collective-permute-start(bf16[64,384]{1,0:T(8,128)(2,1)S(1)} %reduce_sum.110), channel_id=1, source_target_pairs={{256,0},{0,256},{257,1},{1,257},{258,2},{2,258},{259,3},{3,259},{2... | collective-permute-start | bytes 147464 | tf_op jit(solution)/shard_map/ppermute | solution.py:18
  262.3 2.8 collective-permute-done.20
  266.3 5.2 %all-to-all-start.9 = ((f32[32,1,384]{2,1,0:T(1,128)}), f32[32,1,384]{2,1,0:T(1,128)S(1)}, u32[]{:S(2)}, u32[]{:S(2)}) async-start(f32[32,1,384]{2,1,0:T(1,128)} %broadcast_in_dim.20), calls=%async_computation.9 | async-start | bytes 98304 | tf_op jit(solution)/shard_map/all_to_all | solution.py:23
  271.7 8.9 %all-to-all-done.9 = f32[32,1,384]{2,1,0:T(1,128)S(1)} async-done(((f32[32,1,384]{2,1,0:T(1,128)}), f32[32,1,384]{2,1,0:T(1,128)S(1)}, u32[]{:S(2)}, u32[]{:S(2)}) %all-to-all-start.9) | async-done | bytes 49184 | tf_op jit(solution)/shard_map/all_to_all | solution.py:23
  281.7 6.6 %all-to-all-start.7 = ((bf16[8,32,2048]{2,1,0:T(8,128)(2,1)}), bf16[8,32,2048]{2,1,0:T(8,128)(2,1)S(1)}, u32[]{:S(2)}, u32[]{:S(2)}) async-start(bf16[8,32,2048]{2,1,0:T(8,128)(2,1)} %broadcast_in_dim.19), calls=%async_computation.7 | async-start | bytes 2097152 | tf_op jit(solution)/shard_map/all_to_all | solution.py:23
  289.0 14.3 %all-to-all-done.7 = bf16[8,32,2048]{2,1,0:T(8,128)(2,1)S(1)} async-done(((bf16[8,32,2048]{2,1,0:T(8,128)(2,1)}), bf16[8,32,2048]{2,1,0:T(8,128)(2,1)S(1)}, u32[]{:S(2)}, u32[]{:S(2)}) %all-to-all-start.7) | async-done | bytes 1048608 | tf_op jit(solution)/shard_map/all_to_all | solution.py:23
  (122 shorter events, 49.0 us)
Async XLA Ops:
  2.4 7.9 %copy-start = (bf16[256,2048]{1,0:T(8,128)(2,1)S(1)}, bf16[256,2048]{1,0:T(8,128)(2,1)}, u32[]{:S(2)}) copy-start(bf16[256,2048]{1,0:T(8,128)(2,1)} %param.12) | copy-start | bytes 3145732
  2.4 28.9 %all-to-all-start = ((bf16[8,64,768]{2,1,0:T(8,128)(2,1)}), bf16[8,64,768]{2,1,0:T(8,128)(2,1)S(1)}, u32[]{:S(2)}, u32[]{:S(2)}) async-start(bf16[8,64,768]{2,1,0:T(8,128)(2,1)} %broadcast_in_dim.14), calls=%async_computation | async-start | bytes 1572864 | tf_op jit(solution)/shard_map/all_to_all | solution.py:23
  10.2 36.2 %copy-start.12 = (bf16[64,384]{1,0:T(8,128)(2,1)S(1)}, bf16[64,384]{1,0:T(8,128)(2,1)}, u32[]{:S(2)}) copy-start(bf16[64,384]{1,0:T(8,128)(2,1)} %param.15) | copy-start | bytes 147460
  10.2 36.2 %copy-start.13 = (bf16[64,384]{1,0:T(8,128)(2,1)S(1)}, bf16[64,384]{1,0:T(8,128)(2,1)}, u32[]{:S(2)}) copy-start(bf16[64,384]{1,0:T(8,128)(2,1)} %param.14) | copy-start | bytes 147460
  10.2 36.2 %copy-start.10 = (bf16[384,64]{0,1:T(8,128)(2,1)S(1)}, bf16[384,64]{0,1:T(8,128)(2,1)}, u32[]{:S(2)}) copy-start(bf16[384,64]{0,1:T(8,128)(2,1)} %param.19) | copy-start | bytes 147460
  31.3 35.1 %collective-permute-start = (bf16[512,768]{1,0:T(8,128)(2,1)S(1)}, bf16[512,768]{1,0:T(8,128)(2,1)}, u32[]{:S(2)}, u32[]{:S(2)}) collective-permute-start(bf16[512,768]{1,0:T(8,128)(2,1)S(1)} %bitcast.59), channel_id=1, source_target_pairs={{64,0},{128,64},{192,128},{256,192},{320,256},{384,320},{448,384},... | collective-permute-start | bytes 2359304 | tf_op jit(solution)/shard_map/ppermute | solution.py:18
  44.4 22.0 %collective-permute-start.1 = (bf16[512,768]{1,0:T(8,128)(2,1)S(1)}, bf16[512,768]{1,0:T(8,128)(2,1)}, u32[]{:S(2)}, u32[]{:S(2)}) collective-permute-start(bf16[512,768]{1,0:T(8,128)(2,1)S(1)} %bitcast.60), channel_id=1, source_target_pairs={{448,0},{0,64},{64,128},{128,192},{192,256},{256,320},{320,384},{3... | collective-permute-start | bytes 2359304 | tf_op jit(solution)/shard_map/ppermute | solution.py:18
  47.2 19.2 %all-to-all-start.1 = ((bf16[8,64,384]{2,1,0:T(8,128)(2,1)}), bf16[8,64,384]{2,1,0:T(8,128)(2,1)}, u32[]{:S(2)}, u32[]{:S(2)}) async-start(bf16[8,64,384]{2,1,0:T(8,128)(2,1)} %broadcast_in_dim.15), calls=%async_computation.1 | async-start | bytes 786432 | tf_op jit(solution)/shard_map/all_to_all | solution.py:23
  66.4 23.8 %collective-permute-start.3 = (bf16[512,384]{1,0:T(8,128)(2,1)}, bf16[512,384]{1,0:T(8,128)(2,1)}, u32[]{:S(2)}, u32[]{:S(2)}) collective-permute-start(bf16[512,384]{1,0:T(8,128)(2,1)} %bitcast.2), channel_id=1, source_target_pairs={{448,0},{0,64},{64,128},{128,192},{192,256},{256,320},{320,384},{3... | collective-permute-start | bytes 1179656 | tf_op jit(solution)/shard_map/ppermute | solution.py:18
  68.3 24.8 %collective-permute-start.2 = (bf16[512,384]{1,0:T(8,128)(2,1)}, bf16[512,384]{1,0:T(8,128)(2,1)S(1)}, u32[]{:S(2)}, u32[]{:S(2)}) collective-permute-start(bf16[512,384]{1,0:T(8,128)(2,1)} %bitcast.2), channel_id=1, source_target_pairs={{64,0},{128,64},{192,128},{256,192},{320,256},{384,320},{448,384},... | collective-permute-start | bytes 1179656 | tf_op jit(solution)/shard_map/ppermute | solution.py:18
  74.6 23.2 %collective-permute-start.7 = (bf16[256,768]{1,0:T(8,128)(2,1)}, bf16[256,768]{1,0:T(8,128)(2,1)}, u32[]{:S(2)}, u32[]{:S(2)}) collective-permute-start(bf16[256,768]{1,0:T(8,128)(2,1)} %slice.59), channel_id=1, source_target_pairs={{448,0},{0,64},{64,128},{128,192},{192,256},{256,320},{320,384},{3... | collective-permute-start | bytes 1179656 | tf_op jit(solution)/shard_map/ppermute | solution.py:18
  78.8 32.4 %all-to-all-start.4 = ((bf16[8,64,768]{2,1,0:T(8,128)(2,1)}), bf16[8,64,768]{2,1,0:T(8,128)(2,1)}, u32[]{:S(2)}, u32[]{:S(2)}) async-start(bf16[8,64,768]{2,1,0:T(8,128)(2,1)} %broadcast_in_dim.17), calls=%async_computation.4 | async-start | bytes 1572864 | tf_op jit(solution)/shard_map/all_to_all | solution.py:23
  83.0 5.7 %copy-start.3 = (f32[256,768]{1,0:T(8,128)S(1)}, f32[256,768]{1,0:T(8,128)}, u32[]{:S(2)}) copy-start(f32[256,768]{1,0:T(8,128)} %fusion.60) | copy-start | bytes 2359300
  84.1 15.0 %collective-permute-start.6 = (bf16[256,768]{1,0:T(8,128)(2,1)S(1)}, bf16[256,768]{1,0:T(8,128)(2,1)S(1)}, u32[]{:S(2)}, u32[]{:S(2)}) collective-permute-start(bf16[256,768]{1,0:T(8,128)(2,1)S(1)} %slice.58), channel_id=1, source_target_pairs={{64,0},{128,64},{192,128},{256,192},{320,256},{384,320},{448,384},... | collective-permute-start | bytes 1179656 | tf_op jit(solution)/shard_map/ppermute | solution.py:18
  91.2 11.4 %collective-permute-start.5 = (bf16[256,384]{1,0:T(8,128)(2,1)S(1)}, bf16[256,384]{1,0:T(8,128)(2,1)S(1)}, u32[]{:S(2)}, u32[]{:S(2)}) collective-permute-start(bf16[256,384]{1,0:T(8,128)(2,1)S(1)} %slice.57), channel_id=1, source_target_pairs={{448,0},{0,64},{64,128},{128,192},{192,256},{256,320},{320,384},{3... | collective-permute-start | bytes 589832 | tf_op jit(solution)/shard_map/ppermute | solution.py:18
  93.1 6.3 %copy-start.4 = (bf16[256,2048]{1,0:T(8,128)(2,1)S(1)}, bf16[256,2048]{1,0:T(8,128)(2,1)}, u32[]{:S(2)}) copy-start(bf16[256,2048]{1,0:T(8,128)(2,1)} %param.13) | copy-start | bytes 3145732
  93.1 9.6 %collective-permute-start.4 = (bf16[256,384]{1,0:T(8,128)(2,1)S(1)}, bf16[256,384]{1,0:T(8,128)(2,1)S(1)}, u32[]{:S(2)}, u32[]{:S(2)}) collective-permute-start(bf16[256,384]{1,0:T(8,128)(2,1)S(1)} %slice.56), channel_id=1, source_target_pairs={{64,0},{128,64},{192,128},{256,192},{320,256},{384,320},{448,384},... | collective-permute-start | bytes 589832 | tf_op jit(solution)/shard_map/ppermute | solution.py:18
  111.1 7.3 %copy-start.1 = (bf16[256,2048]{1,0:T(8,128)(2,1)S(1)}, bf16[256,2048]{1,0:T(8,128)(2,1)}, u32[]{:S(2)}) copy-start(bf16[256,2048]{1,0:T(8,128)(2,1)} %param.11) | copy-start | bytes 3145732
  111.1 22.3 %all-to-all-start.2 = ((bf16[8,32,2048]{2,1,0:T(8,128)(2,1)}), bf16[8,32,2048]{2,1,0:T(8,128)(2,1)S(1)}, u32[]{:S(2)}, u32[]{:S(2)}) async-start(bf16[8,32,2048]{2,1,0:T(8,128)(2,1)} %bitcast.47), calls=%async_computation.2 | async-start | bytes 2097152 | tf_op jit(solution)/shard_map/all_to_all | solution.py:77
  118.8 14.7 %copy-start.11 = (bf16[384,64]{0,1:T(8,128)(2,1)S(1)}, bf16[384,64]{0,1:T(8,128)(2,1)}, u32[]{:S(2)}) copy-start(bf16[384,64]{0,1:T(8,128)(2,1)} %param.16) | copy-start | bytes 147460
  120.0 41.2 %collective-permute-start.8 = (bf16[512,768]{1,0:T(8,128)(2,1)}, bf16[512,768]{1,0:T(8,128)(2,1)}, u32[]{:S(2)}, u32[]{:S(2)}) collective-permute-start(bf16[512,768]{1,0:T(8,128)(2,1)} %bitcast.6), channel_id=1, source_target_pairs={{64,0},{128,64},{192,128},{256,192},{320,256},{384,320},{448,384},... | collective-permute-start | bytes 2359304 | tf_op jit(solution)/shard_map/ppermute | solution.py:18
  123.5 37.7 %collective-permute-start.9 = (bf16[512,768]{1,0:T(8,128)(2,1)}, bf16[512,768]{1,0:T(8,128)(2,1)}, u32[]{:S(2)}, u32[]{:S(2)}) collective-permute-start(bf16[512,768]{1,0:T(8,128)(2,1)} %bitcast.6), channel_id=1, source_target_pairs={{448,0},{0,64},{64,128},{128,192},{192,256},{256,320},{320,384},{3... | collective-permute-start | bytes 2359304 | tf_op jit(solution)/shard_map/ppermute | solution.py:18
  134.2 20.3 %all-to-all-start.5 = ((bf16[8,64,384]{2,1,0:T(8,128)(2,1)}), bf16[8,64,384]{2,1,0:T(8,128)(2,1)S(1)}, u32[]{:S(2)}, u32[]{:S(2)}) async-start(bf16[8,64,384]{2,1,0:T(8,128)(2,1)} %broadcast_in_dim.18), calls=%async_computation.5 | async-start | bytes 786432 | tf_op jit(solution)/shard_map/all_to_all | solution.py:23
  155.6 34.3 %all-to-all-start.3 = ((bf16[8,32,2048]{2,1,0:T(8,128)(2,1)}), bf16[8,32,2048]{2,1,0:T(8,128)(2,1)S(1)}, u32[]{:S(2)}, u32[]{:S(2)}) async-start(bf16[8,32,2048]{2,1,0:T(8,128)(2,1)} %broadcast_in_dim.16), calls=%async_computation.3 | async-start | bytes 2097152 | tf_op jit(solution)/shard_map/all_to_all | solution.py:23
  161.2 14.2 %copy-start.2 = (bf16[256,2048]{1,0:T(8,128)(2,1)S(1)}, bf16[256,2048]{1,0:T(8,128)(2,1)}, u32[]{:S(2)}) copy-start(bf16[256,2048]{1,0:T(8,128)(2,1)} %fusion.3) | copy-start | bytes 3145732
  161.2 17.2 %collective-permute-start.10 = (bf16[512,384]{1,0:T(8,128)(2,1)S(1)}, bf16[512,384]{1,0:T(8,128)(2,1)S(1)}, u32[]{:S(2)}, u32[]{:S(2)}) collective-permute-start(bf16[512,384]{1,0:T(8,128)(2,1)S(1)} %bitcast.63), channel_id=1, source_target_pairs={{64,0},{128,64},{192,128},{256,192},{320,256},{384,320},{448,384},... | collective-permute-start | bytes 1179656 | tf_op jit(solution)/shard_map/ppermute | solution.py:18
  164.9 18.1 %collective-permute-start.11 = (bf16[512,384]{1,0:T(8,128)(2,1)S(1)}, bf16[512,384]{1,0:T(8,128)(2,1)S(1)}, u32[]{:S(2)}, u32[]{:S(2)}) collective-permute-start(bf16[512,384]{1,0:T(8,128)(2,1)S(1)} %bitcast.64), channel_id=1, source_target_pairs={{448,0},{0,64},{64,128},{128,192},{192,256},{256,320},{320,384},{3... | collective-permute-start | bytes 1179656 | tf_op jit(solution)/shard_map/ppermute | solution.py:18
  167.9 17.8 %collective-permute-start.14 = (bf16[256,768]{1,0:T(8,128)(2,1)S(1)}, bf16[256,768]{1,0:T(8,128)(2,1)S(1)}, u32[]{:S(2)}, u32[]{:S(2)}) collective-permute-start(bf16[256,768]{1,0:T(8,128)(2,1)S(1)} %slice.64), channel_id=1, source_target_pairs={{64,0},{128,64},{192,128},{256,192},{320,256},{384,320},{448,384},... | collective-permute-start | bytes 1179656 | tf_op jit(solution)/shard_map/ppermute | solution.py:18
  173.5 12.8 %collective-permute-start.15 = (bf16[256,768]{1,0:T(8,128)(2,1)S(1)}, bf16[256,768]{1,0:T(8,128)(2,1)S(1)}, u32[]{:S(2)}, u32[]{:S(2)}) collective-permute-start(bf16[256,768]{1,0:T(8,128)(2,1)S(1)} %slice.65), channel_id=1, source_target_pairs={{448,0},{0,64},{64,128},{128,192},{192,256},{256,320},{320,384},{3... | collective-permute-start | bytes 1179656 | tf_op jit(solution)/shard_map/ppermute | solution.py:18
  178.5 12.0 %collective-permute-start.12 = (bf16[256,384]{1,0:T(8,128)(2,1)S(1)}, bf16[256,384]{1,0:T(8,128)(2,1)}, u32[]{:S(2)}, u32[]{:S(2)}) collective-permute-start(bf16[256,384]{1,0:T(8,128)(2,1)S(1)} %slice.62), channel_id=1, source_target_pairs={{64,0},{128,64},{192,128},{256,192},{320,256},{384,320},{448,384},... | collective-permute-start | bytes 589832 | tf_op jit(solution)/shard_map/ppermute | solution.py:18
  183.8 8.4 %collective-permute-start.13 = (bf16[256,384]{1,0:T(8,128)(2,1)}, bf16[256,384]{1,0:T(8,128)(2,1)}, u32[]{:S(2)}, u32[]{:S(2)}) collective-permute-start(bf16[256,384]{1,0:T(8,128)(2,1)} %slice.63), channel_id=1, source_target_pairs={{448,0},{0,64},{64,128},{128,192},{192,256},{256,320},{320,384},{3... | collective-permute-start | bytes 589832 | tf_op jit(solution)/shard_map/ppermute | solution.py:18
  185.7 0.8 copy-start.6
  186.5 0.7 copy-start.8
  190.2 3.1 %copy-start.5 = (f32[256,768]{1,0:T(8,128)S(1)}, f32[256,768]{1,0:T(8,128)}, u32[]{:S(2)}) copy-start(f32[256,768]{1,0:T(8,128)} %fusion.6) | copy-start | bytes 2359300
  193.7 10.4 %copy-start.14 = (bf16[256,384]{1,0:T(8,128)(2,1)}, bf16[256,384]{1,0:T(8,128)(2,1)S(1)}, u32[]{:S(2)}) copy-start(bf16[256,384]{1,0:T(8,128)(2,1)S(1)} %get-tuple-element.20) | copy-start | bytes 589828
  195.9 37.9 %collective-permute-start.16 = (bf16[512,384]{1,0:T(8,128)(2,1)}, bf16[512,384]{1,0:T(8,128)(2,1)S(1)}, u32[]{:S(2)}, u32[]{:S(2)}) collective-permute-start(bf16[512,384]{1,0:T(8,128)(2,1)} %fusion.9), channel_id=1, source_target_pairs={{448,0},{0,64},{64,128},{128,192},{192,256},{256,320},{320,384},{3... | collective-permute-start | bytes 1179656 | tf_op jit(solution)/shard_map/ppermute | solution.py:18
  197.9 36.0 %collective-permute-start.17 = (bf16[512,384]{1,0:T(8,128)(2,1)}, bf16[512,384]{1,0:T(8,128)(2,1)}, u32[]{:S(2)}, u32[]{:S(2)}) collective-permute-start(bf16[512,384]{1,0:T(8,128)(2,1)} %fusion.10), channel_id=1, source_target_pairs={{64,0},{128,64},{192,128},{256,192},{320,256},{384,320},{448,384},... | collective-permute-start | bytes 1179656 | tf_op jit(solution)/shard_map/ppermute | solution.py:18
  204.2 1.6 copy-start.7
  205.8 1.0 copy-start.9
  210.2 25.8 %all-to-all-start.6 = ((bf16[8,32,2048]{2,1,0:T(8,128)(2,1)}), bf16[8,32,2048]{2,1,0:T(8,128)(2,1)S(1)}, u32[]{:S(2)}, u32[]{:S(2)}) async-start(bf16[8,32,2048]{2,1,0:T(8,128)(2,1)} %bitcast.8), calls=%async_computation.6 | async-start | bytes 2097152 | tf_op jit(solution)/shard_map/all_to_all | solution.py:77
  217.7 16.1 %copy-start.15 = (bf16[256,384]{1,0:T(8,128)(2,1)S(1)}, bf16[256,384]{1,0:T(8,128)(2,1)}, u32[]{:S(2)}) copy-start(bf16[256,384]{1,0:T(8,128)(2,1)} %copy-done.14) | copy-start | bytes 589828
  219.1 13.1 %collective-permute-start.18 = (bf16[256,384]{1,0:T(8,128)(2,1)S(1)}, bf16[256,384]{1,0:T(8,128)(2,1)S(1)}, u32[]{:S(2)}, u32[]{:S(2)}) collective-permute-start(bf16[256,384]{1,0:T(8,128)(2,1)S(1)} %get-tuple-element.21), channel_id=1, source_target_pairs={{384,0},{448,64},{0,128},{64,192},{128,256},{192,320},{256,384},{3... | collective-permute-start | bytes 589832 | tf_op jit(solution)/shard_map/ppermute | solution.py:18
  221.0 12.8 %collective-permute-start.19 = (bf16[256,384]{1,0:T(8,128)(2,1)S(1)}, bf16[256,384]{1,0:T(8,128)(2,1)S(1)}, u32[]{:S(2)}, u32[]{:S(2)}) collective-permute-start(bf16[256,384]{1,0:T(8,128)(2,1)S(1)} %get-tuple-element.22), channel_id=1, source_target_pairs={{128,0},{192,64},{256,128},{320,192},{384,256},{448,320},{0,384},{... | collective-permute-start | bytes 589832 | tf_op jit(solution)/shard_map/ppermute | solution.py:18
  236.0 19.2 %all-to-all-start.8 = ((bf16[8,64,384]{2,1,0:T(8,128)(2,1)}), bf16[8,64,384]{2,1,0:T(8,128)(2,1)}, u32[]{:S(2)}, u32[]{:S(2)}) async-start(bf16[8,64,384]{2,1,0:T(8,128)(2,1)} %bitcast.10), calls=%async_computation.8 | async-start | bytes 786432 | tf_op jit(solution)/shard_map/all_to_all | solution.py:123
  256.3 8.7 %collective-permute-start.20 = (bf16[64,384]{1,0:T(8,128)(2,1)S(1)}, bf16[64,384]{1,0:T(8,128)(2,1)S(1)}, u32[]{:S(2)}, u32[]{:S(2)}) collective-permute-start(bf16[64,384]{1,0:T(8,128)(2,1)S(1)} %reduce_sum.110), channel_id=1, source_target_pairs={{256,0},{0,256},{257,1},{1,257},{258,2},{2,258},{259,3},{3,259},{2... | collective-permute-start | bytes 147464 | tf_op jit(solution)/shard_map/ppermute | solution.py:18
  266.3 14.3 %all-to-all-start.9 = ((f32[32,1,384]{2,1,0:T(1,128)}), f32[32,1,384]{2,1,0:T(1,128)S(1)}, u32[]{:S(2)}, u32[]{:S(2)}) async-start(f32[32,1,384]{2,1,0:T(1,128)} %broadcast_in_dim.20), calls=%async_computation.9 | async-start | bytes 98304 | tf_op jit(solution)/shard_map/all_to_all | solution.py:23
  281.7 21.6 %all-to-all-start.7 = ((bf16[8,32,2048]{2,1,0:T(8,128)(2,1)}), bf16[8,32,2048]{2,1,0:T(8,128)(2,1)S(1)}, u32[]{:S(2)}, u32[]{:S(2)}) async-start(bf16[8,32,2048]{2,1,0:T(8,128)(2,1)} %broadcast_in_dim.19), calls=%async_computation.7 | async-start | bytes 2097152 | tf_op jit(solution)/shard_map/all_to_all | solution.py:23

commit v3 on v2

v3 whole, which is shorter than its diff:
```python
import jax
import jax.numpy as jnp
from jax import lax
from jax.experimental import pallas as pl
from jax.experimental.pallas import tpu as pltpu
from jax.sharding import Mesh
from jax.sharding import PartitionSpec as P


FS = ("fs_0", "fs_1")
Z = ("rep", "fs_0")
REP_FS = ("rep", "fs_0", "fs_1")
f32 = jnp.float32
bf16 = jnp.bfloat16

eps = 1e-06
PIECES = ((0, None), (1, None), (3, None), (2, 0), (2, 1))
ROWS_ROWS = (((1,), (1,)), ((), ()))


def take_from(value, axis, step):
    n = lax.axis_size(axis)
    return lax.ppermute(value, axis, [((i + step) % n, i) for i in range(n)])


def from_everyone(value, axis):
    n = lax.axis_size(axis)
    return lax.all_to_all(
        jnp.broadcast_to(value[None], (n, *value.shape)), axis, 0, 0, tiled=True
    )


def along_y(value):
    whole = from_everyone(value, "fs_1")
    return whole.reshape(-1, value.shape[1])


def along_z(value):
    half = value.shape[0] // 2
    next_ = take_from(value, Z, 1)
    last = take_from(value, Z, -1)
    top = take_from(next_[:half], Z, 1)
    bottom = take_from(last[half:], Z, -1)
    return (value, next_, last, top, bottom)


def after(value, *others):
    return lax.optimization_barrier((value, *others))[0]


def span_of(z, piece, width):
    m, half = piece
    quarter = width // 4
    start = lax.rem(z + m, 4) * quarter
    if half is None:
        return pl.ds(pl.multiple_of(start, quarter), quarter)
    return pl.ds(pl.multiple_of(start + half * (quarter // 2), quarter // 2), quarter // 2)


def forward_body(z_ref, u_ref, w0, w1, w2, w3, w4, both_ref, hidden_ref):
    z = z_ref[0]
    width = u_ref.shape[1]
    field = u_ref[...].astype(f32)
    scale = lax.rsqrt(jnp.mean(field * field, axis=1, keepdims=True) + eps)
    total = None
    for piece, w in zip(PIECES, (w0, w1, w2, w3, w4)):
        normed_b = (u_ref[:, span_of(z, piece, width)].astype(f32) * scale).astype(bf16)
        part = jnp.dot(normed_b, w[...], preferred_element_type=f32)
        total = part if total is None else total + part
    both_ref[...] = total
    n = total.shape[1] // 2
    gate, upper = total[:, :n], total[:, n:]
    hidden_ref[...] = (gate * jax.nn.sigmoid(gate) * upper).astype(bf16)


def backward_body(z_ref, c_ref, both_ref, d0, d1, d2, d3, d4, w0, w1, w2, w3, w4, out_ref):
    z = z_ref[0]
    width = c_ref.shape[1]
    total = None
    for piece, w in zip(PIECES, (d0, d1, d2, d3, d4)):
        part = jnp.dot(
            c_ref[:, span_of(z, piece, width)], w[...], preferred_element_type=f32
        )
        total = part if total is None else total + part
    back = 0.5 * total
    n = back.shape[1]
    gate, upper = both_ref[:, :n], both_ref[:, n:]
    logistic = jax.nn.sigmoid(gate)
    d_gate = (back * upper * logistic * (1.0 + gate * (1.0 - logistic))).astype(bf16)
    d_up = (back * (gate * logistic)).astype(bf16)
    d_both = jnp.concatenate([d_gate, d_up], axis=1)
    for piece, w in zip(PIECES, (w0, w1, w2, w3, w4)):
        part = lax.dot_general(d_both, w[...], ROWS_ROWS, preferred_element_type=f32)
        out_ref[:, span_of(z, piece, width)] = part.astype(bf16)


SMEM = pl.BlockSpec(memory_space=pltpu.SMEM)
VMEM = pl.BlockSpec(memory_space=pltpu.VMEM)


def forward(z, u, gate_up):
    tokens, n = u.shape[0], gate_up[0].shape[1]
    return pl.pallas_call(
        forward_body,
        in_specs=[SMEM] + [VMEM] * 6,
        out_specs=(VMEM, VMEM),
        out_shape=(
            jax.ShapeDtypeStruct((tokens, n), f32),
            jax.ShapeDtypeStruct((tokens, n // 2), bf16),
        ),
        cost_estimate=pl.CostEstimate(
            flops=2 * tokens * u.shape[1] * n, bytes_accessed=5 << 20, transcendentals=0
        ),
    )(z, u, *gate_up)


def backward(z, c, both, down, gate_up):
    return pl.pallas_call(
        backward_body,
        in_specs=[SMEM] + [VMEM] * 12,
        out_specs=VMEM,
        out_shape=jax.ShapeDtypeStruct(c.shape, bf16),
        cost_estimate=pl.CostEstimate(
            flops=3 * c.shape[0] * c.shape[1] * both.shape[1],
            bytes_accessed=8 << 20,
            transcendentals=0,
        ),
    )(z, c, both, *down, *gate_up)


def own_rows(partial, u, c, tp):
    n = lax.axis_size("tp")
    pieces = partial.reshape(n, -1, partial.shape[1])
    pieces = lax.all_to_all(pieces, "tp", 0, 0, tiled=True)
    d_normed = pieces.astype(f32).sum(axis=0)
    rows = u.shape[0] // n
    field = lax.dynamic_slice_in_dim(u, tp * rows, rows, axis=0).astype(f32)
    scale = lax.rsqrt(jnp.mean(field * field, axis=1, keepdims=True) + eps)
    normed = field * scale
    carried = lax.dynamic_slice_in_dim(c, tp * rows, rows, axis=0).astype(f32)
    d_field = carried + scale * (
        d_normed - normed * jnp.mean(d_normed * normed, axis=1, keepdims=True)
    )
    return d_field.astype(bf16)


def all_rows(value, tp):
    n = lax.axis_size("tp")
    rows = value.shape[0]
    core, x = tp % 2, tp // 2
    quarters = [value]
    for j in (1, 2, 3):
        quarters.append(lax.ppermute(value, "tp", [((i + 2 * j) % n, i) for i in range(n)]))
    mine = jnp.stack(quarters)
    other = lax.ppermute(mine, "tp", [(i, i ^ 1) for i in range(n)])
    pair = jnp.where(core == 0, jnp.stack([mine, other], 1), jnp.stack([other, mine], 1))
    return jnp.roll(pair, x, axis=0).reshape(n * rows, -1)


def down_column(hidden, grad, z):
    span = grad.shape[1] // 4
    half = span // 2

    def part(m):
        cols = lax.dynamic_slice_in_dim(grad, ((z + m) % 4) * span, span, axis=1)
        return 0.5 * lax.dot_general(
            cols, hidden, (((0,), (0,)), ((), ())), preferred_element_type=f32
        )

    far = part(2).astype(bf16)
    top = take_from(far[:half], Z, -2).astype(f32)
    bottom = take_from(far[half:], Z, 2).astype(f32)
    next_ = take_from(part(1).astype(bf16), Z, -1).astype(f32)
    last = take_from(part(3).astype(bf16), Z, 1).astype(f32)
    column = part(0) + next_ + last + jnp.concatenate([top, bottom], axis=0)
    return column.astype(bf16).reshape(lax.axis_size("fs_1"), -1, hidden.shape[1])


def step(
    tokens,
    mid_tokens,
    out_grad,
    gate_first,
    up_first,
    down_first,
    gate_second,
    up_second,
    down_second,
):
    z = lax.axis_index("fs_0")
    zs = z.astype(jnp.int32).reshape(1)
    tp = lax.axis_index("tp")

    gu2 = along_y(jnp.concatenate([gate_second, up_second], axis=1))
    dn2 = along_y(after(down_second.T, gu2))
    gu1 = along_y(after(jnp.concatenate([gate_first, up_first], axis=1), dn2))
    dn1 = along_y(after(down_first.T, gu1))
    gate_up_2 = along_z(gu2)
    down_2 = along_z(after(dn2, gate_up_2[1], gate_up_2[2]))
    both_2, _ = forward(zs, mid_tokens, gate_up_2)
    partial_2 = backward(zs, out_grad, both_2, down_2, gate_up_2)

    gate_up_1 = along_z(after(gu1, down_2[1], down_2[2]))
    down_1 = along_z(after(dn1, gate_up_1[1], gate_up_1[2]))
    rows_2 = own_rows(after(partial_2, dn1), mid_tokens, out_grad, tp)
    mid_grad = from_everyone(rows_2, "tp").reshape(mid_tokens.shape)

    both_1, hidden = forward(zs, tokens, gate_up_1)
    column = down_column(hidden, mid_grad, z)
    partial_1 = backward(zs, mid_grad, both_1, down_1, gate_up_1)
    rows_1 = own_rows(partial_1, tokens, mid_grad, tp)
    column = after(column, rows_1)
    share = lax.all_to_all(column, "fs_1", 0, 0, tiled=True)
    share = share.astype(f32).sum(axis=0).astype(bf16)
    input_grad = all_rows(rows_1, tp)
    share = share.astype(f32) + take_from(share, "rep", 1).astype(f32)
    norms = from_everyone(jnp.sum(share * share, axis=0), FS).sum(axis=0)
    return (input_grad, share.T, norms)


def solution(mesh):
    torus = Mesh(
        mesh.devices.reshape(mesh.shape["rep"], 4, 8, mesh.shape["tp"]),
        ("rep", "fs_0", "fs_1", "tp"),
    )
    placed = (
        P(REP_FS, None),
        P(REP_FS, None),
        P(REP_FS, None),
        P(FS, "tp"),
        P(FS, "tp"),
        P("tp", FS),
        P(FS, "tp"),
        P(FS, "tp"),
        P("tp", FS),
    )
    return jax.shard_map(
        step,
        mesh=torus,
        in_specs=placed,
        out_specs=(P(REP_FS, None), P("tp", FS), P("tp")),
        check_vma=False,
    )
```

time: 307 us -> 283 us (0.922)
  waiting for transfers between devices: 104 us -> 69.1 us
  matrix products: 34.6 us -> 4.72 us
  blocking collectives: 0 us -> 28.1 us
  Pallas kernels: 0 us -> 19.6 us
  starting transfers between devices: 138 us -> 130 us
    all_to_all x7 -> x5, waiting for transfers between devices: 70.7 us -> 18.8 us  [from_everyone(): lax.all_to_all(jnp.broadcast_to(value[None], (n, *value.shape)), axis, 0,...]
    dot_general x30 -> x0, matrix products: 28.9 us -> none  [the longest x20 18.6 us: contract(): part = jnp.dot(columns(x, z, piece), piece[2], preferred_element_type=f32)]
    all_to_all x0 -> x1, blocking collectives: none -> 28.1 us  [from_everyone(): lax.all_to_all(jnp.broadcast_to(value[None], (n, *value.shape)), axis, 0,...]
    ppermute x21, waiting for transfers between devices: 10.9 us -> 32.9 us  [take_from(): return lax.ppermute(value, axis, [((i + step) % n, i) for i in range(n)])]
    pallas_call x0 -> x4, Pallas kernels: none -> 19.6 us  [the longest x2 11 us: backward(): pl.pallas_call(backward_body, in_specs=[SMEM] + [VMEM] * 12, out_specs=VM...]
    all_to_all x7 -> x5, starting transfers between devices: 40.3 us -> 22.8 us  [from_everyone(): lax.all_to_all(jnp.broadcast_to(value[None], (n, *value.shape)), axis, 0,...]
    ppermute x0 -> x4, starting transfers between devices: none -> 15.1 us  [the longest x3 11.3 us: all_rows(): lax.ppermute(value, 'tp', [((i + 2 * j) % n, i) for i in range(n)])]
    ppermute x21, starting transfers between devices: 78.6 us -> 67.5 us  [take_from(): return lax.ppermute(value, axis, [((i + step) % n, i) for i in range(n)])]
  transfers between devices with their start and end apart: 31 -> 33, of which waited for: 12 -> 13; matrix products, arithmetic and copies ran while one was open for 16% -> 8% of each run, Pallas kernels for 0% -> 5%
where the time goes in v3:
time: 283 us; the launch traced here: 279 us
  starting transfers between devices  130 us (46%)
  waiting for transfers between devices  69.1 us (24%)
  blocking collectives  28.1 us (10%)
  Pallas kernels  19.6 us (7%)
  local copies, waits for them, and re-layouts  16.6 us (6%)
  other arithmetic  9.63 us (3%)
  matrix products  4.72 us (2%)
    ppermute x21, starting transfers between devices, take_from(): return lax.ppermute(value, axis, [((i + step) % n, i) for i in range(n)])  67.5 us
    ppermute x21, waiting for transfers between devices, take_from(): return lax.ppermute(value, axis, [((i + step) % n, i) for i in range(n)])  32.9 us
    all_to_all x1, blocking collectives, from_everyone(): lax.all_to_all(jnp.broadcast_to(value[None], (n, *value.shape)), axis, 0,...  28.1 us
    all_to_all x5, starting transfers between devices, from_everyone(): lax.all_to_all(jnp.broadcast_to(value[None], (n, *value.shape)), axis, 0,...  22.8 us
    all_to_all x5, waiting for transfers between devices, from_everyone(): lax.all_to_all(jnp.broadcast_to(value[None], (n, *value.shape)), axis, 0,...  18.8 us
    all_to_all x2, starting transfers between devices, own_rows(): pieces = lax.all_to_all(pieces, 'tp', 0, 0, tiled=True)  17.6 us
    ppermute x3, starting transfers between devices, all_rows(): lax.ppermute(value, 'tp', [((i + 2 * j) % n, i) for i in range(n)])  11.3 us
    pallas_call x2, Pallas kernels, backward(): pl.pallas_call(backward_body, in_specs=[SMEM] + [VMEM] * 12, out_specs=VM...  11 us
  transfers between devices with their start and end apart: 33, of which 13 were waited for; matrix products, arithmetic and copies ran while one was open for 8% of the time, Pallas kernels for 5%

profile of v3, /device:TPU:1, one launch (start us, length us, event | category | flops | bytes accessed | tf_op | source)
XLA Modules:
  0.0 279.0 jit_solution(3667552238510726080)
XLA Ops:
  1.6 28.1 %all_to_all.46 = bf16[8,64,768]{2,1,0:T(8,128)(2,1)S(1)} all-to-all(bf16[8,64,768]{2,1,0:T(8,128)(2,1)S(1)} %broadcast_in_dim.12), channel_id=1, replica_groups=mesh['rep'=2,'fs_0'=4,'fs_1'=8,'tp'=8] {'fs_1'}, dimensions={0} | all-to-all | bytes 1572864 | tf_op jit(solution)/shard_map/all_to_all | solution.py:28
  30.5 3.5 %all-to-all-start.1 = ((bf16[8,64,384]{2,1,0:T(8,128)(2,1)}), bf16[8,64,384]{2,1,0:T(8,128)(2,1)S(1)}, u32[]{:S(2)}, u32[]{:S(2)}) async-start(bf16[8,64,384]{2,1,0:T(8,128)(2,1)} %broadcast_in_dim.13), calls=%async_computation.1 | async-start | bytes 786432 | tf_op jit(solution)/shard_map/all_to_all | solution.py:28
  34.0 11.1 %all-to-all-done.1 = bf16[8,64,384]{2,1,0:T(8,128)(2,1)S(1)} async-done(((bf16[8,64,384]{2,1,0:T(8,128)(2,1)}), bf16[8,64,384]{2,1,0:T(8,128)(2,1)S(1)}, u32[]{:S(2)}, u32[]{:S(2)}) %all-to-all-start.1) | async-done | bytes 393248 | tf_op jit(solution)/shard_map/all_to_all | solution.py:28
  46.2 3.5 %all-to-all-start.2 = ((bf16[8,64,768]{2,1,0:T(8,128)(2,1)}), bf16[8,64,768]{2,1,0:T(8,128)(2,1)S(1)}, u32[]{:S(2)}, u32[]{:S(2)}) async-start(bf16[8,64,768]{2,1,0:T(8,128)(2,1)} %broadcast_in_dim.14), calls=%async_computation.2 | async-start | bytes 1572864 | tf_op jit(solution)/shard_map/all_to_all | solution.py:28
  49.7 12.8 %collective-permute-start = (bf16[512,768]{1,0:T(8,128)(2,1)S(1)}, bf16[512,768]{1,0:T(8,128)(2,1)S(1)}, u32[]{:S(2)}, u32[]{:S(2)}) collective-permute-start(bf16[512,768]{1,0:T(8,128)(2,1)S(1)} %bitcast.29), channel_id=1, source_target_pairs={{64,0},{128,64},{192,128},{256,192},{320,256},{384,320},{448,384},... | collective-permute-start | bytes 2359304 | tf_op jit(solution)/shard_map/ppermute | solution.py:23
  62.5 1.9 collective-permute-start.1
  64.4 11.4 %collective-permute-done.w1 = bf16[512,768]{1,0:T(8,128)(2,1)S(1)} collective-permute-done((bf16[512,768]{1,0:T(8,128)(2,1)S(1)}, bf16[512,768]{1,0:T(8,128)(2,1)S(1)}, u32[]{:S(2)}, u32[]{:S(2)}) %collective-permute-start) | collective-permute-done | bytes 786464 | tf_op jit(solution)/shard_map/ppermute | solution.py:23
  75.9 5.1 %collective-permute-done.1.w2 = bf16[512,768]{1,0:T(8,128)(2,1)S(1)} collective-permute-done((bf16[512,768]{1,0:T(8,128)(2,1)S(1)}, bf16[512,768]{1,0:T(8,128)(2,1)S(1)}, u32[]{:S(2)}, u32[]{:S(2)}) %collective-permute-start.1) | collective-permute-done | bytes 786464 | tf_op jit(solution)/shard_map/ppermute | solution.py:23
  80.9 1.9 collective-permute-start.4
  82.8 3.4 %collective-permute-start.5 = (bf16[512,384]{1,0:T(8,128)(2,1)}, bf16[512,384]{1,0:T(8,128)(2,1)}, u32[]{:S(2)}, u32[]{:S(2)}) collective-permute-start(bf16[512,384]{1,0:T(8,128)(2,1)} %bitcast.42), channel_id=1, source_target_pairs={{448,0},{0,64},{64,128},{128,192},{192,256},{256,320},{320,384},{3... | collective-permute-start | bytes 1179656 | tf_op jit(solution)/shard_map/ppermute | solution.py:23
  87.1 6.3 %all-to-all-start.3 = ((bf16[8,64,384]{2,1,0:T(8,128)(2,1)}), bf16[8,64,384]{2,1,0:T(8,128)(2,1)}, u32[]{:S(2)}, u32[]{:S(2)}) async-start(bf16[8,64,384]{2,1,0:T(8,128)(2,1)} %broadcast_in_dim.15), calls=%async_computation.3 | async-start | bytes 786432 | tf_op jit(solution)/shard_map/all_to_all | solution.py:28
  94.2 3.1 %collective-permute-start.2 = (bf16[256,768]{1,0:T(8,128)(2,1)}, bf16[256,768]{1,0:T(8,128)(2,1)S(1)}, u32[]{:S(2)}, u32[]{:S(2)}) collective-permute-start(bf16[256,768]{1,0:T(8,128)(2,1)} %slice.40), channel_id=1, source_target_pairs={{64,0},{128,64},{192,128},{256,192},{320,256},{384,320},{448,384},... | collective-permute-start | bytes 1179656 | tf_op jit(solution)/shard_map/ppermute | solution.py:23
  98.1 2.1 collective-permute-start.3
  101.2 4.3 %collective-permute-start.6 = (bf16[256,384]{1,0:T(8,128)(2,1)S(1)}, bf16[256,384]{1,0:T(8,128)(2,1)S(1)}, u32[]{:S(2)}, u32[]{:S(2)}) collective-permute-start(bf16[256,384]{1,0:T(8,128)(2,1)S(1)} %slice.42), channel_id=1, source_target_pairs={{64,0},{128,64},{192,128},{256,192},{320,256},{384,320},{448,384},... | collective-permute-start | bytes 589832 | tf_op jit(solution)/shard_map/ppermute | solution.py:23
  106.5 1.9 collective-permute-start.7
  109.3 4.3 %shard_map.112 = (f32[256,768]{1,0:T(8,128)}, bf16[256,384]{1,0:T(8,128)(2,1)}) custom-call(s32[1]{0:T(128)} %bitcast.z_ref, bf16[256,2048]{1,0:T(8,128)(2,1)} %u_ref.2, bf16[512,768]{1,0:T(8,128)(2,1)} %bitcast.31, bf16[512,768]{1,0:T(8,128)(2,1)} %copy-done.4, bf16[512,768]{1,0:T(8,128)(2,1)} %copy-done.5, bf16[256,768]{1,0:T(8,128)(2,1)} %copy-done.10, ...), custom_call_target="tpu_custom_call" | custom-call | flops 805306368 | bytes 5242880 | tf_op jit(solution)/shard_map/pallas_call | solution.py:103
  113.6 2.9 %collective-permute-done.7.d4 = bf16[256,384]{1,0:T(8,128)(2,1)S(1)} collective-permute-done((bf16[256,384]{1,0:T(8,128)(2,1)S(1)}, bf16[256,384]{1,0:T(8,128)(2,1)S(1)}, u32[]{:S(2)}, u32[]{:S(2)}) %collective-permute-start.7) | collective-permute-done | bytes 196640 | tf_op jit(solution)/shard_map/ppermute | solution.py:23
  117.2 5.5 %shard_map.113 = bf16[256,2048]{1,0:T(8,128)(2,1)} custom-call(s32[1]{0:T(128)} %bitcast.z_ref, bf16[256,2048]{1,0:T(8,128)(2,1)} %c_ref.1, f32[256,768]{1,0:T(8,128)} %get-tuple-element.14.both_ref, bf16[512,384]{1,0:T(8,128)(2,1)} %bitcast.43, bf16[512,384]{1,0:T(8,128)(2,1)} %collective-permute-done.4.d1, bf16[512,384]{1,0:T(8,128)(2,1)} %collective-permute-done.5.d2, ...), custom_call_target="tpu_custom_call" | custom-call | flops 1207959552 | bytes 8388608 | tf_op jit(solution)/shard_map/pallas_call | solution.py:118
  122.7 9.9 %all-to-all-start.4 = ((bf16[8,32,2048]{2,1,0:T(8,128)(2,1)}), bf16[8,32,2048]{2,1,0:T(8,128)(2,1)S(1)}, u32[]{:S(2)}, u32[]{:S(2)}) async-start(bf16[8,32,2048]{2,1,0:T(8,128)(2,1)} %bitcast.39), calls=%async_computation.4 | async-start | bytes 2097152 | tf_op jit(solution)/shard_map/all_to_all | solution.py:134
  133.7 2.7 collective-permute-start.8
  136.4 2.6 collective-permute-start.9
  139.0 8.6 %all-to-all-done.4 = bf16[8,32,2048]{2,1,0:T(8,128)(2,1)S(1)} async-done(((bf16[8,32,2048]{2,1,0:T(8,128)(2,1)}), bf16[8,32,2048]{2,1,0:T(8,128)(2,1)S(1)}, u32[]{:S(2)}, u32[]{:S(2)}) %all-to-all-start.4) | async-done | bytes 1048608 | tf_op jit(solution)/shard_map/all_to_all | solution.py:134
  151.0 4.4 %all-to-all-start.5 = ((bf16[8,32,2048]{2,1,0:T(8,128)(2,1)}), bf16[8,32,2048]{2,1,0:T(8,128)(2,1)S(1)}, u32[]{:S(2)}, u32[]{:S(2)}) async-start(bf16[8,32,2048]{2,1,0:T(8,128)(2,1)} %broadcast_in_dim.16), calls=%async_computation.5 | async-start | bytes 2097152 | tf_op jit(solution)/shard_map/all_to_all | solution.py:28
  155.5 2.8 %collective-permute-done.9.w2 = bf16[512,768]{1,0:T(8,128)(2,1)S(1)} collective-permute-done((bf16[512,768]{1,0:T(8,128)(2,1)S(1)}, bf16[512,768]{1,0:T(8,128)(2,1)S(1)}, u32[]{:S(2)}, u32[]{:S(2)}) %collective-permute-start.9) | collective-permute-done | bytes 786464 | tf_op jit(solution)/shard_map/ppermute | solution.py:23
  158.3 1.9 collective-permute-start.12
  160.2 3.4 %collective-permute-start.13 = (bf16[512,384]{1,0:T(8,128)(2,1)}, bf16[512,384]{1,0:T(8,128)(2,1)}, u32[]{:S(2)}, u32[]{:S(2)}) collective-permute-start(bf16[512,384]{1,0:T(8,128)(2,1)} %bitcast.6.d0), channel_id=1, source_target_pairs={{448,0},{0,64},{64,128},{128,192},{192,256},{256,320},{320,384},{3... | collective-permute-start | bytes 1179656 | tf_op jit(solution)/shard_map/ppermute | solution.py:23
  164.4 3.1 %collective-permute-start.10 = (bf16[256,768]{1,0:T(8,128)(2,1)}, bf16[256,768]{1,0:T(8,128)(2,1)S(1)}, u32[]{:S(2)}, u32[]{:S(2)}) collective-permute-start(bf16[256,768]{1,0:T(8,128)(2,1)} %slice.44), channel_id=1, source_target_pairs={{64,0},{128,64},{192,128},{256,192},{320,256},{384,320},{448,384},... | collective-permute-start | bytes 1179656 | tf_op jit(solution)/shard_map/ppermute | solution.py:23
  168.3 2.1 collective-permute-start.11
  173.2 4.3 %collective-permute-start.14 = (bf16[256,384]{1,0:T(8,128)(2,1)}, bf16[256,384]{1,0:T(8,128)(2,1)}, u32[]{:S(2)}, u32[]{:S(2)}) collective-permute-start(bf16[256,384]{1,0:T(8,128)(2,1)} %slice.46), channel_id=1, source_target_pairs={{64,0},{128,64},{192,128},{256,192},{320,256},{384,320},{448,384},... | collective-permute-start | bytes 589832 | tf_op jit(solution)/shard_map/ppermute | solution.py:23
  178.5 1.9 collective-permute-start.15
  182.1 4.3 %shard_map.114 = (f32[256,768]{1,0:T(8,128)}, bf16[256,384]{1,0:T(8,128)(2,1)}) custom-call(s32[1]{0:T(128)} %bitcast.z_ref, bf16[256,2048]{1,0:T(8,128)(2,1)} %u_ref.3, bf16[512,768]{1,0:T(8,128)(2,1)} %bitcast.27, bf16[512,768]{1,0:T(8,128)(2,1)} %copy-done.2, bf16[512,768]{1,0:T(8,128)(2,1)} %copy-done.3, bf16[256,768]{1,0:T(8,128)(2,1)} %copy-done.8, ...), custom_call_target="tpu_custom_call" | custom-call | flops 805306368 | bytes 5242880 | tf_op jit(solution)/shard_map/pallas_call | solution.py:103
  187.4 5.5 %shard_map.115 = bf16[256,2048]{1,0:T(8,128)(2,1)} custom-call(s32[1]{0:T(128)} %bitcast.z_ref, bf16[256,2048]{1,0:T(8,128)(2,1)} %bitcast.33, f32[256,768]{1,0:T(8,128)} %get-tuple-element.21.both_ref, bf16[512,384]{1,0:T(8,128)(2,1)} %bitcast.6.d0, bf16[512,384]{1,0:T(8,128)(2,1)} %collective-permute-done.12.d1, ...), custom_call_target="tpu_custom_call" | custom-call | flops 1207959552 | bytes 8388608 | tf_op jit(solution)/shard_map/pallas_call | solution.py:118
  192.9 7.7 %all-to-all-start.6 = ((bf16[8,32,2048]{2,1,0:T(8,128)(2,1)}), bf16[8,32,2048]{2,1,0:T(8,128)(2,1)S(1)}, u32[]{:S(2)}, u32[]{:S(2)}) async-start(bf16[8,32,2048]{2,1,0:T(8,128)(2,1)} %bitcast.40), calls=%async_computation.6 | async-start | bytes 2097152 | tf_op jit(solution)/shard_map/all_to_all | solution.py:134
  201.7 3.9 %collective-permute-start.21 = (bf16[512,384]{1,0:T(8,128)(2,1)}, bf16[512,384]{1,0:T(8,128)(2,1)S(1)}, u32[]{:S(2)}, u32[]{:S(2)}) collective-permute-start(bf16[512,384]{1,0:T(8,128)(2,1)} %fusion.5), channel_id=1, source_target_pairs={{64,0},{128,64},{192,128},{256,192},{320,256},{384,320},{448,384},... | collective-permute-start | bytes 1179656 | tf_op jit(solution)/shard_map/ppermute | solution.py:23
  206.7 1.9 collective-permute-start.20
  209.0 3.1 %collective-permute-start.23 = (bf16[256,384]{1,0:T(8,128)(2,1)S(1)}, bf16[256,384]{1,0:T(8,128)(2,1)}, u32[]{:S(2)}, u32[]{:S(2)}) collective-permute-start(bf16[256,384]{1,0:T(8,128)(2,1)S(1)} %get-tuple-element.28), channel_id=1, source_target_pairs={{128,0},{192,64},{256,128},{320,192},{384,256},{448,320},{0,384},{... | collective-permute-start | bytes 589832 | tf_op jit(solution)/shard_map/ppermute | solution.py:23
  212.1 3.1 %collective-permute-start.22 = (bf16[256,384]{1,0:T(8,128)(2,1)S(1)}, bf16[256,384]{1,0:T(8,128)(2,1)}, u32[]{:S(2)}, u32[]{:S(2)}) collective-permute-start(bf16[256,384]{1,0:T(8,128)(2,1)S(1)} %get-tuple-element.27), channel_id=1, source_target_pairs={{384,0},{448,64},{0,128},{64,192},{128,256},{192,320},{256,384},{3... | collective-permute-start | bytes 589832 | tf_op jit(solution)/shard_map/ppermute | solution.py:23
  217.9 2.9 %collective-permute-start.18 = (bf16[32,2048]{1,0:T(8,128)(2,1)S(1)}, bf16[32,2048]{1,0:T(8,128)(2,1)S(1)}, u32[]{:S(2)}, u32[]{:S(2)}) collective-permute-start(bf16[32,2048]{1,0:T(8,128)(2,1)S(1)} %fusion.16), channel_id=1, source_target_pairs={{6,0},{7,1},{0,2},{1,3},{2,4},{3,5},{4,6},{5,7},{14,8},{15,9},{8,1... | collective-permute-start | bytes 393224 | tf_op jit(solution)/shard_map/ppermute | solution.py:153
  222.6 4.4 %collective-permute-start.17 = (bf16[32,2048]{1,0:T(8,128)(2,1)S(1)}, bf16[32,2048]{1,0:T(8,128)(2,1)S(1)}, u32[]{:S(2)}, u32[]{:S(2)}) collective-permute-start(bf16[32,2048]{1,0:T(8,128)(2,1)S(1)} %fusion.16), channel_id=1, source_target_pairs={{4,0},{5,1},{6,2},{7,3},{0,4},{1,5},{2,6},{3,7},{12,8},{13,9},{14,... | collective-permute-start | bytes 393224 | tf_op jit(solution)/shard_map/ppermute | solution.py:153
  227.8 4.1 %collective-permute-start.16 = (bf16[32,2048]{1,0:T(8,128)(2,1)S(1)}, bf16[32,2048]{1,0:T(8,128)(2,1)S(1)}, u32[]{:S(2)}, u32[]{:S(2)}) collective-permute-start(bf16[32,2048]{1,0:T(8,128)(2,1)S(1)} %fusion.16), channel_id=1, source_target_pairs={{2,0},{3,1},{4,2},{5,3},{6,4},{7,5},{0,6},{1,7},{10,8},{11,9},{12,... | collective-permute-start | bytes 393224 | tf_op jit(solution)/shard_map/ppermute | solution.py:153
  231.9 2.2 fusion.3
  234.1 6.9 %all-to-all-start.7 = ((bf16[8,64,384]{2,1,0:T(8,128)(2,1)}), bf16[8,64,384]{2,1,0:T(8,128)(2,1)S(1)}, u32[]{:S(2)}, u32[]{:S(2)}) async-start(bf16[8,64,384]{2,1,0:T(8,128)(2,1)} %bitcast.17), calls=%async_computation.7 | async-start | bytes 786432 | tf_op jit(solution)/shard_map/all_to_all | solution.py:213
  241.1 3.8 %collective-permute-start.19 = (bf16[4,32,2048]{2,1,0:T(8,128)(2,1)S(1)}, bf16[4,32,2048]{2,1,0:T(8,128)(2,1)S(1)}, u32[]{:S(2)}, u32[]{:S(2)}) collective-permute-start(bf16[4,32,2048]{2,1,0:T(8,128)(2,1)S(1)} %get-tuple-element.26), channel_id=1, source_target_pairs={{0,1},{1,0},{2,3},{3,2},{4,5},{5,4},{6,7},{7,6},{8,9},{9,8},{10,11... | collective-permute-start | bytes 1572872 | tf_op jit(solution)/shard_map/ppermute | solution.py:155
  245.0 8.5 %all-to-all-done.7 = bf16[8,64,384]{2,1,0:T(8,128)(2,1)S(1)} async-done(((bf16[8,64,384]{2,1,0:T(8,128)(2,1)}), bf16[8,64,384]{2,1,0:T(8,128)(2,1)S(1)}, u32[]{:S(2)}, u32[]{:S(2)}) %all-to-all-start.7) | async-done | bytes 393248 | tf_op jit(solution)/shard_map/all_to_all | solution.py:213
  253.5 1.9 collective-permute-start.24
  255.6 7.2 %collective-permute-done.24 = bf16[64,384]{1,0:T(8,128)(2,1)S(1)} collective-permute-done((bf16[64,384]{1,0:T(8,128)(2,1)S(1)}, bf16[64,384]{1,0:T(8,128)(2,1)S(1)}, u32[]{:S(2)}, u32[]{:S(2)}) %collective-permute-start.24) | collective-permute-done | bytes 49184 | tf_op jit(solution)/shard_map/ppermute | solution.py:23
  264.2 5.1 %all-to-all-start.8 = ((f32[32,1,384]{2,1,0:T(1,128)}), f32[32,1,384]{2,1,0:T(1,128)S(1)}, u32[]{:S(2)}, u32[]{:S(2)}) async-start(f32[32,1,384]{2,1,0:T(1,128)} %broadcast_in_dim.17), calls=%async_computation.8 | async-start | bytes 98304 | tf_op jit(solution)/shard_map/all_to_all | solution.py:28
  270.7 7.6 %all-to-all-done.8 = f32[32,1,384]{2,1,0:T(1,128)S(1)} async-done(((f32[32,1,384]{2,1,0:T(1,128)}), f32[32,1,384]{2,1,0:T(1,128)S(1)}, u32[]{:S(2)}, u32[]{:S(2)}) %all-to-all-start.8) | async-done | bytes 49184 | tf_op jit(solution)/shard_map/all_to_all | solution.py:28
  (105 shorter events, 32.6 us)
Async XLA Ops:
  1.5 28.2 %copy-start.16 = (bf16[384,64]{0,1:T(8,128)(2,1)S(1)}, bf16[384,64]{0,1:T(8,128)(2,1)}, u32[]{:S(2)}) copy-start(bf16[384,64]{0,1:T(8,128)(2,1)} %param.17) | copy-start | bytes 147460
  1.5 32.4 %copy-start.18 = (bf16[64,384]{1,0:T(8,128)(2,1)S(1)}, bf16[64,384]{1,0:T(8,128)(2,1)}, u32[]{:S(2)}) copy-start(bf16[64,384]{1,0:T(8,128)(2,1)} %param.13) | copy-start | bytes 147460
  1.6 32.4 %copy-start.19 = (bf16[64,384]{1,0:T(8,128)(2,1)S(1)}, bf16[64,384]{1,0:T(8,128)(2,1)}, u32[]{:S(2)}) copy-start(bf16[64,384]{1,0:T(8,128)(2,1)} %param.12) | copy-start | bytes 147460
  29.6 32.9 %copy-start.1 = (bf16[8,64,768]{2,1,0:T(8,128)(2,1)}, bf16[8,64,768]{2,1,0:T(8,128)(2,1)S(1)}, u32[]{:S(2)}) copy-start(bf16[8,64,768]{2,1,0:T(8,128)(2,1)S(1)} %all_to_all.46) | copy-start | bytes 2359300
  30.5 14.7 %all-to-all-start.1 = ((bf16[8,64,384]{2,1,0:T(8,128)(2,1)}), bf16[8,64,384]{2,1,0:T(8,128)(2,1)S(1)}, u32[]{:S(2)}, u32[]{:S(2)}) async-start(bf16[8,64,384]{2,1,0:T(8,128)(2,1)} %broadcast_in_dim.13), calls=%async_computation.1 | async-start | bytes 786432 | tf_op jit(solution)/shard_map/all_to_all | solution.py:28
  45.1 1.0 copy-start.12
  45.1 41.1 %copy-start.17 = (bf16[384,64]{0,1:T(8,128)(2,1)S(1)}, bf16[384,64]{0,1:T(8,128)(2,1)}, u32[]{:S(2)}) copy-start(bf16[384,64]{0,1:T(8,128)(2,1)} %param.14) | copy-start | bytes 147460
  46.2 40.1 %all-to-all-start.2 = ((bf16[8,64,768]{2,1,0:T(8,128)(2,1)}), bf16[8,64,768]{2,1,0:T(8,128)(2,1)S(1)}, u32[]{:S(2)}, u32[]{:S(2)}) async-start(bf16[8,64,768]{2,1,0:T(8,128)(2,1)} %broadcast_in_dim.14), calls=%async_computation.2 | async-start | bytes 1572864 | tf_op jit(solution)/shard_map/all_to_all | solution.py:28
  49.7 26.2 %collective-permute-start = (bf16[512,768]{1,0:T(8,128)(2,1)S(1)}, bf16[512,768]{1,0:T(8,128)(2,1)S(1)}, u32[]{:S(2)}, u32[]{:S(2)}) collective-permute-start(bf16[512,768]{1,0:T(8,128)(2,1)S(1)} %bitcast.29), channel_id=1, source_target_pairs={{64,0},{128,64},{192,128},{256,192},{320,256},{384,320},{448,384},... | collective-permute-start | bytes 2359304 | tf_op jit(solution)/shard_map/ppermute | solution.py:23
  62.5 18.4 %collective-permute-start.1 = (bf16[512,768]{1,0:T(8,128)(2,1)S(1)}, bf16[512,768]{1,0:T(8,128)(2,1)S(1)}, u32[]{:S(2)}, u32[]{:S(2)}) collective-permute-start(bf16[512,768]{1,0:T(8,128)(2,1)S(1)} %bitcast.30), channel_id=1, source_target_pairs={{448,0},{0,64},{64,128},{128,192},{192,256},{256,320},{320,384},{3... | collective-permute-start | bytes 2359304 | tf_op jit(solution)/shard_map/ppermute | solution.py:23
  75.9 22.2 %copy-start.4 = (bf16[512,768]{1,0:T(8,128)(2,1)}, bf16[512,768]{1,0:T(8,128)(2,1)S(1)}, u32[]{:S(2)}) copy-start(bf16[512,768]{1,0:T(8,128)(2,1)S(1)} %collective-permute-done.w1) | copy-start | bytes 2359300
  80.9 17.2 %copy-start.5 = (bf16[512,768]{1,0:T(8,128)(2,1)}, bf16[512,768]{1,0:T(8,128)(2,1)S(1)}, u32[]{:S(2)}) copy-start(bf16[512,768]{1,0:T(8,128)(2,1)S(1)} %collective-permute-done.1.w2) | copy-start | bytes 2359300
  80.9 19.3 %collective-permute-start.4 = (bf16[512,384]{1,0:T(8,128)(2,1)}, bf16[512,384]{1,0:T(8,128)(2,1)}, u32[]{:S(2)}, u32[]{:S(2)}) collective-permute-start(bf16[512,384]{1,0:T(8,128)(2,1)} %bitcast.41), channel_id=1, source_target_pairs={{64,0},{128,64},{192,128},{256,192},{320,256},{384,320},{448,384},... | collective-permute-start | bytes 1179656 | tf_op jit(solution)/shard_map/ppermute | solution.py:23
  82.8 22.7 %collective-permute-start.5 = (bf16[512,384]{1,0:T(8,128)(2,1)}, bf16[512,384]{1,0:T(8,128)(2,1)}, u32[]{:S(2)}, u32[]{:S(2)}) collective-permute-start(bf16[512,384]{1,0:T(8,128)(2,1)} %bitcast.42), channel_id=1, source_target_pairs={{448,0},{0,64},{64,128},{128,192},{192,256},{256,320},{320,384},{3... | collective-permute-start | bytes 1179656 | tf_op jit(solution)/shard_map/ppermute | solution.py:23
  86.2 50.2 %copy-start = (bf16[8,64,768]{2,1,0:T(8,128)(2,1)}, bf16[8,64,768]{2,1,0:T(8,128)(2,1)S(1)}, u32[]{:S(2)}) copy-start(bf16[8,64,768]{2,1,0:T(8,128)(2,1)S(1)} %all-to-all-done.2) | copy-start | bytes 2359300
  87.1 35.6 %all-to-all-start.3 = ((bf16[8,64,384]{2,1,0:T(8,128)(2,1)}), bf16[8,64,384]{2,1,0:T(8,128)(2,1)}, u32[]{:S(2)}, u32[]{:S(2)}) async-start(bf16[8,64,384]{2,1,0:T(8,128)(2,1)} %broadcast_in_dim.15), calls=%async_computation.3 | async-start | bytes 786432 | tf_op jit(solution)/shard_map/all_to_all | solution.py:28
  94.2 14.3 %collective-permute-start.2 = (bf16[256,768]{1,0:T(8,128)(2,1)}, bf16[256,768]{1,0:T(8,128)(2,1)S(1)}, u32[]{:S(2)}, u32[]{:S(2)}) collective-permute-start(bf16[256,768]{1,0:T(8,128)(2,1)} %slice.40), channel_id=1, source_target_pairs={{64,0},{128,64},{192,128},{256,192},{320,256},{384,320},{448,384},... | collective-permute-start | bytes 1179656 | tf_op jit(solution)/shard_map/ppermute | solution.py:23
  98.1 10.4 %collective-permute-start.3 = (bf16[256,768]{1,0:T(8,128)(2,1)}, bf16[256,768]{1,0:T(8,128)(2,1)S(1)}, u32[]{:S(2)}, u32[]{:S(2)}) collective-permute-start(bf16[256,768]{1,0:T(8,128)(2,1)} %slice.41), channel_id=1, source_target_pairs={{448,0},{0,64},{64,128},{128,192},{192,256},{256,320},{320,384},{3... | collective-permute-start | bytes 1179656 | tf_op jit(solution)/shard_map/ppermute | solution.py:23
  101.2 12.4 %collective-permute-start.6 = (bf16[256,384]{1,0:T(8,128)(2,1)S(1)}, bf16[256,384]{1,0:T(8,128)(2,1)S(1)}, u32[]{:S(2)}, u32[]{:S(2)}) collective-permute-start(bf16[256,384]{1,0:T(8,128)(2,1)S(1)} %slice.42), channel_id=1, source_target_pairs={{64,0},{128,64},{192,128},{256,192},{320,256},{384,320},{448,384},... | collective-permute-start | bytes 589832 | tf_op jit(solution)/shard_map/ppermute | solution.py:23
  106.5 10.0 %collective-permute-start.7 = (bf16[256,384]{1,0:T(8,128)(2,1)S(1)}, bf16[256,384]{1,0:T(8,128)(2,1)S(1)}, u32[]{:S(2)}, u32[]{:S(2)}) collective-permute-start(bf16[256,384]{1,0:T(8,128)(2,1)S(1)} %slice.43), channel_id=1, source_target_pairs={{448,0},{0,64},{64,128},{128,192},{192,256},{256,320},{320,384},{3... | collective-permute-start | bytes 589832 | tf_op jit(solution)/shard_map/ppermute | solution.py:23
  113.6 2.9 %copy-start.13 = (bf16[256,384]{1,0:T(8,128)(2,1)}, bf16[256,384]{1,0:T(8,128)(2,1)S(1)}, u32[]{:S(2)}) copy-start(bf16[256,384]{1,0:T(8,128)(2,1)S(1)} %collective-permute-done.6.d3) | copy-start | bytes 589828
  122.7 24.9 %all-to-all-start.4 = ((bf16[8,32,2048]{2,1,0:T(8,128)(2,1)}), bf16[8,32,2048]{2,1,0:T(8,128)(2,1)S(1)}, u32[]{:S(2)}, u32[]{:S(2)}) async-start(bf16[8,32,2048]{2,1,0:T(8,128)(2,1)} %bitcast.39), calls=%async_computation.4 | async-start | bytes 2097152 | tf_op jit(solution)/shard_map/all_to_all | solution.py:134
  133.7 21.8 %collective-permute-start.8 = (bf16[512,768]{1,0:T(8,128)(2,1)S(1)}, bf16[512,768]{1,0:T(8,128)(2,1)S(1)}, u32[]{:S(2)}, u32[]{:S(2)}) collective-permute-start(bf16[512,768]{1,0:T(8,128)(2,1)S(1)} %bitcast.25), channel_id=1, source_target_pairs={{64,0},{128,64},{192,128},{256,192},{320,256},{384,320},{448,384},... | collective-permute-start | bytes 2359304 | tf_op jit(solution)/shard_map/ppermute | solution.py:23
  136.4 21.9 %collective-permute-start.9 = (bf16[512,768]{1,0:T(8,128)(2,1)S(1)}, bf16[512,768]{1,0:T(8,128)(2,1)S(1)}, u32[]{:S(2)}, u32[]{:S(2)}) collective-permute-start(bf16[512,768]{1,0:T(8,128)(2,1)S(1)} %bitcast.26), channel_id=1, source_target_pairs={{448,0},{0,64},{64,128},{128,192},{192,256},{256,320},{320,384},{3... | collective-permute-start | bytes 2359304 | tf_op jit(solution)/shard_map/ppermute | solution.py:23
  151.0 35.4 %all-to-all-start.5 = ((bf16[8,32,2048]{2,1,0:T(8,128)(2,1)}), bf16[8,32,2048]{2,1,0:T(8,128)(2,1)S(1)}, u32[]{:S(2)}, u32[]{:S(2)}) async-start(bf16[8,32,2048]{2,1,0:T(8,128)(2,1)} %broadcast_in_dim.16), calls=%async_computation.5 | async-start | bytes 2097152 | tf_op jit(solution)/shard_map/all_to_all | solution.py:28
  155.5 17.7 %copy-start.2 = (bf16[512,768]{1,0:T(8,128)(2,1)}, bf16[512,768]{1,0:T(8,128)(2,1)S(1)}, u32[]{:S(2)}) copy-start(bf16[512,768]{1,0:T(8,128)(2,1)S(1)} %collective-permute-done.8.w1) | copy-start | bytes 2359300
  158.3 14.9 %copy-start.3 = (bf16[512,768]{1,0:T(8,128)(2,1)}, bf16[512,768]{1,0:T(8,128)(2,1)S(1)}, u32[]{:S(2)}) copy-start(bf16[512,768]{1,0:T(8,128)(2,1)S(1)} %collective-permute-done.9.w2) | copy-start | bytes 2359300
  158.3 13.3 %collective-permute-start.12 = (bf16[512,384]{1,0:T(8,128)(2,1)}, bf16[512,384]{1,0:T(8,128)(2,1)}, u32[]{:S(2)}, u32[]{:S(2)}) collective-permute-start(bf16[512,384]{1,0:T(8,128)(2,1)} %bitcast.6.d0), channel_id=1, source_target_pairs={{64,0},{128,64},{192,128},{256,192},{320,256},{384,320},{448,384},... | collective-permute-start | bytes 1179656 | tf_op jit(solution)/shard_map/ppermute | solution.py:23
  160.2 17.3 %collective-permute-start.13 = (bf16[512,384]{1,0:T(8,128)(2,1)}, bf16[512,384]{1,0:T(8,128)(2,1)}, u32[]{:S(2)}, u32[]{:S(2)}) collective-permute-start(bf16[512,384]{1,0:T(8,128)(2,1)} %bitcast.6.d0), channel_id=1, source_target_pairs={{448,0},{0,64},{64,128},{128,192},{192,256},{256,320},{320,384},{3... | collective-permute-start | bytes 1179656 | tf_op jit(solution)/shard_map/ppermute | solution.py:23
  164.4 16.0 %collective-permute-start.10 = (bf16[256,768]{1,0:T(8,128)(2,1)}, bf16[256,768]{1,0:T(8,128)(2,1)S(1)}, u32[]{:S(2)}, u32[]{:S(2)}) collective-permute-start(bf16[256,768]{1,0:T(8,128)(2,1)} %slice.44), channel_id=1, source_target_pairs={{64,0},{128,64},{192,128},{256,192},{320,256},{384,320},{448,384},... | collective-permute-start | bytes 1179656 | tf_op jit(solution)/shard_map/ppermute | solution.py:23
  168.3 13.0 %collective-permute-start.11 = (bf16[256,768]{1,0:T(8,128)(2,1)}, bf16[256,768]{1,0:T(8,128)(2,1)S(1)}, u32[]{:S(2)}, u32[]{:S(2)}) collective-permute-start(bf16[256,768]{1,0:T(8,128)(2,1)} %slice.45), channel_id=1, source_target_pairs={{448,0},{0,64},{64,128},{128,192},{192,256},{256,320},{320,384},{3... | collective-permute-start | bytes 1179656 | tf_op jit(solution)/shard_map/ppermute | solution.py:23
  173.2 13.2 %collective-permute-start.14 = (bf16[256,384]{1,0:T(8,128)(2,1)}, bf16[256,384]{1,0:T(8,128)(2,1)}, u32[]{:S(2)}, u32[]{:S(2)}) collective-permute-start(bf16[256,384]{1,0:T(8,128)(2,1)} %slice.46), channel_id=1, source_target_pairs={{64,0},{128,64},{192,128},{256,192},{320,256},{384,320},{448,384},... | collective-permute-start | bytes 589832 | tf_op jit(solution)/shard_map/ppermute | solution.py:23
  178.5 7.9 %collective-permute-start.15 = (bf16[256,384]{1,0:T(8,128)(2,1)S(1)}, bf16[256,384]{1,0:T(8,128)(2,1)S(1)}, u32[]{:S(2)}, u32[]{:S(2)}) collective-permute-start(bf16[256,384]{1,0:T(8,128)(2,1)S(1)} %slice.47), channel_id=1, source_target_pairs={{448,0},{0,64},{64,128},{128,192},{192,256},{256,320},{320,384},{3... | collective-permute-start | bytes 589832 | tf_op jit(solution)/shard_map/ppermute | solution.py:23
  186.4 1.0 copy-start.6
  192.9 7.7 %copy-start.7 = (bf16[8,32,2048]{2,1,0:T(8,128)(2,1)S(1)}, bf16[8,32,2048]{2,1,0:T(8,128)(2,1)}, u32[]{:S(2)}) copy-start(bf16[8,32,2048]{2,1,0:T(8,128)(2,1)} %copy-done.6) | copy-start | bytes 3145732
  192.9 7.7 %copy-start.20 = (bf16[256,384]{1,0:T(8,128)(2,1)S(1)}, bf16[256,384]{1,0:T(8,128)(2,1)}, u32[]{:S(2)}) copy-start(bf16[256,384]{1,0:T(8,128)(2,1)} %get-tuple-element.23) | copy-start | bytes 589828
  192.9 22.6 %all-to-all-start.6 = ((bf16[8,32,2048]{2,1,0:T(8,128)(2,1)}), bf16[8,32,2048]{2,1,0:T(8,128)(2,1)S(1)}, u32[]{:S(2)}, u32[]{:S(2)}) async-start(bf16[8,32,2048]{2,1,0:T(8,128)(2,1)} %bitcast.40), calls=%async_computation.6 | async-start | bytes 2097152 | tf_op jit(solution)/shard_map/all_to_all | solution.py:134
  201.7 30.1 %collective-permute-start.21 = (bf16[512,384]{1,0:T(8,128)(2,1)}, bf16[512,384]{1,0:T(8,128)(2,1)S(1)}, u32[]{:S(2)}, u32[]{:S(2)}) collective-permute-start(bf16[512,384]{1,0:T(8,128)(2,1)} %fusion.5), channel_id=1, source_target_pairs={{64,0},{128,64},{192,128},{256,192},{320,256},{384,320},{448,384},... | collective-permute-start | bytes 1179656 | tf_op jit(solution)/shard_map/ppermute | solution.py:23
  206.7 25.1 %collective-permute-start.20 = (bf16[512,384]{1,0:T(8,128)(2,1)}, bf16[512,384]{1,0:T(8,128)(2,1)S(1)}, u32[]{:S(2)}, u32[]{:S(2)}) collective-permute-start(bf16[512,384]{1,0:T(8,128)(2,1)} %fusion.4), channel_id=1, source_target_pairs={{448,0},{0,64},{64,128},{128,192},{192,256},{256,320},{320,384},{3... | collective-permute-start | bytes 1179656 | tf_op jit(solution)/shard_map/ppermute | solution.py:23
  209.0 13.5 %collective-permute-start.23 = (bf16[256,384]{1,0:T(8,128)(2,1)S(1)}, bf16[256,384]{1,0:T(8,128)(2,1)}, u32[]{:S(2)}, u32[]{:S(2)}) collective-permute-start(bf16[256,384]{1,0:T(8,128)(2,1)S(1)} %get-tuple-element.28), channel_id=1, source_target_pairs={{128,0},{192,64},{256,128},{320,192},{384,256},{448,320},{0,384},{... | collective-permute-start | bytes 589832 | tf_op jit(solution)/shard_map/ppermute | solution.py:23
  212.1 15.6 %collective-permute-start.22 = (bf16[256,384]{1,0:T(8,128)(2,1)S(1)}, bf16[256,384]{1,0:T(8,128)(2,1)}, u32[]{:S(2)}, u32[]{:S(2)}) collective-permute-start(bf16[256,384]{1,0:T(8,128)(2,1)S(1)} %get-tuple-element.27), channel_id=1, source_target_pairs={{384,0},{448,64},{0,128},{64,192},{128,256},{192,320},{256,384},{3... | collective-permute-start | bytes 589832 | tf_op jit(solution)/shard_map/ppermute | solution.py:23
  217.9 23.1 %collective-permute-start.18 = (bf16[32,2048]{1,0:T(8,128)(2,1)S(1)}, bf16[32,2048]{1,0:T(8,128)(2,1)S(1)}, u32[]{:S(2)}, u32[]{:S(2)}) collective-permute-start(bf16[32,2048]{1,0:T(8,128)(2,1)S(1)} %fusion.16), channel_id=1, source_target_pairs={{6,0},{7,1},{0,2},{1,3},{2,4},{3,5},{4,6},{5,7},{14,8},{15,9},{8,1... | collective-permute-start | bytes 393224 | tf_op jit(solution)/shard_map/ppermute | solution.py:153
  222.6 18.5 %collective-permute-start.17 = (bf16[32,2048]{1,0:T(8,128)(2,1)S(1)}, bf16[32,2048]{1,0:T(8,128)(2,1)S(1)}, u32[]{:S(2)}, u32[]{:S(2)}) collective-permute-start(bf16[32,2048]{1,0:T(8,128)(2,1)S(1)} %fusion.16), channel_id=1, source_target_pairs={{4,0},{5,1},{6,2},{7,3},{0,4},{1,5},{2,6},{3,7},{12,8},{13,9},{14,... | collective-permute-start | bytes 393224 | tf_op jit(solution)/shard_map/ppermute | solution.py:153
  227.8 13.2 %collective-permute-start.16 = (bf16[32,2048]{1,0:T(8,128)(2,1)S(1)}, bf16[32,2048]{1,0:T(8,128)(2,1)S(1)}, u32[]{:S(2)}, u32[]{:S(2)}) collective-permute-start(bf16[32,2048]{1,0:T(8,128)(2,1)S(1)} %fusion.16), channel_id=1, source_target_pairs={{2,0},{3,1},{4,2},{5,3},{6,4},{7,5},{0,6},{1,7},{10,8},{11,9},{12,... | collective-permute-start | bytes 393224 | tf_op jit(solution)/shard_map/ppermute | solution.py:153
  234.1 19.4 %all-to-all-start.7 = ((bf16[8,64,384]{2,1,0:T(8,128)(2,1)}), bf16[8,64,384]{2,1,0:T(8,128)(2,1)S(1)}, u32[]{:S(2)}, u32[]{:S(2)}) async-start(bf16[8,64,384]{2,1,0:T(8,128)(2,1)} %bitcast.17), calls=%async_computation.7 | async-start | bytes 786432 | tf_op jit(solution)/shard_map/all_to_all | solution.py:213
  241.1 14.3 %collective-permute-start.19 = (bf16[4,32,2048]{2,1,0:T(8,128)(2,1)S(1)}, bf16[4,32,2048]{2,1,0:T(8,128)(2,1)S(1)}, u32[]{:S(2)}, u32[]{:S(2)}) collective-permute-start(bf16[4,32,2048]{2,1,0:T(8,128)(2,1)S(1)} %get-tuple-element.26), channel_id=1, source_target_pairs={{0,1},{1,0},{2,3},{3,2},{4,5},{5,4},{6,7},{7,6},{8,9},{9,8},{10,11... | collective-permute-start | bytes 1572872 | tf_op jit(solution)/shard_map/ppermute | solution.py:155
  253.5 9.4 %collective-permute-start.24 = (bf16[64,384]{1,0:T(8,128)(2,1)S(1)}, bf16[64,384]{1,0:T(8,128)(2,1)S(1)}, u32[]{:S(2)}, u32[]{:S(2)}) collective-permute-start(bf16[64,384]{1,0:T(8,128)(2,1)S(1)} %reduce_sum.90), channel_id=1, source_target_pairs={{256,0},{0,256},{257,1},{1,257},{258,2},{2,258},{259,3},{3,259},{2... | collective-permute-start | bytes 147464 | tf_op jit(solution)/shard_map/ppermute | solution.py:23
  264.2 14.2 %all-to-all-start.8 = ((f32[32,1,384]{2,1,0:T(1,128)}), f32[32,1,384]{2,1,0:T(1,128)S(1)}, u32[]{:S(2)}, u32[]{:S(2)}) async-start(f32[32,1,384]{2,1,0:T(1,128)} %broadcast_in_dim.17), calls=%async_computation.8 | async-start | bytes 98304 | tf_op jit(solution)/shard_map/all_to_all | solution.py:28
  (6 other events, 4.6 us)

commit v4 on v3

v4 whole, which is shorter than its diff:
```python
import jax
import jax.numpy as jnp
from jax import lax
from jax.experimental import pallas as pl
from jax.experimental.pallas import tpu as pltpu
from jax.sharding import Mesh
from jax.sharding import PartitionSpec as P


FS = ("fs_0", "fs_1")
Z = ("rep", "fs_0")
REP_FS = ("rep", "fs_0", "fs_1")
f32 = jnp.float32
bf16 = jnp.bfloat16

eps = 1e-06
PIECES = ((0, None), (1, None), (3, None), (2, 0), (2, 1))
ROWS_ROWS = (((1,), (1,)), ((), ()))


def take_from(value, axis, step):
    n = lax.axis_size(axis)
    return lax.ppermute(value, axis, [((i + step) % n, i) for i in range(n)])


def from_everyone(value, axis):
    n = lax.axis_size(axis)
    return lax.all_to_all(
        jnp.broadcast_to(value[None], (n, *value.shape)), axis, 0, 0, tiled=True
    )


def along_y(value):
    whole = from_everyone(value, "fs_1")
    return whole.reshape(-1, value.shape[1])


def along_z(value):
    half = value.shape[0] // 2
    next_ = take_from(value, Z, 1)
    last = take_from(value, Z, -1)
    top = take_from(next_[:half], Z, 1)
    bottom = take_from(last[half:], Z, -1)
    return (value, next_, last, top, bottom)


def after(value, *others):
    return lax.optimization_barrier((value, *others))[0]


def span_of(z, piece, width):
    m, half = piece
    quarter = width // 4
    start = lax.rem(z + m, 4) * quarter
    if half is None:
        return pl.ds(pl.multiple_of(start, quarter), quarter)
    return pl.ds(pl.multiple_of(start + half * (quarter // 2), quarter // 2), quarter // 2)


def gate_up_of(z, u_ref, pieces, n):
    width = u_ref.shape[1]
    field = u_ref[...].astype(f32)
    scale = lax.rsqrt(jnp.mean(field * field, axis=1, keepdims=True) + eps)
    total = None
    for piece, w in zip(PIECES, pieces):
        normed_b = (u_ref[:, span_of(z, piece, width)].astype(f32) * scale).astype(bf16)
        part = jnp.dot(normed_b, w[:, : 2 * n], preferred_element_type=f32)
        total = part if total is None else total + part
    return total[:, :n], total[:, n:]


def partial_of(z, c_ref, gate, upper, pieces, out_ref):
    width, n = c_ref.shape[1], gate.shape[1]
    total = None
    for piece, w in zip(PIECES, pieces):
        part = jnp.dot(
            c_ref[:, span_of(z, piece, width)], w[:, 2 * n :], preferred_element_type=f32
        )
        total = part if total is None else total + part
    back = 0.5 * total
    logistic = jax.nn.sigmoid(gate)
    d_gate = (back * upper * logistic * (1.0 + gate * (1.0 - logistic))).astype(bf16)
    d_up = (back * (gate * logistic)).astype(bf16)
    d_both = jnp.concatenate([d_gate, d_up], axis=1)
    for piece, w in zip(PIECES, pieces):
        part = lax.dot_general(d_both, w[:, : 2 * n], ROWS_ROWS, preferred_element_type=f32)
        out_ref[:, span_of(z, piece, width)] = part.astype(bf16)


def block_body(z_ref, u_ref, c_ref, w0, w1, w2, w3, w4, out_ref):
    z, pieces = z_ref[0], (w0, w1, w2, w3, w4)
    gate, upper = gate_up_of(z, u_ref, pieces, w0.shape[1] // 3)
    partial_of(z, c_ref, gate, upper, pieces, out_ref)


def forward_body(z_ref, u_ref, w0, w1, w2, w3, w4, both_ref, hidden_ref):
    n = hidden_ref.shape[1]
    gate, upper = gate_up_of(z_ref[0], u_ref, (w0, w1, w2, w3, w4), n)
    both_ref[:, :n] = gate
    both_ref[:, n:] = upper
    hidden_ref[...] = (gate * jax.nn.sigmoid(gate) * upper).astype(bf16)


def backward_body(z_ref, c_ref, both_ref, w0, w1, w2, w3, w4, out_ref):
    n = both_ref.shape[1] // 2
    pieces = (w0, w1, w2, w3, w4)
    partial_of(z_ref[0], c_ref, both_ref[:, :n], both_ref[:, n:], pieces, out_ref)


SMEM = pl.BlockSpec(memory_space=pltpu.SMEM)
VMEM = pl.BlockSpec(memory_space=pltpu.VMEM)


def kernel(body, outs, matmuls, z, *arrays):
    tokens, width, n = arrays[0].shape[0], arrays[0].shape[1], arrays[-1].shape[1] // 3
    return pl.pallas_call(
        body,
        in_specs=[SMEM] + [VMEM] * len(arrays),
        out_specs=tuple(VMEM for _ in outs),
        out_shape=tuple(jax.ShapeDtypeStruct(*o) for o in outs),
        cost_estimate=pl.CostEstimate(
            flops=2 * tokens * width * n * matmuls, bytes_accessed=6 << 20, transcendentals=0
        ),
    )(z, *arrays)


def gradient_of_rows(d_normed, u, c, tp):
    rows = d_normed.shape[0]
    field = lax.dynamic_slice_in_dim(u, tp * rows, rows, axis=0).astype(f32)
    scale = lax.rsqrt(jnp.mean(field * field, axis=1, keepdims=True) + eps)
    normed = field * scale
    carried = lax.dynamic_slice_in_dim(c, tp * rows, rows, axis=0).astype(f32)
    d_field = carried + scale * (
        d_normed - normed * jnp.mean(d_normed * normed, axis=1, keepdims=True)
    )
    return d_field.astype(bf16)


def own_rows(partial):
    pieces = partial.reshape(lax.axis_size("tp"), -1, partial.shape[1])
    pieces = lax.all_to_all(pieces, "tp", 0, 0, tiled=True)
    return pieces.astype(f32).sum(axis=0)


def swap_cores(value):
    return lax.ppermute(value, "tp", [(i, i ^ 1) for i in range(lax.axis_size("tp"))])


def take_x(value, step):
    n = lax.axis_size("tp")
    return lax.ppermute(value, "tp", [((i + 2 * step) % n, i) for i in range(n)])


def own_rows_by_permutes(partial, core, x):
    rows = partial.shape[0]
    half, n = rows // 2, rows // 8
    other = swap_cores(lax.dynamic_slice_in_dim(partial, (1 - core) * half, half, axis=0))
    mine = lax.dynamic_slice_in_dim(partial, core * half, half, axis=0)
    chip = (mine.astype(f32) + other.astype(f32)).astype(bf16)

    def block(j):
        return lax.dynamic_slice_in_dim(chip, ((x + j) % 4) * n, n, axis=0)

    total = block(0).astype(f32)
    for j in (2, 1, 3):
        total = total + take_x(block(j), -j).astype(f32)
    return total


def all_rows(value, core, x):
    rows = value.shape[0]
    quarters = [value]
    for j in (1, 2, 3):
        quarters.append(take_x(value, j))
    mine = jnp.stack(quarters)
    other = swap_cores(mine)
    pair = jnp.where(core == 0, jnp.stack([mine, other]), jnp.stack([other, mine]))
    return jnp.roll(pair, x, axis=1).reshape(8 * rows, -1)


def step(
    tokens,
    mid_tokens,
    out_grad,
    gate_first,
    up_first,
    down_first,
    gate_second,
    up_second,
    down_second,
):
    zs = lax.axis_index("fs_0").astype(jnp.int32).reshape(1)
    tp = lax.axis_index("tp")
    core, x = tp % 2, tp // 2
    rep = lax.axis_index("rep")
    n, width = gate_first.shape[1], tokens.shape[1]
    like_u = (tokens.shape, bf16)

    all2 = along_y(jnp.concatenate([gate_second, up_second, down_second.T], axis=1))
    all1 = jnp.concatenate([gate_first, up_first, down_first.T], axis=1)
    all1 = along_y(after(all1, all2))
    weight_2 = along_z(all2)
    weight_1 = along_z(after(all1, weight_2[1], weight_2[2]))

    (partial,) = kernel(block_body, (like_u,), 5, zs, mid_tokens, out_grad, *weight_2)
    rows = own_rows(after(partial, all1))
    rows = gradient_of_rows(rows, mid_tokens, out_grad, tp)
    mid_grad = from_everyone(rows, "tp").reshape(mid_tokens.shape)

    both, hidden = kernel(
        forward_body,
        (((tokens.shape[0], 2 * n), f32), ((tokens.shape[0], n), bf16)),
        2,
        zs,
        tokens,
        *weight_1,
    )
    share = 0.5 * lax.dot_general(
        mid_grad, hidden, (((0,), (0,)), ((), ())), preferred_element_type=f32
    )
    share = share.astype(bf16).reshape(width // 64, 2, 32, n).swapaxes(0, 1)
    share = lax.all_to_all(share.reshape(width // 32, 32, n), REP_FS, 0, 0, tiled=True)
    share = share.astype(f32).sum(axis=0)
    twin = take_from(share, "rep", 1)
    norms = from_everyone(jnp.sum(share * share, axis=0), REP_FS).sum(axis=0)
    share = jnp.where(rep == 0, jnp.stack([share, twin]), jnp.stack([twin, share]))

    (partial,) = kernel(backward_body, (like_u,), 3, zs, mid_grad, both, *weight_1)
    rows = own_rows_by_permutes(partial, core, x)
    rows = gradient_of_rows(rows, tokens, mid_grad, core * 4 + x)
    input_grad = all_rows(rows, core, x)
    return (input_grad, share.reshape(64, n).T, norms)


def solution(mesh):
    torus = Mesh(
        mesh.devices.reshape(mesh.shape["rep"], 4, 8, mesh.shape["tp"]),
        ("rep", "fs_0", "fs_1", "tp"),
    )
    placed = (
        P(REP_FS, None),
        P(REP_FS, None),
        P(REP_FS, None),
        P(FS, "tp"),
        P(FS, "tp"),
        P("tp", FS),
        P(FS, "tp"),
        P(FS, "tp"),
        P("tp", FS),
    )
    return jax.shard_map(
        step,
        mesh=torus,
        in_specs=placed,
        out_specs=(P(REP_FS, None), P("tp", FS), P("tp")),
        check_vma=False,
    )
```

time: 283 us -> 269 us (0.951)
  waiting for transfers between devices: 69.1 us -> 118 us
  blocking collectives: 28.1 us -> 0 us
  starting transfers between devices: 130 us -> 103 us
  other arithmetic: 9.63 us -> 13.5 us
  local copies, waits for them, and re-layouts: 16.6 us -> 13 us
    ppermute x21 -> x9, starting transfers between devices: 67.5 us -> 37.7 us  [take_from(): return lax.ppermute(value, axis, [((i + step) % n, i) for i in range(n)])]
    all_to_all x1 -> x0, blocking collectives: 28.1 us -> none  [from_everyone(): lax.all_to_all(jnp.broadcast_to(value[None], (n, *value.shape)), axis, 0,...]
    ppermute x21 -> x9, waiting for transfers between devices: 32.9 us -> 58.1 us  [take_from(): return lax.ppermute(value, axis, [((i + step) % n, i) for i in range(n)])]
    all_to_all x5 -> x4, waiting for transfers between devices: 18.8 us -> 41.2 us  [from_everyone(): lax.all_to_all(jnp.broadcast_to(value[None], (n, *value.shape)), axis, 0,...]
    ppermute x4 -> x8, starting transfers between devices: 15.1 us -> 27 us  [the longest x6 18.9 us: take_x(): lax.ppermute(value, 'tp', [((i + 2 * step) % n, i) for i in range(n)])]
    all_to_all x2 -> x1, starting transfers between devices: 17.6 us -> 6.78 us  [own_rows(): pieces = lax.all_to_all(pieces, 'tp', 0, 0, tiled=True)]
    ppermute x4 -> x8, waiting for transfers between devices: 0.01 us -> 10.5 us  [the longest x6 8.96 us: take_x(): lax.ppermute(value, 'tp', [((i + 2 * step) % n, i) for i in range(n)])]
    all_to_all x1, waiting for transfers between devices: 8.49 us -> 0.01 us  [step(): lax.all_to_all(share.reshape(width // 32, 32, n), REP_FS, 0, 0, tiled=True)]
  transfers between devices with their start and end apart: 33 -> 23, of which waited for: 13 -> 14; matrix products, arithmetic and copies ran while one was open for 8% -> 7% of each run, Pallas kernels for 5% -> 4%
where the time goes in v4:
time: 269 us; the launch traced here: 268 us
  waiting for transfers between devices  118 us (44%)
  starting transfers between devices  103 us (38%)
  Pallas kernels  16.9 us (6%)
  other arithmetic  13.5 us (5%)
  local copies, waits for them, and re-layouts  13 us (5%)
    ppermute x9, waiting for transfers between devices, take_from(): return lax.ppermute(value, axis, [((i + step) % n, i) for i in range(n)])  58.1 us
    all_to_all x4, waiting for transfers between devices, from_everyone(): lax.all_to_all(jnp.broadcast_to(value[None], (n, *value.shape)), axis, 0,...  41.2 us
    ppermute x9, starting transfers between devices, take_from(): return lax.ppermute(value, axis, [((i + step) % n, i) for i in range(n)])  37.7 us
    all_to_all x4, starting transfers between devices, from_everyone(): lax.all_to_all(jnp.broadcast_to(value[None], (n, *value.shape)), axis, 0,...  23.9 us
    ppermute x6, starting transfers between devices, take_x(): lax.ppermute(value, 'tp', [((i + 2 * step) % n, i) for i in range(n)])  18.9 us
    pallas_call x3, Pallas kernels, kernel(): pl.pallas_call(body, in_specs=[SMEM] + [VMEM] * len(arrays), out_specs=tu...  16.9 us
    ppermute x6, waiting for transfers between devices, take_x(): lax.ppermute(value, 'tp', [((i + 2 * step) % n, i) for i in range(n)])  8.96 us
    all_to_all x1, waiting for transfers between devices, own_rows(): pieces = lax.all_to_all(pieces, 'tp', 0, 0, tiled=True)  8.73 us
  transfers between devices with their start and end apart: 23, of which 14 were waited for; matrix products, arithmetic and copies ran while one was open for 7% of the time, Pallas kernels for 4%

profile of v4, /device:TPU:1, one launch (start us, length us, event | category | flops | bytes accessed | tf_op | source)
XLA Modules:
  0.0 267.7 jit_solution(4021618231931174770)
XLA Ops:
  1.5 1.2 broadcast_in_dim.8
  2.7 7.6 %all-to-all-start = ((bf16[8,64,1152]{2,1,0:T(8,128)(2,1)}), bf16[8,64,1152]{2,1,0:T(8,128)(2,1)S(1)}, u32[]{:S(2)}, u32[]{:S(2)}) async-start(bf16[8,64,1152]{2,1,0:T(8,128)(2,1)} %broadcast_in_dim.8), calls=%async_computation | async-start | bytes 2359296 | tf_op jit(solution)/shard_map/all_to_all | solution.py:28
  10.4 31.8 %all-to-all-done = bf16[8,64,1152]{2,1,0:T(8,128)(2,1)S(1)} async-done(((bf16[8,64,1152]{2,1,0:T(8,128)(2,1)}), bf16[8,64,1152]{2,1,0:T(8,128)(2,1)S(1)}, u32[]{:S(2)}, u32[]{:S(2)}) %all-to-all-start) | async-done | bytes 1179680 | tf_op jit(solution)/shard_map/all_to_all | solution.py:28
  42.2 1.3 broadcast_in_dim.9
  43.5 3.6 %all-to-all-start.1 = ((bf16[8,64,1152]{2,1,0:T(8,128)(2,1)}), bf16[8,64,1152]{2,1,0:T(8,128)(2,1)S(1)}, u32[]{:S(2)}, u32[]{:S(2)}) async-start(bf16[8,64,1152]{2,1,0:T(8,128)(2,1)} %broadcast_in_dim.9), calls=%async_computation.1 | async-start | bytes 2359296 | tf_op jit(solution)/shard_map/all_to_all | solution.py:28
  47.1 10.9 %collective-permute-start = (bf16[512,1152]{1,0:T(8,128)(2,1)S(1)}, bf16[512,1152]{1,0:T(8,128)(2,1)S(1)}, u32[]{:S(2)}, u32[]{:S(2)}) collective-permute-start(bf16[512,1152]{1,0:T(8,128)(2,1)S(1)} %bitcast.30), channel_id=1, source_target_pairs={{64,0},{128,64},{192,128},{256,192},{320,256},{384,320},{448,384},... | collective-permute-start | bytes 3538952 | tf_op jit(solution)/shard_map/ppermute | solution.py:23
  58.0 1.9 collective-permute-start.1
  59.9 22.9 %collective-permute-done.w1 = bf16[512,1152]{1,0:T(8,128)(2,1)S(1)} collective-permute-done((bf16[512,1152]{1,0:T(8,128)(2,1)S(1)}, bf16[512,1152]{1,0:T(8,128)(2,1)S(1)}, u32[]{:S(2)}, u32[]{:S(2)}) %collective-permute-start) | collective-permute-done | bytes 1179680 | tf_op jit(solution)/shard_map/ppermute | solution.py:23
  83.7 5.3 %collective-permute-start.2 = (bf16[256,1152]{1,0:T(8,128)(2,1)}, bf16[256,1152]{1,0:T(8,128)(2,1)}, u32[]{:S(2)}, u32[]{:S(2)}) collective-permute-start(bf16[256,1152]{1,0:T(8,128)(2,1)} %slice.16), channel_id=1, source_target_pairs={{64,0},{128,64},{192,128},{256,192},{320,256},{384,320},{448,384},... | collective-permute-start | bytes 1769480 | tf_op jit(solution)/shard_map/ppermute | solution.py:23
  90.1 1.9 collective-permute-start.3
  92.0 8.6 %collective-permute-done.2.w3 = bf16[256,1152]{1,0:T(8,128)(2,1)} collective-permute-done((bf16[256,1152]{1,0:T(8,128)(2,1)}, bf16[256,1152]{1,0:T(8,128)(2,1)}, u32[]{:S(2)}, u32[]{:S(2)}) %collective-permute-start.2) | collective-permute-done | bytes 589856 | tf_op jit(solution)/shard_map/ppermute | solution.py:23
  100.6 5.8 %collective-permute-done.3.w4 = bf16[256,1152]{1,0:T(8,128)(2,1)S(1)} collective-permute-done((bf16[256,1152]{1,0:T(8,128)(2,1)S(1)}, bf16[256,1152]{1,0:T(8,128)(2,1)S(1)}, u32[]{:S(2)}, u32[]{:S(2)}) %collective-permute-start.3) | collective-permute-done | bytes 589856 | tf_op jit(solution)/shard_map/ppermute | solution.py:23
  107.3 6.6 %shard_map.112 = bf16[256,2048]{1,0:T(8,128)(2,1)} custom-call(s32[1]{0:T(128)} %bitcast.z_ref, bf16[256,2048]{1,0:T(8,128)(2,1)} %u_ref.2, bf16[256,2048]{1,0:T(8,128)(2,1)} %c_ref.1, bf16[512,1152]{1,0:T(8,128)(2,1)} %bitcast.32, bf16[512,1152]{1,0:T(8,128)(2,1)} %copy-done.5, bf16[512,1152]{1,0:T(8,128)(2,1)} %copy-done.6, ...), custom_call_target="tpu_custom_call" | custom-call | flops 2013265920 | bytes 6291456 | tf_op jit(solution)/shard_map/pallas_call | solution.py:116
  113.9 6.8 %all-to-all-start.2 = ((bf16[8,32,2048]{2,1,0:T(8,128)(2,1)}), bf16[8,32,2048]{2,1,0:T(8,128)(2,1)}, u32[]{:S(2)}, u32[]{:S(2)}) async-start(bf16[8,32,2048]{2,1,0:T(8,128)(2,1)} %bitcast.33), calls=%async_computation.2 | async-start | bytes 2097152 | tf_op jit(solution)/shard_map/all_to_all | solution.py:141
  121.7 1.9 collective-permute-start.4
  123.6 3.4 %collective-permute-start.5 = (bf16[512,1152]{1,0:T(8,128)(2,1)S(1)}, bf16[512,1152]{1,0:T(8,128)(2,1)S(1)}, u32[]{:S(2)}, u32[]{:S(2)}) collective-permute-start(bf16[512,1152]{1,0:T(8,128)(2,1)S(1)} %bitcast.27), channel_id=1, source_target_pairs={{448,0},{0,64},{64,128},{128,192},{192,256},{256,320},{320,384},{3... | collective-permute-start | bytes 3538952 | tf_op jit(solution)/shard_map/ppermute | solution.py:23
  127.0 8.7 %all-to-all-done.2 = bf16[8,32,2048]{2,1,0:T(8,128)(2,1)} async-done(((bf16[8,32,2048]{2,1,0:T(8,128)(2,1)}), bf16[8,32,2048]{2,1,0:T(8,128)(2,1)}, u32[]{:S(2)}, u32[]{:S(2)}) %all-to-all-start.2) | async-done | bytes 1048608 | tf_op jit(solution)/shard_map/all_to_all | solution.py:141
  135.7 1.4 convert_reduce_fusion.1
  140.4 5.1 %all-to-all-start.3 = ((bf16[8,32,2048]{2,1,0:T(8,128)(2,1)}), bf16[8,32,2048]{2,1,0:T(8,128)(2,1)}, u32[]{:S(2)}, u32[]{:S(2)}) async-start(bf16[8,32,2048]{2,1,0:T(8,128)(2,1)} %broadcast_in_dim.10), calls=%async_computation.3 | async-start | bytes 2097152 | tf_op jit(solution)/shard_map/all_to_all | solution.py:28
  145.5 5.7 %collective-permute-done.4.w1 = bf16[512,1152]{1,0:T(8,128)(2,1)S(1)} collective-permute-done((bf16[512,1152]{1,0:T(8,128)(2,1)S(1)}, bf16[512,1152]{1,0:T(8,128)(2,1)S(1)}, u32[]{:S(2)}, u32[]{:S(2)}) %collective-permute-start.4) | collective-permute-done | bytes 1179680 | tf_op jit(solution)/shard_map/ppermute | solution.py:23
  152.1 3.3 %collective-permute-start.6 = (bf16[256,1152]{1,0:T(8,128)(2,1)}, bf16[256,1152]{1,0:T(8,128)(2,1)}, u32[]{:S(2)}, u32[]{:S(2)}) collective-permute-start(bf16[256,1152]{1,0:T(8,128)(2,1)} %slice.18), channel_id=1, source_target_pairs={{64,0},{128,64},{192,128},{256,192},{320,256},{384,320},{448,384},... | collective-permute-start | bytes 1769480 | tf_op jit(solution)/shard_map/ppermute | solution.py:23
  155.5 2.0 collective-permute-start.7
  157.5 10.9 %collective-permute-done.6.w3 = bf16[256,1152]{1,0:T(8,128)(2,1)} collective-permute-done((bf16[256,1152]{1,0:T(8,128)(2,1)}, bf16[256,1152]{1,0:T(8,128)(2,1)}, u32[]{:S(2)}, u32[]{:S(2)}) %collective-permute-start.6) | collective-permute-done | bytes 589856 | tf_op jit(solution)/shard_map/ppermute | solution.py:23
  168.5 4.2 %collective-permute-done.7.w4 = bf16[256,1152]{1,0:T(8,128)(2,1)S(1)} collective-permute-done((bf16[256,1152]{1,0:T(8,128)(2,1)S(1)}, bf16[256,1152]{1,0:T(8,128)(2,1)S(1)}, u32[]{:S(2)}, u32[]{:S(2)}) %collective-permute-start.7) | collective-permute-done | bytes 589856 | tf_op jit(solution)/shard_map/ppermute | solution.py:23
  173.5 4.8 %shard_map.113 = (f32[256,768]{1,0:T(8,128)}, bf16[256,384]{1,0:T(8,128)(2,1)}) custom-call(s32[1]{0:T(128)} %bitcast.z_ref, bf16[256,2048]{1,0:T(8,128)(2,1)} %u_ref.3, bf16[512,1152]{1,0:T(8,128)(2,1)} %bitcast.28, bf16[512,1152]{1,0:T(8,128)(2,1)} %copy-done.1, bf16[512,1152]{1,0:T(8,128)(2,1)} %copy-done.2, bf16[256,1152]{1,0:T(8,128)(2,1)} %collective-permute-done.6.w3, ...), custom_call_target="tpu_custom_call" | custom-call | flops 805306368 | bytes 6291456 | tf_op jit(solution)/shard_map/pallas_call | solution.py:116
  178.3 5.5 %shard_map.114 = bf16[256,2048]{1,0:T(8,128)(2,1)} custom-call(s32[1]{0:T(128)} %bitcast.z_ref, bf16[256,2048]{1,0:T(8,128)(2,1)} %bitcast.6.c_ref, f32[256,768]{1,0:T(8,128)} %get-tuple-element.11.both_ref, bf16[512,1152]{1,0:T(8,128)(2,1)} %bitcast.29, bf16[512,1152]{1,0:T(8,128)(2,1)} %copy-done.1, bf16[512,1152]{1,0:T(8,128)(2,1)} %copy-done.2, ...), custom_call_target="tpu_custom_call" | custom-call | flops 1207959552 | bytes 6291456 | tf_op jit(solution)/shard_map/pallas_call | solution.py:116
  183.8 1.9 constant_dynamic-slice_fusion.3
  185.7 3.6 %collective-permute-start.8 = (bf16[128,2048]{1,0:T(8,128)(2,1)}, bf16[128,2048]{1,0:T(8,128)(2,1)S(1)}, u32[]{:S(2)}, u32[]{:S(2)}) collective-permute-start(bf16[128,2048]{1,0:T(8,128)(2,1)} %constant_dynamic-slice_fusion.3), channel_id=1, source_target_pairs={{0,1},{1,0},{2,3},{3,2},{4,5},{5,4},{6,7},{7,6},{8,9},{9,8},{10,11... | collective-permute-start | bytes 1572872 | tf_op jit(solution)/shard_map/ppermute | solution.py:146
  189.4 2.0 multiply_convert_fusion
  191.3 1.3 copy.14
  192.7 7.4 %all-to-all-start.4 = ((bf16[64,32,384]{2,1,0:T(8,128)(2,1)}), bf16[64,32,384]{2,1,0:T(8,128)(2,1)S(1)}, u32[]{:S(2)}, u32[]{:S(2)}) async-start(bf16[64,32,384]{2,1,0:T(8,128)(2,1)} %bitcast.16), calls=%async_computation.4 | async-start | bytes 3145728 | tf_op jit(solution)/shard_map/all_to_all | solution.py:222
  201.4 4.2 %collective-permute-start.11 = (bf16[32,2048]{1,0:T(8,128)(2,1)S(1)}, bf16[32,2048]{1,0:T(8,128)(2,1)S(1)}, u32[]{:S(2)}, u32[]{:S(2)}) collective-permute-start(bf16[32,2048]{1,0:T(8,128)(2,1)S(1)} %get-tuple-element.16), channel_id=1, source_target_pairs={{2,0},{3,1},{4,2},{5,3},{6,4},{7,5},{0,6},{1,7},{10,8},{11,9},{12,... | collective-permute-start | bytes 393224 | tf_op jit(solution)/shard_map/ppermute | solution.py:151
  205.6 1.9 collective-permute-start.10
  207.6 3.5 %collective-permute-start.9 = (bf16[32,2048]{1,0:T(8,128)(2,1)S(1)}, bf16[32,2048]{1,0:T(8,128)(2,1)S(1)}, u32[]{:S(2)}, u32[]{:S(2)}) collective-permute-start(bf16[32,2048]{1,0:T(8,128)(2,1)S(1)} %get-tuple-element.15), channel_id=1, source_target_pairs={{4,0},{5,1},{6,2},{7,3},{0,4},{1,5},{2,6},{3,7},{12,8},{13,9},{14,... | collective-permute-start | bytes 393224 | tf_op jit(solution)/shard_map/ppermute | solution.py:151
  211.1 2.1 collective-permute-done.10
  213.2 2.3 collective-permute-done.9
  217.8 2.0 collective-permute-start.14
  219.8 5.3 %collective-permute-start.13 = (bf16[32,2048]{1,0:T(8,128)(2,1)S(1)}, bf16[32,2048]{1,0:T(8,128)(2,1)S(1)}, u32[]{:S(2)}, u32[]{:S(2)}) collective-permute-start(bf16[32,2048]{1,0:T(8,128)(2,1)S(1)} %fusion.9), channel_id=1, source_target_pairs={{4,0},{5,1},{6,2},{7,3},{0,4},{1,5},{2,6},{3,7},{12,8},{13,9},{14,... | collective-permute-start | bytes 393224 | tf_op jit(solution)/shard_map/ppermute | solution.py:151
  225.1 1.9 collective-permute-start.12
  227.0 1.9 collective-permute-done.13
  228.9 2.7 %collective-permute-done.12 = bf16[32,2048]{1,0:T(8,128)(2,1)S(1)} collective-permute-done((bf16[32,2048]{1,0:T(8,128)(2,1)S(1)}, bf16[32,2048]{1,0:T(8,128)(2,1)S(1)}, u32[]{:S(2)}, u32[]{:S(2)}) %collective-permute-start.12) | collective-permute-done | bytes 131104 | tf_op jit(solution)/shard_map/ppermute | solution.py:151
  231.7 4.5 %collective-permute-start.15 = (bf16[4,32,2048]{2,1,0:T(8,128)(2,1)S(1)}, bf16[4,32,2048]{2,1,0:T(8,128)(2,1)S(1)}, u32[]{:S(2)}, u32[]{:S(2)}) collective-permute-start(bf16[4,32,2048]{2,1,0:T(8,128)(2,1)S(1)} %get-tuple-element.14), channel_id=1, source_target_pairs={{0,1},{1,0},{2,3},{3,2},{4,5},{5,4},{6,7},{7,6},{8,9},{9,8},{10,11... | collective-permute-start | bytes 1572872 | tf_op jit(solution)/shard_map/ppermute | solution.py:146
  236.3 1.5 collective-permute-done.15
  238.5 1.4 maximum_select_fusion
  240.3 7.1 %collective-permute-start.16 = (f32[32,384]{1,0:T(8,128)S(1)}, f32[32,384]{1,0:T(8,128)S(1)}, u32[]{:S(2)}, u32[]{:S(2)}) collective-permute-start(f32[32,384]{1,0:T(8,128)S(1)} %convert_reduce_fusion), channel_id=1, source_target_pairs={{256,0},{0,256},{257,1},{1,257},{258,2},{2,258},{259,3},{3,259},{2... | collective-permute-start | bytes 147464 | tf_op jit(solution)/shard_map/ppermute | solution.py:23
  248.1 7.6 %all-to-all-start.5 = ((f32[64,1,384]{2,1,0:T(1,128)}), f32[64,1,384]{2,1,0:T(1,128)S(1)}, u32[]{:S(2)}, u32[]{:S(2)}) async-start(f32[64,1,384]{2,1,0:T(1,128)} %broadcast_in_dim.11), calls=%async_computation.5 | async-start | bytes 196608 | tf_op jit(solution)/shard_map/all_to_all | solution.py:28
  255.7 1.4 fusion
  257.7 9.4 %all-to-all-done.5 = f32[64,1,384]{2,1,0:T(1,128)S(1)} async-done(((f32[64,1,384]{2,1,0:T(1,128)}), f32[64,1,384]{2,1,0:T(1,128)S(1)}, u32[]{:S(2)}, u32[]{:S(2)}) %all-to-all-start.5) | async-done | bytes 98336 | tf_op jit(solution)/shard_map/all_to_all | solution.py:28
  (62 shorter events, 16.5 us)
Async XLA Ops:
  1.5 8.9 %copy-start.10 = (bf16[384,64]{0,1:T(8,128)(2,1)S(1)}, bf16[384,64]{0,1:T(8,128)(2,1)}, u32[]{:S(2)}) copy-start(bf16[384,64]{0,1:T(8,128)(2,1)} %param.14) | copy-start | bytes 147460
  1.5 8.9 %copy-start.11 = (bf16[64,384]{1,0:T(8,128)(2,1)S(1)}, bf16[64,384]{1,0:T(8,128)(2,1)}, u32[]{:S(2)}) copy-start(bf16[64,384]{1,0:T(8,128)(2,1)} %param.13) | copy-start | bytes 147460
  1.5 8.9 %copy-start.12 = (bf16[64,384]{1,0:T(8,128)(2,1)S(1)}, bf16[64,384]{1,0:T(8,128)(2,1)}, u32[]{:S(2)}) copy-start(bf16[64,384]{1,0:T(8,128)(2,1)} %param.12) | copy-start | bytes 147460
  2.7 39.5 %all-to-all-start = ((bf16[8,64,1152]{2,1,0:T(8,128)(2,1)}), bf16[8,64,1152]{2,1,0:T(8,128)(2,1)S(1)}, u32[]{:S(2)}, u32[]{:S(2)}) async-start(bf16[8,64,1152]{2,1,0:T(8,128)(2,1)} %broadcast_in_dim.8), calls=%async_computation | async-start | bytes 2359296 | tf_op jit(solution)/shard_map/all_to_all | solution.py:28
  42.2 15.8 %copy-start.3 = (bf16[8,64,1152]{2,1,0:T(8,128)(2,1)}, bf16[8,64,1152]{2,1,0:T(8,128)(2,1)S(1)}, u32[]{:S(2)}) copy-start(bf16[8,64,1152]{2,1,0:T(8,128)(2,1)S(1)} %all-to-all-done) | copy-start | bytes 3538948
  43.5 70.4 %all-to-all-start.1 = ((bf16[8,64,1152]{2,1,0:T(8,128)(2,1)}), bf16[8,64,1152]{2,1,0:T(8,128)(2,1)S(1)}, u32[]{:S(2)}, u32[]{:S(2)}) async-start(bf16[8,64,1152]{2,1,0:T(8,128)(2,1)} %broadcast_in_dim.9), calls=%async_computation.1 | async-start | bytes 2359296 | tf_op jit(solution)/shard_map/all_to_all | solution.py:28
  47.1 35.7 %collective-permute-start = (bf16[512,1152]{1,0:T(8,128)(2,1)S(1)}, bf16[512,1152]{1,0:T(8,128)(2,1)S(1)}, u32[]{:S(2)}, u32[]{:S(2)}) collective-permute-start(bf16[512,1152]{1,0:T(8,128)(2,1)S(1)} %bitcast.30), channel_id=1, source_target_pairs={{64,0},{128,64},{192,128},{256,192},{320,256},{384,320},{448,384},... | collective-permute-start | bytes 3538952 | tf_op jit(solution)/shard_map/ppermute | solution.py:23
  58.0 31.0 %collective-permute-start.1 = (bf16[512,1152]{1,0:T(8,128)(2,1)S(1)}, bf16[512,1152]{1,0:T(8,128)(2,1)S(1)}, u32[]{:S(2)}, u32[]{:S(2)}) collective-permute-start(bf16[512,1152]{1,0:T(8,128)(2,1)S(1)} %bitcast.31), channel_id=1, source_target_pairs={{448,0},{0,64},{64,128},{128,192},{192,256},{256,320},{320,384},{3... | collective-permute-start | bytes 3538952 | tf_op jit(solution)/shard_map/ppermute | solution.py:23
  82.8 23.7 %copy-start.5 = (bf16[512,1152]{1,0:T(8,128)(2,1)}, bf16[512,1152]{1,0:T(8,128)(2,1)S(1)}, u32[]{:S(2)}) copy-start(bf16[512,1152]{1,0:T(8,128)(2,1)S(1)} %collective-permute-done.w1) | copy-start | bytes 3538948
  83.7 16.9 %collective-permute-start.2 = (bf16[256,1152]{1,0:T(8,128)(2,1)}, bf16[256,1152]{1,0:T(8,128)(2,1)}, u32[]{:S(2)}, u32[]{:S(2)}) collective-permute-start(bf16[256,1152]{1,0:T(8,128)(2,1)} %slice.16), channel_id=1, source_target_pairs={{64,0},{128,64},{192,128},{256,192},{320,256},{384,320},{448,384},... | collective-permute-start | bytes 1769480 | tf_op jit(solution)/shard_map/ppermute | solution.py:23
  89.0 1.0 copy-start.6
  90.1 16.4 %collective-permute-start.3 = (bf16[256,1152]{1,0:T(8,128)(2,1)S(1)}, bf16[256,1152]{1,0:T(8,128)(2,1)S(1)}, u32[]{:S(2)}, u32[]{:S(2)}) collective-permute-start(bf16[256,1152]{1,0:T(8,128)(2,1)S(1)} %slice.17), channel_id=1, source_target_pairs={{448,0},{0,64},{64,128},{128,192},{192,256},{256,320},{320,384},{3... | collective-permute-start | bytes 1769480 | tf_op jit(solution)/shard_map/ppermute | solution.py:23
  106.4 0.8 copy-start.8
  113.9 23.3 %copy-start = (bf16[8,64,1152]{2,1,0:T(8,128)(2,1)}, bf16[8,64,1152]{2,1,0:T(8,128)(2,1)S(1)}, u32[]{:S(2)}) copy-start(bf16[8,64,1152]{2,1,0:T(8,128)(2,1)S(1)} %all-to-all-done.1) | copy-start | bytes 3538948
  113.9 21.9 %all-to-all-start.2 = ((bf16[8,32,2048]{2,1,0:T(8,128)(2,1)}), bf16[8,32,2048]{2,1,0:T(8,128)(2,1)}, u32[]{:S(2)}, u32[]{:S(2)}) async-start(bf16[8,32,2048]{2,1,0:T(8,128)(2,1)} %bitcast.33), calls=%async_computation.2 | async-start | bytes 2097152 | tf_op jit(solution)/shard_map/all_to_all | solution.py:141
  121.7 29.5 %collective-permute-start.4 = (bf16[512,1152]{1,0:T(8,128)(2,1)S(1)}, bf16[512,1152]{1,0:T(8,128)(2,1)S(1)}, u32[]{:S(2)}, u32[]{:S(2)}) collective-permute-start(bf16[512,1152]{1,0:T(8,128)(2,1)S(1)} %bitcast.26), channel_id=1, source_target_pairs={{64,0},{128,64},{192,128},{256,192},{320,256},{384,320},{448,384},... | collective-permute-start | bytes 3538952 | tf_op jit(solution)/shard_map/ppermute | solution.py:23
  123.6 31.8 %collective-permute-start.5 = (bf16[512,1152]{1,0:T(8,128)(2,1)S(1)}, bf16[512,1152]{1,0:T(8,128)(2,1)S(1)}, u32[]{:S(2)}, u32[]{:S(2)}) collective-permute-start(bf16[512,1152]{1,0:T(8,128)(2,1)S(1)} %bitcast.27), channel_id=1, source_target_pairs={{448,0},{0,64},{64,128},{128,192},{192,256},{256,320},{320,384},{3... | collective-permute-start | bytes 3538952 | tf_op jit(solution)/shard_map/ppermute | solution.py:23
  140.4 37.9 %all-to-all-start.3 = ((bf16[8,32,2048]{2,1,0:T(8,128)(2,1)}), bf16[8,32,2048]{2,1,0:T(8,128)(2,1)}, u32[]{:S(2)}, u32[]{:S(2)}) async-start(bf16[8,32,2048]{2,1,0:T(8,128)(2,1)} %broadcast_in_dim.10), calls=%async_computation.3 | async-start | bytes 2097152 | tf_op jit(solution)/shard_map/all_to_all | solution.py:28
  151.2 21.4 %copy-start.1 = (bf16[512,1152]{1,0:T(8,128)(2,1)}, bf16[512,1152]{1,0:T(8,128)(2,1)S(1)}, u32[]{:S(2)}) copy-start(bf16[512,1152]{1,0:T(8,128)(2,1)S(1)} %collective-permute-done.4.w1) | copy-start | bytes 3538948
  152.1 16.3 %collective-permute-start.6 = (bf16[256,1152]{1,0:T(8,128)(2,1)}, bf16[256,1152]{1,0:T(8,128)(2,1)}, u32[]{:S(2)}, u32[]{:S(2)}) collective-permute-start(bf16[256,1152]{1,0:T(8,128)(2,1)} %slice.18), channel_id=1, source_target_pairs={{64,0},{128,64},{192,128},{256,192},{320,256},{384,320},{448,384},... | collective-permute-start | bytes 1769480 | tf_op jit(solution)/shard_map/ppermute | solution.py:23
  155.5 17.2 %copy-start.2 = (bf16[512,1152]{1,0:T(8,128)(2,1)}, bf16[512,1152]{1,0:T(8,128)(2,1)S(1)}, u32[]{:S(2)}) copy-start(bf16[512,1152]{1,0:T(8,128)(2,1)S(1)} %collective-permute-done.5.w2) | copy-start | bytes 3538948
  155.5 17.1 %collective-permute-start.7 = (bf16[256,1152]{1,0:T(8,128)(2,1)S(1)}, bf16[256,1152]{1,0:T(8,128)(2,1)S(1)}, u32[]{:S(2)}, u32[]{:S(2)}) collective-permute-start(bf16[256,1152]{1,0:T(8,128)(2,1)S(1)} %slice.19), channel_id=1, source_target_pairs={{448,0},{0,64},{64,128},{128,192},{192,256},{256,320},{320,384},{3... | collective-permute-start | bytes 1769480 | tf_op jit(solution)/shard_map/ppermute | solution.py:23
  172.7 0.8 copy-start.7
  178.3 11.1 %copy-start.13 = (bf16[256,384]{1,0:T(8,128)(2,1)S(1)}, bf16[256,384]{1,0:T(8,128)(2,1)}, u32[]{:S(2)}) copy-start(bf16[256,384]{1,0:T(8,128)(2,1)} %get-tuple-element.12) | copy-start | bytes 589828
  185.7 15.5 %collective-permute-start.8 = (bf16[128,2048]{1,0:T(8,128)(2,1)}, bf16[128,2048]{1,0:T(8,128)(2,1)S(1)}, u32[]{:S(2)}, u32[]{:S(2)}) collective-permute-start(bf16[128,2048]{1,0:T(8,128)(2,1)} %constant_dynamic-slice_fusion.3), channel_id=1, source_target_pairs={{0,1},{1,0},{2,3},{3,2},{4,5},{5,4},{6,7},{7,6},{8,9},{9,8},{10,11... | collective-permute-start | bytes 1572872 | tf_op jit(solution)/shard_map/ppermute | solution.py:146
  192.7 8.6 %copy-start.4 = (bf16[256,2048]{1,0:T(8,128)(2,1)S(1)}, bf16[256,2048]{1,0:T(8,128)(2,1)}, u32[]{:S(2)}) copy-start(bf16[256,2048]{1,0:T(8,128)(2,1)} %shard_map.114) | copy-start | bytes 3145732
  192.7 47.3 %all-to-all-start.4 = ((bf16[64,32,384]{2,1,0:T(8,128)(2,1)}), bf16[64,32,384]{2,1,0:T(8,128)(2,1)S(1)}, u32[]{:S(2)}, u32[]{:S(2)}) async-start(bf16[64,32,384]{2,1,0:T(8,128)(2,1)} %bitcast.16), calls=%async_computation.4 | async-start | bytes 3145728 | tf_op jit(solution)/shard_map/all_to_all | solution.py:222
  201.4 9.7 %collective-permute-start.11 = (bf16[32,2048]{1,0:T(8,128)(2,1)S(1)}, bf16[32,2048]{1,0:T(8,128)(2,1)S(1)}, u32[]{:S(2)}, u32[]{:S(2)}) collective-permute-start(bf16[32,2048]{1,0:T(8,128)(2,1)S(1)} %get-tuple-element.16), channel_id=1, source_target_pairs={{2,0},{3,1},{4,2},{5,3},{6,4},{7,5},{0,6},{1,7},{10,8},{11,9},{12,... | collective-permute-start | bytes 393224 | tf_op jit(solution)/shard_map/ppermute | solution.py:151
  205.6 7.6 %collective-permute-start.10 = (bf16[32,2048]{1,0:T(8,128)(2,1)S(1)}, bf16[32,2048]{1,0:T(8,128)(2,1)S(1)}, u32[]{:S(2)}, u32[]{:S(2)}) collective-permute-start(bf16[32,2048]{1,0:T(8,128)(2,1)S(1)} %get-tuple-element.17), channel_id=1, source_target_pairs={{6,0},{7,1},{0,2},{1,3},{2,4},{3,5},{4,6},{5,7},{14,8},{15,9},{8,1... | collective-permute-start | bytes 393224 | tf_op jit(solution)/shard_map/ppermute | solution.py:151
  207.6 8.0 %collective-permute-start.9 = (bf16[32,2048]{1,0:T(8,128)(2,1)S(1)}, bf16[32,2048]{1,0:T(8,128)(2,1)S(1)}, u32[]{:S(2)}, u32[]{:S(2)}) collective-permute-start(bf16[32,2048]{1,0:T(8,128)(2,1)S(1)} %get-tuple-element.15), channel_id=1, source_target_pairs={{4,0},{5,1},{6,2},{7,3},{0,4},{1,5},{2,6},{3,7},{12,8},{13,9},{14,... | collective-permute-start | bytes 393224 | tf_op jit(solution)/shard_map/ppermute | solution.py:151
  217.8 9.2 %collective-permute-start.14 = (bf16[32,2048]{1,0:T(8,128)(2,1)S(1)}, bf16[32,2048]{1,0:T(8,128)(2,1)S(1)}, u32[]{:S(2)}, u32[]{:S(2)}) collective-permute-start(bf16[32,2048]{1,0:T(8,128)(2,1)S(1)} %fusion.9), channel_id=1, source_target_pairs={{6,0},{7,1},{0,2},{1,3},{2,4},{3,5},{4,6},{5,7},{14,8},{15,9},{8,1... | collective-permute-start | bytes 393224 | tf_op jit(solution)/shard_map/ppermute | solution.py:151
  219.8 9.1 %collective-permute-start.13 = (bf16[32,2048]{1,0:T(8,128)(2,1)S(1)}, bf16[32,2048]{1,0:T(8,128)(2,1)S(1)}, u32[]{:S(2)}, u32[]{:S(2)}) collective-permute-start(bf16[32,2048]{1,0:T(8,128)(2,1)S(1)} %fusion.9), channel_id=1, source_target_pairs={{4,0},{5,1},{6,2},{7,3},{0,4},{1,5},{2,6},{3,7},{12,8},{13,9},{14,... | collective-permute-start | bytes 393224 | tf_op jit(solution)/shard_map/ppermute | solution.py:151
  225.1 6.5 %collective-permute-start.12 = (bf16[32,2048]{1,0:T(8,128)(2,1)S(1)}, bf16[32,2048]{1,0:T(8,128)(2,1)S(1)}, u32[]{:S(2)}, u32[]{:S(2)}) collective-permute-start(bf16[32,2048]{1,0:T(8,128)(2,1)S(1)} %fusion.9), channel_id=1, source_target_pairs={{2,0},{3,1},{4,2},{5,3},{6,4},{7,5},{0,6},{1,7},{10,8},{11,9},{12,... | collective-permute-start | bytes 393224 | tf_op jit(solution)/shard_map/ppermute | solution.py:151
  231.7 6.1 %collective-permute-start.15 = (bf16[4,32,2048]{2,1,0:T(8,128)(2,1)S(1)}, bf16[4,32,2048]{2,1,0:T(8,128)(2,1)S(1)}, u32[]{:S(2)}, u32[]{:S(2)}) collective-permute-start(bf16[4,32,2048]{2,1,0:T(8,128)(2,1)S(1)} %get-tuple-element.14), channel_id=1, source_target_pairs={{0,1},{1,0},{2,3},{3,2},{4,5},{5,4},{6,7},{7,6},{8,9},{9,8},{10,11... | collective-permute-start | bytes 1572872 | tf_op jit(solution)/shard_map/ppermute | solution.py:146
  237.7 0.8 copy-start.9
  240.3 16.8 %collective-permute-start.16 = (f32[32,384]{1,0:T(8,128)S(1)}, f32[32,384]{1,0:T(8,128)S(1)}, u32[]{:S(2)}, u32[]{:S(2)}) collective-permute-start(f32[32,384]{1,0:T(8,128)S(1)} %convert_reduce_fusion), channel_id=1, source_target_pairs={{256,0},{0,256},{257,1},{1,257},{258,2},{2,258},{259,3},{3,259},{2... | collective-permute-start | bytes 147464 | tf_op jit(solution)/shard_map/ppermute | solution.py:23
  248.1 19.0 %all-to-all-start.5 = ((f32[64,1,384]{2,1,0:T(1,128)}), f32[64,1,384]{2,1,0:T(1,128)S(1)}, u32[]{:S(2)}, u32[]{:S(2)}) async-start(f32[64,1,384]{2,1,0:T(1,128)} %broadcast_in_dim.11), calls=%async_computation.5 | async-start | bytes 196608 | tf_op jit(solution)/shard_map/all_to_all | solution.py:28

commit v5 on v4

v5 whole, which is shorter than its diff:
```python
import jax
import jax.numpy as jnp
from jax import lax
from jax.experimental import pallas as pl
from jax.experimental.pallas import tpu as pltpu
from jax.sharding import Mesh
from jax.sharding import PartitionSpec as P


FS = ("fs_0", "fs_1")
Z = ("rep", "fs_0")
REP_FS = ("rep", "fs_0", "fs_1")
FS_REP = ("fs_0", "fs_1", "rep")
f32 = jnp.float32
bf16 = jnp.bfloat16

eps = 1e-06
LEFT = 640
PIECES = (0, 1, 3, 2)
ROWS_ROWS = (((1,), (1,)), ((), ()))


def take_from(value, axis, step):
    n = lax.axis_size(axis)
    return lax.ppermute(value, axis, [((i + step) % n, i) for i in range(n)])


def from_everyone(value, axis):
    n = lax.axis_size(axis)
    return lax.all_to_all(
        jnp.broadcast_to(value[None], (n, *value.shape)), axis, 0, 0, tiled=True
    )


def along_y(value):
    whole = from_everyone(value, "fs_1")
    return whole.reshape(-1, value.shape[1])


def along_z(value, forward):
    next_ = take_from(value, Z, 1)
    last = take_from(value, Z, -1)
    far = take_from(next_ if forward > 0 else last, Z, forward)
    return (value, next_, last, far)


def after(value, *others):
    return lax.optimization_barrier((value, *others))[0]


def span_of(z, m, width):
    quarter = width // 4
    return pl.ds(pl.multiple_of(lax.rem(z + m, 4) * quarter, quarter), quarter)


def gate_up_of(z, u_ref, left, right, n):
    width = u_ref.shape[1]
    field = u_ref[...].astype(f32)
    scale = lax.rsqrt(jnp.mean(field * field, axis=1, keepdims=True) + eps)
    a = b = None
    for m, wl, wr in zip(PIECES, left, right):
        normed_b = (u_ref[:, span_of(z, m, width)].astype(f32) * scale).astype(bf16)
        part_a = jnp.dot(normed_b, wl[...], preferred_element_type=f32)
        part_b = jnp.dot(normed_b, wr[:, : 2 * n - LEFT], preferred_element_type=f32)
        a = part_a if a is None else a + part_a
        b = part_b if b is None else b + part_b
    return a[:, :n], jnp.concatenate([a[:, n:], b], axis=1)


def partial_of(z, c_ref, gate, upper, left, right, out_ref):
    width, n = c_ref.shape[1], gate.shape[1]
    total = None
    for m, wr in zip(PIECES, right):
        part = jnp.dot(
            c_ref[:, span_of(z, m, width)], wr[:, 2 * n - LEFT :], preferred_element_type=f32
        )
        total = part if total is None else total + part
    back = 0.5 * total
    logistic = jax.nn.sigmoid(gate)
    d_gate = (back * upper * logistic * (1.0 + gate * (1.0 - logistic))).astype(bf16)
    d_up = (back * (gate * logistic)).astype(bf16)
    d_left = jnp.concatenate([d_gate, d_up[:, : LEFT - n]], axis=1)
    d_right = d_up[:, LEFT - n :]
    for m, wl, wr in zip(PIECES, left, right):
        part = lax.dot_general(d_left, wl[...], ROWS_ROWS, preferred_element_type=f32)
        part = part + lax.dot_general(
            d_right, wr[:, : 2 * n - LEFT], ROWS_ROWS, preferred_element_type=f32
        )
        out_ref[:, span_of(z, m, width)] = part.astype(bf16)


def block_body(z_ref, u_ref, c_ref, *refs):
    *weight, out_ref = refs
    z, left, right = z_ref[0], weight[:4], weight[4:]
    gate, upper = gate_up_of(z, u_ref, left, right, (LEFT + right[0].shape[1]) // 3)
    partial_of(z, c_ref, gate, upper, left, right, out_ref)


def forward_body(z_ref, u_ref, *refs):
    *weight, both_ref, hidden_ref = refs
    n = hidden_ref.shape[1]
    gate, upper = gate_up_of(z_ref[0], u_ref, weight[:4], weight[4:], n)
    both_ref[:, :n] = gate
    both_ref[:, n:] = upper
    hidden_ref[...] = (gate * jax.nn.sigmoid(gate) * upper).astype(bf16)


def backward_body(z_ref, c_ref, both_ref, *refs):
    *weight, mine_ref, other_ref, out_ref = refs
    n = both_ref.shape[1] // 2
    gate, upper = both_ref[:, :n], both_ref[:, n:]
    partial_of(z_ref[0], c_ref, gate, upper, weight[:4], weight[4:], out_ref)
    core, (blocks, rows, _) = z_ref[1], mine_ref.shape
    for k in range(blocks):
        mine_ref[k] = out_ref[pl.ds(pl.multiple_of((2 * k + core) * rows, rows), rows), :]
        other_ref[k] = out_ref[pl.ds(pl.multiple_of((2 * k + 1 - core) * rows, rows), rows), :]


def gradient_of(d_normed, u, c):
    field = u.astype(f32)
    scale = lax.rsqrt(jnp.mean(field * field, axis=1, keepdims=True) + eps)
    normed = field * scale
    d_field = c.astype(f32) + scale * (
        d_normed - normed * jnp.mean(d_normed * normed, axis=1, keepdims=True)
    )
    return d_field.astype(bf16)


def spread_rows_body(tp_ref, p_ref, u_ref, c_ref, own_ref, out_ref):
    n, _, _ = p_ref.shape
    d_normed = p_ref[0].astype(f32)
    for k in range(1, n):
        d_normed = d_normed + p_ref[k].astype(f32)
    own = gradient_of(d_normed, u_ref[...], c_ref[...])
    own_ref[...] = own
    for k in range(n):
        out_ref[k] = own


def own_rows_body(tp_ref, p0, p1, p2, p3, u_ref, c_ref, own_ref):
    rows = c_ref.shape[0]
    d_normed = p0[...].astype(f32)
    for p in (p1, p2, p3):
        d_normed = d_normed + p[...].astype(f32)
    u = u_ref[pl.ds(pl.multiple_of(tp_ref[0] * rows, rows), rows), :]
    own_ref[...] = gradient_of(d_normed, u, c_ref[...])


def place_rows_body(tp_ref, q0, q1, q2, q3, other_ref, out_ref):
    rows = q0.shape[0]
    x, core = tp_ref[0] // 2, lax.rem(tp_ref[0], 2)
    for j, q in enumerate((q0, q1, q2, q3)):
        at = lax.rem(x + j, 4) * 2
        out_ref[pl.ds(pl.multiple_of((at + core) * rows, rows), rows), :] = q[...]
        out_ref[pl.ds(pl.multiple_of((at + 1 - core) * rows, rows), rows), :] = other_ref[j]


SMEM = pl.BlockSpec(memory_space=pltpu.SMEM)
VMEM = pl.BlockSpec(memory_space=pltpu.VMEM)


def kernel(body, outs, flops, scalars, *arrays, scratch=()):
    return pl.pallas_call(
        body,
        in_specs=[SMEM] + [VMEM] * len(arrays),
        out_specs=tuple(VMEM for _ in outs),
        out_shape=tuple(jax.ShapeDtypeStruct(*o) for o in outs),
        scratch_shapes=scratch,
        cost_estimate=pl.CostEstimate(
            flops=flops, bytes_accessed=6 << 20, transcendentals=0
        ),
    )(scalars, *arrays)


def own_rows(partial):
    pieces = partial.reshape(lax.axis_size("tp"), -1, partial.shape[1])
    return lax.all_to_all(pieces, "tp", 0, 0, tiled=True)


def swap_cores(value):
    return lax.ppermute(value, "tp", [(i, i ^ 1) for i in range(lax.axis_size("tp"))])


def take_x(value, step):
    n = lax.axis_size("tp")
    return lax.ppermute(value, "tp", [((i + 2 * step) % n, i) for i in range(n)])


def own_rows_by_permutes(mine, other, x):
    other = swap_cores(other)
    chip = (mine.astype(f32) + other.astype(f32)).astype(bf16)

    def block(j):
        return lax.dynamic_index_in_dim(chip, (x + j) % 4, axis=0, keepdims=False)

    pieces = [block(0)]
    for j in (2, 1, 3):
        pieces.append(take_x(block(j), -j))
    return pieces


def all_rows(value, tps):
    quarters = [value]
    for j in (1, 2, 3):
        quarters.append(take_x(value, j))
    stacked = jnp.stack(quarters)
    other = swap_cores(stacked)
    out = ((8 * value.shape[0], value.shape[1]), bf16)
    (whole,) = kernel(place_rows_body, (out,), 1 << 20, tps, *quarters, other)
    return whole


def step(
    tokens,
    mid_tokens,
    out_grad,
    gate_first,
    up_first,
    down_first,
    gate_second,
    up_second,
    down_second,
):
    tp = lax.axis_index("tp")
    tps = tp.astype(jnp.int32).reshape(1)
    zs = jnp.stack([lax.axis_index("fs_0"), tp % 2]).astype(jnp.int32)
    n, width = gate_first.shape[1], tokens.shape[1]
    like_u = (tokens.shape, bf16)

    flops = 2 * tokens.shape[0] * width * n

    def parts(whole):
        return whole[:, :LEFT], whole[:, LEFT:]

    y2 = along_y(jnp.concatenate([gate_second, up_second, down_second.T], axis=1))
    y1 = jnp.concatenate([gate_first, up_first, down_first.T], axis=1)
    y1 = along_y(after(y1, y2))
    a2, b2 = parts(y2)
    a1, b1 = parts(y1)
    a2 = along_z(a2, 1)
    b2 = along_z(b2, -1)
    a1 = along_z(a1, 1)
    b1 = along_z(b1, -1)

    (partial,) = kernel(block_body, (like_u,), 5 * flops, zs, mid_tokens, out_grad, *a2, *b2)
    pieces = own_rows(partial)
    rows, like_rows = pieces.shape[1], (pieces.shape[1:], bf16)
    mid_rows, spread = kernel(
        spread_rows_body,
        (like_rows, (pieces.shape, bf16)),
        1 << 24,
        tps,
        pieces,
        lax.dynamic_slice_in_dim(mid_tokens, tp * rows, rows, axis=0),
        lax.dynamic_slice_in_dim(out_grad, tp * rows, rows, axis=0),
    )
    mid_grad = lax.all_to_all(spread, "tp", 0, 0, tiled=True).reshape(mid_tokens.shape)

    both, hidden = kernel(
        forward_body,
        (((tokens.shape[0], 2 * n), f32), ((tokens.shape[0], n), bf16)),
        2 * flops,
        zs,
        tokens,
        *a1,
        *b1,
    )
    share = 0.5 * lax.dot_general(
        mid_grad, hidden, (((0,), (0,)), ((), ())), preferred_element_type=f32
    )
    share = share.astype(bf16).reshape(lax.axis_size(FS_REP), -1, n)
    share = lax.all_to_all(share, FS_REP, 0, 0, tiled=True)
    share = share.astype(f32).sum(axis=0)
    twin = take_from(share, "rep", 1)
    norms = from_everyone(jnp.sum(share * share, axis=0), FS_REP).sum(axis=0)
    first = lax.axis_index("rep") == 0
    share = jnp.where(first, jnp.stack([share, twin]), jnp.stack([twin, share]))

    half = ((4, rows, width), bf16)
    mine, other = kernel(
        backward_body,
        (half, half),
        3 * flops,
        zs,
        mid_grad,
        both,
        *a1,
        *b1,
        scratch=[pltpu.VMEM(tokens.shape, bf16)],
    )
    pieces = own_rows_by_permutes(mine, other, tp // 2)
    (in_rows,) = kernel(own_rows_body, (like_rows,), 1 << 24, tps, *pieces, tokens, mid_rows)
    input_grad = all_rows(in_rows, tps)
    return (input_grad, share.reshape(-1, n).T, norms)


def solution(mesh):
    torus = Mesh(
        mesh.devices.reshape(mesh.shape["rep"], 4, 8, mesh.shape["tp"]),
        ("rep", "fs_0", "fs_1", "tp"),
    )
    placed = (
        P(REP_FS, None),
        P(REP_FS, None),
        P(REP_FS, None),
        P(FS, "tp"),
        P(FS, "tp"),
        P("tp", FS),
        P(FS, "tp"),
        P(FS, "tp"),
        P("tp", FS),
    )
    return jax.shard_map(
        step,
        mesh=torus,
        in_specs=placed,
        out_specs=(P(REP_FS, None), P("tp", FS), P("tp")),
        check_vma=False,
    )
```

time: 269 us -> 268 us (level)
  starting transfers between devices: 103 us -> 126 us
  waiting for transfers between devices: 118 us -> 95.2 us
  Pallas kernels: 16.9 us -> 25.5 us
  other arithmetic: 13.5 us -> 5.3 us
    ppermute x9 -> x13, starting transfers between devices: 37.7 us -> 52.2 us  [take_from(): return lax.ppermute(value, axis, [((i + step) % n, i) for i in range(n)])]
    ppermute x9 -> x13, waiting for transfers between devices: 58.1 us -> 47.9 us  [take_from(): return lax.ppermute(value, axis, [((i + step) % n, i) for i in range(n)])]
    all_to_all x4 -> x3, waiting for transfers between devices: 41.2 us -> 32.5 us  [from_everyone(): lax.all_to_all(jnp.broadcast_to(value[None], (n, *value.shape)), axis, 0,...]
    pallas_call x3 -> x6, Pallas kernels: 16.9 us -> 25.5 us  [kernel(): pl.pallas_call(body, in_specs=[SMEM] + [VMEM] * len(arrays), out_specs=tu...]
    all_to_all x2 -> x3, starting transfers between devices: 14.2 us -> 21.3 us  [the longest x1 10.4 us: step(): share = lax.all_to_all(share, FS_REP, 0, 0, tiled=True)]
    reduce_sum x7 -> x2, other arithmetic: 6.41 us -> 0.7 us  [step(): norms = from_everyone(jnp.sum(share * share, axis=0), FS_REP).sum(axis=0)]
    all_to_all x2 -> x3, waiting for transfers between devices: 8.73 us -> 5.79 us  [the longest x1 5.78 us: own_rows(): return lax.all_to_all(pieces, 'tp', 0, 0, tiled=True)]
    all_to_all x4 -> x3, starting transfers between devices: 23.9 us -> 23.5 us  [from_everyone(): lax.all_to_all(jnp.broadcast_to(value[None], (n, *value.shape)), axis, 0,...]
  transfers between devices with their start and end apart: 23 -> 27, of which waited for: 14 -> 11; matrix products, arithmetic and copies ran while one was open for 7% -> 3% of each run, Pallas kernels for 4% -> 10%
where the time goes in v5:
time: 268 us; the launch traced here: 267 us
  starting transfers between devices  126 us (47%)
  waiting for transfers between devices  95.2 us (36%)
  Pallas kernels  25.5 us (10%)
  local copies, waits for them, and re-layouts  10.5 us (4%)
  other arithmetic  5.3 us (2%)
  matrix products  3.06 us (1%)
    ppermute x13, starting transfers between devices, take_from(): return lax.ppermute(value, axis, [((i + step) % n, i) for i in range(n)])  52.2 us
    ppermute x13, waiting for transfers between devices, take_from(): return lax.ppermute(value, axis, [((i + step) % n, i) for i in range(n)])  47.9 us
    all_to_all x3, waiting for transfers between devices, from_everyone(): lax.all_to_all(jnp.broadcast_to(value[None], (n, *value.shape)), axis, 0,...  32.5 us
    pallas_call x6, Pallas kernels, kernel(): pl.pallas_call(body, in_specs=[SMEM] + [VMEM] * len(arrays), out_specs=tu...  25.5 us
    all_to_all x3, starting transfers between devices, from_everyone(): lax.all_to_all(jnp.broadcast_to(value[None], (n, *value.shape)), axis, 0,...  23.5 us
    ppermute x6, starting transfers between devices, take_x(): lax.ppermute(value, 'tp', [((i + 2 * step) % n, i) for i in range(n)])  21 us
    all_to_all x1, starting transfers between devices, step(): share = lax.all_to_all(share, FS_REP, 0, 0, tiled=True)  10.4 us
    ppermute x2, starting transfers between devices, swap_cores(): lax.ppermute(value, 'tp', [(i, i ^ 1) for i in range(lax.axis_size('tp'))])  8.07 us
  transfers between devices with their start and end apart: 27, of which 11 were waited for; matrix products, arithmetic and copies ran while one was open for 3% of the time, Pallas kernels for 10%

profile of v5, /device:TPU:1, one launch (start us, length us, event | category | flops | bytes accessed | tf_op | source)
XLA Modules:
  0.0 266.9 jit_solution(13863837323159592020)
XLA Ops:
  1.5 1.2 broadcast_in_dim.6
  2.7 7.6 %all-to-all-start = ((bf16[8,64,1152]{2,1,0:T(8,128)(2,1)}), bf16[8,64,1152]{2,1,0:T(8,128)(2,1)S(1)}, u32[]{:S(2)}, u32[]{:S(2)}) async-start(bf16[8,64,1152]{2,1,0:T(8,128)(2,1)} %broadcast_in_dim.6), calls=%async_computation | async-start | bytes 2359296 | tf_op jit(solution)/shard_map/all_to_all | solution.py:30
  10.4 31.8 %all-to-all-done = bf16[8,64,1152]{2,1,0:T(8,128)(2,1)S(1)} async-done(((bf16[8,64,1152]{2,1,0:T(8,128)(2,1)}), bf16[8,64,1152]{2,1,0:T(8,128)(2,1)S(1)}, u32[]{:S(2)}, u32[]{:S(2)}) %all-to-all-start) | async-done | bytes 1179680 | tf_op jit(solution)/shard_map/all_to_all | solution.py:30
  42.2 1.2 broadcast_in_dim.7
  43.4 3.6 %all-to-all-start.3 = ((bf16[8,64,1152]{2,1,0:T(8,128)(2,1)}), bf16[8,64,1152]{2,1,0:T(8,128)(2,1)S(1)}, u32[]{:S(2)}, u32[]{:S(2)}) async-start(bf16[8,64,1152]{2,1,0:T(8,128)(2,1)} %broadcast_in_dim.7), calls=%async_computation.3 | async-start | bytes 2359296 | tf_op jit(solution)/shard_map/all_to_all | solution.py:30
  47.1 10.9 %collective-permute-start = (bf16[512,640]{1,0:T(8,128)(2,1)S(1)}, bf16[512,640]{1,0:T(8,128)(2,1)}, u32[]{:S(2)}, u32[]{:S(2)}) collective-permute-start(bf16[512,640]{1,0:T(8,128)(2,1)S(1)} %slice.16.refs_0_), channel_id=1, source_target_pairs={{64,0},{128,64},{192,128},{256,192},{320,256},{384,320},{448,384},... | collective-permute-start | bytes 1966088 | tf_op jit(solution)/shard_map/ppermute | solution.py:25
  58.0 1.9 collective-permute-start.4
  59.9 1.9 collective-permute-start.1
  61.9 9.7 %collective-permute-done.refs_1_ = bf16[512,640]{1,0:T(8,128)(2,1)} collective-permute-done((bf16[512,640]{1,0:T(8,128)(2,1)S(1)}, bf16[512,640]{1,0:T(8,128)(2,1)}, u32[]{:S(2)}, u32[]{:S(2)}) %collective-permute-start) | collective-permute-done | bytes 655392 | tf_op jit(solution)/shard_map/ppermute | solution.py:25
  71.5 5.4 %collective-permute-start.2 = (bf16[512,640]{1,0:T(8,128)(2,1)}, bf16[512,640]{1,0:T(8,128)(2,1)}, u32[]{:S(2)}, u32[]{:S(2)}) collective-permute-start(bf16[512,640]{1,0:T(8,128)(2,1)} %collective-permute-done.refs_1_), channel_id=1, source_target_pairs={{64,0},{128,64},{192,128},{256,192},{320,256},{384,320},{448,384},... | collective-permute-start | bytes 1966088 | tf_op jit(solution)/shard_map/ppermute | solution.py:25
  77.0 1.9 collective-permute-start.3
  78.9 3.4 %collective-permute-start.5 = (bf16[512,512]{1,0:T(8,128)(2,1)S(1)}, bf16[512,512]{1,0:T(8,128)(2,1)}, u32[]{:S(2)}, u32[]{:S(2)}) collective-permute-start(bf16[512,512]{1,0:T(8,128)(2,1)S(1)} %collective-permute-done.4.refs_6_), channel_id=1, source_target_pairs={{448,0},{0,64},{64,128},{128,192},{192,256},{256,320},{320,384},{3... | collective-permute-start | bytes 1572872 | tf_op jit(solution)/shard_map/ppermute | solution.py:25
  82.9 18.2 %collective-permute-done.3.refs_5_ = bf16[512,512]{1,0:T(8,128)(2,1)} collective-permute-done((bf16[512,512]{1,0:T(8,128)(2,1)S(1)}, bf16[512,512]{1,0:T(8,128)(2,1)}, u32[]{:S(2)}, u32[]{:S(2)}) %collective-permute-start.3) | collective-permute-done | bytes 524320 | tf_op jit(solution)/shard_map/ppermute | solution.py:25
  102.0 7.2 %shard_map.112 = bf16[256,2048]{1,0:T(8,128)(2,1)} custom-call(s32[2]{0:T(128)} %pad_add_fusion.z_ref, bf16[256,2048]{1,0:T(8,128)(2,1)} %u_ref.3, bf16[256,2048]{1,0:T(8,128)(2,1)} %c_ref.1, bf16[512,640]{1,0:T(8,128)(2,1)} %copy-done.5, bf16[512,640]{1,0:T(8,128)(2,1)} %collective-permute-done.refs_1_, bf16[512,640]{1,0:T(8,128)(2,1)} %copy-done.10, ...), custom_call_target="tpu_custom_call" | custom-call | flops 2013265920 | bytes 6291456 | tf_op jit(solution)/shard_map/pallas_call | solution.py:163
  109.1 6.5 %all-to-all-start.1 = ((bf16[8,32,2048]{2,1,0:T(8,128)(2,1)}), bf16[8,32,2048]{2,1,0:T(8,128)(2,1)S(1)}, u32[]{:S(2)}, u32[]{:S(2)}) async-start(bf16[8,32,2048]{2,1,0:T(8,128)(2,1)} %bitcast.33), calls=%async_computation.1 | async-start | bytes 2097152 | tf_op jit(solution)/shard_map/all_to_all | solution.py:177
  115.7 5.4 %collective-permute-start.6 = (bf16[512,640]{1,0:T(8,128)(2,1)S(1)}, bf16[512,640]{1,0:T(8,128)(2,1)}, u32[]{:S(2)}, u32[]{:S(2)}) collective-permute-start(bf16[512,640]{1,0:T(8,128)(2,1)S(1)} %slice.18.refs_0_), channel_id=1, source_target_pairs={{64,0},{128,64},{192,128},{256,192},{320,256},{384,320},{448,384},... | collective-permute-start | bytes 1966088 | tf_op jit(solution)/shard_map/ppermute | solution.py:25
  121.2 1.9 collective-permute-start.10
  123.1 1.7 constant_dynamic-slice_fusion
  124.8 5.8 %all-to-all-done.1.p_ref = bf16[8,32,2048]{2,1,0:T(8,128)(2,1)S(1)} async-done(((bf16[8,32,2048]{2,1,0:T(8,128)(2,1)}), bf16[8,32,2048]{2,1,0:T(8,128)(2,1)S(1)}, u32[]{:S(2)}, u32[]{:S(2)}) %all-to-all-start.1) | async-done | bytes 1048608 | tf_op jit(solution)/shard_map/all_to_all | solution.py:177
  131.5 2.7 shard_map.113
  134.2 4.4 %all-to-all-start.2 = ((bf16[8,32,2048]{2,1,0:T(8,128)(2,1)}), bf16[8,32,2048]{2,1,0:T(8,128)(2,1)S(1)}, u32[]{:S(2)}, u32[]{:S(2)}) async-start(bf16[8,32,2048]{2,1,0:T(8,128)(2,1)} %get-tuple-element.10), calls=%async_computation.2 | async-start | bytes 2097152 | tf_op jit(solution)/shard_map/all_to_all | solution.py:257
  138.6 1.9 collective-permute-start.7
  140.6 5.4 %collective-permute-start.8 = (bf16[512,640]{1,0:T(8,128)(2,1)}, bf16[512,640]{1,0:T(8,128)(2,1)}, u32[]{:S(2)}, u32[]{:S(2)}) collective-permute-start(bf16[512,640]{1,0:T(8,128)(2,1)} %collective-permute-done.6.refs_1_), channel_id=1, source_target_pairs={{64,0},{128,64},{192,128},{256,192},{320,256},{384,320},{448,384},... | collective-permute-start | bytes 1966088 | tf_op jit(solution)/shard_map/ppermute | solution.py:25
  146.0 3.4 %collective-permute-start.9 = (bf16[512,512]{1,0:T(8,128)(2,1)S(1)}, bf16[512,512]{1,0:T(8,128)(2,1)S(1)}, u32[]{:S(2)}, u32[]{:S(2)}) collective-permute-start(bf16[512,512]{1,0:T(8,128)(2,1)S(1)} %slice.19.refs_4_), channel_id=1, source_target_pairs={{64,0},{128,64},{192,128},{256,192},{320,256},{384,320},{448,384},... | collective-permute-start | bytes 1572872 | tf_op jit(solution)/shard_map/ppermute | solution.py:25
  149.4 1.9 collective-permute-start.11
  151.3 20.1 %collective-permute-done.9.refs_5_ = bf16[512,512]{1,0:T(8,128)(2,1)S(1)} collective-permute-done((bf16[512,512]{1,0:T(8,128)(2,1)S(1)}, bf16[512,512]{1,0:T(8,128)(2,1)S(1)}, u32[]{:S(2)}, u32[]{:S(2)}) %collective-permute-start.9) | collective-permute-done | bytes 524320 | tf_op jit(solution)/shard_map/ppermute | solution.py:25
  173.0 5.1 %shard_map.114 = (f32[256,768]{1,0:T(8,128)}, bf16[256,384]{1,0:T(8,128)(2,1)}) custom-call(s32[2]{0:T(128)} %pad_add_fusion.z_ref, bf16[256,2048]{1,0:T(8,128)(2,1)} %u_ref.5, bf16[512,640]{1,0:T(8,128)(2,1)} %copy-done, bf16[512,640]{1,0:T(8,128)(2,1)} %collective-permute-done.6.refs_1_, bf16[512,640]{1,0:T(8,128)(2,1)} %copy-done.4, ...), custom_call_target="tpu_custom_call" | custom-call | flops 805306368 | bytes 6291456 | tf_op jit(solution)/shard_map/pallas_call | solution.py:163
  178.1 3.1 %multiply_convert_fusion = bf16[2048,384]{1,0:T(8,128)(2,1)} fusion(bf16[256,2048]{1,0:T(8,128)(2,1)S(1)} %bitcast.34, bf16[256,384]{1,0:T(8,128)(2,1)} %get-tuple-element.16), kind=kOutput, calls=%fused_computation.1 | convolution fusion | flops 404226048 | bytes 2818048 | tf_op jit(solution)/shard_map/dot_general | solution.py:268
  181.1 10.4 %all-to-all-start.4 = ((bf16[64,32,384]{2,1,0:T(8,128)(2,1)}), bf16[64,32,384]{2,1,0:T(8,128)(2,1)S(1)}, u32[]{:S(2)}, u32[]{:S(2)}) async-start(bf16[64,32,384]{2,1,0:T(8,128)(2,1)} %bitcast.36), calls=%async_computation.4 | async-start | bytes 3145728 | tf_op jit(solution)/shard_map/all_to_all | solution.py:272
  191.6 5.9 %shard_map.115 = (bf16[4,32,2048]{2,1,0:T(8,128)(2,1)}, bf16[4,32,2048]{2,1,0:T(8,128)(2,1)}) custom-call(s32[2]{0:T(128)} %pad_add_fusion.z_ref, bf16[256,2048]{1,0:T(8,128)(2,1)} %bitcast.35, f32[256,768]{1,0:T(8,128)} %get-tuple-element.12.both_ref, bf16[512,640]{1,0:T(8,128)(2,1)} %copy-done, bf16[512,640]{1,0:T(8,128)(2,1)} %collective-permute-done.6.refs_1_, ...), custom_call_target="tpu_custom_call" | custom-call | flops 1207959552 | bytes 6291456 | tf_op jit(solution)/shard_map/pallas_call | solution.py:163
  197.4 3.2 %collective-permute-start.12 = (bf16[4,32,2048]{2,1,0:T(8,128)(2,1)}, bf16[4,32,2048]{2,1,0:T(8,128)(2,1)S(1)}, u32[]{:S(2)}, u32[]{:S(2)}) collective-permute-start(bf16[4,32,2048]{2,1,0:T(8,128)(2,1)} %get-tuple-element.14), channel_id=1, source_target_pairs={{0,1},{1,0},{2,3},{3,2},{4,5},{5,4},{6,7},{7,6},{8,9},{9,8},{10,11... | collective-permute-start | bytes 1572872 | tf_op jit(solution)/shard_map/ppermute | solution.py:181
  200.7 1.6 collective-permute-done.12
  202.3 1.2 add_convert_fusion
  204.2 4.8 %collective-permute-start.13 = (bf16[32,2048]{1,0:T(8,128)(2,1)S(1)}, bf16[32,2048]{1,0:T(8,128)(2,1)S(1)}, u32[]{:S(2)}, u32[]{:S(2)}) collective-permute-start(bf16[32,2048]{1,0:T(8,128)(2,1)S(1)} %get-tuple-element.19), channel_id=1, source_target_pairs={{4,0},{5,1},{6,2},{7,3},{0,4},{1,5},{2,6},{3,7},{12,8},{13,9},{14,... | collective-permute-start | bytes 393224 | tf_op jit(solution)/shard_map/ppermute | solution.py:186
  209.0 2.2 collective-permute-start.14
  211.2 4.3 %collective-permute-start.15 = (bf16[32,2048]{1,0:T(8,128)(2,1)S(1)}, bf16[32,2048]{1,0:T(8,128)(2,1)S(1)}, u32[]{:S(2)}, u32[]{:S(2)}) collective-permute-start(bf16[32,2048]{1,0:T(8,128)(2,1)S(1)} %get-tuple-element.17), channel_id=1, source_target_pairs={{2,0},{3,1},{4,2},{5,3},{6,4},{7,5},{0,6},{1,7},{10,8},{11,9},{12,... | collective-permute-start | bytes 393224 | tf_op jit(solution)/shard_map/ppermute | solution.py:186
  215.5 1.0 collective-permute-done.14.p2
  218.1 2.4 shard_map.116.q0
  220.5 5.3 %collective-permute-start.16 = (bf16[32,2048]{1,0:T(8,128)(2,1)}, bf16[32,2048]{1,0:T(8,128)(2,1)S(1)}, u32[]{:S(2)}, u32[]{:S(2)}) collective-permute-start(bf16[32,2048]{1,0:T(8,128)(2,1)} %shard_map.116.q0), channel_id=1, source_target_pairs={{2,0},{3,1},{4,2},{5,3},{6,4},{7,5},{0,6},{1,7},{10,8},{11,9},{12,... | collective-permute-start | bytes 393224 | tf_op jit(solution)/shard_map/ppermute | solution.py:186
  225.8 1.9 collective-permute-start.17
  227.7 2.5 collective-permute-start.18
  230.2 3.0 %collective-permute-done.17.q2 = bf16[32,2048]{1,0:T(8,128)(2,1)S(1)} collective-permute-done((bf16[32,2048]{1,0:T(8,128)(2,1)}, bf16[32,2048]{1,0:T(8,128)(2,1)S(1)}, u32[]{:S(2)}, u32[]{:S(2)}) %collective-permute-start.17) | collective-permute-done | bytes 131104 | tf_op jit(solution)/shard_map/ppermute | solution.py:186
  233.2 2.4 collective-permute-done.18.q3
  235.6 1.0 pad_maximum_fusion
  236.7 4.9 %collective-permute-start.19 = (bf16[4,32,2048]{2,1,0:T(8,128)(2,1)S(1)}, bf16[4,32,2048]{2,1,0:T(8,128)(2,1)S(1)}, u32[]{:S(2)}, u32[]{:S(2)}) collective-permute-start(bf16[4,32,2048]{2,1,0:T(8,128)(2,1)S(1)} %pad_maximum_fusion), channel_id=1, source_target_pairs={{0,1},{1,0},{2,3},{3,2},{4,5},{5,4},{6,7},{7,6},{8,9},{9,8},{10,11... | collective-permute-start | bytes 1572872 | tf_op jit(solution)/shard_map/ppermute | solution.py:181
  242.5 12.3 %all-to-all-start.5 = ((f32[64,1,384]{2,1,0:T(1,128)}), f32[64,1,384]{2,1,0:T(1,128)S(1)}, u32[]{:S(2)}, u32[]{:S(2)}) async-start(f32[64,1,384]{2,1,0:T(1,128)} %broadcast_in_dim.8), calls=%async_computation.5 | async-start | bytes 196608 | tf_op jit(solution)/shard_map/all_to_all | solution.py:30
  254.8 6.8 %collective-permute-start.20 = (f32[32,384]{1,0:T(8,128)S(1)}, f32[32,384]{1,0:T(8,128)S(1)}, u32[]{:S(2)}, u32[]{:S(2)}) collective-permute-start(f32[32,384]{1,0:T(8,128)S(1)} %convert_reduce_fusion), channel_id=1, source_target_pairs={{256,0},{0,256},{257,1},{1,257},{258,2},{2,258},{259,3},{3,259},{2... | collective-permute-start | bytes 147464 | tf_op jit(solution)/shard_map/ppermute | solution.py:25
  262.5 2.4 shard_map.117
  (75 shorter events, 11.2 us)
Async XLA Ops:
  1.5 8.9 %copy-start.19 = (bf16[384,64]{0,1:T(8,128)(2,1)S(1)}, bf16[384,64]{0,1:T(8,128)(2,1)}, u32[]{:S(2)}) copy-start(bf16[384,64]{0,1:T(8,128)(2,1)} %param.14) | copy-start | bytes 147460
  1.5 8.9 %copy-start.20 = (bf16[64,384]{1,0:T(8,128)(2,1)S(1)}, bf16[64,384]{1,0:T(8,128)(2,1)}, u32[]{:S(2)}) copy-start(bf16[64,384]{1,0:T(8,128)(2,1)} %param.13) | copy-start | bytes 147460
  1.5 8.9 %copy-start.21 = (bf16[64,384]{1,0:T(8,128)(2,1)S(1)}, bf16[64,384]{1,0:T(8,128)(2,1)}, u32[]{:S(2)}) copy-start(bf16[64,384]{1,0:T(8,128)(2,1)} %param.12) | copy-start | bytes 147460
  2.7 39.5 %all-to-all-start = ((bf16[8,64,1152]{2,1,0:T(8,128)(2,1)}), bf16[8,64,1152]{2,1,0:T(8,128)(2,1)S(1)}, u32[]{:S(2)}, u32[]{:S(2)}) async-start(bf16[8,64,1152]{2,1,0:T(8,128)(2,1)} %broadcast_in_dim.6), calls=%async_computation | async-start | bytes 2359296 | tf_op jit(solution)/shard_map/all_to_all | solution.py:30
  43.4 65.7 %all-to-all-start.3 = ((bf16[8,64,1152]{2,1,0:T(8,128)(2,1)}), bf16[8,64,1152]{2,1,0:T(8,128)(2,1)S(1)}, u32[]{:S(2)}, u32[]{:S(2)}) async-start(bf16[8,64,1152]{2,1,0:T(8,128)(2,1)} %broadcast_in_dim.7), calls=%async_computation.3 | async-start | bytes 2359296 | tf_op jit(solution)/shard_map/all_to_all | solution.py:30
  47.1 54.1 %copy-start.5 = (bf16[512,640]{1,0:T(8,128)(2,1)}, bf16[512,640]{1,0:T(8,128)(2,1)S(1)}, u32[]{:S(2)}) copy-start(bf16[512,640]{1,0:T(8,128)(2,1)S(1)} %slice.16.refs_0_) | copy-start | bytes 1966084
  47.1 24.5 %collective-permute-start = (bf16[512,640]{1,0:T(8,128)(2,1)S(1)}, bf16[512,640]{1,0:T(8,128)(2,1)}, u32[]{:S(2)}, u32[]{:S(2)}) collective-permute-start(bf16[512,640]{1,0:T(8,128)(2,1)S(1)} %slice.16.refs_0_), channel_id=1, source_target_pairs={{64,0},{128,64},{192,128},{256,192},{320,256},{384,320},{448,384},... | collective-permute-start | bytes 1966088 | tf_op jit(solution)/shard_map/ppermute | solution.py:25
  58.0 43.1 %copy-start.6 = (bf16[512,512]{1,0:T(8,128)(2,1)}, bf16[512,512]{1,0:T(8,128)(2,1)S(1)}, u32[]{:S(2)}) copy-start(bf16[512,512]{1,0:T(8,128)(2,1)S(1)} %slice.17.refs_4_) | copy-start | bytes 1572868
  58.0 20.9 %collective-permute-start.4 = (bf16[512,512]{1,0:T(8,128)(2,1)S(1)}, bf16[512,512]{1,0:T(8,128)(2,1)S(1)}, u32[]{:S(2)}, u32[]{:S(2)}) collective-permute-start(bf16[512,512]{1,0:T(8,128)(2,1)S(1)} %slice.17.refs_4_), channel_id=1, source_target_pairs={{448,0},{0,64},{64,128},{128,192},{192,256},{256,320},{320,384},{3... | collective-permute-start | bytes 1572872 | tf_op jit(solution)/shard_map/ppermute | solution.py:25
  59.9 41.2 %collective-permute-start.1 = (bf16[512,640]{1,0:T(8,128)(2,1)S(1)}, bf16[512,640]{1,0:T(8,128)(2,1)S(1)}, u32[]{:S(2)}, u32[]{:S(2)}) collective-permute-start(bf16[512,640]{1,0:T(8,128)(2,1)S(1)} %slice.16.refs_0_), channel_id=1, source_target_pairs={{448,0},{0,64},{64,128},{128,192},{192,256},{256,320},{320,384},{3... | collective-permute-start | bytes 1966088 | tf_op jit(solution)/shard_map/ppermute | solution.py:25
  71.5 29.6 %collective-permute-start.2 = (bf16[512,640]{1,0:T(8,128)(2,1)}, bf16[512,640]{1,0:T(8,128)(2,1)}, u32[]{:S(2)}, u32[]{:S(2)}) collective-permute-start(bf16[512,640]{1,0:T(8,128)(2,1)} %collective-permute-done.refs_1_), channel_id=1, source_target_pairs={{64,0},{128,64},{192,128},{256,192},{320,256},{384,320},{448,384},... | collective-permute-start | bytes 1966088 | tf_op jit(solution)/shard_map/ppermute | solution.py:25
  77.0 24.2 %collective-permute-start.3 = (bf16[512,512]{1,0:T(8,128)(2,1)S(1)}, bf16[512,512]{1,0:T(8,128)(2,1)}, u32[]{:S(2)}, u32[]{:S(2)}) collective-permute-start(bf16[512,512]{1,0:T(8,128)(2,1)S(1)} %slice.17.refs_4_), channel_id=1, source_target_pairs={{64,0},{128,64},{192,128},{256,192},{320,256},{384,320},{448,384},... | collective-permute-start | bytes 1572872 | tf_op jit(solution)/shard_map/ppermute | solution.py:25
  78.9 22.3 %copy-start.11 = (bf16[512,512]{1,0:T(8,128)(2,1)}, bf16[512,512]{1,0:T(8,128)(2,1)S(1)}, u32[]{:S(2)}) copy-start(bf16[512,512]{1,0:T(8,128)(2,1)S(1)} %collective-permute-done.4.refs_6_) | copy-start | bytes 1572868
  78.9 22.2 %collective-permute-start.5 = (bf16[512,512]{1,0:T(8,128)(2,1)S(1)}, bf16[512,512]{1,0:T(8,128)(2,1)}, u32[]{:S(2)}, u32[]{:S(2)}) collective-permute-start(bf16[512,512]{1,0:T(8,128)(2,1)S(1)} %collective-permute-done.4.refs_6_), channel_id=1, source_target_pairs={{448,0},{0,64},{64,128},{128,192},{192,256},{256,320},{320,384},{3... | collective-permute-start | bytes 1572872 | tf_op jit(solution)/shard_map/ppermute | solution.py:25
  101.1 0.8 copy-start.10
  109.1 21.5 %all-to-all-start.1 = ((bf16[8,32,2048]{2,1,0:T(8,128)(2,1)}), bf16[8,32,2048]{2,1,0:T(8,128)(2,1)S(1)}, u32[]{:S(2)}, u32[]{:S(2)}) async-start(bf16[8,32,2048]{2,1,0:T(8,128)(2,1)} %bitcast.33), calls=%async_computation.1 | async-start | bytes 2097152 | tf_op jit(solution)/shard_map/all_to_all | solution.py:177
  115.7 23.0 %copy-start = (bf16[512,640]{1,0:T(8,128)(2,1)}, bf16[512,640]{1,0:T(8,128)(2,1)S(1)}, u32[]{:S(2)}) copy-start(bf16[512,640]{1,0:T(8,128)(2,1)S(1)} %slice.18.refs_0_) | copy-start | bytes 1966084
  115.7 24.9 %collective-permute-start.6 = (bf16[512,640]{1,0:T(8,128)(2,1)S(1)}, bf16[512,640]{1,0:T(8,128)(2,1)}, u32[]{:S(2)}, u32[]{:S(2)}) collective-permute-start(bf16[512,640]{1,0:T(8,128)(2,1)S(1)} %slice.18.refs_0_), channel_id=1, source_target_pairs={{64,0},{128,64},{192,128},{256,192},{320,256},{384,320},{448,384},... | collective-permute-start | bytes 1966088 | tf_op jit(solution)/shard_map/ppermute | solution.py:25
  121.2 24.9 %copy-start.1 = (bf16[512,512]{1,0:T(8,128)(2,1)}, bf16[512,512]{1,0:T(8,128)(2,1)S(1)}, u32[]{:S(2)}) copy-start(bf16[512,512]{1,0:T(8,128)(2,1)S(1)} %slice.19.refs_4_) | copy-start | bytes 1572868
  121.2 28.2 %collective-permute-start.10 = (bf16[512,512]{1,0:T(8,128)(2,1)S(1)}, bf16[512,512]{1,0:T(8,128)(2,1)S(1)}, u32[]{:S(2)}, u32[]{:S(2)}) collective-permute-start(bf16[512,512]{1,0:T(8,128)(2,1)S(1)} %slice.19.refs_4_), channel_id=1, source_target_pairs={{448,0},{0,64},{64,128},{128,192},{192,256},{256,320},{320,384},{3... | collective-permute-start | bytes 1572872 | tf_op jit(solution)/shard_map/ppermute | solution.py:25
  130.6 1.0 copy-start.2
  134.2 43.9 %all-to-all-start.2 = ((bf16[8,32,2048]{2,1,0:T(8,128)(2,1)}), bf16[8,32,2048]{2,1,0:T(8,128)(2,1)S(1)}, u32[]{:S(2)}, u32[]{:S(2)}) async-start(bf16[8,32,2048]{2,1,0:T(8,128)(2,1)} %get-tuple-element.10), calls=%async_computation.2 | async-start | bytes 2097152 | tf_op jit(solution)/shard_map/all_to_all | solution.py:257
  138.6 32.8 %collective-permute-start.7 = (bf16[512,640]{1,0:T(8,128)(2,1)S(1)}, bf16[512,640]{1,0:T(8,128)(2,1)S(1)}, u32[]{:S(2)}, u32[]{:S(2)}) collective-permute-start(bf16[512,640]{1,0:T(8,128)(2,1)S(1)} %slice.18.refs_0_), channel_id=1, source_target_pairs={{448,0},{0,64},{64,128},{128,192},{192,256},{256,320},{320,384},{3... | collective-permute-start | bytes 1966088 | tf_op jit(solution)/shard_map/ppermute | solution.py:25
  140.6 32.4 %collective-permute-start.8 = (bf16[512,640]{1,0:T(8,128)(2,1)}, bf16[512,640]{1,0:T(8,128)(2,1)}, u32[]{:S(2)}, u32[]{:S(2)}) collective-permute-start(bf16[512,640]{1,0:T(8,128)(2,1)} %collective-permute-done.6.refs_1_), channel_id=1, source_target_pairs={{64,0},{128,64},{192,128},{256,192},{320,256},{384,320},{448,384},... | collective-permute-start | bytes 1966088 | tf_op jit(solution)/shard_map/ppermute | solution.py:25
  146.0 25.4 %collective-permute-start.9 = (bf16[512,512]{1,0:T(8,128)(2,1)S(1)}, bf16[512,512]{1,0:T(8,128)(2,1)S(1)}, u32[]{:S(2)}, u32[]{:S(2)}) collective-permute-start(bf16[512,512]{1,0:T(8,128)(2,1)S(1)} %slice.19.refs_4_), channel_id=1, source_target_pairs={{64,0},{128,64},{192,128},{256,192},{320,256},{384,320},{448,384},... | collective-permute-start | bytes 1572872 | tf_op jit(solution)/shard_map/ppermute | solution.py:25
  149.4 23.6 %copy-start.7 = (bf16[512,512]{1,0:T(8,128)(2,1)}, bf16[512,512]{1,0:T(8,128)(2,1)S(1)}, u32[]{:S(2)}) copy-start(bf16[512,512]{1,0:T(8,128)(2,1)S(1)} %collective-permute-done.10.refs_6_) | copy-start | bytes 1572868
  149.4 22.0 %collective-permute-start.11 = (bf16[512,512]{1,0:T(8,128)(2,1)S(1)}, bf16[512,512]{1,0:T(8,128)(2,1)S(1)}, u32[]{:S(2)}, u32[]{:S(2)}) collective-permute-start(bf16[512,512]{1,0:T(8,128)(2,1)S(1)} %collective-permute-done.10.refs_6_), channel_id=1, source_target_pairs={{448,0},{0,64},{64,128},{128,192},{192,256},{256,320},{320,384},{3... | collective-permute-start | bytes 1572872 | tf_op jit(solution)/shard_map/ppermute | solution.py:25
  171.4 0.8 copy-start.8
  171.4 1.6 copy-start.4
  172.2 0.8 copy-start.9
  178.1 3.1 %copy-start.3 = (bf16[8,32,2048]{2,1,0:T(8,128)(2,1)}, bf16[8,32,2048]{2,1,0:T(8,128)(2,1)S(1)}, u32[]{:S(2)}) copy-start(bf16[8,32,2048]{2,1,0:T(8,128)(2,1)S(1)} %all-to-all-done.2) | copy-start | bytes 3145732
  181.1 60.4 %all-to-all-start.4 = ((bf16[64,32,384]{2,1,0:T(8,128)(2,1)}), bf16[64,32,384]{2,1,0:T(8,128)(2,1)S(1)}, u32[]{:S(2)}, u32[]{:S(2)}) async-start(bf16[64,32,384]{2,1,0:T(8,128)(2,1)} %bitcast.36), calls=%async_computation.4 | async-start | bytes 3145728 | tf_op jit(solution)/shard_map/all_to_all | solution.py:272
  197.4 4.9 %collective-permute-start.12 = (bf16[4,32,2048]{2,1,0:T(8,128)(2,1)}, bf16[4,32,2048]{2,1,0:T(8,128)(2,1)S(1)}, u32[]{:S(2)}, u32[]{:S(2)}) collective-permute-start(bf16[4,32,2048]{2,1,0:T(8,128)(2,1)} %get-tuple-element.14), channel_id=1, source_target_pairs={{0,1},{1,0},{2,3},{3,2},{4,5},{5,4},{6,7},{7,6},{8,9},{9,8},{10,11... | collective-permute-start | bytes 1572872 | tf_op jit(solution)/shard_map/ppermute | solution.py:181
  204.2 11.3 %collective-permute-start.13 = (bf16[32,2048]{1,0:T(8,128)(2,1)S(1)}, bf16[32,2048]{1,0:T(8,128)(2,1)S(1)}, u32[]{:S(2)}, u32[]{:S(2)}) collective-permute-start(bf16[32,2048]{1,0:T(8,128)(2,1)S(1)} %get-tuple-element.19), channel_id=1, source_target_pairs={{4,0},{5,1},{6,2},{7,3},{0,4},{1,5},{2,6},{3,7},{12,8},{13,9},{14,... | collective-permute-start | bytes 393224 | tf_op jit(solution)/shard_map/ppermute | solution.py:186
  209.0 7.5 %collective-permute-start.14 = (bf16[32,2048]{1,0:T(8,128)(2,1)S(1)}, bf16[32,2048]{1,0:T(8,128)(2,1)S(1)}, u32[]{:S(2)}, u32[]{:S(2)}) collective-permute-start(bf16[32,2048]{1,0:T(8,128)(2,1)S(1)} %get-tuple-element.18), channel_id=1, source_target_pairs={{6,0},{7,1},{0,2},{1,3},{2,4},{3,5},{4,6},{5,7},{14,8},{15,9},{8,1... | collective-permute-start | bytes 393224 | tf_op jit(solution)/shard_map/ppermute | solution.py:186
  211.2 6.2 %collective-permute-start.15 = (bf16[32,2048]{1,0:T(8,128)(2,1)S(1)}, bf16[32,2048]{1,0:T(8,128)(2,1)S(1)}, u32[]{:S(2)}, u32[]{:S(2)}) collective-permute-start(bf16[32,2048]{1,0:T(8,128)(2,1)S(1)} %get-tuple-element.17), channel_id=1, source_target_pairs={{2,0},{3,1},{4,2},{5,3},{6,4},{7,5},{0,6},{1,7},{10,8},{11,9},{12,... | collective-permute-start | bytes 393224 | tf_op jit(solution)/shard_map/ppermute | solution.py:186
  215.5 1.9 copy-start.16
  216.5 0.9 copy-start.17
  220.5 9.7 %collective-permute-start.16 = (bf16[32,2048]{1,0:T(8,128)(2,1)}, bf16[32,2048]{1,0:T(8,128)(2,1)S(1)}, u32[]{:S(2)}, u32[]{:S(2)}) collective-permute-start(bf16[32,2048]{1,0:T(8,128)(2,1)} %shard_map.116.q0), channel_id=1, source_target_pairs={{2,0},{3,1},{4,2},{5,3},{6,4},{7,5},{0,6},{1,7},{10,8},{11,9},{12,... | collective-permute-start | bytes 393224 | tf_op jit(solution)/shard_map/ppermute | solution.py:186
  225.8 7.4 %collective-permute-start.17 = (bf16[32,2048]{1,0:T(8,128)(2,1)}, bf16[32,2048]{1,0:T(8,128)(2,1)S(1)}, u32[]{:S(2)}, u32[]{:S(2)}) collective-permute-start(bf16[32,2048]{1,0:T(8,128)(2,1)} %shard_map.116.q0), channel_id=1, source_target_pairs={{4,0},{5,1},{6,2},{7,3},{0,4},{1,5},{2,6},{3,7},{12,8},{13,9},{14,... | collective-permute-start | bytes 393224 | tf_op jit(solution)/shard_map/ppermute | solution.py:186
  227.7 7.9 %collective-permute-start.18 = (bf16[32,2048]{1,0:T(8,128)(2,1)}, bf16[32,2048]{1,0:T(8,128)(2,1)S(1)}, u32[]{:S(2)}, u32[]{:S(2)}) collective-permute-start(bf16[32,2048]{1,0:T(8,128)(2,1)} %shard_map.116.q0), channel_id=1, source_target_pairs={{6,0},{7,1},{0,2},{1,3},{2,4},{3,5},{4,6},{5,7},{14,8},{15,9},{8,1... | collective-permute-start | bytes 393224 | tf_op jit(solution)/shard_map/ppermute | solution.py:186
  230.2 31.5 %copy-start.13 = (bf16[32,2048]{1,0:T(8,128)(2,1)}, bf16[32,2048]{1,0:T(8,128)(2,1)S(1)}, u32[]{:S(2)}) copy-start(bf16[32,2048]{1,0:T(8,128)(2,1)S(1)} %collective-permute-done.16.q1) | copy-start | bytes 393220
  233.2 28.5 %copy-start.14 = (bf16[32,2048]{1,0:T(8,128)(2,1)}, bf16[32,2048]{1,0:T(8,128)(2,1)S(1)}, u32[]{:S(2)}) copy-start(bf16[32,2048]{1,0:T(8,128)(2,1)S(1)} %collective-permute-done.17.q2) | copy-start | bytes 393220
  235.6 26.1 %copy-start.15 = (bf16[32,2048]{1,0:T(8,128)(2,1)}, bf16[32,2048]{1,0:T(8,128)(2,1)S(1)}, u32[]{:S(2)}) copy-start(bf16[32,2048]{1,0:T(8,128)(2,1)S(1)} %collective-permute-done.18.q3) | copy-start | bytes 393220
  236.7 25.0 %collective-permute-start.19 = (bf16[4,32,2048]{2,1,0:T(8,128)(2,1)S(1)}, bf16[4,32,2048]{2,1,0:T(8,128)(2,1)S(1)}, u32[]{:S(2)}, u32[]{:S(2)}) collective-permute-start(bf16[4,32,2048]{2,1,0:T(8,128)(2,1)S(1)} %pad_maximum_fusion), channel_id=1, source_target_pairs={{0,1},{1,0},{2,3},{3,2},{4,5},{5,4},{6,7},{7,6},{8,9},{9,8},{10,11... | collective-permute-start | bytes 1572872 | tf_op jit(solution)/shard_map/ppermute | solution.py:181
  242.5 23.7 %all-to-all-start.5 = ((f32[64,1,384]{2,1,0:T(1,128)}), f32[64,1,384]{2,1,0:T(1,128)S(1)}, u32[]{:S(2)}, u32[]{:S(2)}) async-start(f32[64,1,384]{2,1,0:T(1,128)} %broadcast_in_dim.8), calls=%async_computation.5 | async-start | bytes 196608 | tf_op jit(solution)/shard_map/all_to_all | solution.py:30
  254.8 10.0 %collective-permute-start.20 = (f32[32,384]{1,0:T(8,128)S(1)}, f32[32,384]{1,0:T(8,128)S(1)}, u32[]{:S(2)}, u32[]{:S(2)}) collective-permute-start(f32[32,384]{1,0:T(8,128)S(1)} %convert_reduce_fusion), channel_id=1, source_target_pairs={{256,0},{0,256},{257,1},{1,257},{258,2},{2,258},{259,3},{3,259},{2... | collective-permute-start | bytes 147464 | tf_op jit(solution)/shard_map/ppermute | solution.py:25
  261.7 0.8 copy-start.12
  (1 other events, 0.7 us)

commit v6 on v5

--- a/solution.py
+++ b/solution.py
@@ -53,29 +53,37 @@
     return pl.ds(pl.multiple_of(lax.rem(z + m, 4) * quarter, quarter), quarter)
 
 
-def gate_up_of(z, u_ref, left, right, n):
+def scale_of(u_ref):
+    field = u_ref[...].astype(f32)
+    return lax.rsqrt(jnp.mean(field * field, axis=1, keepdims=True) + eps)
+
+
+def gate_up_of(z, u_ref, scale, places, left, right, n):
     width = u_ref.shape[1]
-    field = u_ref[...].astype(f32)
-    scale = lax.rsqrt(jnp.mean(field * field, axis=1, keepdims=True) + eps)
     a = b = None
-    for m, wl, wr in zip(PIECES, left, right):
+    for m, wl, wr in zip(places, left, right):
         normed_b = (u_ref[:, span_of(z, m, width)].astype(f32) * scale).astype(bf16)
         part_a = jnp.dot(normed_b, wl[...], preferred_element_type=f32)
         part_b = jnp.dot(normed_b, wr[:, : 2 * n - LEFT], preferred_element_type=f32)
         a = part_a if a is None else a + part_a
         b = part_b if b is None else b + part_b
-    return a[:, :n], jnp.concatenate([a[:, n:], b], axis=1)
-
-
-def partial_of(z, c_ref, gate, upper, left, right, out_ref):
-    width, n = c_ref.shape[1], gate.shape[1]
+    return a, b
+
+
+def back_of(z, c_ref, places, right, n):
+    width = c_ref.shape[1]
     total = None
-    for m, wr in zip(PIECES, right):
+    for m, wr in zip(places, right):
         part = jnp.dot(
             c_ref[:, span_of(z, m, width)], wr[:, 2 * n - LEFT :], preferred_element_type=f32
         )
         total = part if total is None else total + part
-    back = 0.5 * total
+    return total
+
+
+def partial_of(z, back, gate, upper, left, right, out_ref):
+    width, n = out_ref.shape[1], gate.shape[1]
+    back = 0.5 * back
     logistic = jax.nn.sigmoid(gate)
     d_gate = (back * upper * logistic * (1.0 + gate * (1.0 - logistic))).astype(bf16)
     d_up = (back * (gate * logistic)).astype(bf16)
@@ -89,19 +97,46 @@
         out_ref[:, span_of(z, m, width)] = part.astype(bf16)
 
 
-def block_body(z_ref, u_ref, c_ref, *refs):
+def near_body(z_ref, u_ref, c_ref, *refs):
+    *weight, sums_ref, scale_ref = refs
+    z, left, right = z_ref[0], weight[:3], weight[3:]
+    n = sums_ref.shape[1] // 3
+    scale = scale_of(u_ref)
+    a, b = gate_up_of(z, u_ref, scale, PIECES[:3], left, right, n)
+    sums_ref[:, :LEFT] = a
+    sums_ref[:, LEFT : 2 * n] = b
+    sums_ref[:, 2 * n :] = back_of(z, c_ref, PIECES[:3], right, n)
+    scale_ref[...] = jnp.broadcast_to(scale, scale_ref.shape)
+
+
+def block_body(z_ref, u_ref, c_ref, sums_ref, scale_ref, *refs):
     *weight, out_ref = refs
     z, left, right = z_ref[0], weight[:4], weight[4:]
-    gate, upper = gate_up_of(z, u_ref, left, right, (LEFT + right[0].shape[1]) // 3)
-    partial_of(z, c_ref, gate, upper, left, right, out_ref)
-
-
-def forward_body(z_ref, u_ref, *refs):
-    *weight, both_ref, hidden_ref = refs
+    n = sums_ref.shape[1] // 3
+    a, b = gate_up_of(z, u_ref, scale_ref[:, :1], PIECES[3:], left[3:], right[3:], n)
+    a, b = a + sums_ref[:, :LEFT], b + sums_ref[:, LEFT : 2 * n]
+    back = back_of(z, c_ref, PIECES[3:], right[3:], n) + sums_ref[:, 2 * n :]
+    upper = jnp.concatenate([a[:, n:], b], axis=1)
+    partial_of(z, back, a[:, :n], upper, left, right, out_ref)
+
+
+def near_forward_body(z_ref, u_ref, *refs):
+    *weight, sums_ref, scale_ref = refs
+    scale = scale_of(u_ref)
+    n = sums_ref.shape[1] // 2
+    a, b = gate_up_of(z_ref[0], u_ref, scale, PIECES[:3], weight[:3], weight[3:], n)
+    sums_ref[:, :LEFT] = a
+    sums_ref[:, LEFT:] = b
+    scale_ref[...] = jnp.broadcast_to(scale, scale_ref.shape)
+
+
+def forward_body(z_ref, u_ref, sums_ref, scale_ref, left_ref, right_ref, both_ref, hidden_ref):
     n = hidden_ref.shape[1]
-    gate, upper = gate_up_of(z_ref[0], u_ref, weight[:4], weight[4:], n)
-    both_ref[:, :n] = gate
-    both_ref[:, n:] = upper
+    scale = scale_ref[:, :1]
+    a, b = gate_up_of(z_ref[0], u_ref, scale, PIECES[3:], [left_ref], [right_ref], n)
+    total = jnp.concatenate([a, b], axis=1) + sums_ref[...]
+    gate, upper = total[:, :n], total[:, n:]
+    both_ref[...] = total
     hidden_ref[...] = (gate * jax.nn.sigmoid(gate) * upper).astype(bf16)
 
 
@@ -109,7 +144,8 @@
     *weight, mine_ref, other_ref, out_ref = refs
     n = both_ref.shape[1] // 2
     gate, upper = both_ref[:, :n], both_ref[:, n:]
-    partial_of(z_ref[0], c_ref, gate, upper, weight[:4], weight[4:], out_ref)
+    back = back_of(z_ref[0], c_ref, PIECES, weight[4:], n)
+    partial_of(z_ref[0], back, gate, upper, weight[:4], weight[4:], out_ref)
     core, (blocks, rows, _) = z_ref[1], mine_ref.shape
     for k in range(blocks):
         mine_ref[k] = out_ref[pl.ds(pl.multiple_of((2 * k + core) * rows, rows), rows), :]
@@ -159,7 +195,11 @@
 VMEM = pl.BlockSpec(memory_space=pltpu.VMEM)
 
 
-def kernel(body, outs, flops, scalars, *arrays, scratch=()):
+def kernel(body, outs, flops, scalars, *arrays, scratch=(), near=()):
+    arrays = [
+        pltpu.with_memory_space_constraint(a, pltpu.MemorySpace.VMEM) if i in near else a
+        for i, a in enumerate(arrays)
+    ]
     return pl.pallas_call(
         body,
         in_specs=[SMEM] + [VMEM] * len(arrays),
@@ -206,7 +246,7 @@
     stacked = jnp.stack(quarters)
     other = swap_cores(stacked)
     out = ((8 * value.shape[0], value.shape[1]), bf16)
-    (whole,) = kernel(place_rows_body, (out,), 1 << 20, tps, *quarters, other)
+    (whole,) = kernel(place_rows_body, (out,), 1 << 20, tps, *quarters, other, near=range(5))
     return whole
 
 
@@ -242,7 +282,19 @@
     a1 = along_z(a1, 1)
     b1 = along_z(b1, -1)
 
-    (partial,) = kernel(block_body, (like_u,), 5 * flops, zs, mid_tokens, out_grad, *a2, *b2)
+    sums, scale = kernel(
+        near_body,
+        (((tokens.shape[0], 3 * n), f32), ((tokens.shape[0], 128), f32)),
+        2 * flops,
+        zs,
+        mid_tokens,
+        out_grad,
+        *a2[:3],
+        *b2[:3],
+    )
+    (partial,) = kernel(
+        block_body, (like_u,), 3 * flops, zs, mid_tokens, out_grad, sums, scale, *a2, *b2
+    )
     pieces = own_rows(partial)
     rows, like_rows = pieces.shape[1], (pieces.shape[1:], bf16)
     mid_rows, spread = kernel(
@@ -253,17 +305,30 @@
         pieces,
         lax.dynamic_slice_in_dim(mid_tokens, tp * rows, rows, axis=0),
         lax.dynamic_slice_in_dim(out_grad, tp * rows, rows, axis=0),
+        near=(0,),
     )
     mid_grad = lax.all_to_all(spread, "tp", 0, 0, tiled=True).reshape(mid_tokens.shape)
 
+    sums_1, scale_1 = kernel(
+        near_forward_body,
+        (((tokens.shape[0], 2 * n), f32), ((tokens.shape[0], 128), f32)),
+        flops,
+        zs,
+        tokens,
+        *a1[:3],
+        *b1[:3],
+    )
     both, hidden = kernel(
         forward_body,
         (((tokens.shape[0], 2 * n), f32), ((tokens.shape[0], n), bf16)),
-        2 * flops,
+        flops,
         zs,
         tokens,
-        *a1,
-        *b1,
+        sums_1,
+        scale_1,
+        a1[3],
+        b1[3],
+        near=(3, 4),
     )
     share = 0.5 * lax.dot_general(
         mid_grad, hidden, (((0,), (0,)), ((), ())), preferred_element_type=f32
@@ -272,7 +337,8 @@
     share = lax.all_to_all(share, FS_REP, 0, 0, tiled=True)
     share = share.astype(f32).sum(axis=0)
     twin = take_from(share, "rep", 1)
-    norms = from_everyone(jnp.sum(share * share, axis=0), FS_REP).sum(axis=0)
+    norms = from_everyone(jnp.sum(share * share, axis=0), FS_REP)
+    norms = norms.sum(axis=0)
     first = lax.axis_index("rep") == 0
     share = jnp.where(first, jnp.stack([share, twin]), jnp.stack([twin, share]))
 
@@ -289,7 +355,9 @@
         scratch=[pltpu.VMEM(tokens.shape, bf16)],
     )
     pieces = own_rows_by_permutes(mine, other, tp // 2)
-    (in_rows,) = kernel(own_rows_body, (like_rows,), 1 << 24, tps, *pieces, tokens, mid_rows)
+    (in_rows,) = kernel(
+        own_rows_body, (like_rows,), 1 << 24, tps, *pieces, tokens, mid_rows, near=range(4)
+    )
     input_grad = all_rows(in_rows, tps)
     return (input_grad, share.reshape(-1, n).T, norms)
 

time: 268 us -> 272 us (1.015)
  Pallas kernels: 25.5 us -> 30.5 us
  local copies, waits for them, and re-layouts: 10.5 us -> 6.68 us
    pallas_call x6 -> x8, Pallas kernels: 25.5 us -> 30.5 us  [kernel(): pl.pallas_call(body, in_specs=[SMEM] + [VMEM] * len(arrays), out_specs=tu...]
    unnamed x44 -> x28, local copies, waits for them, and re-layouts: 4.83 us -> 1.71 us
  transfers between devices with their start and end apart: 27 -> 27, of which waited for: 11 -> 12; matrix products, arithmetic and copies ran while one was open for 3% -> 2% of each run, Pallas kernels for 10% -> 11%
where the time goes in v6:
time: 272 us; the launch traced here: 270 us
  starting transfers between devices  126 us (46%)
  waiting for transfers between devices  97.4 us (36%)
  Pallas kernels  30.5 us (11%)
  local copies, waits for them, and re-layouts  6.68 us (2%)
  other arithmetic  5.19 us (2%)
  matrix products  3.05 us (1%)
    ppermute x13, starting transfers between devices, take_from(): return lax.ppermute(value, axis, [((i + step) % n, i) for i in range(n)])  52.2 us
    ppermute x13, waiting for transfers between devices, take_from(): return lax.ppermute(value, axis, [((i + step) % n, i) for i in range(n)])  49.9 us
    all_to_all x3, waiting for transfers between devices, from_everyone(): lax.all_to_all(jnp.broadcast_to(value[None], (n, *value.shape)), axis, 0,...  32.7 us
    pallas_call x8, Pallas kernels, kernel(): pl.pallas_call(body, in_specs=[SMEM] + [VMEM] * len(arrays), out_specs=tu...  30.5 us
    all_to_all x3, starting transfers between devices, from_everyone(): lax.all_to_all(jnp.broadcast_to(value[None], (n, *value.shape)), axis, 0,...  23.5 us
    ppermute x6, starting transfers between devices, take_x(): lax.ppermute(value, 'tp', [((i + 2 * step) % n, i) for i in range(n)])  21.1 us
    all_to_all x1, starting transfers between devices, step(): share = lax.all_to_all(share, FS_REP, 0, 0, tiled=True)  10.4 us
    ppermute x2, starting transfers between devices, swap_cores(): lax.ppermute(value, 'tp', [(i, i ^ 1) for i in range(lax.axis_size('tp'))])  8.07 us
  transfers between devices with their start and end apart: 27, of which 12 were waited for; matrix products, arithmetic and copies ran while one was open for 2% of the time, Pallas kernels for 11%

profile of v6, /device:TPU:1, one launch (start us, length us, event | category | flops | bytes accessed | tf_op | source)
XLA Modules:
  0.0 270.2 jit_solution(15866864977288811569)
XLA Ops:
  1.5 1.2 broadcast_in_dim.6
  2.7 7.6 %all-to-all-start = ((bf16[8,64,1152]{2,1,0:T(8,128)(2,1)}), bf16[8,64,1152]{2,1,0:T(8,128)(2,1)S(1)}, u32[]{:S(2)}, u32[]{:S(2)}) async-start(bf16[8,64,1152]{2,1,0:T(8,128)(2,1)} %broadcast_in_dim.6), calls=%async_computation | async-start | bytes 2359296 | tf_op jit(solution)/shard_map/all_to_all | solution.py:30
  10.4 31.8 %all-to-all-done = bf16[8,64,1152]{2,1,0:T(8,128)(2,1)S(1)} async-done(((bf16[8,64,1152]{2,1,0:T(8,128)(2,1)}), bf16[8,64,1152]{2,1,0:T(8,128)(2,1)S(1)}, u32[]{:S(2)}, u32[]{:S(2)}) %all-to-all-start) | async-done | bytes 1179680 | tf_op jit(solution)/shard_map/all_to_all | solution.py:30
  42.2 1.2 broadcast_in_dim.7
  43.4 3.6 %all-to-all-start.3 = ((bf16[8,64,1152]{2,1,0:T(8,128)(2,1)}), bf16[8,64,1152]{2,1,0:T(8,128)(2,1)S(1)}, u32[]{:S(2)}, u32[]{:S(2)}) async-start(bf16[8,64,1152]{2,1,0:T(8,128)(2,1)} %broadcast_in_dim.7), calls=%async_computation.3 | async-start | bytes 2359296 | tf_op jit(solution)/shard_map/all_to_all | solution.py:30
  47.0 10.9 %collective-permute-start = (bf16[512,640]{1,0:T(8,128)(2,1)S(1)}, bf16[512,640]{1,0:T(8,128)(2,1)}, u32[]{:S(2)}, u32[]{:S(2)}) collective-permute-start(bf16[512,640]{1,0:T(8,128)(2,1)S(1)} %slice.16.refs_0_), channel_id=1, source_target_pairs={{64,0},{128,64},{192,128},{256,192},{320,256},{384,320},{448,384},... | collective-permute-start | bytes 1966088 | tf_op jit(solution)/shard_map/ppermute | solution.py:25
  58.0 1.9 collective-permute-start.3
  59.9 1.9 collective-permute-start.1
  61.8 9.7 %collective-permute-done.refs_1_ = bf16[512,640]{1,0:T(8,128)(2,1)} collective-permute-done((bf16[512,640]{1,0:T(8,128)(2,1)S(1)}, bf16[512,640]{1,0:T(8,128)(2,1)}, u32[]{:S(2)}, u32[]{:S(2)}) %collective-permute-start) | collective-permute-done | bytes 655392 | tf_op jit(solution)/shard_map/ppermute | solution.py:25
  71.5 5.4 %collective-permute-start.4 = (bf16[512,640]{1,0:T(8,128)(2,1)}, bf16[512,640]{1,0:T(8,128)(2,1)}, u32[]{:S(2)}, u32[]{:S(2)}) collective-permute-start(bf16[512,640]{1,0:T(8,128)(2,1)} %collective-permute-done.refs_1_), channel_id=1, source_target_pairs={{64,0},{128,64},{192,128},{256,192},{320,256},{384,320},{448,384},... | collective-permute-start | bytes 1966088 | tf_op jit(solution)/shard_map/ppermute | solution.py:25
  76.9 1.9 collective-permute-start.2
  78.9 3.4 %collective-permute-start.5 = (bf16[512,512]{1,0:T(8,128)(2,1)S(1)}, bf16[512,512]{1,0:T(8,128)(2,1)}, u32[]{:S(2)}, u32[]{:S(2)}) collective-permute-start(bf16[512,512]{1,0:T(8,128)(2,1)S(1)} %collective-permute-done.3.refs_5_.refs_6_), channel_id=1, source_target_pairs={{448,0},{0,64},{64,128},{128,192},{192,256},{256,320},{320,384},{3... | collective-permute-start | bytes 1572872 | tf_op jit(solution)/shard_map/ppermute | solution.py:25
  82.8 18.2 %collective-permute-done.2.refs_4_.refs_5_ = bf16[512,512]{1,0:T(8,128)(2,1)} collective-permute-done((bf16[512,512]{1,0:T(8,128)(2,1)S(1)}, bf16[512,512]{1,0:T(8,128)(2,1)}, u32[]{:S(2)}, u32[]{:S(2)}) %collective-permute-start.2) | collective-permute-done | bytes 524320 | tf_op jit(solution)/shard_map/ppermute | solution.py:25
  101.9 5.3 %shard_map.112 = (f32[256,1152]{1,0:T(8,128)}, f32[256,128]{1,0:T(8,128)}) custom-call(s32[2]{0:T(128)} %pad_add_fusion.z_ref, bf16[256,2048]{1,0:T(8,128)(2,1)} %u_ref.6, bf16[256,2048]{1,0:T(8,128)(2,1)} %c_ref.3, bf16[512,640]{1,0:T(8,128)(2,1)} %copy-done.3, bf16[512,640]{1,0:T(8,128)(2,1)} %collective-permute-done.refs_1_, bf16[512,640]{1,0:T(8,128)(2,1)} %copy-done.8, ...), custom_call_target="tpu_custom_call" | custom-call | flops 805306368 | bytes 6291456 | tf_op jit(solution)/shard_map/pallas_call | solution.py:203
  107.2 6.1 %shard_map.113 = bf16[256,2048]{1,0:T(8,128)(2,1)} custom-call(s32[2]{0:T(128)} %pad_add_fusion.z_ref, bf16[256,2048]{1,0:T(8,128)(2,1)} %u_ref.6, bf16[256,2048]{1,0:T(8,128)(2,1)} %c_ref.3, f32[256,1152]{1,0:T(8,128)} %get-tuple-element.14.sums_ref, f32[256,128]{1,0:T(8,128)} %get-tuple-element.15.scale_ref, bf16[512,640]{1,0:T(8,128)(2,1)} %copy-done.3, ...), custom_call_target="tpu_custom_call" | custom-call | flops 1207959552 | bytes 6291456 | tf_op jit(solution)/shard_map/pallas_call | solution.py:203
  113.3 6.5 %all-to-all-start.1 = ((bf16[8,32,2048]{2,1,0:T(8,128)(2,1)}), bf16[8,32,2048]{2,1,0:T(8,128)(2,1)S(1)}, u32[]{:S(2)}, u32[]{:S(2)}) async-start(bf16[8,32,2048]{2,1,0:T(8,128)(2,1)} %bitcast.37), calls=%async_computation.1 | async-start | bytes 2097152 | tf_op jit(solution)/shard_map/all_to_all | solution.py:217
  119.9 5.4 %collective-permute-start.6 = (bf16[512,640]{1,0:T(8,128)(2,1)S(1)}, bf16[512,640]{1,0:T(8,128)(2,1)}, u32[]{:S(2)}, u32[]{:S(2)}) collective-permute-start(bf16[512,640]{1,0:T(8,128)(2,1)S(1)} %slice.18.refs_0_), channel_id=1, source_target_pairs={{64,0},{128,64},{192,128},{256,192},{320,256},{384,320},{448,384},... | collective-permute-start | bytes 1966088 | tf_op jit(solution)/shard_map/ppermute | solution.py:25
  125.4 1.9 collective-permute-start.9
  127.3 1.7 constant_dynamic-slice_fusion
  129.0 5.8 %all-to-all-done.1.p_ref = bf16[8,32,2048]{2,1,0:T(8,128)(2,1)S(1)} async-done(((bf16[8,32,2048]{2,1,0:T(8,128)(2,1)}), bf16[8,32,2048]{2,1,0:T(8,128)(2,1)S(1)}, u32[]{:S(2)}, u32[]{:S(2)}) %all-to-all-start.1) | async-done | bytes 1048608 | tf_op jit(solution)/shard_map/all_to_all | solution.py:217
  134.8 2.3 shard_map.114
  137.1 4.4 %all-to-all-start.2 = ((bf16[8,32,2048]{2,1,0:T(8,128)(2,1)}), bf16[8,32,2048]{2,1,0:T(8,128)(2,1)S(1)}, u32[]{:S(2)}, u32[]{:S(2)}) async-start(bf16[8,32,2048]{2,1,0:T(8,128)(2,1)} %get-tuple-element.16), calls=%async_computation.2 | async-start | bytes 2097152 | tf_op jit(solution)/shard_map/all_to_all | solution.py:310
  141.5 1.9 collective-permute-start.7
  143.4 5.4 %collective-permute-start.10 = (bf16[512,640]{1,0:T(8,128)(2,1)}, bf16[512,640]{1,0:T(8,128)(2,1)S(1)}, u32[]{:S(2)}, u32[]{:S(2)}) collective-permute-start(bf16[512,640]{1,0:T(8,128)(2,1)} %collective-permute-done.6.refs_1_), channel_id=1, source_target_pairs={{64,0},{128,64},{192,128},{256,192},{320,256},{384,320},{448,384},... | collective-permute-start | bytes 1966088 | tf_op jit(solution)/shard_map/ppermute | solution.py:25
  148.9 3.4 %collective-permute-start.8 = (bf16[512,512]{1,0:T(8,128)(2,1)S(1)}, bf16[512,512]{1,0:T(8,128)(2,1)S(1)}, u32[]{:S(2)}, u32[]{:S(2)}) collective-permute-start(bf16[512,512]{1,0:T(8,128)(2,1)S(1)} %slice.19.refs_3_.refs_4_), channel_id=1, source_target_pairs={{64,0},{128,64},{192,128},{256,192},{320,256},{384,320},{448,384},... | collective-permute-start | bytes 1572872 | tf_op jit(solution)/shard_map/ppermute | solution.py:25
  152.3 1.9 collective-permute-start.11
  154.2 20.1 %collective-permute-done.8.refs_4_.refs_5_ = bf16[512,512]{1,0:T(8,128)(2,1)S(1)} collective-permute-done((bf16[512,512]{1,0:T(8,128)(2,1)S(1)}, bf16[512,512]{1,0:T(8,128)(2,1)S(1)}, u32[]{:S(2)}, u32[]{:S(2)}) %collective-permute-start.8) | collective-permute-done | bytes 524320 | tf_op jit(solution)/shard_map/ppermute | solution.py:25
  175.1 4.4 %shard_map.115 = (f32[256,768]{1,0:T(8,128)}, f32[256,128]{1,0:T(8,128)}) custom-call(s32[2]{0:T(128)} %pad_add_fusion.z_ref, bf16[256,2048]{1,0:T(8,128)(2,1)} %u_ref.9, bf16[512,640]{1,0:T(8,128)(2,1)} %copy-done.4, bf16[512,640]{1,0:T(8,128)(2,1)} %collective-permute-done.6.refs_1_, bf16[512,640]{1,0:T(8,128)(2,1)} %collective-permute-done.7.refs_2_, ...), custom_call_target="tpu_custom_call" | custom-call | flops 402653184 | bytes 6291456 | tf_op jit(solution)/shard_map/pallas_call | solution.py:203
  179.5 3.3 %shard_map.116 = (f32[256,768]{1,0:T(8,128)}, bf16[256,384]{1,0:T(8,128)(2,1)}) custom-call(s32[2]{0:T(128)} %pad_add_fusion.z_ref, bf16[256,2048]{1,0:T(8,128)(2,1)} %u_ref.9, f32[256,768]{1,0:T(8,128)} %get-tuple-element.18.sums_ref, f32[256,128]{1,0:T(8,128)} %get-tuple-element.19.scale_ref, ...), custom_call_target="tpu_custom_call" | custom-call | flops 402653184 | bytes 6291456 | tf_op jit(solution)/shard_map/pallas_call | solution.py:203
  182.8 3.1 %multiply_convert_fusion = bf16[2048,384]{1,0:T(8,128)(2,1)} fusion(bf16[256,2048]{1,0:T(8,128)(2,1)S(1)} %bitcast.38, bf16[256,384]{1,0:T(8,128)(2,1)} %get-tuple-element.24), kind=kOutput, calls=%fused_computation.1 | convolution fusion | flops 404226048 | bytes 2818048 | tf_op jit(solution)/shard_map/dot_general | solution.py:333
  185.9 10.4 %all-to-all-start.4 = ((bf16[64,32,384]{2,1,0:T(8,128)(2,1)}), bf16[64,32,384]{2,1,0:T(8,128)(2,1)S(1)}, u32[]{:S(2)}, u32[]{:S(2)}) async-start(bf16[64,32,384]{2,1,0:T(8,128)(2,1)} %bitcast.17), calls=%async_computation.4 | async-start | bytes 3145728 | tf_op jit(solution)/shard_map/all_to_all | solution.py:337
  196.3 5.9 %shard_map.117 = (bf16[4,32,2048]{2,1,0:T(8,128)(2,1)}, bf16[4,32,2048]{2,1,0:T(8,128)(2,1)}) custom-call(s32[2]{0:T(128)} %pad_add_fusion.z_ref, bf16[256,2048]{1,0:T(8,128)(2,1)} %bitcast.39, f32[256,768]{1,0:T(8,128)} %get-tuple-element.20.both_ref, bf16[512,640]{1,0:T(8,128)(2,1)} %copy-done.4, bf16[512,640]{1,0:T(8,128)(2,1)} %collective-permute-done.6.refs_1_, ...), custom_call_target="tpu_custom_call" | custom-call | flops 1207959552 | bytes 6291456 | tf_op jit(solution)/shard_map/pallas_call | solution.py:203
  202.2 3.2 %collective-permute-start.12 = (bf16[4,32,2048]{2,1,0:T(8,128)(2,1)}, bf16[4,32,2048]{2,1,0:T(8,128)(2,1)S(1)}, u32[]{:S(2)}, u32[]{:S(2)}) collective-permute-start(bf16[4,32,2048]{2,1,0:T(8,128)(2,1)} %get-tuple-element.22), channel_id=1, source_target_pairs={{0,1},{1,0},{2,3},{3,2},{4,5},{5,4},{6,7},{7,6},{8,9},{9,8},{10,11... | collective-permute-start | bytes 1572872 | tf_op jit(solution)/shard_map/ppermute | solution.py:221
  205.5 1.6 collective-permute-done.12
  207.1 1.2 add_convert_fusion
  208.3 4.8 %collective-permute-start.13 = (bf16[32,2048]{1,0:T(8,128)(2,1)S(1)}, bf16[32,2048]{1,0:T(8,128)(2,1)S(1)}, u32[]{:S(2)}, u32[]{:S(2)}) collective-permute-start(bf16[32,2048]{1,0:T(8,128)(2,1)S(1)} %get-tuple-element.27), channel_id=1, source_target_pairs={{4,0},{5,1},{6,2},{7,3},{0,4},{1,5},{2,6},{3,7},{12,8},{13,9},{14,... | collective-permute-start | bytes 393224 | tf_op jit(solution)/shard_map/ppermute | solution.py:226
  213.1 2.2 collective-permute-start.14
  215.4 4.3 %collective-permute-start.15 = (bf16[32,2048]{1,0:T(8,128)(2,1)S(1)}, bf16[32,2048]{1,0:T(8,128)(2,1)S(1)}, u32[]{:S(2)}, u32[]{:S(2)}) collective-permute-start(bf16[32,2048]{1,0:T(8,128)(2,1)S(1)} %get-tuple-element.25), channel_id=1, source_target_pairs={{2,0},{3,1},{4,2},{5,3},{6,4},{7,5},{0,6},{1,7},{10,8},{11,9},{12,... | collective-permute-start | bytes 393224 | tf_op jit(solution)/shard_map/ppermute | solution.py:226
  221.6 2.1 shard_map.118.q0
  223.7 5.4 %collective-permute-start.16 = (bf16[32,2048]{1,0:T(8,128)(2,1)}, bf16[32,2048]{1,0:T(8,128)(2,1)S(1)}, u32[]{:S(2)}, u32[]{:S(2)}) collective-permute-start(bf16[32,2048]{1,0:T(8,128)(2,1)} %shard_map.118.q0), channel_id=1, source_target_pairs={{2,0},{3,1},{4,2},{5,3},{6,4},{7,5},{0,6},{1,7},{10,8},{11,9},{12,... | collective-permute-start | bytes 393224 | tf_op jit(solution)/shard_map/ppermute | solution.py:226
  229.1 1.9 collective-permute-start.17
  231.1 2.5 collective-permute-start.18
  233.6 3.3 %collective-permute-done.17.q2 = bf16[32,2048]{1,0:T(8,128)(2,1)S(1)} collective-permute-done((bf16[32,2048]{1,0:T(8,128)(2,1)}, bf16[32,2048]{1,0:T(8,128)(2,1)S(1)}, u32[]{:S(2)}, u32[]{:S(2)}) %collective-permute-start.17) | collective-permute-done | bytes 131104 | tf_op jit(solution)/shard_map/ppermute | solution.py:226
  236.8 2.1 collective-permute-done.18.q3
  240.0 4.9 %collective-permute-start.19 = (bf16[4,32,2048]{2,1,0:T(8,128)(2,1)S(1)}, bf16[4,32,2048]{2,1,0:T(8,128)(2,1)S(1)}, u32[]{:S(2)}, u32[]{:S(2)}) collective-permute-start(bf16[4,32,2048]{2,1,0:T(8,128)(2,1)S(1)} %pad_maximum_fusion), channel_id=1, source_target_pairs={{0,1},{1,0},{2,3},{3,2},{4,5},{5,4},{6,7},{7,6},{8,9},{9,8},{10,11... | collective-permute-start | bytes 1572872 | tf_op jit(solution)/shard_map/ppermute | solution.py:221
  245.8 12.3 %all-to-all-start.5 = ((f32[64,1,384]{2,1,0:T(1,128)}), f32[64,1,384]{2,1,0:T(1,128)S(1)}, u32[]{:S(2)}, u32[]{:S(2)}) async-start(f32[64,1,384]{2,1,0:T(1,128)} %broadcast_in_dim.8), calls=%async_computation.5 | async-start | bytes 196608 | tf_op jit(solution)/shard_map/all_to_all | solution.py:30
  258.1 6.8 %collective-permute-start.20 = (f32[32,384]{1,0:T(8,128)S(1)}, f32[32,384]{1,0:T(8,128)S(1)}, u32[]{:S(2)}, u32[]{:S(2)}) collective-permute-start(f32[32,384]{1,0:T(8,128)S(1)} %convert_reduce_fusion), channel_id=1, source_target_pairs={{256,0},{0,256},{257,1},{1,257},{258,2},{2,258},{259,3},{3,259},{2... | collective-permute-start | bytes 147464 | tf_op jit(solution)/shard_map/ppermute | solution.py:25
  266.1 1.9 collective-permute-done.20
  (61 shorter events, 10.6 us)
Async XLA Ops:
  1.5 8.9 %copy-start.11 = (bf16[384,64]{0,1:T(8,128)(2,1)S(1)}, bf16[384,64]{0,1:T(8,128)(2,1)}, u32[]{:S(2)}) copy-start(bf16[384,64]{0,1:T(8,128)(2,1)} %param.14) | copy-start | bytes 147460
  1.5 8.9 %copy-start.12 = (bf16[64,384]{1,0:T(8,128)(2,1)S(1)}, bf16[64,384]{1,0:T(8,128)(2,1)}, u32[]{:S(2)}) copy-start(bf16[64,384]{1,0:T(8,128)(2,1)} %param.13) | copy-start | bytes 147460
  1.5 8.8 %copy-start.13 = (bf16[64,384]{1,0:T(8,128)(2,1)S(1)}, bf16[64,384]{1,0:T(8,128)(2,1)}, u32[]{:S(2)}) copy-start(bf16[64,384]{1,0:T(8,128)(2,1)} %param.12) | copy-start | bytes 147460
  2.7 39.5 %all-to-all-start = ((bf16[8,64,1152]{2,1,0:T(8,128)(2,1)}), bf16[8,64,1152]{2,1,0:T(8,128)(2,1)S(1)}, u32[]{:S(2)}, u32[]{:S(2)}) async-start(bf16[8,64,1152]{2,1,0:T(8,128)(2,1)} %broadcast_in_dim.6), calls=%async_computation | async-start | bytes 2359296 | tf_op jit(solution)/shard_map/all_to_all | solution.py:30
  43.4 69.9 %all-to-all-start.3 = ((bf16[8,64,1152]{2,1,0:T(8,128)(2,1)}), bf16[8,64,1152]{2,1,0:T(8,128)(2,1)S(1)}, u32[]{:S(2)}, u32[]{:S(2)}) async-start(bf16[8,64,1152]{2,1,0:T(8,128)(2,1)} %broadcast_in_dim.7), calls=%async_computation.3 | async-start | bytes 2359296 | tf_op jit(solution)/shard_map/all_to_all | solution.py:30
  47.0 54.1 %copy-start.3 = (bf16[512,640]{1,0:T(8,128)(2,1)}, bf16[512,640]{1,0:T(8,128)(2,1)S(1)}, u32[]{:S(2)}) copy-start(bf16[512,640]{1,0:T(8,128)(2,1)S(1)} %slice.16.refs_0_) | copy-start | bytes 1966084
  47.0 24.5 %collective-permute-start = (bf16[512,640]{1,0:T(8,128)(2,1)S(1)}, bf16[512,640]{1,0:T(8,128)(2,1)}, u32[]{:S(2)}, u32[]{:S(2)}) collective-permute-start(bf16[512,640]{1,0:T(8,128)(2,1)S(1)} %slice.16.refs_0_), channel_id=1, source_target_pairs={{64,0},{128,64},{192,128},{256,192},{320,256},{384,320},{448,384},... | collective-permute-start | bytes 1966088 | tf_op jit(solution)/shard_map/ppermute | solution.py:25
  57.9 43.1 %copy-start.5 = (bf16[512,512]{1,0:T(8,128)(2,1)}, bf16[512,512]{1,0:T(8,128)(2,1)S(1)}, u32[]{:S(2)}) copy-start(bf16[512,512]{1,0:T(8,128)(2,1)S(1)} %slice.17.refs_3_.refs_4_) | copy-start | bytes 1572868
  58.0 20.9 %collective-permute-start.3 = (bf16[512,512]{1,0:T(8,128)(2,1)S(1)}, bf16[512,512]{1,0:T(8,128)(2,1)S(1)}, u32[]{:S(2)}, u32[]{:S(2)}) collective-permute-start(bf16[512,512]{1,0:T(8,128)(2,1)S(1)} %slice.17.refs_3_.refs_4_), channel_id=1, source_target_pairs={{448,0},{0,64},{64,128},{128,192},{192,256},{256,320},{320,384},{3... | collective-permute-start | bytes 1572872 | tf_op jit(solution)/shard_map/ppermute | solution.py:25
  59.9 41.2 %collective-permute-start.1 = (bf16[512,640]{1,0:T(8,128)(2,1)S(1)}, bf16[512,640]{1,0:T(8,128)(2,1)S(1)}, u32[]{:S(2)}, u32[]{:S(2)}) collective-permute-start(bf16[512,640]{1,0:T(8,128)(2,1)S(1)} %slice.16.refs_0_), channel_id=1, source_target_pairs={{448,0},{0,64},{64,128},{128,192},{192,256},{256,320},{320,384},{3... | collective-permute-start | bytes 1966088 | tf_op jit(solution)/shard_map/ppermute | solution.py:25
  71.5 35.7 %collective-permute-start.4 = (bf16[512,640]{1,0:T(8,128)(2,1)}, bf16[512,640]{1,0:T(8,128)(2,1)}, u32[]{:S(2)}, u32[]{:S(2)}) collective-permute-start(bf16[512,640]{1,0:T(8,128)(2,1)} %collective-permute-done.refs_1_), channel_id=1, source_target_pairs={{64,0},{128,64},{192,128},{256,192},{320,256},{384,320},{448,384},... | collective-permute-start | bytes 1966088 | tf_op jit(solution)/shard_map/ppermute | solution.py:25
  76.9 24.2 %collective-permute-start.2 = (bf16[512,512]{1,0:T(8,128)(2,1)S(1)}, bf16[512,512]{1,0:T(8,128)(2,1)}, u32[]{:S(2)}, u32[]{:S(2)}) collective-permute-start(bf16[512,512]{1,0:T(8,128)(2,1)S(1)} %slice.17.refs_3_.refs_4_), channel_id=1, source_target_pairs={{64,0},{128,64},{192,128},{256,192},{320,256},{384,320},{448,384},... | collective-permute-start | bytes 1572872 | tf_op jit(solution)/shard_map/ppermute | solution.py:25
  78.8 22.2 %copy-start.9 = (bf16[512,512]{1,0:T(8,128)(2,1)}, bf16[512,512]{1,0:T(8,128)(2,1)S(1)}, u32[]{:S(2)}) copy-start(bf16[512,512]{1,0:T(8,128)(2,1)S(1)} %collective-permute-done.3.refs_5_.refs_6_) | copy-start | bytes 1572868
  78.9 28.3 %collective-permute-start.5 = (bf16[512,512]{1,0:T(8,128)(2,1)S(1)}, bf16[512,512]{1,0:T(8,128)(2,1)}, u32[]{:S(2)}, u32[]{:S(2)}) collective-permute-start(bf16[512,512]{1,0:T(8,128)(2,1)S(1)} %collective-permute-done.3.refs_5_.refs_6_), channel_id=1, source_target_pairs={{448,0},{0,64},{64,128},{128,192},{192,256},{256,320},{320,384},{3... | collective-permute-start | bytes 1572872 | tf_op jit(solution)/shard_map/ppermute | solution.py:25
  101.1 0.8 copy-start.8
  113.3 21.5 %all-to-all-start.1 = ((bf16[8,32,2048]{2,1,0:T(8,128)(2,1)}), bf16[8,32,2048]{2,1,0:T(8,128)(2,1)S(1)}, u32[]{:S(2)}, u32[]{:S(2)}) async-start(bf16[8,32,2048]{2,1,0:T(8,128)(2,1)} %bitcast.37), calls=%async_computation.1 | async-start | bytes 2097152 | tf_op jit(solution)/shard_map/all_to_all | solution.py:217
  119.9 21.6 %copy-start.4 = (bf16[512,640]{1,0:T(8,128)(2,1)}, bf16[512,640]{1,0:T(8,128)(2,1)S(1)}, u32[]{:S(2)}) copy-start(bf16[512,640]{1,0:T(8,128)(2,1)S(1)} %slice.18.refs_0_) | copy-start | bytes 1966084
  119.9 23.5 %collective-permute-start.6 = (bf16[512,640]{1,0:T(8,128)(2,1)S(1)}, bf16[512,640]{1,0:T(8,128)(2,1)}, u32[]{:S(2)}, u32[]{:S(2)}) collective-permute-start(bf16[512,640]{1,0:T(8,128)(2,1)S(1)} %slice.18.refs_0_), channel_id=1, source_target_pairs={{64,0},{128,64},{192,128},{256,192},{320,256},{384,320},{448,384},... | collective-permute-start | bytes 1966088 | tf_op jit(solution)/shard_map/ppermute | solution.py:25
  125.4 23.5 %copy-start.6 = (bf16[512,512]{1,0:T(8,128)(2,1)}, bf16[512,512]{1,0:T(8,128)(2,1)S(1)}, u32[]{:S(2)}) copy-start(bf16[512,512]{1,0:T(8,128)(2,1)S(1)} %slice.19.refs_3_.refs_4_) | copy-start | bytes 1572868
  125.4 26.9 %collective-permute-start.9 = (bf16[512,512]{1,0:T(8,128)(2,1)S(1)}, bf16[512,512]{1,0:T(8,128)(2,1)}, u32[]{:S(2)}, u32[]{:S(2)}) collective-permute-start(bf16[512,512]{1,0:T(8,128)(2,1)S(1)} %slice.19.refs_3_.refs_4_), channel_id=1, source_target_pairs={{448,0},{0,64},{64,128},{128,192},{192,256},{256,320},{320,384},{3... | collective-permute-start | bytes 1572872 | tf_op jit(solution)/shard_map/ppermute | solution.py:25
  137.1 45.7 %all-to-all-start.2 = ((bf16[8,32,2048]{2,1,0:T(8,128)(2,1)}), bf16[8,32,2048]{2,1,0:T(8,128)(2,1)S(1)}, u32[]{:S(2)}, u32[]{:S(2)}) async-start(bf16[8,32,2048]{2,1,0:T(8,128)(2,1)} %get-tuple-element.16), calls=%async_computation.2 | async-start | bytes 2097152 | tf_op jit(solution)/shard_map/all_to_all | solution.py:310
  141.5 33.6 %collective-permute-start.7 = (bf16[512,640]{1,0:T(8,128)(2,1)S(1)}, bf16[512,640]{1,0:T(8,128)(2,1)}, u32[]{:S(2)}, u32[]{:S(2)}) collective-permute-start(bf16[512,640]{1,0:T(8,128)(2,1)S(1)} %slice.18.refs_0_), channel_id=1, source_target_pairs={{448,0},{0,64},{64,128},{128,192},{192,256},{256,320},{320,384},{3... | collective-permute-start | bytes 1966088 | tf_op jit(solution)/shard_map/ppermute | solution.py:25
  143.4 36.0 %collective-permute-start.10 = (bf16[512,640]{1,0:T(8,128)(2,1)}, bf16[512,640]{1,0:T(8,128)(2,1)S(1)}, u32[]{:S(2)}, u32[]{:S(2)}) collective-permute-start(bf16[512,640]{1,0:T(8,128)(2,1)} %collective-permute-done.6.refs_1_), channel_id=1, source_target_pairs={{64,0},{128,64},{192,128},{256,192},{320,256},{384,320},{448,384},... | collective-permute-start | bytes 1966088 | tf_op jit(solution)/shard_map/ppermute | solution.py:25
  148.9 25.4 %collective-permute-start.8 = (bf16[512,512]{1,0:T(8,128)(2,1)S(1)}, bf16[512,512]{1,0:T(8,128)(2,1)S(1)}, u32[]{:S(2)}, u32[]{:S(2)}) collective-permute-start(bf16[512,512]{1,0:T(8,128)(2,1)S(1)} %slice.19.refs_3_.refs_4_), channel_id=1, source_target_pairs={{64,0},{128,64},{192,128},{256,192},{320,256},{384,320},{448,384},... | collective-permute-start | bytes 1572872 | tf_op jit(solution)/shard_map/ppermute | solution.py:25
  152.3 27.2 %collective-permute-start.11 = (bf16[512,512]{1,0:T(8,128)(2,1)}, bf16[512,512]{1,0:T(8,128)(2,1)S(1)}, u32[]{:S(2)}, u32[]{:S(2)}) collective-permute-start(bf16[512,512]{1,0:T(8,128)(2,1)} %collective-permute-done.9.refs_5_.refs_6_), channel_id=1, source_target_pairs={{448,0},{0,64},{64,128},{128,192},{192,256},{256,320},{320,384},{3... | collective-permute-start | bytes 1572872 | tf_op jit(solution)/shard_map/ppermute | solution.py:25
  174.3 0.8 copy-start.10
  179.5 3.4 %copy-start.1 = (bf16[512,512]{1,0:T(8,128)(2,1)}, bf16[512,512]{1,0:T(8,128)(2,1)S(1)}, u32[]{:S(2)}) copy-start(bf16[512,512]{1,0:T(8,128)(2,1)S(1)} %collective-permute-done.11.right_ref.refs_7_) | copy-start | bytes 1572868
  179.5 3.3 %copy-start = (bf16[512,640]{1,0:T(8,128)(2,1)}, bf16[512,640]{1,0:T(8,128)(2,1)S(1)}, u32[]{:S(2)}) copy-start(bf16[512,640]{1,0:T(8,128)(2,1)S(1)} %collective-permute-done.10.left_ref.refs_3_) | copy-start | bytes 1966084
  182.8 3.1 %copy-start.7 = (bf16[8,32,2048]{2,1,0:T(8,128)(2,1)}, bf16[8,32,2048]{2,1,0:T(8,128)(2,1)S(1)}, u32[]{:S(2)}) copy-start(bf16[8,32,2048]{2,1,0:T(8,128)(2,1)S(1)} %all-to-all-done.2) | copy-start | bytes 3145732
  185.9 59.0 %all-to-all-start.4 = ((bf16[64,32,384]{2,1,0:T(8,128)(2,1)}), bf16[64,32,384]{2,1,0:T(8,128)(2,1)S(1)}, u32[]{:S(2)}, u32[]{:S(2)}) async-start(bf16[64,32,384]{2,1,0:T(8,128)(2,1)} %bitcast.17), calls=%async_computation.4 | async-start | bytes 3145728 | tf_op jit(solution)/shard_map/all_to_all | solution.py:337
  202.2 4.9 %collective-permute-start.12 = (bf16[4,32,2048]{2,1,0:T(8,128)(2,1)}, bf16[4,32,2048]{2,1,0:T(8,128)(2,1)S(1)}, u32[]{:S(2)}, u32[]{:S(2)}) collective-permute-start(bf16[4,32,2048]{2,1,0:T(8,128)(2,1)} %get-tuple-element.22), channel_id=1, source_target_pairs={{0,1},{1,0},{2,3},{3,2},{4,5},{5,4},{6,7},{7,6},{8,9},{9,8},{10,11... | collective-permute-start | bytes 1572872 | tf_op jit(solution)/shard_map/ppermute | solution.py:221
  208.3 11.3 %collective-permute-start.13 = (bf16[32,2048]{1,0:T(8,128)(2,1)S(1)}, bf16[32,2048]{1,0:T(8,128)(2,1)S(1)}, u32[]{:S(2)}, u32[]{:S(2)}) collective-permute-start(bf16[32,2048]{1,0:T(8,128)(2,1)S(1)} %get-tuple-element.27), channel_id=1, source_target_pairs={{4,0},{5,1},{6,2},{7,3},{0,4},{1,5},{2,6},{3,7},{12,8},{13,9},{14,... | collective-permute-start | bytes 393224 | tf_op jit(solution)/shard_map/ppermute | solution.py:226
  213.1 7.5 %collective-permute-start.14 = (bf16[32,2048]{1,0:T(8,128)(2,1)S(1)}, bf16[32,2048]{1,0:T(8,128)(2,1)S(1)}, u32[]{:S(2)}, u32[]{:S(2)}) collective-permute-start(bf16[32,2048]{1,0:T(8,128)(2,1)S(1)} %get-tuple-element.26), channel_id=1, source_target_pairs={{6,0},{7,1},{0,2},{1,3},{2,4},{3,5},{4,6},{5,7},{14,8},{15,9},{8,1... | collective-permute-start | bytes 393224 | tf_op jit(solution)/shard_map/ppermute | solution.py:226
  215.4 6.2 %collective-permute-start.15 = (bf16[32,2048]{1,0:T(8,128)(2,1)S(1)}, bf16[32,2048]{1,0:T(8,128)(2,1)S(1)}, u32[]{:S(2)}, u32[]{:S(2)}) collective-permute-start(bf16[32,2048]{1,0:T(8,128)(2,1)S(1)} %get-tuple-element.25), channel_id=1, source_target_pairs={{2,0},{3,1},{4,2},{5,3},{6,4},{7,5},{0,6},{1,7},{10,8},{11,9},{12,... | collective-permute-start | bytes 393224 | tf_op jit(solution)/shard_map/ppermute | solution.py:226
  223.7 41.3 %copy-start.2 = (bf16[32,2048]{1,0:T(8,128)(2,1)S(1)}, bf16[32,2048]{1,0:T(8,128)(2,1)}, u32[]{:S(2)}) copy-start(bf16[32,2048]{1,0:T(8,128)(2,1)} %shard_map.118.q0) | copy-start | bytes 393220
  223.7 9.8 %collective-permute-start.16 = (bf16[32,2048]{1,0:T(8,128)(2,1)}, bf16[32,2048]{1,0:T(8,128)(2,1)S(1)}, u32[]{:S(2)}, u32[]{:S(2)}) collective-permute-start(bf16[32,2048]{1,0:T(8,128)(2,1)} %shard_map.118.q0), channel_id=1, source_target_pairs={{2,0},{3,1},{4,2},{5,3},{6,4},{7,5},{0,6},{1,7},{10,8},{11,9},{12,... | collective-permute-start | bytes 393224 | tf_op jit(solution)/shard_map/ppermute | solution.py:226
  229.1 7.7 %collective-permute-start.17 = (bf16[32,2048]{1,0:T(8,128)(2,1)}, bf16[32,2048]{1,0:T(8,128)(2,1)S(1)}, u32[]{:S(2)}, u32[]{:S(2)}) collective-permute-start(bf16[32,2048]{1,0:T(8,128)(2,1)} %shard_map.118.q0), channel_id=1, source_target_pairs={{4,0},{5,1},{6,2},{7,3},{0,4},{1,5},{2,6},{3,7},{12,8},{13,9},{14,... | collective-permute-start | bytes 393224 | tf_op jit(solution)/shard_map/ppermute | solution.py:226
  231.1 7.9 %collective-permute-start.18 = (bf16[32,2048]{1,0:T(8,128)(2,1)}, bf16[32,2048]{1,0:T(8,128)(2,1)S(1)}, u32[]{:S(2)}, u32[]{:S(2)}) collective-permute-start(bf16[32,2048]{1,0:T(8,128)(2,1)} %shard_map.118.q0), channel_id=1, source_target_pairs={{6,0},{7,1},{0,2},{1,3},{2,4},{3,5},{4,6},{5,7},{14,8},{15,9},{8,1... | collective-permute-start | bytes 393224 | tf_op jit(solution)/shard_map/ppermute | solution.py:226
  240.0 25.0 %collective-permute-start.19 = (bf16[4,32,2048]{2,1,0:T(8,128)(2,1)S(1)}, bf16[4,32,2048]{2,1,0:T(8,128)(2,1)S(1)}, u32[]{:S(2)}, u32[]{:S(2)}) collective-permute-start(bf16[4,32,2048]{2,1,0:T(8,128)(2,1)S(1)} %pad_maximum_fusion), channel_id=1, source_target_pairs={{0,1},{1,0},{2,3},{3,2},{4,5},{5,4},{6,7},{7,6},{8,9},{9,8},{10,11... | collective-permute-start | bytes 1572872 | tf_op jit(solution)/shard_map/ppermute | solution.py:221
  245.8 23.7 %all-to-all-start.5 = ((f32[64,1,384]{2,1,0:T(1,128)}), f32[64,1,384]{2,1,0:T(1,128)S(1)}, u32[]{:S(2)}, u32[]{:S(2)}) async-start(f32[64,1,384]{2,1,0:T(1,128)} %broadcast_in_dim.8), calls=%async_computation.5 | async-start | bytes 196608 | tf_op jit(solution)/shard_map/all_to_all | solution.py:30
  258.1 9.8 %collective-permute-start.20 = (f32[32,384]{1,0:T(8,128)S(1)}, f32[32,384]{1,0:T(8,128)S(1)}, u32[]{:S(2)}, u32[]{:S(2)}) collective-permute-start(f32[32,384]{1,0:T(8,128)S(1)} %convert_reduce_fusion), channel_id=1, source_target_pairs={{256,0},{0,256},{257,1},{1,257},{258,2},{2,258},{259,3},{3,259},{2... | collective-permute-start | bytes 147464 | tf_op jit(solution)/shard_map/ppermute | solution.py:25

commit v7 on v6

--- a/solution.py
+++ b/solution.py
@@ -32,9 +32,9 @@
     )
 
 
-def along_y(value):
-    whole = from_everyone(value, "fs_1")
-    return whole.reshape(-1, value.shape[1])
+def along_y(copies):
+    whole = lax.all_to_all(copies, "fs_1", 0, 0, tiled=True)
+    return whole.reshape(-1, copies.shape[2])
 
 
 def along_z(value, forward):
@@ -51,6 +51,13 @@
 def span_of(z, m, width):
     quarter = width // 4
     return pl.ds(pl.multiple_of(lax.rem(z + m, 4) * quarter, quarter), quarter)
+
+
+def pack_body(_, gate_ref, up_ref, down_ref, out_ref):
+    n = gate_ref.shape[1]
+    for k in range(out_ref.shape[0]):
+        for j, ref in enumerate((gate_ref, up_ref, down_ref)):
+            out_ref[k, :, j * n : (j + 1) * n] = ref[...]
 
 
 def scale_of(u_ref):
@@ -171,6 +178,14 @@
     own_ref[...] = own
     for k in range(n):
         out_ref[k] = own
+
+
+def outer_body(_, hidden_ref, grad_ref, out_ref):
+    blocks, rows, n = out_ref.shape
+    share = lax.dot_general(
+        grad_ref[...], hidden_ref[...], (((0,), (0,)), ((), ())), preferred_element_type=f32
+    )
+    out_ref[...] = (0.5 * share).astype(bf16).reshape(blocks, rows, n)
 
 
 def own_rows_body(tp_ref, p0, p1, p2, p3, u_ref, c_ref, own_ref):
@@ -269,11 +284,16 @@
 
     flops = 2 * tokens.shape[0] * width * n
 
+    def packed(gate, up, down):
+        out = ((lax.axis_size("fs_1"), gate.shape[0], 3 * n), bf16)
+        return kernel(pack_body, (out,), 1 << 20, tps, gate, up, down.T)[0]
+
     def parts(whole):
-        return whole[:, :LEFT], whole[:, LEFT:]
-
-    y2 = along_y(jnp.concatenate([gate_second, up_second, down_second.T], axis=1))
-    y1 = jnp.concatenate([gate_first, up_first, down_first.T], axis=1)
+        left = whole[:, :LEFT]
+        return left, whole[:, LEFT:]
+
+    y2 = along_y(packed(gate_second, up_second, down_second))
+    y1 = packed(gate_first, up_first, down_first)
     y1 = along_y(after(y1, y2))
     a2, b2 = parts(y2)
     a1, b1 = parts(y1)
@@ -297,14 +317,16 @@
     )
     pieces = own_rows(partial)
     rows, like_rows = pieces.shape[1], (pieces.shape[1:], bf16)
+    u_rows = lax.dynamic_slice_in_dim(mid_tokens, tp * rows, rows, axis=0)
+    c_rows = lax.dynamic_slice_in_dim(out_grad, tp * rows, rows, axis=0)
     mid_rows, spread = kernel(
         spread_rows_body,
         (like_rows, (pieces.shape, bf16)),
         1 << 24,
         tps,
         pieces,
-        lax.dynamic_slice_in_dim(mid_tokens, tp * rows, rows, axis=0),
-        lax.dynamic_slice_in_dim(out_grad, tp * rows, rows, axis=0),
+        u_rows,
+        c_rows,
         near=(0,),
     )
     mid_grad = lax.all_to_all(spread, "tp", 0, 0, tiled=True).reshape(mid_tokens.shape)
@@ -330,10 +352,9 @@
         b1[3],
         near=(3, 4),
     )
-    share = 0.5 * lax.dot_general(
-        mid_grad, hidden, (((0,), (0,)), ((), ())), preferred_element_type=f32
-    )
-    share = share.astype(bf16).reshape(lax.axis_size(FS_REP), -1, n)
+    blocks = lax.axis_size(FS_REP)
+    out = ((blocks, width // blocks, n), bf16)
+    (share,) = kernel(outer_body, (out,), flops, tps, hidden, mid_grad, near=(1,))
     share = lax.all_to_all(share, FS_REP, 0, 0, tiled=True)
     share = share.astype(f32).sum(axis=0)
     twin = take_from(share, "rep", 1)

time: 272 us -> 270 us (level)
  Pallas kernels: 30.5 us -> 37.5 us
  matrix products: 3.05 us -> 0 us
    all_to_all x3 -> x1, waiting for transfers between devices: 32.7 us -> 1 us  [from_everyone(): lax.all_to_all(jnp.broadcast_to(value[None], (n, *value.shape)), axis, 0,...]
    all_to_all x0 -> x2, waiting for transfers between devices: none -> 29.8 us  [along_y(): whole = lax.all_to_all(copies, 'fs_1', 0, 0, tiled=True)]
    all_to_all x0 -> x2, starting transfers between devices: none -> 11.2 us  [along_y(): whole = lax.all_to_all(copies, 'fs_1', 0, 0, tiled=True)]
    all_to_all x3 -> x1, starting transfers between devices: 23.5 us -> 12.3 us  [from_everyone(): lax.all_to_all(jnp.broadcast_to(value[None], (n, *value.shape)), axis, 0,...]
    pallas_call x8 -> x11, Pallas kernels: 30.5 us -> 37.5 us  [kernel(): pl.pallas_call(body, in_specs=[SMEM] + [VMEM] * len(arrays), out_specs=tu...]
    dot_general x1 -> x0, matrix products: 3.05 us -> none  [step(): lax.dot_general(mid_grad, hidden, (((0,), (0,)), ((), ())), preferred_ele...]
  transfers between devices with their start and end apart: 27 -> 27, of which waited for: 12 -> 12; matrix products, arithmetic and copies ran while one was open for 2% -> 2% of each run, Pallas kernels for 11% -> 12%
where the time goes in v7:
time: 270 us; the launch traced here: 269 us
  starting transfers between devices  126 us (47%)
  waiting for transfers between devices  95.4 us (35%)
  Pallas kernels  37.5 us (14%)
  other arithmetic  4.34 us (2%)
  local copies, waits for them, and re-layouts  4.31 us (2%)
    ppermute x13, starting transfers between devices, take_from(): return lax.ppermute(value, axis, [((i + step) % n, i) for i in range(n)])  52.2 us
    ppermute x13, waiting for transfers between devices, take_from(): return lax.ppermute(value, axis, [((i + step) % n, i) for i in range(n)])  49.8 us
    pallas_call x11, Pallas kernels, kernel(): pl.pallas_call(body, in_specs=[SMEM] + [VMEM] * len(arrays), out_specs=tu...  37.5 us
    all_to_all x2, waiting for transfers between devices, along_y(): whole = lax.all_to_all(copies, 'fs_1', 0, 0, tiled=True)  29.8 us
    ppermute x6, starting transfers between devices, take_x(): lax.ppermute(value, 'tp', [((i + 2 * step) % n, i) for i in range(n)])  21 us
    all_to_all x1, starting transfers between devices, from_everyone(): lax.all_to_all(jnp.broadcast_to(value[None], (n, *value.shape)), axis, 0,...  12.3 us
    all_to_all x2, starting transfers between devices, along_y(): whole = lax.all_to_all(copies, 'fs_1', 0, 0, tiled=True)  11.2 us
    all_to_all x1, starting transfers between devices, step(): share = lax.all_to_all(share, FS_REP, 0, 0, tiled=True)  10.4 us
  transfers between devices with their start and end apart: 27, of which 12 were waited for; matrix products, arithmetic and copies ran while one was open for 2% of the time, Pallas kernels for 12%

profile of v7, /device:TPU:1, one launch (start us, length us, event | category | flops | bytes accessed | tf_op | source)
XLA Modules:
  0.0 269.0 jit_solution(6889498955978972722)
XLA Ops:
  0.6 2.0 shard_map.112
  2.6 7.6 %all-to-all-start = ((bf16[8,64,1152]{2,1,0:T(8,128)(2,1)}), bf16[8,64,1152]{2,1,0:T(8,128)(2,1)S(1)}, u32[]{:S(2)}, u32[]{:S(2)}) async-start(bf16[8,64,1152]{2,1,0:T(8,128)(2,1)} %shard_map.112), calls=%async_computation | async-start | bytes 2359296 | tf_op jit(solution)/shard_map/all_to_all | solution.py:36
  10.3 2.0 shard_map.116
  12.3 29.8 %all-to-all-done = bf16[8,64,1152]{2,1,0:T(8,128)(2,1)S(1)} async-done(((bf16[8,64,1152]{2,1,0:T(8,128)(2,1)}), bf16[8,64,1152]{2,1,0:T(8,128)(2,1)S(1)}, u32[]{:S(2)}, u32[]{:S(2)}) %all-to-all-start) | async-done | bytes 1179680 | tf_op jit(solution)/shard_map/all_to_all | solution.py:36
  42.1 3.6 %all-to-all-start.3 = ((bf16[8,64,1152]{2,1,0:T(8,128)(2,1)}), bf16[8,64,1152]{2,1,0:T(8,128)(2,1)S(1)}, u32[]{:S(2)}, u32[]{:S(2)}) async-start(bf16[8,64,1152]{2,1,0:T(8,128)(2,1)} %shard_map.116), calls=%async_computation.3 | async-start | bytes 2359296 | tf_op jit(solution)/shard_map/all_to_all | solution.py:36
  45.7 10.9 %collective-permute-start = (bf16[512,640]{1,0:T(8,128)(2,1)S(1)}, bf16[512,640]{1,0:T(8,128)(2,1)}, u32[]{:S(2)}, u32[]{:S(2)}) collective-permute-start(bf16[512,640]{1,0:T(8,128)(2,1)S(1)} %slice.16.refs_0_), channel_id=1, source_target_pairs={{64,0},{128,64},{192,128},{256,192},{320,256},{384,320},{448,384},... | collective-permute-start | bytes 1966088 | tf_op jit(solution)/shard_map/ppermute | solution.py:25
  56.7 1.9 collective-permute-start.3
  58.6 1.9 collective-permute-start.1
  60.5 9.7 %collective-permute-done.refs_1_ = bf16[512,640]{1,0:T(8,128)(2,1)} collective-permute-done((bf16[512,640]{1,0:T(8,128)(2,1)S(1)}, bf16[512,640]{1,0:T(8,128)(2,1)}, u32[]{:S(2)}, u32[]{:S(2)}) %collective-permute-start) | collective-permute-done | bytes 655392 | tf_op jit(solution)/shard_map/ppermute | solution.py:25
  70.2 5.4 %collective-permute-start.4 = (bf16[512,640]{1,0:T(8,128)(2,1)}, bf16[512,640]{1,0:T(8,128)(2,1)}, u32[]{:S(2)}, u32[]{:S(2)}) collective-permute-start(bf16[512,640]{1,0:T(8,128)(2,1)} %collective-permute-done.refs_1_), channel_id=1, source_target_pairs={{64,0},{128,64},{192,128},{256,192},{320,256},{384,320},{448,384},... | collective-permute-start | bytes 1966088 | tf_op jit(solution)/shard_map/ppermute | solution.py:25
  75.6 1.9 collective-permute-start.2
  77.6 3.4 %collective-permute-start.5 = (bf16[512,512]{1,0:T(8,128)(2,1)S(1)}, bf16[512,512]{1,0:T(8,128)(2,1)}, u32[]{:S(2)}, u32[]{:S(2)}) collective-permute-start(bf16[512,512]{1,0:T(8,128)(2,1)S(1)} %collective-permute-done.3.refs_5_.refs_6_), channel_id=1, source_target_pairs={{448,0},{0,64},{64,128},{128,192},{192,256},{256,320},{320,384},{3... | collective-permute-start | bytes 1572872 | tf_op jit(solution)/shard_map/ppermute | solution.py:25
  81.6 18.2 %collective-permute-done.2.refs_4_.refs_5_ = bf16[512,512]{1,0:T(8,128)(2,1)} collective-permute-done((bf16[512,512]{1,0:T(8,128)(2,1)S(1)}, bf16[512,512]{1,0:T(8,128)(2,1)}, u32[]{:S(2)}, u32[]{:S(2)}) %collective-permute-start.2) | collective-permute-done | bytes 524320 | tf_op jit(solution)/shard_map/ppermute | solution.py:25
  100.7 5.2 %shard_map.113 = (f32[256,1152]{1,0:T(8,128)}, f32[256,128]{1,0:T(8,128)}) custom-call(s32[2]{0:T(128)} %pad_add_fusion.z_ref, bf16[256,2048]{1,0:T(8,128)(2,1)} %u_ref.6, bf16[256,2048]{1,0:T(8,128)(2,1)} %c_ref.3, bf16[512,640]{1,0:T(8,128)(2,1)} %copy-done.4, bf16[512,640]{1,0:T(8,128)(2,1)} %collective-permute-done.refs_1_, bf16[512,640]{1,0:T(8,128)(2,1)} %copy-done.8, ...), custom_call_target="tpu_custom_call" | custom-call | flops 805306368 | bytes 6291456 | tf_op jit(solution)/shard_map/pallas_call | solution.py:218
  105.9 6.1 %shard_map.114 = bf16[256,2048]{1,0:T(8,128)(2,1)} custom-call(s32[2]{0:T(128)} %pad_add_fusion.z_ref, bf16[256,2048]{1,0:T(8,128)(2,1)} %u_ref.6, bf16[256,2048]{1,0:T(8,128)(2,1)} %c_ref.3, f32[256,1152]{1,0:T(8,128)} %get-tuple-element.14.sums_ref, f32[256,128]{1,0:T(8,128)} %get-tuple-element.15.scale_ref, bf16[512,640]{1,0:T(8,128)(2,1)} %copy-done.4, ...), custom_call_target="tpu_custom_call" | custom-call | flops 1207959552 | bytes 6291456 | tf_op jit(solution)/shard_map/pallas_call | solution.py:218
  112.0 6.5 %all-to-all-start.1 = ((bf16[8,32,2048]{2,1,0:T(8,128)(2,1)}), bf16[8,32,2048]{2,1,0:T(8,128)(2,1)S(1)}, u32[]{:S(2)}, u32[]{:S(2)}) async-start(bf16[8,32,2048]{2,1,0:T(8,128)(2,1)} %bitcast.36), calls=%async_computation.1 | async-start | bytes 2097152 | tf_op jit(solution)/shard_map/all_to_all | solution.py:232
  118.6 5.4 %collective-permute-start.6 = (bf16[512,640]{1,0:T(8,128)(2,1)S(1)}, bf16[512,640]{1,0:T(8,128)(2,1)}, u32[]{:S(2)}, u32[]{:S(2)}) collective-permute-start(bf16[512,640]{1,0:T(8,128)(2,1)S(1)} %slice.18.refs_0_), channel_id=1, source_target_pairs={{64,0},{128,64},{192,128},{256,192},{320,256},{384,320},{448,384},... | collective-permute-start | bytes 1966088 | tf_op jit(solution)/shard_map/ppermute | solution.py:25
  124.1 1.9 collective-permute-start.9
  126.0 1.7 constant_dynamic-slice_fusion
  127.7 5.8 %all-to-all-done.1.p_ref = bf16[8,32,2048]{2,1,0:T(8,128)(2,1)S(1)} async-done(((bf16[8,32,2048]{2,1,0:T(8,128)(2,1)}), bf16[8,32,2048]{2,1,0:T(8,128)(2,1)S(1)}, u32[]{:S(2)}, u32[]{:S(2)}) %all-to-all-start.1) | async-done | bytes 1048608 | tf_op jit(solution)/shard_map/all_to_all | solution.py:232
  133.5 2.3 shard_map.115
  135.8 4.4 %all-to-all-start.2 = ((bf16[8,32,2048]{2,1,0:T(8,128)(2,1)}), bf16[8,32,2048]{2,1,0:T(8,128)(2,1)S(1)}, u32[]{:S(2)}, u32[]{:S(2)}) async-start(bf16[8,32,2048]{2,1,0:T(8,128)(2,1)} %get-tuple-element.16), calls=%async_computation.2 | async-start | bytes 2097152 | tf_op jit(solution)/shard_map/all_to_all | solution.py:332
  140.2 1.9 collective-permute-start.7
  142.1 5.4 %collective-permute-start.10 = (bf16[512,640]{1,0:T(8,128)(2,1)}, bf16[512,640]{1,0:T(8,128)(2,1)S(1)}, u32[]{:S(2)}, u32[]{:S(2)}) collective-permute-start(bf16[512,640]{1,0:T(8,128)(2,1)} %collective-permute-done.6.refs_1_), channel_id=1, source_target_pairs={{64,0},{128,64},{192,128},{256,192},{320,256},{384,320},{448,384},... | collective-permute-start | bytes 1966088 | tf_op jit(solution)/shard_map/ppermute | solution.py:25
  147.6 3.4 %collective-permute-start.8 = (bf16[512,512]{1,0:T(8,128)(2,1)S(1)}, bf16[512,512]{1,0:T(8,128)(2,1)S(1)}, u32[]{:S(2)}, u32[]{:S(2)}) collective-permute-start(bf16[512,512]{1,0:T(8,128)(2,1)S(1)} %slice.19.refs_3_.refs_4_), channel_id=1, source_target_pairs={{64,0},{128,64},{192,128},{256,192},{320,256},{384,320},{448,384},... | collective-permute-start | bytes 1572872 | tf_op jit(solution)/shard_map/ppermute | solution.py:25
  151.0 1.9 collective-permute-start.11
  152.9 20.1 %collective-permute-done.8.refs_4_.refs_5_ = bf16[512,512]{1,0:T(8,128)(2,1)S(1)} collective-permute-done((bf16[512,512]{1,0:T(8,128)(2,1)S(1)}, bf16[512,512]{1,0:T(8,128)(2,1)S(1)}, u32[]{:S(2)}, u32[]{:S(2)}) %collective-permute-start.8) | collective-permute-done | bytes 524320 | tf_op jit(solution)/shard_map/ppermute | solution.py:25
  173.8 4.4 %shard_map.117 = (f32[256,768]{1,0:T(8,128)}, f32[256,128]{1,0:T(8,128)}) custom-call(s32[2]{0:T(128)} %pad_add_fusion.z_ref, bf16[256,2048]{1,0:T(8,128)(2,1)} %u_ref.9, bf16[512,640]{1,0:T(8,128)(2,1)} %copy-done.5, bf16[512,640]{1,0:T(8,128)(2,1)} %collective-permute-done.6.refs_1_, bf16[512,640]{1,0:T(8,128)(2,1)} %collective-permute-done.7.refs_2_, ...), custom_call_target="tpu_custom_call" | custom-call | flops 402653184 | bytes 6291456 | tf_op jit(solution)/shard_map/pallas_call | solution.py:218
  178.2 3.3 %shard_map.118 = (f32[256,768]{1,0:T(8,128)}, bf16[256,384]{1,0:T(8,128)(2,1)}) custom-call(s32[2]{0:T(128)} %pad_add_fusion.z_ref, bf16[256,2048]{1,0:T(8,128)(2,1)} %u_ref.9, f32[256,768]{1,0:T(8,128)} %get-tuple-element.18.sums_ref, f32[256,128]{1,0:T(8,128)} %get-tuple-element.19.scale_ref, ...), custom_call_target="tpu_custom_call" | custom-call | flops 402653184 | bytes 6291456 | tf_op jit(solution)/shard_map/pallas_call | solution.py:218
  181.5 3.1 %shard_map.122 = bf16[64,32,384]{2,1,0:T(8,128)(2,1)} custom-call(s32[1]{0:T(128)} %bitcast._.tp_ref, bf16[256,384]{1,0:T(8,128)(2,1)} %get-tuple-element.24.hidden_ref, bf16[256,2048]{1,0:T(8,128)(2,1)S(1)} %bitcast.26), custom_call_target="tpu_custom_call" | custom-call | flops 402653184 | bytes 6291456 | tf_op jit(solution)/shard_map/pallas_call | solution.py:218
  184.6 10.4 %all-to-all-start.4 = ((bf16[64,32,384]{2,1,0:T(8,128)(2,1)}), bf16[64,32,384]{2,1,0:T(8,128)(2,1)S(1)}, u32[]{:S(2)}, u32[]{:S(2)}) async-start(bf16[64,32,384]{2,1,0:T(8,128)(2,1)} %shard_map.122), calls=%async_computation.4 | async-start | bytes 3145728 | tf_op jit(solution)/shard_map/all_to_all | solution.py:358
  195.1 5.9 %shard_map.119 = (bf16[4,32,2048]{2,1,0:T(8,128)(2,1)}, bf16[4,32,2048]{2,1,0:T(8,128)(2,1)}) custom-call(s32[2]{0:T(128)} %pad_add_fusion.z_ref, bf16[256,2048]{1,0:T(8,128)(2,1)} %bitcast.27, f32[256,768]{1,0:T(8,128)} %get-tuple-element.20.both_ref, bf16[512,640]{1,0:T(8,128)(2,1)} %copy-done.5, bf16[512,640]{1,0:T(8,128)(2,1)} %collective-permute-done.6.refs_1_, ...), custom_call_target="tpu_custom_call" | custom-call | flops 1207959552 | bytes 6291456 | tf_op jit(solution)/shard_map/pallas_call | solution.py:218
  201.0 3.2 %collective-permute-start.12 = (bf16[4,32,2048]{2,1,0:T(8,128)(2,1)}, bf16[4,32,2048]{2,1,0:T(8,128)(2,1)S(1)}, u32[]{:S(2)}, u32[]{:S(2)}) collective-permute-start(bf16[4,32,2048]{2,1,0:T(8,128)(2,1)} %get-tuple-element.22), channel_id=1, source_target_pairs={{0,1},{1,0},{2,3},{3,2},{4,5},{5,4},{6,7},{7,6},{8,9},{9,8},{10,11... | collective-permute-start | bytes 1572872 | tf_op jit(solution)/shard_map/ppermute | solution.py:236
  204.2 1.6 collective-permute-done.12
  205.8 1.2 add_convert_fusion
  207.1 4.8 %collective-permute-start.13 = (bf16[32,2048]{1,0:T(8,128)(2,1)S(1)}, bf16[32,2048]{1,0:T(8,128)(2,1)S(1)}, u32[]{:S(2)}, u32[]{:S(2)}) collective-permute-start(bf16[32,2048]{1,0:T(8,128)(2,1)S(1)} %get-tuple-element.27), channel_id=1, source_target_pairs={{4,0},{5,1},{6,2},{7,3},{0,4},{1,5},{2,6},{3,7},{12,8},{13,9},{14,... | collective-permute-start | bytes 393224 | tf_op jit(solution)/shard_map/ppermute | solution.py:241
  211.9 2.2 collective-permute-start.14
  214.1 4.3 %collective-permute-start.15 = (bf16[32,2048]{1,0:T(8,128)(2,1)S(1)}, bf16[32,2048]{1,0:T(8,128)(2,1)S(1)}, u32[]{:S(2)}, u32[]{:S(2)}) collective-permute-start(bf16[32,2048]{1,0:T(8,128)(2,1)S(1)} %get-tuple-element.25), channel_id=1, source_target_pairs={{2,0},{3,1},{4,2},{5,3},{6,4},{7,5},{0,6},{1,7},{10,8},{11,9},{12,... | collective-permute-start | bytes 393224 | tf_op jit(solution)/shard_map/ppermute | solution.py:241
  220.3 2.1 shard_map.120.q0
  222.4 5.3 %collective-permute-start.16 = (bf16[32,2048]{1,0:T(8,128)(2,1)}, bf16[32,2048]{1,0:T(8,128)(2,1)S(1)}, u32[]{:S(2)}, u32[]{:S(2)}) collective-permute-start(bf16[32,2048]{1,0:T(8,128)(2,1)} %shard_map.120.q0), channel_id=1, source_target_pairs={{2,0},{3,1},{4,2},{5,3},{6,4},{7,5},{0,6},{1,7},{10,8},{11,9},{12,... | collective-permute-start | bytes 393224 | tf_op jit(solution)/shard_map/ppermute | solution.py:241
  227.7 1.9 collective-permute-start.17
  229.6 2.5 collective-permute-start.18
  232.2 3.3 %collective-permute-done.17.q2 = bf16[32,2048]{1,0:T(8,128)(2,1)S(1)} collective-permute-done((bf16[32,2048]{1,0:T(8,128)(2,1)}, bf16[32,2048]{1,0:T(8,128)(2,1)S(1)}, u32[]{:S(2)}, u32[]{:S(2)}) %collective-permute-start.17) | collective-permute-done | bytes 131104 | tf_op jit(solution)/shard_map/ppermute | solution.py:241
  235.4 2.1 collective-permute-done.18.q3
  238.6 5.0 %collective-permute-start.19 = (bf16[4,32,2048]{2,1,0:T(8,128)(2,1)S(1)}, bf16[4,32,2048]{2,1,0:T(8,128)(2,1)S(1)}, u32[]{:S(2)}, u32[]{:S(2)}) collective-permute-start(bf16[4,32,2048]{2,1,0:T(8,128)(2,1)S(1)} %pad_maximum_fusion), channel_id=1, source_target_pairs={{0,1},{1,0},{2,3},{3,2},{4,5},{5,4},{6,7},{7,6},{8,9},{9,8},{10,11... | collective-permute-start | bytes 1572872 | tf_op jit(solution)/shard_map/ppermute | solution.py:236
  244.6 12.3 %all-to-all-start.5 = ((f32[64,1,384]{2,1,0:T(1,128)}), f32[64,1,384]{2,1,0:T(1,128)S(1)}, u32[]{:S(2)}, u32[]{:S(2)}) async-start(f32[64,1,384]{2,1,0:T(1,128)} %broadcast_in_dim.2), calls=%async_computation.5 | async-start | bytes 196608 | tf_op jit(solution)/shard_map/all_to_all | solution.py:30
  256.9 6.8 %collective-permute-start.20 = (f32[32,384]{1,0:T(8,128)S(1)}, f32[32,384]{1,0:T(8,128)S(1)}, u32[]{:S(2)}, u32[]{:S(2)}) collective-permute-start(f32[32,384]{1,0:T(8,128)S(1)} %convert_reduce_fusion), channel_id=1, source_target_pairs={{256,0},{0,256},{257,1},{1,257},{258,2},{2,258},{259,3},{3,259},{2... | collective-permute-start | bytes 147464 | tf_op jit(solution)/shard_map/ppermute | solution.py:25
  264.8 1.9 collective-permute-done.20
  (53 shorter events, 9.8 us)
Async XLA Ops:
  2.6 39.5 %all-to-all-start = ((bf16[8,64,1152]{2,1,0:T(8,128)(2,1)}), bf16[8,64,1152]{2,1,0:T(8,128)(2,1)S(1)}, u32[]{:S(2)}, u32[]{:S(2)}) async-start(bf16[8,64,1152]{2,1,0:T(8,128)(2,1)} %shard_map.112), calls=%async_computation | async-start | bytes 2359296 | tf_op jit(solution)/shard_map/all_to_all | solution.py:36
  42.1 69.9 %all-to-all-start.3 = ((bf16[8,64,1152]{2,1,0:T(8,128)(2,1)}), bf16[8,64,1152]{2,1,0:T(8,128)(2,1)S(1)}, u32[]{:S(2)}, u32[]{:S(2)}) async-start(bf16[8,64,1152]{2,1,0:T(8,128)(2,1)} %shard_map.116), calls=%async_computation.3 | async-start | bytes 2359296 | tf_op jit(solution)/shard_map/all_to_all | solution.py:36
  45.7 54.1 %copy-start.4 = (bf16[512,640]{1,0:T(8,128)(2,1)}, bf16[512,640]{1,0:T(8,128)(2,1)S(1)}, u32[]{:S(2)}) copy-start(bf16[512,640]{1,0:T(8,128)(2,1)S(1)} %slice.16.refs_0_) | copy-start | bytes 1966084
  45.7 24.5 %collective-permute-start = (bf16[512,640]{1,0:T(8,128)(2,1)S(1)}, bf16[512,640]{1,0:T(8,128)(2,1)}, u32[]{:S(2)}, u32[]{:S(2)}) collective-permute-start(bf16[512,640]{1,0:T(8,128)(2,1)S(1)} %slice.16.refs_0_), channel_id=1, source_target_pairs={{64,0},{128,64},{192,128},{256,192},{320,256},{384,320},{448,384},... | collective-permute-start | bytes 1966088 | tf_op jit(solution)/shard_map/ppermute | solution.py:25
  56.7 43.1 %copy-start.6 = (bf16[512,512]{1,0:T(8,128)(2,1)}, bf16[512,512]{1,0:T(8,128)(2,1)S(1)}, u32[]{:S(2)}) copy-start(bf16[512,512]{1,0:T(8,128)(2,1)S(1)} %slice.17.refs_3_.refs_4_) | copy-start | bytes 1572868
  56.7 20.9 %collective-permute-start.3 = (bf16[512,512]{1,0:T(8,128)(2,1)S(1)}, bf16[512,512]{1,0:T(8,128)(2,1)S(1)}, u32[]{:S(2)}, u32[]{:S(2)}) collective-permute-start(bf16[512,512]{1,0:T(8,128)(2,1)S(1)} %slice.17.refs_3_.refs_4_), channel_id=1, source_target_pairs={{448,0},{0,64},{64,128},{128,192},{192,256},{256,320},{320,384},{3... | collective-permute-start | bytes 1572872 | tf_op jit(solution)/shard_map/ppermute | solution.py:25
  58.6 41.2 %collective-permute-start.1 = (bf16[512,640]{1,0:T(8,128)(2,1)S(1)}, bf16[512,640]{1,0:T(8,128)(2,1)S(1)}, u32[]{:S(2)}, u32[]{:S(2)}) collective-permute-start(bf16[512,640]{1,0:T(8,128)(2,1)S(1)} %slice.16.refs_0_), channel_id=1, source_target_pairs={{448,0},{0,64},{64,128},{128,192},{192,256},{256,320},{320,384},{3... | collective-permute-start | bytes 1966088 | tf_op jit(solution)/shard_map/ppermute | solution.py:25
  70.2 35.7 %collective-permute-start.4 = (bf16[512,640]{1,0:T(8,128)(2,1)}, bf16[512,640]{1,0:T(8,128)(2,1)}, u32[]{:S(2)}, u32[]{:S(2)}) collective-permute-start(bf16[512,640]{1,0:T(8,128)(2,1)} %collective-permute-done.refs_1_), channel_id=1, source_target_pairs={{64,0},{128,64},{192,128},{256,192},{320,256},{384,320},{448,384},... | collective-permute-start | bytes 1966088 | tf_op jit(solution)/shard_map/ppermute | solution.py:25
  75.6 24.2 %collective-permute-start.2 = (bf16[512,512]{1,0:T(8,128)(2,1)S(1)}, bf16[512,512]{1,0:T(8,128)(2,1)}, u32[]{:S(2)}, u32[]{:S(2)}) collective-permute-start(bf16[512,512]{1,0:T(8,128)(2,1)S(1)} %slice.17.refs_3_.refs_4_), channel_id=1, source_target_pairs={{64,0},{128,64},{192,128},{256,192},{320,256},{384,320},{448,384},... | collective-permute-start | bytes 1572872 | tf_op jit(solution)/shard_map/ppermute | solution.py:25
  77.6 22.2 %copy-start.9 = (bf16[512,512]{1,0:T(8,128)(2,1)}, bf16[512,512]{1,0:T(8,128)(2,1)S(1)}, u32[]{:S(2)}) copy-start(bf16[512,512]{1,0:T(8,128)(2,1)S(1)} %collective-permute-done.3.refs_5_.refs_6_) | copy-start | bytes 1572868
  77.6 28.3 %collective-permute-start.5 = (bf16[512,512]{1,0:T(8,128)(2,1)S(1)}, bf16[512,512]{1,0:T(8,128)(2,1)}, u32[]{:S(2)}, u32[]{:S(2)}) collective-permute-start(bf16[512,512]{1,0:T(8,128)(2,1)S(1)} %collective-permute-done.3.refs_5_.refs_6_), channel_id=1, source_target_pairs={{448,0},{0,64},{64,128},{128,192},{192,256},{256,320},{320,384},{3... | collective-permute-start | bytes 1572872 | tf_op jit(solution)/shard_map/ppermute | solution.py:25
  99.8 0.9 copy-start.8
  112.0 21.5 %all-to-all-start.1 = ((bf16[8,32,2048]{2,1,0:T(8,128)(2,1)}), bf16[8,32,2048]{2,1,0:T(8,128)(2,1)S(1)}, u32[]{:S(2)}, u32[]{:S(2)}) async-start(bf16[8,32,2048]{2,1,0:T(8,128)(2,1)} %bitcast.36), calls=%async_computation.1 | async-start | bytes 2097152 | tf_op jit(solution)/shard_map/all_to_all | solution.py:232
  118.6 21.6 %copy-start.5 = (bf16[512,640]{1,0:T(8,128)(2,1)}, bf16[512,640]{1,0:T(8,128)(2,1)S(1)}, u32[]{:S(2)}) copy-start(bf16[512,640]{1,0:T(8,128)(2,1)S(1)} %slice.18.refs_0_) | copy-start | bytes 1966084
  118.6 23.5 %collective-permute-start.6 = (bf16[512,640]{1,0:T(8,128)(2,1)S(1)}, bf16[512,640]{1,0:T(8,128)(2,1)}, u32[]{:S(2)}, u32[]{:S(2)}) collective-permute-start(bf16[512,640]{1,0:T(8,128)(2,1)S(1)} %slice.18.refs_0_), channel_id=1, source_target_pairs={{64,0},{128,64},{192,128},{256,192},{320,256},{384,320},{448,384},... | collective-permute-start | bytes 1966088 | tf_op jit(solution)/shard_map/ppermute | solution.py:25
  124.1 23.5 %copy-start.7 = (bf16[512,512]{1,0:T(8,128)(2,1)}, bf16[512,512]{1,0:T(8,128)(2,1)S(1)}, u32[]{:S(2)}) copy-start(bf16[512,512]{1,0:T(8,128)(2,1)S(1)} %slice.19.refs_3_.refs_4_) | copy-start | bytes 1572868
  124.1 26.9 %collective-permute-start.9 = (bf16[512,512]{1,0:T(8,128)(2,1)S(1)}, bf16[512,512]{1,0:T(8,128)(2,1)}, u32[]{:S(2)}, u32[]{:S(2)}) collective-permute-start(bf16[512,512]{1,0:T(8,128)(2,1)S(1)} %slice.19.refs_3_.refs_4_), channel_id=1, source_target_pairs={{448,0},{0,64},{64,128},{128,192},{192,256},{256,320},{320,384},{3... | collective-permute-start | bytes 1572872 | tf_op jit(solution)/shard_map/ppermute | solution.py:25
  135.8 45.7 %all-to-all-start.2 = ((bf16[8,32,2048]{2,1,0:T(8,128)(2,1)}), bf16[8,32,2048]{2,1,0:T(8,128)(2,1)S(1)}, u32[]{:S(2)}, u32[]{:S(2)}) async-start(bf16[8,32,2048]{2,1,0:T(8,128)(2,1)} %get-tuple-element.16), calls=%async_computation.2 | async-start | bytes 2097152 | tf_op jit(solution)/shard_map/all_to_all | solution.py:332
  140.2 33.6 %collective-permute-start.7 = (bf16[512,640]{1,0:T(8,128)(2,1)S(1)}, bf16[512,640]{1,0:T(8,128)(2,1)}, u32[]{:S(2)}, u32[]{:S(2)}) collective-permute-start(bf16[512,640]{1,0:T(8,128)(2,1)S(1)} %slice.18.refs_0_), channel_id=1, source_target_pairs={{448,0},{0,64},{64,128},{128,192},{192,256},{256,320},{320,384},{3... | collective-permute-start | bytes 1966088 | tf_op jit(solution)/shard_map/ppermute | solution.py:25
  142.1 36.0 %collective-permute-start.10 = (bf16[512,640]{1,0:T(8,128)(2,1)}, bf16[512,640]{1,0:T(8,128)(2,1)S(1)}, u32[]{:S(2)}, u32[]{:S(2)}) collective-permute-start(bf16[512,640]{1,0:T(8,128)(2,1)} %collective-permute-done.6.refs_1_), channel_id=1, source_target_pairs={{64,0},{128,64},{192,128},{256,192},{320,256},{384,320},{448,384},... | collective-permute-start | bytes 1966088 | tf_op jit(solution)/shard_map/ppermute | solution.py:25
  147.6 25.4 %collective-permute-start.8 = (bf16[512,512]{1,0:T(8,128)(2,1)S(1)}, bf16[512,512]{1,0:T(8,128)(2,1)S(1)}, u32[]{:S(2)}, u32[]{:S(2)}) collective-permute-start(bf16[512,512]{1,0:T(8,128)(2,1)S(1)} %slice.19.refs_3_.refs_4_), channel_id=1, source_target_pairs={{64,0},{128,64},{192,128},{256,192},{320,256},{384,320},{448,384},... | collective-permute-start | bytes 1572872 | tf_op jit(solution)/shard_map/ppermute | solution.py:25
  151.0 27.2 %collective-permute-start.11 = (bf16[512,512]{1,0:T(8,128)(2,1)}, bf16[512,512]{1,0:T(8,128)(2,1)S(1)}, u32[]{:S(2)}, u32[]{:S(2)}) collective-permute-start(bf16[512,512]{1,0:T(8,128)(2,1)} %collective-permute-done.9.refs_5_.refs_6_), channel_id=1, source_target_pairs={{448,0},{0,64},{64,128},{128,192},{192,256},{256,320},{320,384},{3... | collective-permute-start | bytes 1572872 | tf_op jit(solution)/shard_map/ppermute | solution.py:25
  173.0 0.8 copy-start.10
  178.2 3.4 %copy-start.2 = (bf16[512,512]{1,0:T(8,128)(2,1)}, bf16[512,512]{1,0:T(8,128)(2,1)S(1)}, u32[]{:S(2)}) copy-start(bf16[512,512]{1,0:T(8,128)(2,1)S(1)} %collective-permute-done.11.right_ref.refs_7_) | copy-start | bytes 1572868
  178.2 3.3 %copy-start.1 = (bf16[512,640]{1,0:T(8,128)(2,1)}, bf16[512,640]{1,0:T(8,128)(2,1)S(1)}, u32[]{:S(2)}) copy-start(bf16[512,640]{1,0:T(8,128)(2,1)S(1)} %collective-permute-done.10.left_ref.refs_3_) | copy-start | bytes 1966084
  181.5 3.1 %copy-start = (bf16[8,32,2048]{2,1,0:T(8,128)(2,1)}, bf16[8,32,2048]{2,1,0:T(8,128)(2,1)S(1)}, u32[]{:S(2)}) copy-start(bf16[8,32,2048]{2,1,0:T(8,128)(2,1)S(1)} %all-to-all-done.2) | copy-start | bytes 3145732
  184.6 59.0 %all-to-all-start.4 = ((bf16[64,32,384]{2,1,0:T(8,128)(2,1)}), bf16[64,32,384]{2,1,0:T(8,128)(2,1)S(1)}, u32[]{:S(2)}, u32[]{:S(2)}) async-start(bf16[64,32,384]{2,1,0:T(8,128)(2,1)} %shard_map.122), calls=%async_computation.4 | async-start | bytes 3145728 | tf_op jit(solution)/shard_map/all_to_all | solution.py:358
  201.0 4.9 %collective-permute-start.12 = (bf16[4,32,2048]{2,1,0:T(8,128)(2,1)}, bf16[4,32,2048]{2,1,0:T(8,128)(2,1)S(1)}, u32[]{:S(2)}, u32[]{:S(2)}) collective-permute-start(bf16[4,32,2048]{2,1,0:T(8,128)(2,1)} %get-tuple-element.22), channel_id=1, source_target_pairs={{0,1},{1,0},{2,3},{3,2},{4,5},{5,4},{6,7},{7,6},{8,9},{9,8},{10,11... | collective-permute-start | bytes 1572872 | tf_op jit(solution)/shard_map/ppermute | solution.py:236
  207.1 11.3 %collective-permute-start.13 = (bf16[32,2048]{1,0:T(8,128)(2,1)S(1)}, bf16[32,2048]{1,0:T(8,128)(2,1)S(1)}, u32[]{:S(2)}, u32[]{:S(2)}) collective-permute-start(bf16[32,2048]{1,0:T(8,128)(2,1)S(1)} %get-tuple-element.27), channel_id=1, source_target_pairs={{4,0},{5,1},{6,2},{7,3},{0,4},{1,5},{2,6},{3,7},{12,8},{13,9},{14,... | collective-permute-start | bytes 393224 | tf_op jit(solution)/shard_map/ppermute | solution.py:241
  211.9 7.5 %collective-permute-start.14 = (bf16[32,2048]{1,0:T(8,128)(2,1)S(1)}, bf16[32,2048]{1,0:T(8,128)(2,1)S(1)}, u32[]{:S(2)}, u32[]{:S(2)}) collective-permute-start(bf16[32,2048]{1,0:T(8,128)(2,1)S(1)} %get-tuple-element.26), channel_id=1, source_target_pairs={{6,0},{7,1},{0,2},{1,3},{2,4},{3,5},{4,6},{5,7},{14,8},{15,9},{8,1... | collective-permute-start | bytes 393224 | tf_op jit(solution)/shard_map/ppermute | solution.py:241
  214.1 6.2 %collective-permute-start.15 = (bf16[32,2048]{1,0:T(8,128)(2,1)S(1)}, bf16[32,2048]{1,0:T(8,128)(2,1)S(1)}, u32[]{:S(2)}, u32[]{:S(2)}) collective-permute-start(bf16[32,2048]{1,0:T(8,128)(2,1)S(1)} %get-tuple-element.25), channel_id=1, source_target_pairs={{2,0},{3,1},{4,2},{5,3},{6,4},{7,5},{0,6},{1,7},{10,8},{11,9},{12,... | collective-permute-start | bytes 393224 | tf_op jit(solution)/shard_map/ppermute | solution.py:241
  222.4 9.7 %collective-permute-start.16 = (bf16[32,2048]{1,0:T(8,128)(2,1)}, bf16[32,2048]{1,0:T(8,128)(2,1)S(1)}, u32[]{:S(2)}, u32[]{:S(2)}) collective-permute-start(bf16[32,2048]{1,0:T(8,128)(2,1)} %shard_map.120.q0), channel_id=1, source_target_pairs={{2,0},{3,1},{4,2},{5,3},{6,4},{7,5},{0,6},{1,7},{10,8},{11,9},{12,... | collective-permute-start | bytes 393224 | tf_op jit(solution)/shard_map/ppermute | solution.py:241
  227.7 7.7 %collective-permute-start.17 = (bf16[32,2048]{1,0:T(8,128)(2,1)}, bf16[32,2048]{1,0:T(8,128)(2,1)S(1)}, u32[]{:S(2)}, u32[]{:S(2)}) collective-permute-start(bf16[32,2048]{1,0:T(8,128)(2,1)} %shard_map.120.q0), channel_id=1, source_target_pairs={{4,0},{5,1},{6,2},{7,3},{0,4},{1,5},{2,6},{3,7},{12,8},{13,9},{14,... | collective-permute-start | bytes 393224 | tf_op jit(solution)/shard_map/ppermute | solution.py:241
  229.6 7.9 %collective-permute-start.18 = (bf16[32,2048]{1,0:T(8,128)(2,1)}, bf16[32,2048]{1,0:T(8,128)(2,1)S(1)}, u32[]{:S(2)}, u32[]{:S(2)}) collective-permute-start(bf16[32,2048]{1,0:T(8,128)(2,1)} %shard_map.120.q0), channel_id=1, source_target_pairs={{6,0},{7,1},{0,2},{1,3},{2,4},{3,5},{4,6},{5,7},{14,8},{15,9},{8,1... | collective-permute-start | bytes 393224 | tf_op jit(solution)/shard_map/ppermute | solution.py:241
  238.5 25.2 %copy-start.3 = (bf16[32,2048]{1,0:T(8,128)(2,1)S(1)}, bf16[32,2048]{1,0:T(8,128)(2,1)}, u32[]{:S(2)}) copy-start(bf16[32,2048]{1,0:T(8,128)(2,1)} %shard_map.120.q0) | copy-start | bytes 393220
  238.6 25.2 %collective-permute-start.19 = (bf16[4,32,2048]{2,1,0:T(8,128)(2,1)S(1)}, bf16[4,32,2048]{2,1,0:T(8,128)(2,1)S(1)}, u32[]{:S(2)}, u32[]{:S(2)}) collective-permute-start(bf16[4,32,2048]{2,1,0:T(8,128)(2,1)S(1)} %pad_maximum_fusion), channel_id=1, source_target_pairs={{0,1},{1,0},{2,3},{3,2},{4,5},{5,4},{6,7},{7,6},{8,9},{9,8},{10,11... | collective-permute-start | bytes 1572872 | tf_op jit(solution)/shard_map/ppermute | solution.py:236
  244.6 23.7 %all-to-all-start.5 = ((f32[64,1,384]{2,1,0:T(1,128)}), f32[64,1,384]{2,1,0:T(1,128)S(1)}, u32[]{:S(2)}, u32[]{:S(2)}) async-start(f32[64,1,384]{2,1,0:T(1,128)} %broadcast_in_dim.2), calls=%async_computation.5 | async-start | bytes 196608 | tf_op jit(solution)/shard_map/all_to_all | solution.py:30
  256.9 9.8 %collective-permute-start.20 = (f32[32,384]{1,0:T(8,128)S(1)}, f32[32,384]{1,0:T(8,128)S(1)}, u32[]{:S(2)}, u32[]{:S(2)}) collective-permute-start(f32[32,384]{1,0:T(8,128)S(1)} %convert_reduce_fusion), channel_id=1, source_target_pairs={{256,0},{0,256},{257,1},{1,257},{258,2},{2,258},{259,3},{3,259},{2... | collective-permute-start | bytes 147464 | tf_op jit(solution)/shard_map/ppermute | solution.py:25

commit v8 on v7

--- a/solution.py
+++ b/solution.py
@@ -17,6 +17,7 @@
 eps = 1e-06
 LEFT = 640
 PIECES = (0, 1, 3, 2)
+NEAR_2 = 2
 ROWS_ROWS = (((1,), (1,)), ((), ()))
 
 
@@ -106,13 +107,14 @@
 
 def near_body(z_ref, u_ref, c_ref, *refs):
     *weight, sums_ref, scale_ref = refs
-    z, left, right = z_ref[0], weight[:3], weight[3:]
+    k = len(weight) // 2
+    z, left, right = z_ref[0], weight[:k], weight[k:]
     n = sums_ref.shape[1] // 3
     scale = scale_of(u_ref)
-    a, b = gate_up_of(z, u_ref, scale, PIECES[:3], left, right, n)
+    a, b = gate_up_of(z, u_ref, scale, PIECES[:k], left, right, n)
     sums_ref[:, :LEFT] = a
     sums_ref[:, LEFT : 2 * n] = b
-    sums_ref[:, 2 * n :] = back_of(z, c_ref, PIECES[:3], right, n)
+    sums_ref[:, 2 * n :] = back_of(z, c_ref, PIECES[:k], right, n)
     scale_ref[...] = jnp.broadcast_to(scale, scale_ref.shape)
 
 
@@ -120,9 +122,10 @@
     *weight, out_ref = refs
     z, left, right = z_ref[0], weight[:4], weight[4:]
     n = sums_ref.shape[1] // 3
-    a, b = gate_up_of(z, u_ref, scale_ref[:, :1], PIECES[3:], left[3:], right[3:], n)
+    k = NEAR_2
+    a, b = gate_up_of(z, u_ref, scale_ref[:, :1], PIECES[k:], left[k:], right[k:], n)
     a, b = a + sums_ref[:, :LEFT], b + sums_ref[:, LEFT : 2 * n]
-    back = back_of(z, c_ref, PIECES[3:], right[3:], n) + sums_ref[:, 2 * n :]
+    back = back_of(z, c_ref, PIECES[k:], right[k:], n) + sums_ref[:, 2 * n :]
     upper = jnp.concatenate([a[:, n:], b], axis=1)
     partial_of(z, back, a[:, :n], upper, left, right, out_ref)
 
@@ -188,13 +191,11 @@
     out_ref[...] = (0.5 * share).astype(bf16).reshape(blocks, rows, n)
 
 
-def own_rows_body(tp_ref, p0, p1, p2, p3, u_ref, c_ref, own_ref):
-    rows = c_ref.shape[0]
+def own_rows_body(_, p0, p1, p2, p3, u_ref, c_ref, own_ref):
     d_normed = p0[...].astype(f32)
     for p in (p1, p2, p3):
         d_normed = d_normed + p[...].astype(f32)
-    u = u_ref[pl.ds(pl.multiple_of(tp_ref[0] * rows, rows), rows), :]
-    own_ref[...] = gradient_of(d_normed, u, c_ref[...])
+    own_ref[...] = gradient_of(d_normed, u_ref[...], c_ref[...])
 
 
 def place_rows_body(tp_ref, q0, q1, q2, q3, other_ref, out_ref):
@@ -309,8 +310,8 @@
         zs,
         mid_tokens,
         out_grad,
-        *a2[:3],
-        *b2[:3],
+        *a2[:NEAR_2],
+        *b2[:NEAR_2],
     )
     (partial,) = kernel(
         block_body, (like_u,), 3 * flops, zs, mid_tokens, out_grad, sums, scale, *a2, *b2
@@ -319,6 +320,7 @@
     rows, like_rows = pieces.shape[1], (pieces.shape[1:], bf16)
     u_rows = lax.dynamic_slice_in_dim(mid_tokens, tp * rows, rows, axis=0)
     c_rows = lax.dynamic_slice_in_dim(out_grad, tp * rows, rows, axis=0)
+    own_tokens = lax.dynamic_slice_in_dim(tokens, tp * rows, rows, axis=0)
     mid_rows, spread = kernel(
         spread_rows_body,
         (like_rows, (pieces.shape, bf16)),
@@ -354,7 +356,7 @@
     )
     blocks = lax.axis_size(FS_REP)
     out = ((blocks, width // blocks, n), bf16)
-    (share,) = kernel(outer_body, (out,), flops, tps, hidden, mid_grad, near=(1,))
+    (share,) = kernel(outer_body, (out,), flops, tps, hidden, mid_grad, near=(0, 1))
     share = lax.all_to_all(share, FS_REP, 0, 0, tiled=True)
     share = share.astype(f32).sum(axis=0)
     twin = take_from(share, "rep", 1)
@@ -377,7 +379,7 @@
     )
     pieces = own_rows_by_permutes(mine, other, tp // 2)
     (in_rows,) = kernel(
-        own_rows_body, (like_rows,), 1 << 24, tps, *pieces, tokens, mid_rows, near=range(4)
+        own_rows_body, (like_rows,), 1 << 24, tps, *pieces, own_tokens, mid_rows, near=range(4)
     )
     input_grad = all_rows(in_rows, tps)
     return (input_grad, share.reshape(-1, n).T, norms)

time: 270 us -> 270 us (level)
  local copies, waits for them, and re-layouts: 4.31 us -> 7.78 us
  transfers between devices with their start and end apart: 27 -> 27, of which waited for: 12 -> 11; matrix products, arithmetic and copies ran while one was open for 2% -> 3% of each run, Pallas kernels for 12% -> 12%
where the time goes in v8:
time: 270 us; the launch traced here: 269 us
  starting transfers between devices  126 us (47%)
  waiting for transfers between devices  94 us (35%)
  Pallas kernels  35.7 us (13%)
  local copies, waits for them, and re-layouts  7.78 us (3%)
  other arithmetic  4.34 us (2%)
    ppermute x13, starting transfers between devices, take_from(): return lax.ppermute(value, axis, [((i + step) % n, i) for i in range(n)])  52 us
    ppermute x13, waiting for transfers between devices, take_from(): return lax.ppermute(value, axis, [((i + step) % n, i) for i in range(n)])  49.8 us
    pallas_call x11, Pallas kernels, kernel(): pl.pallas_call(body, in_specs=[SMEM] + [VMEM] * len(arrays), out_specs=tu...  35.7 us
    all_to_all x2, waiting for transfers between devices, along_y(): whole = lax.all_to_all(copies, 'fs_1', 0, 0, tiled=True)  29.8 us
    ppermute x6, starting transfers between devices, take_x(): lax.ppermute(value, 'tp', [((i + 2 * step) % n, i) for i in range(n)])  21 us
    all_to_all x1, starting transfers between devices, from_everyone(): lax.all_to_all(jnp.broadcast_to(value[None], (n, *value.shape)), axis, 0,...  12.3 us
    all_to_all x2, starting transfers between devices, along_y(): whole = lax.all_to_all(copies, 'fs_1', 0, 0, tiled=True)  11.2 us
    all_to_all x1, starting transfers between devices, step(): share = lax.all_to_all(share, FS_REP, 0, 0, tiled=True)  10.4 us
  transfers between devices with their start and end apart: 27, of which 11 were waited for; matrix products, arithmetic and copies ran while one was open for 3% of the time, Pallas kernels for 12%

profile of v8, /device:TPU:1, one launch (start us, length us, event | category | flops | bytes accessed | tf_op | source)
XLA Modules:
  0.0 269.0 jit_solution(12430143953336459106)
XLA Ops:
  0.6 2.0 shard_map.112
  2.6 7.6 %all-to-all-start = ((bf16[8,64,1152]{2,1,0:T(8,128)(2,1)}), bf16[8,64,1152]{2,1,0:T(8,128)(2,1)S(1)}, u32[]{:S(2)}, u32[]{:S(2)}) async-start(bf16[8,64,1152]{2,1,0:T(8,128)(2,1)} %shard_map.112), calls=%async_computation | async-start | bytes 2359296 | tf_op jit(solution)/shard_map/all_to_all | solution.py:37
  10.3 2.0 shard_map.116
  12.3 29.8 %all-to-all-done = bf16[8,64,1152]{2,1,0:T(8,128)(2,1)S(1)} async-done(((bf16[8,64,1152]{2,1,0:T(8,128)(2,1)}), bf16[8,64,1152]{2,1,0:T(8,128)(2,1)S(1)}, u32[]{:S(2)}, u32[]{:S(2)}) %all-to-all-start) | async-done | bytes 1179680 | tf_op jit(solution)/shard_map/all_to_all | solution.py:37
  42.1 3.6 %all-to-all-start.3 = ((bf16[8,64,1152]{2,1,0:T(8,128)(2,1)}), bf16[8,64,1152]{2,1,0:T(8,128)(2,1)S(1)}, u32[]{:S(2)}, u32[]{:S(2)}) async-start(bf16[8,64,1152]{2,1,0:T(8,128)(2,1)} %shard_map.116), calls=%async_computation.3 | async-start | bytes 2359296 | tf_op jit(solution)/shard_map/all_to_all | solution.py:37
  45.8 10.9 %collective-permute-start = (bf16[512,640]{1,0:T(8,128)(2,1)S(1)}, bf16[512,640]{1,0:T(8,128)(2,1)}, u32[]{:S(2)}, u32[]{:S(2)}) collective-permute-start(bf16[512,640]{1,0:T(8,128)(2,1)S(1)} %slice.16.refs_0_), channel_id=1, source_target_pairs={{64,0},{128,64},{192,128},{256,192},{320,256},{384,320},{448,384},... | collective-permute-start | bytes 1966088 | tf_op jit(solution)/shard_map/ppermute | solution.py:26
  56.7 1.9 collective-permute-start.4
  58.6 1.9 collective-permute-start.2
  60.6 9.7 %collective-permute-done.refs_1_ = bf16[512,640]{1,0:T(8,128)(2,1)} collective-permute-done((bf16[512,640]{1,0:T(8,128)(2,1)S(1)}, bf16[512,640]{1,0:T(8,128)(2,1)}, u32[]{:S(2)}, u32[]{:S(2)}) %collective-permute-start) | collective-permute-done | bytes 655392 | tf_op jit(solution)/shard_map/ppermute | solution.py:26
  70.2 5.4 %collective-permute-start.3 = (bf16[512,640]{1,0:T(8,128)(2,1)}, bf16[512,640]{1,0:T(8,128)(2,1)}, u32[]{:S(2)}, u32[]{:S(2)}) collective-permute-start(bf16[512,640]{1,0:T(8,128)(2,1)} %collective-permute-done.refs_1_), channel_id=1, source_target_pairs={{64,0},{128,64},{192,128},{256,192},{320,256},{384,320},{448,384},... | collective-permute-start | bytes 1966088 | tf_op jit(solution)/shard_map/ppermute | solution.py:26
  75.6 1.9 collective-permute-start.1
  77.6 3.4 %collective-permute-start.5 = (bf16[512,512]{1,0:T(8,128)(2,1)}, bf16[512,512]{1,0:T(8,128)(2,1)}, u32[]{:S(2)}, u32[]{:S(2)}) collective-permute-start(bf16[512,512]{1,0:T(8,128)(2,1)} %collective-permute-done.4.refs_6_), channel_id=1, source_target_pairs={{448,0},{0,64},{64,128},{128,192},{192,256},{256,320},{320,384},{3... | collective-permute-start | bytes 1572872 | tf_op jit(solution)/shard_map/ppermute | solution.py:26
  81.6 18.2 %collective-permute-done.1.refs_3_.refs_5_ = bf16[512,512]{1,0:T(8,128)(2,1)S(1)} collective-permute-done((bf16[512,512]{1,0:T(8,128)(2,1)S(1)}, bf16[512,512]{1,0:T(8,128)(2,1)S(1)}, u32[]{:S(2)}, u32[]{:S(2)}) %collective-permute-start.1) | collective-permute-done | bytes 524320 | tf_op jit(solution)/shard_map/ppermute | solution.py:26
  100.6 4.5 %shard_map.113 = (f32[256,1152]{1,0:T(8,128)}, f32[256,128]{1,0:T(8,128)}) custom-call(s32[2]{0:T(128)} %pad_add_fusion.z_ref, bf16[256,2048]{1,0:T(8,128)(2,1)} %u_ref.5, bf16[256,2048]{1,0:T(8,128)(2,1)} %c_ref.3, bf16[512,640]{1,0:T(8,128)(2,1)} %copy-done.5, bf16[512,640]{1,0:T(8,128)(2,1)} %collective-permute-done.refs_1_, bf16[512,512]{1,0:T(8,128)(2,1)} %copy-done.7, ...), custom_call_target="tpu_custom_call" | custom-call | flops 805306368 | bytes 6291456 | tf_op jit(solution)/shard_map/pallas_call | solution.py:219
  105.9 6.6 %shard_map.114 = bf16[256,2048]{1,0:T(8,128)(2,1)} custom-call(s32[2]{0:T(128)} %pad_add_fusion.z_ref, bf16[256,2048]{1,0:T(8,128)(2,1)} %u_ref.5, bf16[256,2048]{1,0:T(8,128)(2,1)} %c_ref.3, f32[256,1152]{1,0:T(8,128)} %get-tuple-element.14.sums_ref, f32[256,128]{1,0:T(8,128)} %get-tuple-element.15.scale_ref, bf16[512,640]{1,0:T(8,128)(2,1)} %copy-done.5, ...), custom_call_target="tpu_custom_call" | custom-call | flops 1207959552 | bytes 6291456 | tf_op jit(solution)/shard_map/pallas_call | solution.py:219
  112.5 6.5 %all-to-all-start.1 = ((bf16[8,32,2048]{2,1,0:T(8,128)(2,1)}), bf16[8,32,2048]{2,1,0:T(8,128)(2,1)S(1)}, u32[]{:S(2)}, u32[]{:S(2)}) async-start(bf16[8,32,2048]{2,1,0:T(8,128)(2,1)} %bitcast.36), calls=%async_computation.1 | async-start | bytes 2097152 | tf_op jit(solution)/shard_map/all_to_all | solution.py:233
  119.1 5.3 %collective-permute-start.6 = (bf16[512,640]{1,0:T(8,128)(2,1)S(1)}, bf16[512,640]{1,0:T(8,128)(2,1)}, u32[]{:S(2)}, u32[]{:S(2)}) collective-permute-start(bf16[512,640]{1,0:T(8,128)(2,1)S(1)} %slice.18.refs_0_), channel_id=1, source_target_pairs={{64,0},{128,64},{192,128},{256,192},{320,256},{384,320},{448,384},... | collective-permute-start | bytes 1966088 | tf_op jit(solution)/shard_map/ppermute | solution.py:26
  124.4 1.9 collective-permute-start.9
  126.4 1.7 constant_dynamic-slice_fusion.1
  128.1 5.9 %all-to-all-done.1.p_ref = bf16[8,32,2048]{2,1,0:T(8,128)(2,1)S(1)} async-done(((bf16[8,32,2048]{2,1,0:T(8,128)(2,1)}), bf16[8,32,2048]{2,1,0:T(8,128)(2,1)S(1)}, u32[]{:S(2)}, u32[]{:S(2)}) %all-to-all-start.1) | async-done | bytes 1048608 | tf_op jit(solution)/shard_map/all_to_all | solution.py:233
  134.0 2.3 shard_map.115
  136.2 4.4 %all-to-all-start.2 = ((bf16[8,32,2048]{2,1,0:T(8,128)(2,1)}), bf16[8,32,2048]{2,1,0:T(8,128)(2,1)S(1)}, u32[]{:S(2)}, u32[]{:S(2)}) async-start(bf16[8,32,2048]{2,1,0:T(8,128)(2,1)} %get-tuple-element.16), calls=%async_computation.2 | async-start | bytes 2097152 | tf_op jit(solution)/shard_map/all_to_all | solution.py:334
  140.7 1.9 collective-permute-start.7
  142.6 5.3 %collective-permute-start.10 = (bf16[512,640]{1,0:T(8,128)(2,1)}, bf16[512,640]{1,0:T(8,128)(2,1)S(1)}, u32[]{:S(2)}, u32[]{:S(2)}) collective-permute-start(bf16[512,640]{1,0:T(8,128)(2,1)} %collective-permute-done.6.refs_1_), channel_id=1, source_target_pairs={{64,0},{128,64},{192,128},{256,192},{320,256},{384,320},{448,384},... | collective-permute-start | bytes 1966088 | tf_op jit(solution)/shard_map/ppermute | solution.py:26
  147.9 3.4 %collective-permute-start.8 = (bf16[512,512]{1,0:T(8,128)(2,1)S(1)}, bf16[512,512]{1,0:T(8,128)(2,1)S(1)}, u32[]{:S(2)}, u32[]{:S(2)}) collective-permute-start(bf16[512,512]{1,0:T(8,128)(2,1)S(1)} %slice.19.refs_3_.refs_4_), channel_id=1, source_target_pairs={{64,0},{128,64},{192,128},{256,192},{320,256},{384,320},{448,384},... | collective-permute-start | bytes 1572872 | tf_op jit(solution)/shard_map/ppermute | solution.py:26
  151.3 1.9 collective-permute-start.11
  153.3 20.1 %collective-permute-done.8.refs_4_.refs_5_ = bf16[512,512]{1,0:T(8,128)(2,1)S(1)} collective-permute-done((bf16[512,512]{1,0:T(8,128)(2,1)S(1)}, bf16[512,512]{1,0:T(8,128)(2,1)S(1)}, u32[]{:S(2)}, u32[]{:S(2)}) %collective-permute-start.8) | collective-permute-done | bytes 524320 | tf_op jit(solution)/shard_map/ppermute | solution.py:26
  174.1 4.4 %shard_map.117 = (f32[256,768]{1,0:T(8,128)}, f32[256,128]{1,0:T(8,128)}) custom-call(s32[2]{0:T(128)} %pad_add_fusion.z_ref, bf16[256,2048]{1,0:T(8,128)(2,1)} %u_ref.7, bf16[512,640]{1,0:T(8,128)(2,1)} %copy-done.6, bf16[512,640]{1,0:T(8,128)(2,1)} %collective-permute-done.6.refs_1_, bf16[512,640]{1,0:T(8,128)(2,1)} %collective-permute-done.7.refs_2_, ...), custom_call_target="tpu_custom_call" | custom-call | flops 402653184 | bytes 6291456 | tf_op jit(solution)/shard_map/pallas_call | solution.py:219
  178.5 3.3 %shard_map.118 = (f32[256,768]{1,0:T(8,128)}, bf16[256,384]{1,0:T(8,128)(2,1)}) custom-call(s32[2]{0:T(128)} %pad_add_fusion.z_ref, bf16[256,2048]{1,0:T(8,128)(2,1)} %u_ref.7, f32[256,768]{1,0:T(8,128)} %get-tuple-element.18.sums_ref, f32[256,128]{1,0:T(8,128)} %get-tuple-element.19.scale_ref, ...), custom_call_target="tpu_custom_call" | custom-call | flops 402653184 | bytes 6291456 | tf_op jit(solution)/shard_map/pallas_call | solution.py:219
  183.0 1.9 shard_map.122
  185.0 10.4 %all-to-all-start.4 = ((bf16[64,32,384]{2,1,0:T(8,128)(2,1)}), bf16[64,32,384]{2,1,0:T(8,128)(2,1)S(1)}, u32[]{:S(2)}, u32[]{:S(2)}) async-start(bf16[64,32,384]{2,1,0:T(8,128)(2,1)} %shard_map.122), calls=%async_computation.4 | async-start | bytes 3145728 | tf_op jit(solution)/shard_map/all_to_all | solution.py:360
  195.4 5.9 %shard_map.119 = (bf16[4,32,2048]{2,1,0:T(8,128)(2,1)}, bf16[4,32,2048]{2,1,0:T(8,128)(2,1)}) custom-call(s32[2]{0:T(128)} %pad_add_fusion.z_ref, bf16[256,2048]{1,0:T(8,128)(2,1)} %bitcast.27, f32[256,768]{1,0:T(8,128)} %get-tuple-element.20.both_ref, bf16[512,640]{1,0:T(8,128)(2,1)} %copy-done.6, bf16[512,640]{1,0:T(8,128)(2,1)} %collective-permute-done.6.refs_1_, ...), custom_call_target="tpu_custom_call" | custom-call | flops 1207959552 | bytes 6291456 | tf_op jit(solution)/shard_map/pallas_call | solution.py:219
  201.3 3.2 %collective-permute-start.12 = (bf16[4,32,2048]{2,1,0:T(8,128)(2,1)}, bf16[4,32,2048]{2,1,0:T(8,128)(2,1)S(1)}, u32[]{:S(2)}, u32[]{:S(2)}) collective-permute-start(bf16[4,32,2048]{2,1,0:T(8,128)(2,1)} %get-tuple-element.22), channel_id=1, source_target_pairs={{0,1},{1,0},{2,3},{3,2},{4,5},{5,4},{6,7},{7,6},{8,9},{9,8},{10,11... | collective-permute-start | bytes 1572872 | tf_op jit(solution)/shard_map/ppermute | solution.py:237
  204.5 1.6 collective-permute-done.12
  207.4 4.8 %collective-permute-start.13 = (bf16[32,2048]{1,0:T(8,128)(2,1)S(1)}, bf16[32,2048]{1,0:T(8,128)(2,1)S(1)}, u32[]{:S(2)}, u32[]{:S(2)}) collective-permute-start(bf16[32,2048]{1,0:T(8,128)(2,1)S(1)} %get-tuple-element.27), channel_id=1, source_target_pairs={{4,0},{5,1},{6,2},{7,3},{0,4},{1,5},{2,6},{3,7},{12,8},{13,9},{14,... | collective-permute-start | bytes 393224 | tf_op jit(solution)/shard_map/ppermute | solution.py:242
  212.2 2.2 collective-permute-start.14
  214.4 4.3 %collective-permute-start.15 = (bf16[32,2048]{1,0:T(8,128)(2,1)S(1)}, bf16[32,2048]{1,0:T(8,128)(2,1)S(1)}, u32[]{:S(2)}, u32[]{:S(2)}) collective-permute-start(bf16[32,2048]{1,0:T(8,128)(2,1)S(1)} %get-tuple-element.25), channel_id=1, source_target_pairs={{2,0},{3,1},{4,2},{5,3},{6,4},{7,5},{0,6},{1,7},{10,8},{11,9},{12,... | collective-permute-start | bytes 393224 | tf_op jit(solution)/shard_map/ppermute | solution.py:242
  218.7 1.6 constant_dynamic-slice_fusion.u_ref
  220.6 1.9 shard_map.120.q0
  222.5 5.3 %collective-permute-start.16 = (bf16[32,2048]{1,0:T(8,128)(2,1)}, bf16[32,2048]{1,0:T(8,128)(2,1)S(1)}, u32[]{:S(2)}, u32[]{:S(2)}) collective-permute-start(bf16[32,2048]{1,0:T(8,128)(2,1)} %shard_map.120.q0), channel_id=1, source_target_pairs={{2,0},{3,1},{4,2},{5,3},{6,4},{7,5},{0,6},{1,7},{10,8},{11,9},{12,... | collective-permute-start | bytes 393224 | tf_op jit(solution)/shard_map/ppermute | solution.py:242
  227.8 1.9 collective-permute-start.17
  229.7 2.5 collective-permute-start.18
  232.2 3.3 %collective-permute-done.17.q2 = bf16[32,2048]{1,0:T(8,128)(2,1)S(1)} collective-permute-done((bf16[32,2048]{1,0:T(8,128)(2,1)}, bf16[32,2048]{1,0:T(8,128)(2,1)S(1)}, u32[]{:S(2)}, u32[]{:S(2)}) %collective-permute-start.17) | collective-permute-done | bytes 131104 | tf_op jit(solution)/shard_map/ppermute | solution.py:242
  235.5 2.1 collective-permute-done.18.q3
  238.6 5.0 %collective-permute-start.19 = (bf16[4,32,2048]{2,1,0:T(8,128)(2,1)S(1)}, bf16[4,32,2048]{2,1,0:T(8,128)(2,1)S(1)}, u32[]{:S(2)}, u32[]{:S(2)}) collective-permute-start(bf16[4,32,2048]{2,1,0:T(8,128)(2,1)S(1)} %pad_maximum_fusion), channel_id=1, source_target_pairs={{0,1},{1,0},{2,3},{3,2},{4,5},{5,4},{6,7},{7,6},{8,9},{9,8},{10,11... | collective-permute-start | bytes 1572872 | tf_op jit(solution)/shard_map/ppermute | solution.py:237
  244.6 12.3 %all-to-all-start.5 = ((f32[64,1,384]{2,1,0:T(1,128)}), f32[64,1,384]{2,1,0:T(1,128)S(1)}, u32[]{:S(2)}, u32[]{:S(2)}) async-start(f32[64,1,384]{2,1,0:T(1,128)} %broadcast_in_dim.2), calls=%async_computation.5 | async-start | bytes 196608 | tf_op jit(solution)/shard_map/all_to_all | solution.py:31
  256.9 6.8 %collective-permute-start.20 = (f32[32,384]{1,0:T(8,128)S(1)}, f32[32,384]{1,0:T(8,128)S(1)}, u32[]{:S(2)}, u32[]{:S(2)}) collective-permute-start(f32[32,384]{1,0:T(8,128)S(1)} %convert_reduce_fusion), channel_id=1, source_target_pairs={{256,0},{0,256},{257,1},{1,257},{258,2},{2,258},{259,3},{3,259},{2... | collective-permute-start | bytes 147464 | tf_op jit(solution)/shard_map/ppermute | solution.py:26
  264.8 1.9 collective-permute-done.20
  (56 shorter events, 11.2 us)
Async XLA Ops:
  2.6 39.5 %all-to-all-start = ((bf16[8,64,1152]{2,1,0:T(8,128)(2,1)}), bf16[8,64,1152]{2,1,0:T(8,128)(2,1)S(1)}, u32[]{:S(2)}, u32[]{:S(2)}) async-start(bf16[8,64,1152]{2,1,0:T(8,128)(2,1)} %shard_map.112), calls=%async_computation | async-start | bytes 2359296 | tf_op jit(solution)/shard_map/all_to_all | solution.py:37
  42.1 70.4 %all-to-all-start.3 = ((bf16[8,64,1152]{2,1,0:T(8,128)(2,1)}), bf16[8,64,1152]{2,1,0:T(8,128)(2,1)S(1)}, u32[]{:S(2)}, u32[]{:S(2)}) async-start(bf16[8,64,1152]{2,1,0:T(8,128)(2,1)} %shard_map.116), calls=%async_computation.3 | async-start | bytes 2359296 | tf_op jit(solution)/shard_map/all_to_all | solution.py:37
  45.8 54.1 %copy-start.5 = (bf16[512,640]{1,0:T(8,128)(2,1)}, bf16[512,640]{1,0:T(8,128)(2,1)S(1)}, u32[]{:S(2)}) copy-start(bf16[512,640]{1,0:T(8,128)(2,1)S(1)} %slice.16.refs_0_) | copy-start | bytes 1966084
  45.8 24.5 %collective-permute-start = (bf16[512,640]{1,0:T(8,128)(2,1)S(1)}, bf16[512,640]{1,0:T(8,128)(2,1)}, u32[]{:S(2)}, u32[]{:S(2)}) collective-permute-start(bf16[512,640]{1,0:T(8,128)(2,1)S(1)} %slice.16.refs_0_), channel_id=1, source_target_pairs={{64,0},{128,64},{192,128},{256,192},{320,256},{384,320},{448,384},... | collective-permute-start | bytes 1966088 | tf_op jit(solution)/shard_map/ppermute | solution.py:26
  56.7 43.1 %copy-start.7 = (bf16[512,512]{1,0:T(8,128)(2,1)}, bf16[512,512]{1,0:T(8,128)(2,1)S(1)}, u32[]{:S(2)}) copy-start(bf16[512,512]{1,0:T(8,128)(2,1)S(1)} %slice.17.refs_2_.refs_4_) | copy-start | bytes 1572868
  56.7 20.9 %collective-permute-start.4 = (bf16[512,512]{1,0:T(8,128)(2,1)S(1)}, bf16[512,512]{1,0:T(8,128)(2,1)}, u32[]{:S(2)}, u32[]{:S(2)}) collective-permute-start(bf16[512,512]{1,0:T(8,128)(2,1)S(1)} %slice.17.refs_2_.refs_4_), channel_id=1, source_target_pairs={{448,0},{0,64},{64,128},{128,192},{192,256},{256,320},{320,384},{3... | collective-permute-start | bytes 1572872 | tf_op jit(solution)/shard_map/ppermute | solution.py:26
  58.6 46.4 %collective-permute-start.2 = (bf16[512,640]{1,0:T(8,128)(2,1)S(1)}, bf16[512,640]{1,0:T(8,128)(2,1)S(1)}, u32[]{:S(2)}, u32[]{:S(2)}) collective-permute-start(bf16[512,640]{1,0:T(8,128)(2,1)S(1)} %slice.16.refs_0_), channel_id=1, source_target_pairs={{448,0},{0,64},{64,128},{128,192},{192,256},{256,320},{320,384},{3... | collective-permute-start | bytes 1966088 | tf_op jit(solution)/shard_map/ppermute | solution.py:26
  70.2 34.9 %collective-permute-start.3 = (bf16[512,640]{1,0:T(8,128)(2,1)}, bf16[512,640]{1,0:T(8,128)(2,1)}, u32[]{:S(2)}, u32[]{:S(2)}) collective-permute-start(bf16[512,640]{1,0:T(8,128)(2,1)} %collective-permute-done.refs_1_), channel_id=1, source_target_pairs={{64,0},{128,64},{192,128},{256,192},{320,256},{384,320},{448,384},... | collective-permute-start | bytes 1966088 | tf_op jit(solution)/shard_map/ppermute | solution.py:26
  75.6 24.2 %collective-permute-start.1 = (bf16[512,512]{1,0:T(8,128)(2,1)S(1)}, bf16[512,512]{1,0:T(8,128)(2,1)S(1)}, u32[]{:S(2)}, u32[]{:S(2)}) collective-permute-start(bf16[512,512]{1,0:T(8,128)(2,1)S(1)} %slice.17.refs_2_.refs_4_), channel_id=1, source_target_pairs={{64,0},{128,64},{192,128},{256,192},{320,256},{384,320},{448,384},... | collective-permute-start | bytes 1572872 | tf_op jit(solution)/shard_map/ppermute | solution.py:26
  77.6 27.5 %collective-permute-start.5 = (bf16[512,512]{1,0:T(8,128)(2,1)}, bf16[512,512]{1,0:T(8,128)(2,1)}, u32[]{:S(2)}, u32[]{:S(2)}) collective-permute-start(bf16[512,512]{1,0:T(8,128)(2,1)} %collective-permute-done.4.refs_6_), channel_id=1, source_target_pairs={{448,0},{0,64},{64,128},{128,192},{192,256},{256,320},{320,384},{3... | collective-permute-start | bytes 1572872 | tf_op jit(solution)/shard_map/ppermute | solution.py:26
  99.8 0.8 copy-start.9
  105.1 0.9 copy-start.11
  112.5 21.5 %all-to-all-start.1 = ((bf16[8,32,2048]{2,1,0:T(8,128)(2,1)}), bf16[8,32,2048]{2,1,0:T(8,128)(2,1)S(1)}, u32[]{:S(2)}, u32[]{:S(2)}) async-start(bf16[8,32,2048]{2,1,0:T(8,128)(2,1)} %bitcast.36), calls=%async_computation.1 | async-start | bytes 2097152 | tf_op jit(solution)/shard_map/all_to_all | solution.py:233
  119.0 21.6 %copy-start.6 = (bf16[512,640]{1,0:T(8,128)(2,1)}, bf16[512,640]{1,0:T(8,128)(2,1)S(1)}, u32[]{:S(2)}) copy-start(bf16[512,640]{1,0:T(8,128)(2,1)S(1)} %slice.18.refs_0_) | copy-start | bytes 1966084
  119.1 23.5 %collective-permute-start.6 = (bf16[512,640]{1,0:T(8,128)(2,1)S(1)}, bf16[512,640]{1,0:T(8,128)(2,1)}, u32[]{:S(2)}, u32[]{:S(2)}) collective-permute-start(bf16[512,640]{1,0:T(8,128)(2,1)S(1)} %slice.18.refs_0_), channel_id=1, source_target_pairs={{64,0},{128,64},{192,128},{256,192},{320,256},{384,320},{448,384},... | collective-permute-start | bytes 1966088 | tf_op jit(solution)/shard_map/ppermute | solution.py:26
  124.4 23.5 %copy-start.8 = (bf16[512,512]{1,0:T(8,128)(2,1)}, bf16[512,512]{1,0:T(8,128)(2,1)S(1)}, u32[]{:S(2)}) copy-start(bf16[512,512]{1,0:T(8,128)(2,1)S(1)} %slice.19.refs_3_.refs_4_) | copy-start | bytes 1572868
  124.4 26.9 %collective-permute-start.9 = (bf16[512,512]{1,0:T(8,128)(2,1)S(1)}, bf16[512,512]{1,0:T(8,128)(2,1)}, u32[]{:S(2)}, u32[]{:S(2)}) collective-permute-start(bf16[512,512]{1,0:T(8,128)(2,1)S(1)} %slice.19.refs_3_.refs_4_), channel_id=1, source_target_pairs={{448,0},{0,64},{64,128},{128,192},{192,256},{256,320},{320,384},{3... | collective-permute-start | bytes 1572872 | tf_op jit(solution)/shard_map/ppermute | solution.py:26
  136.2 45.6 %all-to-all-start.2 = ((bf16[8,32,2048]{2,1,0:T(8,128)(2,1)}), bf16[8,32,2048]{2,1,0:T(8,128)(2,1)S(1)}, u32[]{:S(2)}, u32[]{:S(2)}) async-start(bf16[8,32,2048]{2,1,0:T(8,128)(2,1)} %get-tuple-element.16), calls=%async_computation.2 | async-start | bytes 2097152 | tf_op jit(solution)/shard_map/all_to_all | solution.py:334
  140.7 33.5 %collective-permute-start.7 = (bf16[512,640]{1,0:T(8,128)(2,1)S(1)}, bf16[512,640]{1,0:T(8,128)(2,1)}, u32[]{:S(2)}, u32[]{:S(2)}) collective-permute-start(bf16[512,640]{1,0:T(8,128)(2,1)S(1)} %slice.18.refs_0_), channel_id=1, source_target_pairs={{448,0},{0,64},{64,128},{128,192},{192,256},{256,320},{320,384},{3... | collective-permute-start | bytes 1966088 | tf_op jit(solution)/shard_map/ppermute | solution.py:26
  142.6 35.9 %collective-permute-start.10 = (bf16[512,640]{1,0:T(8,128)(2,1)}, bf16[512,640]{1,0:T(8,128)(2,1)S(1)}, u32[]{:S(2)}, u32[]{:S(2)}) collective-permute-start(bf16[512,640]{1,0:T(8,128)(2,1)} %collective-permute-done.6.refs_1_), channel_id=1, source_target_pairs={{64,0},{128,64},{192,128},{256,192},{320,256},{384,320},{448,384},... | collective-permute-start | bytes 1966088 | tf_op jit(solution)/shard_map/ppermute | solution.py:26
  147.9 25.4 %collective-permute-start.8 = (bf16[512,512]{1,0:T(8,128)(2,1)S(1)}, bf16[512,512]{1,0:T(8,128)(2,1)S(1)}, u32[]{:S(2)}, u32[]{:S(2)}) collective-permute-start(bf16[512,512]{1,0:T(8,128)(2,1)S(1)} %slice.19.refs_3_.refs_4_), channel_id=1, source_target_pairs={{64,0},{128,64},{192,128},{256,192},{320,256},{384,320},{448,384},... | collective-permute-start | bytes 1572872 | tf_op jit(solution)/shard_map/ppermute | solution.py:26
  151.3 27.2 %collective-permute-start.11 = (bf16[512,512]{1,0:T(8,128)(2,1)}, bf16[512,512]{1,0:T(8,128)(2,1)S(1)}, u32[]{:S(2)}, u32[]{:S(2)}) collective-permute-start(bf16[512,512]{1,0:T(8,128)(2,1)} %collective-permute-done.9.refs_5_.refs_6_), channel_id=1, source_target_pairs={{448,0},{0,64},{64,128},{128,192},{192,256},{256,320},{320,384},{3... | collective-permute-start | bytes 1572872 | tf_op jit(solution)/shard_map/ppermute | solution.py:26
  173.3 0.8 copy-start.10
  178.5 3.4 %copy-start.2 = (bf16[512,512]{1,0:T(8,128)(2,1)}, bf16[512,512]{1,0:T(8,128)(2,1)S(1)}, u32[]{:S(2)}) copy-start(bf16[512,512]{1,0:T(8,128)(2,1)S(1)} %collective-permute-done.11.right_ref.refs_7_) | copy-start | bytes 1572868
  178.5 3.3 %copy-start.1 = (bf16[512,640]{1,0:T(8,128)(2,1)}, bf16[512,640]{1,0:T(8,128)(2,1)S(1)}, u32[]{:S(2)}) copy-start(bf16[512,640]{1,0:T(8,128)(2,1)S(1)} %collective-permute-done.10.left_ref.refs_3_) | copy-start | bytes 1966084
  181.9 3.1 %copy-start = (bf16[8,32,2048]{2,1,0:T(8,128)(2,1)}, bf16[8,32,2048]{2,1,0:T(8,128)(2,1)S(1)}, u32[]{:S(2)}) copy-start(bf16[8,32,2048]{2,1,0:T(8,128)(2,1)S(1)} %all-to-all-done.2) | copy-start | bytes 3145732
  181.9 1.1 copy-start.4
  185.0 58.7 %all-to-all-start.4 = ((bf16[64,32,384]{2,1,0:T(8,128)(2,1)}), bf16[64,32,384]{2,1,0:T(8,128)(2,1)S(1)}, u32[]{:S(2)}, u32[]{:S(2)}) async-start(bf16[64,32,384]{2,1,0:T(8,128)(2,1)} %shard_map.122), calls=%async_computation.4 | async-start | bytes 3145728 | tf_op jit(solution)/shard_map/all_to_all | solution.py:360
  201.3 4.9 %collective-permute-start.12 = (bf16[4,32,2048]{2,1,0:T(8,128)(2,1)}, bf16[4,32,2048]{2,1,0:T(8,128)(2,1)S(1)}, u32[]{:S(2)}, u32[]{:S(2)}) collective-permute-start(bf16[4,32,2048]{2,1,0:T(8,128)(2,1)} %get-tuple-element.22), channel_id=1, source_target_pairs={{0,1},{1,0},{2,3},{3,2},{4,5},{5,4},{6,7},{7,6},{8,9},{9,8},{10,11... | collective-permute-start | bytes 1572872 | tf_op jit(solution)/shard_map/ppermute | solution.py:237
  207.4 12.9 %collective-permute-start.13 = (bf16[32,2048]{1,0:T(8,128)(2,1)S(1)}, bf16[32,2048]{1,0:T(8,128)(2,1)S(1)}, u32[]{:S(2)}, u32[]{:S(2)}) collective-permute-start(bf16[32,2048]{1,0:T(8,128)(2,1)S(1)} %get-tuple-element.27), channel_id=1, source_target_pairs={{4,0},{5,1},{6,2},{7,3},{0,4},{1,5},{2,6},{3,7},{12,8},{13,9},{14,... | collective-permute-start | bytes 393224 | tf_op jit(solution)/shard_map/ppermute | solution.py:242
  212.2 8.1 %collective-permute-start.14 = (bf16[32,2048]{1,0:T(8,128)(2,1)S(1)}, bf16[32,2048]{1,0:T(8,128)(2,1)S(1)}, u32[]{:S(2)}, u32[]{:S(2)}) collective-permute-start(bf16[32,2048]{1,0:T(8,128)(2,1)S(1)} %get-tuple-element.26), channel_id=1, source_target_pairs={{6,0},{7,1},{0,2},{1,3},{2,4},{3,5},{4,6},{5,7},{14,8},{15,9},{8,1... | collective-permute-start | bytes 393224 | tf_op jit(solution)/shard_map/ppermute | solution.py:242
  214.4 6.2 %collective-permute-start.15 = (bf16[32,2048]{1,0:T(8,128)(2,1)S(1)}, bf16[32,2048]{1,0:T(8,128)(2,1)S(1)}, u32[]{:S(2)}, u32[]{:S(2)}) collective-permute-start(bf16[32,2048]{1,0:T(8,128)(2,1)S(1)} %get-tuple-element.25), channel_id=1, source_target_pairs={{2,0},{3,1},{4,2},{5,3},{6,4},{7,5},{0,6},{1,7},{10,8},{11,9},{12,... | collective-permute-start | bytes 393224 | tf_op jit(solution)/shard_map/ppermute | solution.py:242
  222.5 9.7 %collective-permute-start.16 = (bf16[32,2048]{1,0:T(8,128)(2,1)}, bf16[32,2048]{1,0:T(8,128)(2,1)S(1)}, u32[]{:S(2)}, u32[]{:S(2)}) collective-permute-start(bf16[32,2048]{1,0:T(8,128)(2,1)} %shard_map.120.q0), channel_id=1, source_target_pairs={{2,0},{3,1},{4,2},{5,3},{6,4},{7,5},{0,6},{1,7},{10,8},{11,9},{12,... | collective-permute-start | bytes 393224 | tf_op jit(solution)/shard_map/ppermute | solution.py:242
  227.8 7.7 %collective-permute-start.17 = (bf16[32,2048]{1,0:T(8,128)(2,1)}, bf16[32,2048]{1,0:T(8,128)(2,1)S(1)}, u32[]{:S(2)}, u32[]{:S(2)}) collective-permute-start(bf16[32,2048]{1,0:T(8,128)(2,1)} %shard_map.120.q0), channel_id=1, source_target_pairs={{4,0},{5,1},{6,2},{7,3},{0,4},{1,5},{2,6},{3,7},{12,8},{13,9},{14,... | collective-permute-start | bytes 393224 | tf_op jit(solution)/shard_map/ppermute | solution.py:242
  229.7 7.9 %collective-permute-start.18 = (bf16[32,2048]{1,0:T(8,128)(2,1)}, bf16[32,2048]{1,0:T(8,128)(2,1)S(1)}, u32[]{:S(2)}, u32[]{:S(2)}) collective-permute-start(bf16[32,2048]{1,0:T(8,128)(2,1)} %shard_map.120.q0), channel_id=1, source_target_pairs={{6,0},{7,1},{0,2},{1,3},{2,4},{3,5},{4,6},{5,7},{14,8},{15,9},{8,1... | collective-permute-start | bytes 393224 | tf_op jit(solution)/shard_map/ppermute | solution.py:242
  238.6 25.2 %copy-start.3 = (bf16[32,2048]{1,0:T(8,128)(2,1)S(1)}, bf16[32,2048]{1,0:T(8,128)(2,1)}, u32[]{:S(2)}) copy-start(bf16[32,2048]{1,0:T(8,128)(2,1)} %shard_map.120.q0) | copy-start | bytes 393220
  238.6 25.2 %collective-permute-start.19 = (bf16[4,32,2048]{2,1,0:T(8,128)(2,1)S(1)}, bf16[4,32,2048]{2,1,0:T(8,128)(2,1)S(1)}, u32[]{:S(2)}, u32[]{:S(2)}) collective-permute-start(bf16[4,32,2048]{2,1,0:T(8,128)(2,1)S(1)} %pad_maximum_fusion), channel_id=1, source_target_pairs={{0,1},{1,0},{2,3},{3,2},{4,5},{5,4},{6,7},{7,6},{8,9},{9,8},{10,11... | collective-permute-start | bytes 1572872 | tf_op jit(solution)/shard_map/ppermute | solution.py:237
  244.6 23.7 %all-to-all-start.5 = ((f32[64,1,384]{2,1,0:T(1,128)}), f32[64,1,384]{2,1,0:T(1,128)S(1)}, u32[]{:S(2)}, u32[]{:S(2)}) async-start(f32[64,1,384]{2,1,0:T(1,128)} %broadcast_in_dim.2), calls=%async_computation.5 | async-start | bytes 196608 | tf_op jit(solution)/shard_map/all_to_all | solution.py:31
  256.9 9.8 %collective-permute-start.20 = (f32[32,384]{1,0:T(8,128)S(1)}, f32[32,384]{1,0:T(8,128)S(1)}, u32[]{:S(2)}, u32[]{:S(2)}) collective-permute-start(f32[32,384]{1,0:T(8,128)S(1)} %convert_reduce_fusion), channel_id=1, source_target_pairs={{256,0},{0,256},{257,1},{1,257},{258,2},{2,258},{259,3},{3,259},{2... | collective-permute-start | bytes 147464 | tf_op jit(solution)/shard_map/ppermute | solution.py:26
